TPU v7x, 256 devices: a whole 4x4x8 slice. The times are simulated.
256 devices in a mesh: ep: 32 (over z, x), tp: 8 (over y, core).
Axes of the slice: x: 4, y: 4, z: 8, core: 2. Of those that a mesh axis runs over, the one named last changes fastest.
Arguments:
- tokens: bfloat16 [1536, 2048], P('ep'), may hold values from -6 to 6
- state: float32 [1536, 8, 128, 128], P('ep', 'tp'), may hold values from -4 to 4
- norm_gain: float32 [2048], replicated, may hold values from 0.1 to 1.9
- w_query: bfloat16 [2048, 1024], P('ep', 'tp'), may hold values from -0.125 to 0.125
- w_forget: bfloat16 [2048, 1024], P('ep', 'tp'), may hold values from -0.125 to 0.125
- w_input: bfloat16 [2048, 1024], P('ep', 'tp'), may hold values from -0.125 to 0.125
- w_outgate: bfloat16 [2048, 1024], P('ep', 'tp'), may hold values from -0.125 to 0.125
- lower_bound: float32 [1024], P('tp'), may hold values from 0 to 0.9
- head_gain: float32 [1024], P('tp'), may hold values from 0.1 to 1.9
- w_output: bfloat16 [1024, 2048], P('tp'), may hold values from -0.1875 to 0.1875
- ffn_gain: float32 [2048], replicated, may hold values from 0.1 to 1.9
- route_ids: int32 [1536, 4], P('ep'), may hold values from 0 to 63, all different within a row; in each aligned block of 48 rows (0 to 47, 48 to 95, ...) at most 6 rows name the same one
- route_weight: float32 [1536, 4], P('ep'), may hold values from 0.2 to 1
- expert_gate: bfloat16 [64, 2048, 1024], P('ep', None, 'tp'), may hold values from -0.125 to 0.125
- expert_up: bfloat16 [64, 2048, 1024], P('ep', None, 'tp'), may hold values from -0.125 to 0.125
- expert_down: bfloat16 [64, 1024, 2048], P('ep', 'tp'), may hold values from -0.1875 to 0.1875
- shared_gate: bfloat16 [2048, 1024], P(None, 'tp'), may hold values from -0.125 to 0.125
- shared_up: bfloat16 [2048, 1024], P(None, 'tp'), may hold values from -0.125 to 0.125
- shared_down: bfloat16 [1024, 2048], P('tp'), may hold values from -0.1875 to 0.1875
- dense_gate: bfloat16 [2048, 8192], P('tp', 'ep'), may hold values from -0.125 to 0.125
- dense_up: bfloat16 [2048, 8192], P('tp', 'ep'), may hold values from -0.125 to 0.125
- dense_down: bfloat16 [8192, 2048], P('ep', 'tp'), may hold values from -0.0625 to 0.0625
- dense_mix: float32 [2048], P('tp'), may hold values from -6 to 6
Outputs:
- mixed: bfloat16 [1536, 2048], P('ep', 'tp')
- new_state: float32 [1536, 8, 128, 128], P('ep', 'tp')
Inputs may be any that keep to these rules, and one draw needn't show every extreme that they name: `route_ids`: each row names 4 different experts. Among the rows of one device no expert is named more than 6 times, and in every draw some expert is named exactly 6 times by some device's rows.
All inputs are finite; a program needn't handle non-finite values.
Results may differ from a plain program's by a relative error of at most 0.025.
Values may be sent and summed in bfloat16 or wider, within the bound.
No kernel may reach another device: no remote copies, remote signals or barrier semaphores. Data moves between devices by JAX's collectives and lax.ppermute only.
A program may use at most 64 MiB of HBM per device.

v0:
```python
import jax
import jax.numpy as jnp
from jax import lax
from jax.sharding import Mesh
from jax.sharding import PartitionSpec as P

EP = ("ep_0", "ep_1")


EPS = 1e-06


def side_by_side(arrays, axis, dim, along):
    ends, at = ([], 0)
    for a in arrays[:-1]:
        at += a.shape[along]
        ends.append(at)
    both = jnp.concatenate(arrays, axis=along)
    return tuple(jnp.split(lax.all_gather(both, axis, axis=dim, tiled=True), ends, axis=along))


def from_everyone(x, axis):
    copies = jnp.broadcast_to(x, (lax.axis_size(axis), *x.shape))
    return lax.all_to_all(copies, axis, split_axis=0, concat_axis=0, tiled=True)


def over_copies(x, axis):
    return from_everyone(x, axis).astype(jnp.float32).sum(axis=0)


def split_up(x, dim, size):
    shape = x.shape
    parts = x.reshape(*shape[:dim], size, shape[dim] // size, *shape[dim + 1 :])
    return jnp.moveaxis(parts, dim, 0)


def sum_at_owner(x, axis, dim):
    parts = split_up(x, dim, lax.axis_size(axis))
    arrived = lax.all_to_all(parts, axis, split_axis=0, concat_axis=0, tiled=True)
    return arrived.astype(jnp.float32).sum(axis=0)


def joined_along(parts, dim):
    shape = list(parts.shape[1:])
    shape[dim] *= parts.shape[0]
    return jnp.moveaxis(parts, 0, dim).reshape(shape)


def collect(x, axis, dim):
    return joined_along(from_everyone(x, axis), dim)


def padded_to(lines, size):
    spare = -len(lines) % size
    return jnp.pad(lines, [(0, spare)] + [(0, 0)] * (lines.ndim - 1))


def total_of(x, axis):
    lines = x.reshape(-1, *x.shape[1:][-1:])
    own = lax.psum_scatter(
        padded_to(lines, lax.axis_size(axis)), axis, scatter_dimension=0, tiled=True
    )
    whole = lax.all_gather(own, axis).reshape(-1, *lines.shape[1:])
    return lax.slice_in_dim(whole, 0, len(lines)).reshape(x.shape)


def sum_by_axis(terms, axes):
    subtotal = terms.astype(jnp.bfloat16)
    for axis in axes:
        subtotal = lax.psum_scatter(subtotal, axis, scatter_dimension=0, tiled=True)
    return subtotal.astype(jnp.float32)


def rms_scale(values, gain):
    values = values.astype(jnp.float32)
    return values * lax.rsqrt(jnp.mean(values * values, axis=-1, keepdims=True) + EPS) * gain


def rounded(values):
    return lax.optimization_barrier(values.astype(jnp.bfloat16)).astype(jnp.float32)


def local(
    tokens,
    state,
    norm_gain,
    w_query,
    w_forget,
    w_input,
    w_outgate,
    lower_bound,
    head_gain,
    w_output,
    ffn_gain,
    route_ids,
    route_weight,
    expert_gate,
    expert_up,
    expert_down,
    shared_gate,
    shared_up,
    shared_down,
    dense_gate,
    dense_up,
    dense_down,
    dense_mix,
):
    ep_size = lax.axis_size(EP)
    tp_size = lax.axis_size("tp")
    seq_local, width = tokens.shape
    mix_local = w_query.shape[1]
    heads_local = state.shape[1]
    head_dim = state.shape[2]
    width_local = width // tp_size
    tp_index = lax.axis_index("tp")
    normed = rms_scale(tokens, norm_gain).astype(jnp.bfloat16)
    block = normed
    joined = jnp.concatenate(
        side_by_side((w_query, w_forget, w_input, w_outgate), EP, 0, 1), axis=1
    )
    projected = jnp.dot(block, joined, preferred_element_type=jnp.float32)
    projected = rounded(projected)
    query, forget_pre, values, out_gate = jnp.split(projected, 4, axis=1)
    shape = (seq_local, heads_local, head_dim)
    forget_sig = jax.nn.sigmoid(forget_pre)
    decay = (lower_bound + (1.0 - lower_bound) * forget_sig).reshape(shape)
    keygate = ((1.0 - lower_bound) * (1.0 - forget_sig)).reshape(shape)
    new_state = decay[..., None] * state + keygate[..., None] * values.reshape(shape)[:, :, None, :]
    readout = jnp.einsum("bhk,bhkv->bhv", query.reshape(shape), new_state)
    readout = readout * lax.rsqrt(jnp.mean(readout * readout, axis=-1, keepdims=True) + EPS)
    head_out = (readout.reshape(seq_local, mix_local) * head_gain * jax.nn.silu(out_gate)).astype(
        jnp.bfloat16
    )
    head_part = rounded(jnp.dot(head_out, w_output, preferred_element_type=jnp.float32))
    resid = tokens.astype(jnp.float32) + over_copies(head_part.astype(jnp.bfloat16), "tp").astype(
        jnp.float32
    )
    moe_in = rms_scale(resid, ffn_gain).astype(jnp.bfloat16)
    exp_local = expert_gate.shape[0]
    experts = exp_local * ep_size
    topk = route_ids.shape[1]
    capacity = max(2, 2 * seq_local * topk // experts)
    flat_ids = route_ids.reshape(-1)
    onehot = (flat_ids[:, None] == jnp.arange(experts, dtype=jnp.int32)[None, :]).astype(jnp.int32)
    slot_rank = jnp.sum((jnp.cumsum(onehot, axis=0) - onehot) * onehot, axis=1)
    slot_index = (flat_ids * capacity + slot_rank).reshape(seq_local, topk)
    slot_ids = jnp.arange(experts * capacity, dtype=jnp.int32)
    slot_hits = slot_index[None, :, :] == slot_ids[:, None, None]
    dispatch = jnp.sum(slot_hits.astype(jnp.bfloat16), axis=2)
    outgoing = jnp.dot(dispatch, moe_in, preferred_element_type=jnp.float32).astype(jnp.bfloat16)
    outgoing = outgoing.reshape(experts, capacity, width)
    incoming = lax.all_to_all(outgoing, EP, split_axis=0, concat_axis=0, tiled=True)
    count = incoming.shape[1]
    grouped = incoming.reshape(ep_size, exp_local, count, width)
    gate_pre = jnp.einsum(
        "sexd,edf->sexf", grouped, expert_gate, preferred_element_type=jnp.float32
    )
    up_pre = jnp.einsum("sexd,edf->sexf", grouped, expert_up, preferred_element_type=jnp.float32)
    hidden = (jax.nn.silu(gate_pre) * up_pre).astype(jnp.bfloat16)
    partial_value = rounded(
        jnp.einsum("sexf,efd->sexd", hidden, expert_down, preferred_element_type=jnp.float32)
    )
    summed = sum_at_owner(partial_value.astype(jnp.bfloat16), "tp", 3).astype(jnp.bfloat16)
    results = lax.all_to_all(
        summed.reshape(experts, count, width_local), EP, split_axis=0, concat_axis=0, tiled=True
    )
    combine = jnp.sum(
        jnp.where(
            slot_index[:, :, None] == slot_ids[None, None, :],
            route_weight[:, :, None],
            jnp.float32(0.0),
        ),
        axis=1,
    )
    routed = jnp.dot(combine, results.reshape(experts * capacity, width_local).astype(jnp.float32))
    shared_hidden = (
        jax.nn.silu(jnp.dot(moe_in, shared_gate, preferred_element_type=jnp.float32))
        * jnp.dot(moe_in, shared_up, preferred_element_type=jnp.float32)
    ).astype(jnp.bfloat16)
    shared_part = rounded(jnp.dot(shared_hidden, shared_down, preferred_element_type=jnp.float32))
    shared_out = sum_at_owner(shared_part.astype(jnp.bfloat16), "tp", 1)
    own_columns = lax.dynamic_slice_in_dim(moe_in, tp_index * width_local, width_local, 1)
    dense_joined = jnp.concatenate([dense_gate, dense_up], axis=1)
    dense_pre = jnp.dot(
        collect(own_columns, EP, 0), dense_joined, preferred_element_type=jnp.float32
    )
    dense_pre = total_of(rounded(dense_pre).astype(jnp.bfloat16), "tp").astype(jnp.float32)
    dense_pre_gate, dense_pre_up = jnp.split(dense_pre, 2, axis=1)
    dense_hidden = (jax.nn.silu(dense_pre_gate) * dense_pre_up).astype(jnp.bfloat16)
    block = dense_hidden
    dense_out = sum_by_axis(jnp.dot(block, dense_down, preferred_element_type=jnp.float32), EP)
    own_resid = lax.dynamic_slice_in_dim(resid, tp_index * width_local, width_local, 1)
    mixed = (own_resid + routed + shared_out + jax.nn.sigmoid(dense_mix) * dense_out).astype(
        jnp.bfloat16
    )
    return (mixed, new_state)


def solution(mesh):
    torus = Mesh(mesh.devices.reshape(8, 4, mesh.shape["tp"]), ("ep_0", "ep_1", "tp"))
    return jax.shard_map(
        local,
        mesh=torus,
        in_specs=(
            P(EP, None),
            P(EP, "tp", None, None),
            P(),
            P(EP, "tp"),
            P(EP, "tp"),
            P(EP, "tp"),
            P(EP, "tp"),
            P("tp"),
            P("tp"),
            P("tp", None),
            P(),
            P(EP, None),
            P(EP, None),
            P(EP, None, "tp"),
            P(EP, None, "tp"),
            P(EP, "tp", None),
            P(None, "tp"),
            P(None, "tp"),
            P("tp", None),
            P("tp", EP),
            P("tp", EP),
            P(EP, "tp"),
            P("tp"),
        ),
        out_specs=(P(EP, "tp"), P(EP, "tp", None, None)),
        check_vma=False,
    )
```

profile of v0, /device:TPU:8, one launch (start us, length us, event | category | flops | bytes accessed | tf_op | source)
XLA Modules:
  0.0 300.8 jit_solution(5604684566299326197)
XLA Ops:
  7.2 1.5 pad_maximum_fusion
  8.7 1.1 fusion.18
  9.8 0.7 broadcast_subtract_fusion
  10.5 81.5 %all-gather.4.cloned.1.call-done = bf16[2048,512]{1,0:T(8,128)(2,1)} async-done(((bf16[64,512]{1,0:T(8,128)(2,1)}), bf16[2048,512]{1,0:T(8,128)(2,1)}) %all-gather.4.cloned.1.call-update) | async-done | bytes 2097168 | tf_op jit(solution)/shard_map/all_gather | solution.py:19
  92.0 2.2 convolution_convert_fusion.6
  94.3 3.5 %fusion = f32[48,1,128]{2,1,0:T(1,128)S(1)} fusion(bf16[48,128,1]{1,0,2:T(8,128)(2,1)S(1)} %slice_bitcast_fusion, f32[48,128]{1,0:T(8,128)S(1)} %split.30, f32[48,128]{1,0:T(8,128)S(1)} %get-tuple-element.5, f32[48,1,128,128]{3,2,1,0:T(8,128)} %param.24, f32[48,128]{1,0:T(8,128)S(1)} %get-tuple-element.4), kind=kOutput, calls=%fused_computation | convolution fusion | flops 3932160 | bytes 3256320 | tf_op jit(solution)/shard_map/bhk,bhkv->bhv/dot_general | solution.py:129
  98.2 1.3 broadcast_in_dim.12
  99.5 5.0 %all-to-all-start = ((bf16[8,48,2048]{2,1,0:T(8,128)(2,1)}), bf16[8,48,2048]{2,1,0:T(8,128)(2,1)S(1)}, u32[]{:S(2)}, u32[]{:S(2)}) async-start(bf16[8,48,2048]{2,1,0:T(8,128)(2,1)} %broadcast_in_dim.12), calls=%async_computation | async-start | bytes 3145728 | tf_op jit(solution)/shard_map/all_to_all | solution.py:24
  104.5 20.1 %all-to-all-done = bf16[8,48,2048]{2,1,0:T(8,128)(2,1)S(1)} async-done(((bf16[8,48,2048]{2,1,0:T(8,128)(2,1)}), bf16[8,48,2048]{2,1,0:T(8,128)(2,1)S(1)}, u32[]{:S(2)}, u32[]{:S(2)}) %all-to-all-start) | async-done | bytes 1572896 | tf_op jit(solution)/shard_map/all_to_all | solution.py:24
  125.8 28.3 %all_to_all.30 = bf16[32,48,256]{2,1,0:T(8,128)(2,1)S(1)} all-to-all(bf16[32,48,256]{2,1,0:T(8,128)(2,1)S(1)} %broadcast_in_dim.15), channel_id=1, replica_groups=mesh['ep_0'=8,'ep_1'=4,'tp'=8] {'ep_0','ep_1'}, dimensions={0} | all-to-all | bytes 1572864 | tf_op jit(solution)/shard_map/all_to_all | solution.py:24
  154.1 1.7 convolution_convert_fusion
  158.0 1.6 reshape.116
  159.6 5.0 %all-to-all-start.1 = ((bf16[64,6,2048]{2,1,0:T(8,128)(2,1)}), bf16[64,6,2048]{2,1,0:T(8,128)(2,1)S(1)}, u32[]{:S(2)}, u32[]{:S(2)}) async-start(bf16[64,6,2048]{2,1,0:T(8,128)(2,1)} %reshape.116), calls=%async_computation.1 | async-start | bytes 4194304 | tf_op jit(solution)/shard_map/all_to_all | solution.py:152
  164.6 19.8 %reduce-scatter.4.cloned.1.call-done = bf16[192,512]{1,0:T(8,128)(2,1)} async-done(((bf16[1536,512]{1,0:T(8,128)(2,1)}), bf16[192,512]{1,0:T(8,128)(2,1)}) %reduce-scatter.4.cloned.1.call-update) | async-done | bytes 196624 | tf_op jit(solution)/shard_map/reduce_scatter | solution.py:60
  184.4 29.2 %all-to-all-done.1 = bf16[64,6,2048]{2,1,0:T(8,128)(2,1)S(1)} async-done(((bf16[64,6,2048]{2,1,0:T(8,128)(2,1)}), bf16[64,6,2048]{2,1,0:T(8,128)(2,1)S(1)}, u32[]{:S(2)}, u32[]{:S(2)}) %all-to-all-start.1) | async-done | bytes 1572896 | tf_op jit(solution)/shard_map/all_to_all | solution.py:152
  213.6 3.0 %convolution_bitcast_fusion.1 = f32[32,2,6,128]{3,0,2,1:T(8,128)} fusion(bf16[32,2,6,2048]{3,2,1,0:T(8,128)(2,1)S(1)} %bitcast.86, bf16[2,2048,128]{2,1,0:T(8,128)(2,1)} %param.36), kind=kOutput, calls=%fused_computation.16 | convolution fusion | flops 201326592 | bytes 2818048 | tf_op jit(solution)/shard_map/sexd,edf->sexf/dot_general | solution.py:155
  216.7 4.0 %fusion.2 = bf16[32,2,6,2048]{3,0,2,1:T(8,128)(2,1)} fusion(bf16[32,2,6,2048]{3,2,1,0:T(8,128)(2,1)S(1)} %bitcast.87, bf16[2,128,2048]{2,1,0:T(8,128)(2,1)S(1)} %copy-done, bf16[2,2048,128]{2,1,0:T(8,128)(2,1)} %param.37, f32[32,2,6,128]{3,0,2,1:T(8,128)} %convolution_bitcast_fusion.1), kind=kOutput, calls=%fused_computation.7 | convolution fusion | flops 403734528 | bytes 5439488 | tf_op jit(solution)/shard_map/sexf,efd->sexd/dot_general | solution.py:161
  220.7 2.8 copy.129
  223.5 4.9 %all-to-all-start.2 = ((bf16[8,32,2,6,256]{4,1,3,2,0:T(8,128)(2,1)}), bf16[8,32,2,6,256]{4,1,3,2,0:T(8,128)(2,1)S(1)}, u32[]{:S(2)}, u32[]{:S(2)}) async-start(bf16[8,32,2,6,256]{4,1,3,2,0:T(8,128)(2,1)} %bitcast.88), calls=%async_computation.2 | async-start | bytes 3145728 | tf_op jit(solution)/shard_map/all_to_all | solution.py:39
  228.4 1.8 convert_element_type.112
  230.3 2.4 convolution_convert_fusion.3
  232.9 1.6 convolution_convert_fusion.4
  234.5 0.7 copy.130
  235.2 13.3 %all-to-all-done.2 = bf16[8,32,2,6,256]{4,1,3,2,0:T(8,128)(2,1)S(1)} async-done(((bf16[8,32,2,6,256]{4,1,3,2,0:T(8,128)(2,1)}), bf16[8,32,2,6,256]{4,1,3,2,0:T(8,128)(2,1)S(1)}, u32[]{:S(2)}, u32[]{:S(2)}) %all-to-all-start.2) | async-done | bytes 1572896 | tf_op jit(solution)/shard_map/all_to_all | solution.py:39
  248.5 4.7 %all-to-all-start.4 = ((bf16[8,48,256]{2,1,0:T(8,128)(2,1)}), bf16[8,48,256]{2,1,0:T(8,128)(2,1)S(1)}, u32[]{:S(2)}, u32[]{:S(2)}) async-start(bf16[8,48,256]{2,1,0:T(8,128)(2,1)} %bitcast.85), calls=%async_computation.4 | async-start | bytes 393216 | tf_op jit(solution)/shard_map/all_to_all | solution.py:39
  253.7 0.8 copy.111
  254.5 14.0 %reduce-scatter.6.cloned.1.call-done = bf16[192,256]{1,0:T(8,128)(2,1)} async-done(((bf16[1536,256]{1,0:T(8,128)(2,1)}), bf16[192,256]{1,0:T(8,128)(2,1)}) %reduce-scatter.6.cloned.1.call-update) | async-done | bytes 98320 | tf_op jit(solution)/shard_map/reduce_scatter | solution.py:70
  268.6 7.1 %all-to-all-start.3 = ((bf16[64,6,256]{2,1,0:T(8,128)(2,1)}), bf16[64,6,256]{2,1,0:T(8,128)(2,1)S(1)}, u32[]{:S(2)}, u32[]{:S(2)}) async-start(bf16[64,6,256]{2,1,0:T(8,128)(2,1)} %bitcast.16), calls=%async_computation.3 | async-start | bytes 524288 | tf_op jit(solution)/shard_map/all_to_all | solution.py:164
  275.7 5.1 %multiply_add_fusion = f32[48,1,128,128]{3,2,1,0:T(8,128)} fusion(f32[48,1,128,128]{3,2,1,0:T(8,128)} %param.24, f32[48,128]{1,0:T(8,128)S(1)} %split.30, f32[48,128]{1,0:T(8,128)S(1)} %get-tuple-element.5, f32[48,128]{1,0:T(8,128)S(1)} %get-tuple-element.4), kind=kLoop, calls=%fused_computation.3 | loop fusion | flops 2359296 | bytes 6365184 | tf_op jit(solution)/shard_map/add | solution.py:128
  280.8 6.5 %all-to-all-done.3 = bf16[64,6,256]{2,1,0:T(8,128)(2,1)S(1)} async-done(((bf16[64,6,256]{2,1,0:T(8,128)(2,1)}), bf16[64,6,256]{2,1,0:T(8,128)(2,1)S(1)}, u32[]{:S(2)}, u32[]{:S(2)}) %all-to-all-start.3) | async-done | bytes 196640 | tf_op jit(solution)/shard_map/all_to_all | solution.py:164
  287.3 5.4 %reduce-scatter.8.cloned.1.call-done = bf16[48,256]{1,0:T(8,128)(2,1)} async-done(((bf16[192,256]{1,0:T(8,128)(2,1)}), bf16[48,256]{1,0:T(8,128)(2,1)}) %reduce-scatter.8.cloned.1.call-update) | async-done | bytes 24592 | tf_op jit(solution)/shard_map/reduce_scatter | solution.py:70
  292.7 1.6 fusion.11
  (73 shorter events, 4.6 us)
Async XLA Ops:
  7.2 209.5 %copy-start = (bf16[2,128,2048]{2,1,0:T(8,128)(2,1)S(1)}, bf16[2,128,2048]{2,1,0:T(8,128)(2,1)}, u32[]{:S(2)}) copy-start(bf16[2,128,2048]{2,1,0:T(8,128)(2,1)} %param.38) | copy-start | bytes 3145732
  7.2 87.1 %copy-start.11 = (f32[128]{0:T(128)S(1)}, f32[128]{0:T(128)}, u32[]{:S(2)}) copy-start(f32[128]{0:T(128)} %param.30) | copy-start | bytes 1540
  7.2 84.8 %all-gather.4.cloned.1.call-start = ((), (), s32[]{:S(2)}) async-start(), calls=%async_computation.9 | async-start | bytes 2162688 | tf_op jit(solution)/shard_map/all_gather | solution.py:19
  94.2 3.7 %copy-start.3 = (bf16[128,2048]{1,0:T(8,128)(2,1)S(1)}, bf16[128,2048]{1,0:T(8,128)(2,1)}, u32[]{:S(2)}) copy-start(bf16[128,2048]{1,0:T(8,128)(2,1)} %param.32) | copy-start | bytes 1572868
  94.2 3.7 %copy-start.12 = (f32[128]{0:T(128)S(1)}, f32[128]{0:T(128)}, u32[]{:S(2)}) copy-start(f32[128]{0:T(128)} %param.31) | copy-start | bytes 1540
  99.5 25.3 %copy-start.2 = (bf16[48,2048]{1,0:T(8,128)(2,1)S(1)}, bf16[48,2048]{1,0:T(8,128)(2,1)}, u32[]{:S(2)}) copy-start(bf16[48,2048]{1,0:T(8,128)(2,1)} %param.23) | copy-start | bytes 589828
  99.5 25.1 %all-to-all-start = ((bf16[8,48,2048]{2,1,0:T(8,128)(2,1)}), bf16[8,48,2048]{2,1,0:T(8,128)(2,1)S(1)}, u32[]{:S(2)}, u32[]{:S(2)}) async-start(bf16[8,48,2048]{2,1,0:T(8,128)(2,1)} %broadcast_in_dim.12), calls=%async_computation | async-start | bytes 3145728 | tf_op jit(solution)/shard_map/all_to_all | solution.py:24
  104.5 20.5 %copy-start.7 = (f32[2048]{0:T(1024)S(1)}, f32[2048]{0:T(1024)}, u32[]{:S(2)}) copy-start(f32[2048]{0:T(1024)} %param.33) | copy-start | bytes 24580
  104.5 79.9 %reduce-scatter.4.cloned.1.call-start = ((), (), s32[]{:S(2)}) async-start(), calls=%async_computation.10 | async-start | bytes 1769472 | tf_op jit(solution)/shard_map/reduce_scatter | solution.py:60
  124.8 29.3 %copy-start.5 = (bf16[256,256]{1,0:T(8,128)(2,1)S(1)}, bf16[256,256]{1,0:T(8,128)(2,1)}, u32[]{:S(2)}) copy-start(bf16[256,256]{1,0:T(8,128)(2,1)} %param.43) | copy-start | bytes 393220
  124.8 29.3 %copy-start.6 = (bf16[256,256]{1,0:T(8,128)(2,1)S(1)}, bf16[256,256]{1,0:T(8,128)(2,1)}, u32[]{:S(2)}) copy-start(bf16[256,256]{1,0:T(8,128)(2,1)} %param.42) | copy-start | bytes 393220
  125.0 0.7 copy-start.1
  154.1 1.8 copy-start.8
  159.6 54.1 %all-to-all-start.1 = ((bf16[64,6,2048]{2,1,0:T(8,128)(2,1)}), bf16[64,6,2048]{2,1,0:T(8,128)(2,1)S(1)}, u32[]{:S(2)}, u32[]{:S(2)}) async-start(bf16[64,6,2048]{2,1,0:T(8,128)(2,1)} %reshape.116), calls=%async_computation.1 | async-start | bytes 4194304 | tf_op jit(solution)/shard_map/all_to_all | solution.py:152
  164.6 63.8 %all-gather.6.cloned.1.call-start = ((), (), s32[]{:S(2)}) async-start(), calls=%async_computation.13 | async-start | bytes 1769472 | tf_op jit(solution)/shard_map/all_gather | solution.py:63
  223.5 25.1 %all-to-all-start.2 = ((bf16[8,32,2,6,256]{4,1,3,2,0:T(8,128)(2,1)}), bf16[8,32,2,6,256]{4,1,3,2,0:T(8,128)(2,1)S(1)}, u32[]{:S(2)}, u32[]{:S(2)}) async-start(bf16[8,32,2,6,256]{4,1,3,2,0:T(8,128)(2,1)} %bitcast.88), calls=%async_computation.2 | async-start | bytes 3145728 | tf_op jit(solution)/shard_map/all_to_all | solution.py:39
  228.4 40.2 %reduce-scatter.6.cloned.1.call-start = ((), (), s32[]{:S(2)}) async-start(), calls=%async_computation.11 | async-start | bytes 884736 | tf_op jit(solution)/shard_map/reduce_scatter | solution.py:70
  230.2 2.4 copy-start.4
  232.7 20.6 %copy-start.10 = (f32[256]{0:T(256)S(1)}, f32[256]{0:T(256)}, u32[]{:S(2)}) copy-start(f32[256]{0:T(256)} %param.45) | copy-start | bytes 3076
  232.7 20.6 %copy-start.9 = (f32[48,4]{0,1:T(4,128)S(1)}, f32[48,4]{0,1:T(4,128)}, u32[]{:S(2)}) copy-start(f32[48,4]{0,1:T(4,128)} %param.35) | copy-start | bytes 2308
  248.5 20.1 %all-to-all-start.4 = ((bf16[8,48,256]{2,1,0:T(8,128)(2,1)}), bf16[8,48,256]{2,1,0:T(8,128)(2,1)S(1)}, u32[]{:S(2)}, u32[]{:S(2)}) async-start(bf16[8,48,256]{2,1,0:T(8,128)(2,1)} %bitcast.85), calls=%async_computation.4 | async-start | bytes 393216 | tf_op jit(solution)/shard_map/all_to_all | solution.py:39
  253.3 39.5 %reduce-scatter.8.cloned.1.call-start = ((), (), s32[]{:S(2)}) async-start(), calls=%async_computation.12 | async-start | bytes 122880 | tf_op jit(solution)/shard_map/reduce_scatter | solution.py:70
  268.6 18.7 %all-to-all-start.3 = ((bf16[64,6,256]{2,1,0:T(8,128)(2,1)}), bf16[64,6,256]{2,1,0:T(8,128)(2,1)S(1)}, u32[]{:S(2)}, u32[]{:S(2)}) async-start(bf16[64,6,256]{2,1,0:T(8,128)(2,1)} %bitcast.16), calls=%async_computation.3 | async-start | bytes 524288 | tf_op jit(solution)/shard_map/all_to_all | solution.py:164
Sparse Core Ops, SparseCore 0:
  11.2 80.7 all-gather.3
  156.0 28.3 reduce-scatter.3
  186.2 27.3 all-gather.5
  232.8 35.6 reduce-scatter.5
  270.9 21.7 reduce-scatter.7
where the time goes:
time: 302 us; the launch traced here: 301 us
  waiting for transfers between devices  190 us (63%)
  blocking collectives  28.3 us (9%)
  starting transfers between devices  26.8 us (9%)
  matrix products  21.1 us (7%)
  between operations  14.1 us (5%)
  other arithmetic  12.1 us (4%)
  local copies, waits for them, and re-layouts  8.57 us (3%)
    all_gather x1, waiting for transfers between devices, side_by_side(): lax.all_gather(both, axis, axis=dim, tiled=True)  81.5 us
    all_to_all x1, waiting for transfers between devices, local(): lax.all_to_all(outgoing, EP, split_axis=0, concat_axis=0, tiled=True)  29.2 us
    all_to_all x1, blocking collectives, from_everyone(): return lax.all_to_all(copies, axis, split_axis=0, concat_axis=0, tiled=True)  28.3 us
    all_to_all x1, waiting for transfers between devices, from_everyone(): return lax.all_to_all(copies, axis, split_axis=0, concat_axis=0, tiled=True)  20.1 us
    reduce_scatter x1, waiting for transfers between devices, total_of(): lax.psum_scatter(padded_to(lines, lax.axis_size(axis)), axis, scatter_dim...  19.8 us
    reduce_scatter x2, waiting for transfers between devices, sum_by_axis(): subtotal = lax.psum_scatter(subtotal, axis, scatter_dimension=0, tiled=True)  19.4 us
    all_to_all x2, waiting for transfers between devices, sum_at_owner(): lax.all_to_all(parts, axis, split_axis=0, concat_axis=0, tiled=True)  13.3 us
    all_to_all x2, starting transfers between devices, sum_at_owner(): lax.all_to_all(parts, axis, split_axis=0, concat_axis=0, tiled=True)  9.7 us
  transfers between devices with their start and end apart: 10, of which 8 were waited for; matrix products, arithmetic and copies ran while one was open for 9% of the time, Pallas kernels for 0%

commit v1 on v0

v1 whole, which is shorter than its diff:
```python
import jax
import jax.numpy as jnp
from jax import lax
from jax.sharding import Mesh
from jax.sharding import PartitionSpec as P

EP = ("z", "x")
TP = ("y", "c")
HUB = ("z", "x", "c")

EPS = 1e-06
BF = jnp.bfloat16
F32 = jnp.float32


def swap(x, axis):
    return lax.all_to_all(x, axis, split_axis=0, concat_axis=0, tiled=True)


def spread(x, axis):
    return swap(jnp.broadcast_to(x, (lax.axis_size(axis), *x.shape)), axis)


def partner(x):
    return lax.ppermute(x, "c", [(0, 1), (1, 0)])


def dot(a, b):
    return jnp.dot(a, b, preferred_element_type=F32)


def local(
    tokens,
    state,
    norm_gain,
    w_query,
    w_forget,
    w_input,
    w_outgate,
    lower_bound,
    head_gain,
    w_output,
    ffn_gain,
    route_ids,
    route_weight,
    expert_gate,
    expert_up,
    expert_down,
    shared_gate,
    shared_up,
    shared_down,
    dense_gate,
    dense_up,
    dense_down,
    dense_mix,
):
    nz, nx, ny, nc = (lax.axis_size(a) for a in ("z", "x", "y", "c"))
    y, c = lax.axis_index("y"), lax.axis_index("c")
    seq, width = tokens.shape
    rows_w, chan = w_query.shape
    head_dim = state.shape[2]
    cols = width // (ny * nc)
    own_at = (y * nc + c) * cols

    joined = jnp.concatenate([w_query, w_forget, w_input, w_outgate], axis=1)
    weights = spread(joined, "z").reshape(nz * rows_w, 4 * chan)
    wide = tokens.astype(F32)
    normed = wide * lax.rsqrt(jnp.mean(wide * wide, axis=-1, keepdims=True) + EPS) * norm_gain
    normed = normed.astype(BF).reshape(seq, nz, nx, rows_w)
    normed = jnp.transpose(normed, (2, 0, 1, 3)).reshape(nx, seq, nz * rows_w)
    mine = swap(normed, "x").reshape(nx * seq, nz * rows_w)
    part = dot(mine, weights).astype(BF).reshape(nx, seq, 4 * chan)
    projected = swap(part, "x").astype(F32).sum(axis=0)
    projected = lax.optimization_barrier(projected.astype(BF)).astype(F32)
    query, forget_pre, values, out_gate = jnp.split(projected, 4, axis=1)

    dense_own = spread(jnp.stack([dense_gate, dense_up, dense_down]), "x")
    dense_other = partner(dense_own)

    def paired(stack, axis):
        keep = lax.dynamic_index_in_dim(stack, c, 0, keepdims=False)
        other = partner(lax.dynamic_index_in_dim(stack, 1 - c, 0, keepdims=False))
        return jnp.concatenate([keep, other], axis=axis)

    gate_w, up_w, down_w = (
        paired(expert_gate, 1),
        paired(expert_up, 1),
        paired(expert_down, 0),
    )

    def side(stack, index):
        picked = stack[:, index]
        return jnp.moveaxis(picked, 0, 1).reshape(picked.shape[1], -1)

    dense_in_w = jnp.concatenate(
        [
            jnp.concatenate([side(s, 0), side(s, 1)], axis=1)
            for s in (dense_own, dense_other)
        ],
        axis=0,
    )
    dense_out_w = jnp.concatenate(
        [s[:, 2].reshape(-1, cols) for s in (dense_own, dense_other)], axis=1
    )

    forget_sig = jax.nn.sigmoid(forget_pre)
    shape = (seq, 1, head_dim)
    decay = (lower_bound + (1.0 - lower_bound) * forget_sig).reshape(shape)
    keygate = ((1.0 - lower_bound) * (1.0 - forget_sig)).reshape(shape)
    new_state = decay[..., None] * state + keygate[..., None] * values.reshape(shape)[:, :, None, :]
    readout = jnp.einsum("bhk,bhkv->bhv", query.reshape(shape), new_state)
    readout = readout * lax.rsqrt(jnp.mean(readout * readout, axis=-1, keepdims=True) + EPS)
    head_out = (readout.reshape(seq, chan) * head_gain * jax.nn.silu(out_gate)).astype(BF)

    head_part = dot(head_out, w_output).astype(BF)
    head_part = jnp.moveaxis(head_part.reshape(seq, ny * nc, cols), 1, 0)
    resid = swap(head_part, TP).astype(F32).sum(axis=0)
    resid = resid + lax.dynamic_slice_in_dim(tokens, own_at, cols, 1).astype(F32)
    own = resid.astype(BF)

    topk = route_ids.shape[1]
    experts = nz * nx * nc
    cap = max(2, 2 * seq * topk // experts)
    flat_ids = route_ids.reshape(-1)
    onehot = (flat_ids[:, None] == jnp.arange(experts, dtype=jnp.int32)[None, :]).astype(jnp.int32)
    rank = jnp.sum((jnp.cumsum(onehot, axis=0) - onehot) * onehot, axis=1)
    slots = 2 * cap
    slot_index = (flat_ids * slots + rank).reshape(seq, topk)
    slot_ids = jnp.arange(experts * slots, dtype=jnp.int32)
    place = slot_ids % slots
    line = (slot_ids // slots) % (nx * nc) * cap + place - cap
    is_dense = place >= cap
    token_ids = jnp.arange(seq, dtype=jnp.int32)
    dense_hits = is_dense[None, :] & (line[None, :] == token_ids[:, None])
    hits = slot_index[:, :, None] == slot_ids[None, None, :]
    routed_hits = jnp.any(hits, axis=1)
    select = (routed_hits | dense_hits).astype(BF)
    half = cols // 2

    def to_lines(rows):
        rows = rows.reshape(experts, slots, 2, half)
        return jnp.transpose(rows, (0, 2, 1, 3)).reshape(experts, 2 * slots, half)

    def from_lines(lines):
        return jnp.transpose(lines.reshape(experts, 2, slots, half), (0, 2, 1, 3)).reshape(
            experts, slots, cols
        )

    outgoing = jnp.einsum("bs,bw->sw", select, own, preferred_element_type=F32).astype(BF)
    arrived = from_lines(swap(to_lines(outgoing), HUB)).reshape(nz * nx, nc, slots, cols)
    arrived_first, arrived_second = arrived[:, 0], arrived[:, 1]
    count = nz * nx * cap

    routed_rows = jnp.concatenate([arrived_first[:, :cap], arrived_second[:, :cap]], axis=2)
    routed_rows = routed_rows.reshape(count, nc * cols)
    other = partner(own)
    shared_rows = jnp.concatenate(
        [jnp.where(c == 0, own, other), jnp.where(c == 0, other, own)], axis=1
    )
    both = jnp.concatenate([routed_rows, shared_rows], axis=0)
    whole = spread(both, "y")
    whole = jnp.moveaxis(whole, 0, 1).reshape(count + seq, width).astype(F32)
    scale = lax.rsqrt(jnp.mean(whole * whole, axis=-1, keepdims=True) + EPS)
    moe_in = (whole * scale * ffn_gain).astype(BF)

    dense_own_rows = jnp.where(c == 0, arrived_first[:, cap:], arrived_second[:, cap:])
    dense_other_rows = jnp.where(c == 0, arrived_second[:, cap:], arrived_first[:, cap:])
    gain_own = lax.dynamic_slice_in_dim(ffn_gain, own_at, cols, 0)
    gain_other = lax.dynamic_slice_in_dim(ffn_gain, (y * nc + 1 - c) * cols, cols, 0)
    dense_rows = jnp.concatenate([dense_own_rows, dense_other_rows], axis=2)
    dense_rows = dense_rows.reshape(count, nc * cols).astype(F32)
    square = jnp.sum(dense_rows * dense_rows, axis=-1, keepdims=True)
    square_high = square.astype(BF)
    square_low = (square - square_high.astype(F32)).astype(BF)
    dense_scaled = (dense_rows * jnp.concatenate([gain_own, gain_other])).astype(BF)
    dense_pre = dot(dense_scaled, dense_in_w).astype(BF)
    lanes = 128
    dense_pre = jnp.concatenate(
        [
            dense_pre,
            jnp.broadcast_to(square_high, (count, lanes // 2)),
            jnp.broadcast_to(square_low, (count, lanes // 2)),
        ],
        axis=1,
    )
    dense_pre = swap(dense_pre.reshape(ny, count // ny, -1), "y").astype(F32).sum(axis=0)
    hidden_width = dense_in_w.shape[1] // 2
    total = dense_pre[:, 2 * hidden_width] + dense_pre[:, 2 * hidden_width + lanes // 2]
    dense_scale = lax.rsqrt(total / width + EPS)[:, None]
    dense_gate_pre = dense_pre[:, :hidden_width] * dense_scale
    dense_up_pre = dense_pre[:, hidden_width : 2 * hidden_width] * dense_scale
    dense_hidden = (jax.nn.silu(dense_gate_pre) * dense_up_pre).astype(BF)
    dense_hidden = spread(dense_hidden, "y").reshape(count, hidden_width)
    dense_part = dot(dense_hidden, dense_out_w).astype(BF).reshape(nz * nx, cap, nc, cols)
    dense_first = jnp.where(c == 0, dense_part[:, :, 0], dense_part[:, :, 1])
    dense_second = jnp.where(c == 0, dense_part[:, :, 1], dense_part[:, :, 0])

    routed_in, shared_in = moe_in[:count], moe_in[count:]
    hidden = (jax.nn.silu(dot(routed_in, gate_w)) * dot(routed_in, up_w)).astype(BF)
    expert_part = dot(hidden, down_w).astype(BF)
    shared_hidden = (
        jax.nn.silu(dot(shared_in, shared_gate)) * dot(shared_in, shared_up)
    ).astype(BF)
    shared_part = dot(shared_hidden, shared_down).astype(BF)
    parts = jnp.concatenate([expert_part, shared_part], axis=0)
    parts = jnp.moveaxis(parts.reshape(count + seq, ny, nc * cols), 1, 0)
    summed = swap(parts, "y").astype(F32).sum(axis=0)
    expert_out = summed[:count].astype(BF).reshape(nz * nx, cap, nc, cols)
    shared_sum = summed[count:]
    shared_own = jnp.where(c == 0, shared_sum[:, :cols], shared_sum[:, cols:])
    shared_send = jnp.where(c == 0, shared_sum[:, cols:], shared_sum[:, :cols])
    shared_out = shared_own + partner(shared_send.astype(BF)).astype(F32)

    first = jnp.concatenate([expert_out[:, :, 0], dense_first], axis=1)
    second = jnp.concatenate([expert_out[:, :, 1], dense_second], axis=1)
    back = jnp.stack([first, second], axis=1).reshape(experts * slots, cols)
    results = from_lines(swap(to_lines(back), HUB)).reshape(experts * slots, cols)
    combine = jnp.sum(jnp.where(hits, route_weight[:, :, None], F32(0.0)), axis=1)
    routed = dot(combine.astype(BF), results)
    dense_out = dot(dense_hits.astype(BF), results)
    mixed = (resid + routed + shared_out + jax.nn.sigmoid(dense_mix) * dense_out).astype(BF)
    return (mixed, new_state)


def solution(mesh):
    torus = Mesh(mesh.devices.reshape(8, 4, 4, 2), ("z", "x", "y", "c"))
    return jax.shard_map(
        local,
        mesh=torus,
        in_specs=(
            P(EP, None),
            P(EP, TP, None, None),
            P(),
            P(EP, TP),
            P(EP, TP),
            P(EP, TP),
            P(EP, TP),
            P(TP),
            P(TP),
            P(TP, None),
            P(),
            P(EP, None),
            P(EP, None),
            P(EP, None, TP),
            P(EP, None, TP),
            P(EP, TP, None),
            P(None, TP),
            P(None, TP),
            P(TP, None),
            P(TP, EP),
            P(TP, EP),
            P(EP, TP),
            P(TP),
        ),
        out_specs=(P(EP, TP), P(EP, TP, None, None)),
        check_vma=False,
    )
```

time: 302 us -> 217 us (0.72)
  waiting for transfers between devices: 190 us -> 89.3 us
  starting transfers between devices: 26.8 us -> 58.2 us
  blocking collectives: 28.3 us -> 0 us
  local copies, waits for them, and re-layouts: 8.57 us -> 33.4 us
  between operations: 14.1 us -> 1.55 us
  matrix products: 21.1 us -> 17.2 us
    all_gather x2 -> x0, waiting for transfers between devices: 81.5 us -> none  [the longest x1 81.5 us: side_by_side(): lax.all_gather(both, axis, axis=dim, tiled=True)]
    reduce_scatter x3 -> x0, waiting for transfers between devices: 39.2 us -> none  [the longest x1 19.8 us: total_of(): lax.psum_scatter(padded_to(lines, lax.axis_size(axis)), axis, scatter_dim...]
    all_to_all x5 -> x11, starting transfers between devices: 26.7 us -> 56.9 us  [swap(): return lax.all_to_all(x, axis, split_axis=0, concat_axis=0, tiled=True)]
    all_to_all x1 -> x0, blocking collectives: 28.3 us -> none  [from_everyone(): return lax.all_to_all(copies, axis, split_axis=0, concat_axis=0, tiled=True)]
    all_to_all x5 -> x11, waiting for transfers between devices: 69.1 us -> 89.3 us  [swap(): return lax.all_to_all(x, axis, split_axis=0, concat_axis=0, tiled=True)]
    slice x1 -> x9, local copies, waits for them, and re-layouts: 0.18 us -> 7.94 us  [the longest x3 5.29 us: local(): s[:, 2].reshape(-1, cols)]
    dot_general x10 -> x11, matrix products: 17.7 us -> 13.8 us  [the longest x10 12.8 us: dot(): return jnp.dot(a, b, preferred_element_type=F32)]
    unnamed x27 -> x69, local copies, waits for them, and re-layouts: 0.77 us -> 4.5 us
  transfers between devices with their start and end apart: 10 -> 17, of which waited for: 8 -> 11; matrix products, arithmetic and copies ran while one was open for 9% -> 20% of each run, Pallas kernels for 0% -> 0%
where the time goes in v1:
time: 217 us; the launch traced here: 213 us
  waiting for transfers between devices  89.3 us (41%)
  starting transfers between devices  58.2 us (27%)
  local copies, waits for them, and re-layouts  33.4 us (15%)
  matrix products  17.2 us (8%)
  other arithmetic  13.7 us (6%)
    all_to_all x11, waiting for transfers between devices, swap(): return lax.all_to_all(x, axis, split_axis=0, concat_axis=0, tiled=True)  89.3 us
    all_to_all x11, starting transfers between devices, swap(): return lax.all_to_all(x, axis, split_axis=0, concat_axis=0, tiled=True)  56.9 us
    dot_general x10, matrix products, dot(): return jnp.dot(a, b, preferred_element_type=F32)  12.8 us
    slice x3, local copies, waits for them, and re-layouts, local(): s[:, 2].reshape(-1, cols)  5.29 us
    add x1, other arithmetic, local(): decay[..., None] * state  5.07 us
    unnamed x69, local copies, waits for them, and re-layouts  4.5 us
  transfers between devices with their start and end apart: 17, of which 11 were waited for; matrix products, arithmetic and copies ran while one was open for 20% of the time, Pallas kernels for 0%

profile of v1, /device:TPU:8, one launch (start us, length us, event | category | flops | bytes accessed | tf_op | source)
XLA Modules:
  0.0 213.4 jit_solution(339402540370744096)
XLA Ops:
  4.3 4.4 %all-to-all-start = ((bf16[4,48,512]{2,1,0:T(8,128)(2,1)}), bf16[4,48,512]{2,1,0:T(8,128)(2,1)S(1)}, u32[]{:S(2)}, u32[]{:S(2)}) async-start(bf16[4,48,512]{2,1,0:T(8,128)(2,1)} %reshape.214), calls=%async_computation | async-start | bytes 393216 | tf_op jit(solution)/shard_map/all_to_all | solution.py:17
  9.0 6.1 %all-to-all-done = bf16[4,48,512]{2,1,0:T(8,128)(2,1)S(1)} async-done(((bf16[4,48,512]{2,1,0:T(8,128)(2,1)}), bf16[4,48,512]{2,1,0:T(8,128)(2,1)S(1)}, u32[]{:S(2)}, u32[]{:S(2)}) %all-to-all-start) | async-done | bytes 196640 | tf_op jit(solution)/shard_map/all_to_all | solution.py:17
  15.9 8.5 %all-to-all-start.1 = ((bf16[8,64,512]{2,1,0:T(8,128)(2,1)}), bf16[8,64,512]{2,1,0:T(8,128)(2,1)S(1)}, u32[]{:S(2)}, u32[]{:S(2)}) async-start(bf16[8,64,512]{2,1,0:T(8,128)(2,1)} %broadcast_in_dim.20), calls=%async_computation.1 | async-start | bytes 1048576 | tf_op jit(solution)/shard_map/all_to_all | solution.py:17
  25.5 14.9 %all-to-all-done.1 = bf16[8,64,512]{2,1,0:T(8,128)(2,1)S(1)} async-done(((bf16[8,64,512]{2,1,0:T(8,128)(2,1)}), bf16[8,64,512]{2,1,0:T(8,128)(2,1)S(1)}, u32[]{:S(2)}, u32[]{:S(2)}) %all-to-all-start.1) | async-done | bytes 524320 | tf_op jit(solution)/shard_map/all_to_all | solution.py:17
  41.4 3.5 %all-to-all-start.2 = ((bf16[4,48,512]{2,1,0:T(8,128)(2,1)}), bf16[4,48,512]{2,1,0:T(8,128)(2,1)S(1)}, u32[]{:S(2)}, u32[]{:S(2)}) async-start(bf16[4,48,512]{2,1,0:T(8,128)(2,1)} %bitcast.3), calls=%async_computation.2 | async-start | bytes 393216 | tf_op jit(solution)/shard_map/all_to_all | solution.py:17
  44.9 6.2 %all-to-all-done.2 = bf16[4,48,512]{2,1,0:T(8,128)(2,1)S(1)} async-done(((bf16[4,48,512]{2,1,0:T(8,128)(2,1)}), bf16[4,48,512]{2,1,0:T(8,128)(2,1)S(1)}, u32[]{:S(2)}, u32[]{:S(2)}) %all-to-all-start.2) | async-done | bytes 196640 | tf_op jit(solution)/shard_map/all_to_all | solution.py:17
  51.3 3.4 %fusion = f32[48,1,128]{2,1,0:T(1,128)S(1)} fusion(bf16[48,128,1]{1,0,2:T(8,128)(2,1)S(1)} %slice_bitcast_fusion, f32[48,128]{1,0:T(8,128)S(1)} %split.18, f32[48,128]{1,0:T(8,128)S(1)} %get-tuple-element.28, f32[48,1,128,128]{3,2,1,0:T(8,128)} %param.24, f32[48,128]{1,0:T(8,128)S(1)} %get-tuple-element.27), kind=kOutput, calls=%fused_computation | convolution fusion | flops 3932160 | bytes 3256320 | tf_op jit(solution)/shard_map/bhk,bhkv->bhv/dot_general | solution.py:111
  55.8 4.9 %all-to-all-start.3 = ((bf16[8,48,256]{2,1,0:T(8,128)(2,1)}), bf16[8,48,256]{2,1,0:T(8,128)(2,1)S(1)}, u32[]{:S(2)}, u32[]{:S(2)}) async-start(bf16[8,48,256]{2,1,0:T(8,128)(2,1)} %bitcast.141), calls=%async_computation.3 | async-start | bytes 393216 | tf_op jit(solution)/shard_map/all_to_all | solution.py:17
  60.9 5.2 %all-to-all-done.3 = bf16[8,48,256]{2,1,0:T(8,128)(2,1)S(1)} async-done(((bf16[8,48,256]{2,1,0:T(8,128)(2,1)}), bf16[8,48,256]{2,1,0:T(8,128)(2,1)S(1)}, u32[]{:S(2)}, u32[]{:S(2)}) %all-to-all-start.3) | async-done | bytes 196640 | tf_op jit(solution)/shard_map/all_to_all | solution.py:17
  70.3 4.6 %all-to-all-start.4 = ((bf16[64,24,128]{2,1,0:T(8,128)(2,1)}), bf16[64,24,128]{2,1,0:T(8,128)(2,1)S(1)}, u32[]{:S(2)}, u32[]{:S(2)}) async-start(bf16[64,24,128]{2,1,0:T(8,128)(2,1)} %copy.203), calls=%async_computation.4 | async-start | bytes 786432 | tf_op jit(solution)/shard_map/all_to_all | solution.py:17
  79.6 10.3 %all-to-all-done.4 = bf16[64,24,128]{2,1,0:T(8,128)(2,1)S(1)} async-done(((bf16[64,24,128]{2,1,0:T(8,128)(2,1)}), bf16[64,24,128]{2,1,0:T(8,128)(2,1)S(1)}, u32[]{:S(2)}, u32[]{:S(2)}) %all-to-all-start.4) | async-done | bytes 393248 | tf_op jit(solution)/shard_map/all_to_all | solution.py:17
  91.2 4.1 %all-to-all-start.7 = ((bf16[4,3,256,256]{2,3,1,0:T(8,128)(2,1)}), bf16[4,3,256,256]{2,3,1,0:T(8,128)(2,1)S(1)}, u32[]{:S(2)}, u32[]{:S(2)}) async-start(bf16[4,3,256,256]{2,3,1,0:T(8,128)(2,1)} %broadcast_in_dim.24), calls=%async_computation.7 | async-start | bytes 3145728 | tf_op jit(solution)/shard_map/all_to_all | solution.py:17
  98.0 18.2 %all-to-all-done.7 = bf16[4,3,256,256]{2,3,1,0:T(8,128)(2,1)S(1)} async-done(((bf16[4,3,256,256]{2,3,1,0:T(8,128)(2,1)}), bf16[4,3,256,256]{2,3,1,0:T(8,128)(2,1)S(1)}, u32[]{:S(2)}, u32[]{:S(2)}) %all-to-all-start.7) | async-done | bytes 1572896 | tf_op jit(solution)/shard_map/all_to_all | solution.py:17
  117.3 4.9 %all-to-all-start.5 = ((bf16[4,240,512]{2,1,0:T(8,128)(2,1)}), bf16[4,240,512]{2,1,0:T(8,128)(2,1)S(1)}, u32[]{:S(2)}, u32[]{:S(2)}) async-start(bf16[4,240,512]{2,1,0:T(8,128)(2,1)} %broadcast_in_dim.23), calls=%async_computation.5 | async-start | bytes 1966080 | tf_op jit(solution)/shard_map/all_to_all | solution.py:17
  125.7 1.9 reshape.239
  127.9 6.6 %all-to-all-done.5 = bf16[4,240,512]{2,1,0:T(8,128)(2,1)S(1)} async-done(((bf16[4,240,512]{2,1,0:T(8,128)(2,1)}), bf16[4,240,512]{2,1,0:T(8,128)(2,1)S(1)}, u32[]{:S(2)}, u32[]{:S(2)}) %all-to-all-start.5) | async-done | bytes 983072 | tf_op jit(solution)/shard_map/all_to_all | solution.py:17
  136.2 1.7 convolution_convert_fusion.2
  138.0 2.4 %fusion.103 = (bf16[4,1,256,256]{2,3,0,1:T(8,128)(2,1)}, bf16[4,1,256,256]{2,3,0,1:T(8,128)(2,1)S(1)}, bf16[4,1,256,256]{2,3,0,1:T(8,128)(2,1)S(1)}) fusion(bf16[4,3,256,256]{2,3,0,1:T(8,128)(2,1)} %collective-permute-done.4), kind=kLoop, calls=%fused_computation.176 | loop fusion | bytes 3145728 | tf_op jit(solution)/shard_map/slice | solution.py:103
  142.5 4.9 %all-to-all-start.8 = ((bf16[4,48,2176]{2,1,0:T(8,128)(2,1)}), bf16[4,48,2176]{2,1,0:T(8,128)(2,1)S(1)}, u32[]{:S(2)}, u32[]{:S(2)}) async-start(bf16[4,48,2176]{2,1,0:T(8,128)(2,1)} %bitcast.147), calls=%async_computation.8 | async-start | bytes 1671168 | tf_op jit(solution)/shard_map/all_to_all | solution.py:17
  147.5 1.8 fusion.11
  149.3 3.7 %convolution_convert_fusion.1 = bf16[192,2048]{1,0:T(8,128)(2,1)} fusion(bf16[128,2048]{1,0:T(8,128)(2,1)} %collective-permute-done.3, bf16[128,2048]{1,0:T(8,128)(2,1)} %get-tuple-element.13, f32[192,256]{1,0:T(8,128)S(1)} %fusion.11, bf16[2048,128]{1,0:T(8,128)(2,1)} %collective-permute-done.2, bf16[2048,128]{1,0:T(8,128)(2,1)} %get-tuple-element.9, ...), kind=kOutput, calls=%fused_computation.4 | convolution fusion | flops 407535616 | bytes 3866624 | tf_op jit(solution)/shard_map/dot_general | solution.py:29
  155.2 2.1 all-to-all-done.8
  158.2 4.9 %all-to-all-start.6 = ((bf16[4,240,512]{2,1,0:T(8,128)(2,1)}), bf16[4,240,512]{2,1,0:T(8,128)(2,1)S(1)}, u32[]{:S(2)}, u32[]{:S(2)}) async-start(bf16[4,240,512]{2,1,0:T(8,128)(2,1)} %bitcast.145), calls=%async_computation.6 | async-start | bytes 1966080 | tf_op jit(solution)/shard_map/all_to_all | solution.py:17
  164.0 2.1 %copy.231 = bf16[4,1,256,256]{3,2,0,1:T(8,128)(2,1)} copy(bf16[4,1,256,256]{2,3,1,0:T(8,128)(2,1)} %slice.142) | data formatting | bytes 1048576
  166.1 2.1 copy.217
  168.7 4.7 %all-to-all-done.6 = bf16[4,240,512]{2,1,0:T(8,128)(2,1)S(1)} async-done(((bf16[4,240,512]{2,1,0:T(8,128)(2,1)}), bf16[4,240,512]{2,1,0:T(8,128)(2,1)S(1)}, u32[]{:S(2)}, u32[]{:S(2)}) %all-to-all-start.6) | async-done | bytes 983072 | tf_op jit(solution)/shard_map/all_to_all | solution.py:17
  174.2 4.9 %all-to-all-start.9 = ((bf16[4,48,1024]{2,1,0:T(8,128)(2,1)}), bf16[4,48,1024]{2,1,0:T(8,128)(2,1)S(1)}, u32[]{:S(2)}, u32[]{:S(2)}) async-start(bf16[4,48,1024]{2,1,0:T(8,128)(2,1)} %broadcast_in_dim.27), calls=%async_computation.9 | async-start | bytes 786432 | tf_op jit(solution)/shard_map/all_to_all | solution.py:17
  179.6 5.4 %all-to-all-done.9 = bf16[4,48,1024]{2,1,0:T(8,128)(2,1)S(1)} async-done(((bf16[4,48,1024]{2,1,0:T(8,128)(2,1)}), bf16[4,48,1024]{2,1,0:T(8,128)(2,1)S(1)}, u32[]{:S(2)}, u32[]{:S(2)}) %all-to-all-start.9) | async-done | bytes 393248 | tf_op jit(solution)/shard_map/all_to_all | solution.py:17
  185.0 1.6 convolution_convert_fusion.5
  188.9 7.2 %all-to-all-start.10 = ((bf16[64,24,128]{2,1,0:T(8,128)(2,1)}), bf16[64,24,128]{2,1,0:T(8,128)(2,1)S(1)}, u32[]{:S(2)}, u32[]{:S(2)}) async-start(bf16[64,24,128]{2,1,0:T(8,128)(2,1)} %copy.223), calls=%async_computation.10 | async-start | bytes 786432 | tf_op jit(solution)/shard_map/all_to_all | solution.py:17
  196.3 5.1 %multiply_add_fusion = f32[48,1,128,128]{3,2,1,0:T(8,128)} fusion(f32[48,1,128,128]{3,2,1,0:T(8,128)} %param.24, f32[48,128]{1,0:T(8,128)S(1)} %copy-done.14, f32[48,128]{1,0:T(8,128)S(1)} %copy-done.18, f32[48,128]{1,0:T(8,128)S(1)} %copy-done.16), kind=kLoop, calls=%fused_computation.2 | loop fusion | flops 2359296 | bytes 6365184 | tf_op jit(solution)/shard_map/add | solution.py:110
  201.5 9.5 %all-to-all-done.10 = bf16[64,24,128]{2,1,0:T(8,128)(2,1)S(1)} async-done(((bf16[64,24,128]{2,1,0:T(8,128)(2,1)}), bf16[64,24,128]{2,1,0:T(8,128)(2,1)S(1)}, u32[]{:S(2)}, u32[]{:S(2)}) %all-to-all-start.10) | async-done | bytes 393248 | tf_op jit(solution)/shard_map/all_to_all | solution.py:17
  (185 shorter events, 39.9 us)
Async XLA Ops:
  0.6 54.2 %copy-start = (bf16[128,2048]{1,0:T(8,128)(2,1)S(1)}, bf16[128,2048]{1,0:T(8,128)(2,1)}, u32[]{:S(2)}) copy-start(bf16[128,2048]{1,0:T(8,128)(2,1)} %param.32) | copy-start | bytes 1572868
  0.6 8.1 %copy-start.27 = (s32[48,4]{0,1:T(4,128)S(1)}, s32[48,4]{0,1:T(4,128)}, u32[]{:S(2)}) copy-start(s32[48,4]{0,1:T(4,128)} %param.34) | copy-start | bytes 2308
  0.7 8.3 %copy-start.22 = (bf16[64,128]{1,0:T(8,128)(2,1)S(1)}, bf16[64,128]{1,0:T(8,128)(2,1)}, u32[]{:S(2)}) copy-start(bf16[64,128]{1,0:T(8,128)(2,1)} %param.29) | copy-start | bytes 49156
  0.7 8.3 %copy-start.23 = (bf16[64,128]{1,0:T(8,128)(2,1)S(1)}, bf16[64,128]{1,0:T(8,128)(2,1)}, u32[]{:S(2)}) copy-start(bf16[64,128]{1,0:T(8,128)(2,1)} %param.28) | copy-start | bytes 49156
  0.7 8.3 %copy-start.24 = (bf16[64,128]{1,0:T(8,128)(2,1)S(1)}, bf16[64,128]{1,0:T(8,128)(2,1)}, u32[]{:S(2)}) copy-start(bf16[64,128]{1,0:T(8,128)(2,1)} %param.27) | copy-start | bytes 49156
  0.7 8.3 %copy-start.25 = (bf16[64,128]{1,0:T(8,128)(2,1)S(1)}, bf16[64,128]{1,0:T(8,128)(2,1)}, u32[]{:S(2)}) copy-start(bf16[64,128]{1,0:T(8,128)(2,1)} %param.26) | copy-start | bytes 49156
  4.3 40.6 %copy-start.30 = (f32[128]{0:T(128)S(1)}, f32[128]{0:T(128)}, u32[]{:S(2)}) copy-start(f32[128]{0:T(128)} %param.30) | copy-start | bytes 1540
  4.3 10.8 %all-to-all-start = ((bf16[4,48,512]{2,1,0:T(8,128)(2,1)}), bf16[4,48,512]{2,1,0:T(8,128)(2,1)S(1)}, u32[]{:S(2)}, u32[]{:S(2)}) async-start(bf16[4,48,512]{2,1,0:T(8,128)(2,1)} %reshape.214), calls=%async_computation | async-start | bytes 393216 | tf_op jit(solution)/shard_map/all_to_all | solution.py:17
  15.9 24.5 %all-to-all-start.1 = ((bf16[8,64,512]{2,1,0:T(8,128)(2,1)}), bf16[8,64,512]{2,1,0:T(8,128)(2,1)S(1)}, u32[]{:S(2)}, u32[]{:S(2)}) async-start(bf16[8,64,512]{2,1,0:T(8,128)(2,1)} %broadcast_in_dim.20), calls=%async_computation.1 | async-start | bytes 1048576 | tf_op jit(solution)/shard_map/all_to_all | solution.py:17
  41.4 13.5 %copy-start.31 = (f32[128]{0:T(128)S(1)}, f32[128]{0:T(128)}, u32[]{:S(2)}) copy-start(f32[128]{0:T(128)} %param.31) | copy-start | bytes 1540
  41.4 9.8 %all-to-all-start.2 = ((bf16[4,48,512]{2,1,0:T(8,128)(2,1)}), bf16[4,48,512]{2,1,0:T(8,128)(2,1)S(1)}, u32[]{:S(2)}, u32[]{:S(2)}) async-start(bf16[4,48,512]{2,1,0:T(8,128)(2,1)} %bitcast.3), calls=%async_computation.2 | async-start | bytes 393216 | tf_op jit(solution)/shard_map/all_to_all | solution.py:17
  55.8 10.3 %all-to-all-start.3 = ((bf16[8,48,256]{2,1,0:T(8,128)(2,1)}), bf16[8,48,256]{2,1,0:T(8,128)(2,1)S(1)}, u32[]{:S(2)}, u32[]{:S(2)}) async-start(bf16[8,48,256]{2,1,0:T(8,128)(2,1)} %bitcast.141), calls=%async_computation.3 | async-start | bytes 393216 | tf_op jit(solution)/shard_map/all_to_all | solution.py:17
  60.7 14.2 %copy-start.4 = (bf16[2,128,2048]{2,1,0:T(8,128)(2,1)S(1)}, bf16[2,128,2048]{2,1,0:T(8,128)(2,1)}, u32[]{:S(2)}) copy-start(bf16[2,128,2048]{2,1,0:T(8,128)(2,1)} %param.38) | copy-start | bytes 3145732
  70.3 19.6 %all-to-all-start.4 = ((bf16[64,24,128]{2,1,0:T(8,128)(2,1)}), bf16[64,24,128]{2,1,0:T(8,128)(2,1)S(1)}, u32[]{:S(2)}, u32[]{:S(2)}) async-start(bf16[64,24,128]{2,1,0:T(8,128)(2,1)} %copy.203), calls=%async_computation.4 | async-start | bytes 786432 | tf_op jit(solution)/shard_map/all_to_all | solution.py:17
  76.1 73.2 %collective-permute-start.3 = (bf16[128,2048]{1,0:T(8,128)(2,1)}, bf16[128,2048]{1,0:T(8,128)(2,1)}, u32[]{:S(2)}, u32[]{:S(2)}) collective-permute-start(bf16[128,2048]{1,0:T(8,128)(2,1)} %get-tuple-element.14), channel_id=1, source_target_pairs={{0,1},{1,0},{2,3},{3,2},{4,5},{5,4},{6,7},{7,6},{8,9},{9,8},{10,11... | collective-permute-start | bytes 1572872 | tf_op jit(solution)/shard_map/ppermute | solution.py:25
  77.2 70.2 %collective-permute-start.1 = (bf16[2048,128]{1,0:T(8,128)(2,1)}, bf16[2048,128]{1,0:T(8,128)(2,1)}, u32[]{:S(2)}, u32[]{:S(2)}) collective-permute-start(bf16[2048,128]{1,0:T(8,128)(2,1)} %get-tuple-element.12), channel_id=1, source_target_pairs={{0,1},{1,0},{2,3},{3,2},{4,5},{5,4},{6,7},{7,6},{8,9},{9,8},{10,11... | collective-permute-start | bytes 1572872 | tf_op jit(solution)/shard_map/ppermute | solution.py:25
  78.7 70.6 %collective-permute-start.2 = (bf16[2048,128]{1,0:T(8,128)(2,1)}, bf16[2048,128]{1,0:T(8,128)(2,1)}, u32[]{:S(2)}, u32[]{:S(2)}) collective-permute-start(bf16[2048,128]{1,0:T(8,128)(2,1)} %get-tuple-element.10), channel_id=1, source_target_pairs={{0,1},{1,0},{2,3},{3,2},{4,5},{5,4},{6,7},{7,6},{8,9},{9,8},{10,11... | collective-permute-start | bytes 1572872 | tf_op jit(solution)/shard_map/ppermute | solution.py:25
  78.8 16.5 %collective-permute-start = (bf16[48,256]{1,0:T(8,128)(2,1)}, bf16[48,256]{1,0:T(8,128)(2,1)S(1)}, u32[]{:S(2)}, u32[]{:S(2)}) collective-permute-start(bf16[48,256]{1,0:T(8,128)(2,1)} %fusion.62), channel_id=1, source_target_pairs={{0,1},{1,0},{2,3},{3,2},{4,5},{5,4},{6,7},{7,6},{8,9},{9,8},{10,11... | collective-permute-start | bytes 73736 | tf_op jit(solution)/shard_map/ppermute | solution.py:25
  91.2 25.0 %all-to-all-start.7 = ((bf16[4,3,256,256]{2,3,1,0:T(8,128)(2,1)}), bf16[4,3,256,256]{2,3,1,0:T(8,128)(2,1)S(1)}, u32[]{:S(2)}, u32[]{:S(2)}) async-start(bf16[4,3,256,256]{2,3,1,0:T(8,128)(2,1)} %broadcast_in_dim.24), calls=%async_computation.7 | async-start | bytes 3145728 | tf_op jit(solution)/shard_map/all_to_all | solution.py:17
  117.3 17.2 %all-to-all-start.5 = ((bf16[4,240,512]{2,1,0:T(8,128)(2,1)}), bf16[4,240,512]{2,1,0:T(8,128)(2,1)S(1)}, u32[]{:S(2)}, u32[]{:S(2)}) async-start(bf16[4,240,512]{2,1,0:T(8,128)(2,1)} %broadcast_in_dim.23), calls=%async_computation.5 | async-start | bytes 1966080 | tf_op jit(solution)/shard_map/all_to_all | solution.py:17
  123.5 14.5 %collective-permute-start.4 = (bf16[4,3,256,256]{2,3,0,1:T(8,128)(2,1)}, bf16[4,3,256,256]{2,3,0,1:T(8,128)(2,1)}, u32[]{:S(2)}, u32[]{:S(2)}) collective-permute-start(bf16[4,3,256,256]{2,3,0,1:T(8,128)(2,1)} %copy.212), channel_id=1, source_target_pairs={{0,1},{1,0},{2,3},{3,2},{4,5},{5,4},{6,7},{7,6},{8,9},{9,8},{10,11... | collective-permute-start | bytes 4718600 | tf_op jit(solution)/shard_map/ppermute | solution.py:25
  142.5 14.8 %all-to-all-start.8 = ((bf16[4,48,2176]{2,1,0:T(8,128)(2,1)}), bf16[4,48,2176]{2,1,0:T(8,128)(2,1)S(1)}, u32[]{:S(2)}, u32[]{:S(2)}) async-start(bf16[4,48,2176]{2,1,0:T(8,128)(2,1)} %bitcast.147), calls=%async_computation.8 | async-start | bytes 1671168 | tf_op jit(solution)/shard_map/all_to_all | solution.py:17
  158.2 15.2 %all-to-all-start.6 = ((bf16[4,240,512]{2,1,0:T(8,128)(2,1)}), bf16[4,240,512]{2,1,0:T(8,128)(2,1)S(1)}, u32[]{:S(2)}, u32[]{:S(2)}) async-start(bf16[4,240,512]{2,1,0:T(8,128)(2,1)} %bitcast.145), calls=%async_computation.6 | async-start | bytes 1966080 | tf_op jit(solution)/shard_map/all_to_all | solution.py:17
  174.2 10.8 %all-to-all-start.9 = ((bf16[4,48,1024]{2,1,0:T(8,128)(2,1)}), bf16[4,48,1024]{2,1,0:T(8,128)(2,1)S(1)}, u32[]{:S(2)}, u32[]{:S(2)}) async-start(bf16[4,48,1024]{2,1,0:T(8,128)(2,1)} %broadcast_in_dim.27), calls=%async_computation.9 | async-start | bytes 786432 | tf_op jit(solution)/shard_map/all_to_all | solution.py:17
  187.1 9.0 %copy-start.29 = (f32[256]{0:T(256)S(1)}, f32[256]{0:T(256)}, u32[]{:S(2)}) copy-start(f32[256]{0:T(256)} %param.45) | copy-start | bytes 3076
  187.1 9.1 %copy-start.28 = (f32[48,4]{0,1:T(4,128)S(1)}, f32[48,4]{0,1:T(4,128)}, u32[]{:S(2)}) copy-start(f32[48,4]{0,1:T(4,128)} %param.35) | copy-start | bytes 2308
  187.1 9.2 %copy-start.14 = (f32[48,128]{1,0:T(8,128)S(1)}, f32[48,128]{1,0:T(8,128)}, u32[]{:S(2)}) copy-start(f32[48,128]{1,0:T(8,128)} %copy-done.13) | copy-start | bytes 73732
  187.1 9.2 %copy-start.16 = (f32[48,128]{1,0:T(8,128)S(1)}, f32[48,128]{1,0:T(8,128)}, u32[]{:S(2)}) copy-start(f32[48,128]{1,0:T(8,128)} %copy-done.15) | copy-start | bytes 73732
  187.1 9.2 %copy-start.18 = (f32[48,128]{1,0:T(8,128)S(1)}, f32[48,128]{1,0:T(8,128)}, u32[]{:S(2)}) copy-start(f32[48,128]{1,0:T(8,128)} %copy-done.17) | copy-start | bytes 73732
  188.9 22.2 %all-to-all-start.10 = ((bf16[64,24,128]{2,1,0:T(8,128)(2,1)}), bf16[64,24,128]{2,1,0:T(8,128)(2,1)S(1)}, u32[]{:S(2)}, u32[]{:S(2)}) async-start(bf16[64,24,128]{2,1,0:T(8,128)(2,1)} %copy.223), calls=%async_computation.10 | async-start | bytes 786432 | tf_op jit(solution)/shard_map/all_to_all | solution.py:17
  201.4 10.4 %copy-start.11 = (f32[48,256]{1,0:T(8,128)S(1)}, f32[48,256]{1,0:T(8,128)}, u32[]{:S(2)}) copy-start(f32[48,256]{1,0:T(8,128)} %copy-done.10) | copy-start | bytes 147460
  201.4 10.4 %collective-permute-start.5 = (bf16[48,256]{1,0:T(8,128)(2,1)S(1)}, bf16[48,256]{1,0:T(8,128)(2,1)S(1)}, u32[]{:S(2)}, u32[]{:S(2)}) collective-permute-start(bf16[48,256]{1,0:T(8,128)(2,1)S(1)} %select_convert_fusion), channel_id=1, source_target_pairs={{0,1},{1,0},{2,3},{3,2},{4,5},{5,4},{6,7},{7,6},{8,9},{9,8},{10,11... | collective-permute-start | bytes 73736 | tf_op jit(solution)/shard_map/ppermute | solution.py:25
  (17 other events, 53.0 us)

commit v2 on v1

--- a/solution.py
+++ b/solution.py
@@ -8,6 +8,7 @@
 TP = ("y", "c")
 HUB = ("z", "x", "c")
 
+
 EPS = 1e-06
 BF = jnp.bfloat16
 F32 = jnp.float32
@@ -25,11 +26,20 @@
     return lax.ppermute(x, "c", [(0, 1), (1, 0)])
 
 
+def shift(x, axis, by):
+    size = lax.axis_size(axis)
+    return lax.ppermute(x, axis, [(i, (i + by) % size) for i in range(size)])
+
+
+def pick(x, index):
+    return lax.dynamic_index_in_dim(x, index, 0, keepdims=False)
+
+
 def dot(a, b):
     return jnp.dot(a, b, preferred_element_type=F32)
 
 
-def local(
+def step(
     tokens,
     state,
     norm_gain,
@@ -55,7 +65,7 @@
     dense_mix,
 ):
     nz, nx, ny, nc = (lax.axis_size(a) for a in ("z", "x", "y", "c"))
-    y, c = lax.axis_index("y"), lax.axis_index("c")
+    x, y, c = (lax.axis_index(a) for a in ("x", "y", "c"))
     seq, width = tokens.shape
     rows_w, chan = w_query.shape
     head_dim = state.shape[2]
@@ -68,13 +78,17 @@
     normed = wide * lax.rsqrt(jnp.mean(wide * wide, axis=-1, keepdims=True) + EPS) * norm_gain
     normed = normed.astype(BF).reshape(seq, nz, nx, rows_w)
     normed = jnp.transpose(normed, (2, 0, 1, 3)).reshape(nx, seq, nz * rows_w)
-    mine = swap(normed, "x").reshape(nx * seq, nz * rows_w)
-    part = dot(mine, weights).astype(BF).reshape(nx, seq, 4 * chan)
-    projected = swap(part, "x").astype(F32).sum(axis=0)
+    mine = [pick(normed, x)] + [shift(pick(normed, (x + d) % nx), "x", d) for d in range(1, nx)]
+    part = dot(jnp.concatenate(mine, axis=0), weights).astype(BF)
+    part = part.reshape(nx, seq, 4 * chan)
+    projected = part[0].astype(F32)
+    for d in range(1, nx):
+        projected = projected + shift(part[d], "x", -d).astype(F32)
     projected = lax.optimization_barrier(projected.astype(BF)).astype(F32)
     query, forget_pre, values, out_gate = jnp.split(projected, 4, axis=1)
 
-    dense_own = spread(jnp.stack([dense_gate, dense_up, dense_down]), "x")
+    dense_block = jnp.stack([dense_gate, dense_up, dense_down])
+    dense_own = jnp.stack([dense_block] + [shift(dense_block, "x", d) for d in range(1, nx)])
     dense_other = partner(dense_own)
 
     def paired(stack, axis):
@@ -113,8 +127,12 @@
     head_out = (readout.reshape(seq, chan) * head_gain * jax.nn.silu(out_gate)).astype(BF)
 
     head_part = dot(head_out, w_output).astype(BF)
-    head_part = jnp.moveaxis(head_part.reshape(seq, ny * nc, cols), 1, 0)
-    resid = swap(head_part, TP).astype(F32).sum(axis=0)
+    head_part = jnp.moveaxis(head_part.reshape(seq, ny, nc, cols), 2, 0)
+    head_first, head_second = (jnp.moveaxis(h, 1, 0) for h in (head_part[0], head_part[1]))
+    keep = jnp.where(c == 0, head_first, head_second)
+    give = jnp.where(c == 0, head_second, head_first)
+    pair = (keep.astype(F32) + partner(give).astype(F32)).astype(BF)
+    resid = swap(pair, "y").astype(F32).sum(axis=0)
     resid = resid + lax.dynamic_slice_in_dim(tokens, own_at, cols, 1).astype(F32)
     own = resid.astype(BF)
 
@@ -148,6 +166,9 @@
 
     outgoing = jnp.einsum("bs,bw->sw", select, own, preferred_element_type=F32).astype(BF)
     arrived = from_lines(swap(to_lines(outgoing), HUB)).reshape(nz * nx, nc, slots, cols)
+    arrived, gate_w, up_w, down_w, dense_in_w, dense_out_w = lax.optimization_barrier(
+        (arrived, gate_w, up_w, down_w, dense_in_w, dense_out_w)
+    )
     arrived_first, arrived_second = arrived[:, 0], arrived[:, 1]
     count = nz * nx * cap
 
@@ -183,15 +204,22 @@
         ],
         axis=1,
     )
-    dense_pre = swap(dense_pre.reshape(ny, count // ny, -1), "y").astype(F32).sum(axis=0)
+    quarters = dense_pre.reshape(ny, count // ny, -1)
+    dense_pre = pick(quarters, y).astype(F32)
+    for d in range(1, ny):
+        dense_pre = dense_pre + shift(pick(quarters, (y + d) % ny), "y", d).astype(F32)
     hidden_width = dense_in_w.shape[1] // 2
     total = dense_pre[:, 2 * hidden_width] + dense_pre[:, 2 * hidden_width + lanes // 2]
     dense_scale = lax.rsqrt(total / width + EPS)[:, None]
     dense_gate_pre = dense_pre[:, :hidden_width] * dense_scale
     dense_up_pre = dense_pre[:, hidden_width : 2 * hidden_width] * dense_scale
     dense_hidden = (jax.nn.silu(dense_gate_pre) * dense_up_pre).astype(BF)
-    dense_hidden = spread(dense_hidden, "y").reshape(count, hidden_width)
-    dense_part = dot(dense_hidden, dense_out_w).astype(BF).reshape(nz * nx, cap, nc, cols)
+    dense_hidden = jnp.concatenate(
+        [dense_hidden] + [shift(dense_hidden, "y", d) for d in range(1, ny)], axis=0
+    )
+    dense_part = dot(dense_hidden, dense_out_w).astype(BF).reshape(ny, count // ny, nc * cols)
+    dense_part = jnp.stack([pick(dense_part, (y - q) % ny) for q in range(ny)])
+    dense_part = dense_part.reshape(nz * nx, cap, nc, cols)
     dense_first = jnp.where(c == 0, dense_part[:, :, 0], dense_part[:, :, 1])
     dense_second = jnp.where(c == 0, dense_part[:, :, 1], dense_part[:, :, 0])
 
@@ -225,7 +253,7 @@
 def solution(mesh):
     torus = Mesh(mesh.devices.reshape(8, 4, 4, 2), ("z", "x", "y", "c"))
     return jax.shard_map(
-        local,
+        step,
         mesh=torus,
         in_specs=(
             P(EP, None),

time: 217 us -> 176 us (0.81)
  the two profiles are of different devices: /device:TPU:8 before, /device:TPU:1 now
where the time goes in v2:
time: 176 us; the launch traced here: 175 us
  starting transfers between devices  59.4 us (34%)
  waiting for transfers between devices  47.8 us (27%)
  local copies, waits for them, and re-layouts  26.4 us (15%)
  other arithmetic  25.2 us (14%)
  matrix products  14.3 us (8%)
  between operations  1.97 us (1%)
    all_to_all x6, waiting for transfers between devices, swap(): return lax.all_to_all(x, axis, split_axis=0, concat_axis=0, tiled=True)  41.1 us
    all_to_all x6, starting transfers between devices, swap(): return lax.all_to_all(x, axis, split_axis=0, concat_axis=0, tiled=True)  33.8 us
    ppermute x15, starting transfers between devices, shift(): return lax.ppermute(x, axis, [(i, (i + by) % size) for i in range(size)])  16 us
    dot_general x10, matrix products, dot(): return jnp.dot(a, b, preferred_element_type=F32)  10.6 us
    ppermute x7, starting transfers between devices, partner(): return lax.ppermute(x, 'c', [(0, 1), (1, 0)])  9.56 us
    ppermute x15, waiting for transfers between devices, shift(): return lax.ppermute(x, axis, [(i, (i + by) % size) for i in range(size)])  6.71 us
    concatenate x3, other arithmetic, paired(): return jnp.concatenate([keep, other], axis=axis)  6.63 us
    unnamed x83, local copies, waits for them, and re-layouts  5.36 us
  transfers between devices with their start and end apart: 28, of which 9 were waited for; matrix products, arithmetic and copies ran while one was open for 26% of the time, Pallas kernels for 0%

profile of v2, /device:TPU:1, one launch (start us, length us, event | category | flops | bytes accessed | tf_op | source)
XLA Modules:
  0.0 175.0 jit_solution(13350140915386662865)
XLA Ops:
  4.6 3.3 %collective-permute-start.12 = (bf16[3,256,256]{1,2,0:T(8,128)(2,1)}, bf16[3,256,256]{1,2,0:T(8,128)(2,1)}, u32[]{:S(2)}, u32[]{:S(2)}) collective-permute-start(bf16[3,256,256]{1,2,0:T(8,128)(2,1)} %get-tuple-element.36), channel_id=1, source_target_pairs={{0,24},{8,0},{16,8},{24,16},{1,25},{9,1},{17,9},{25,17},{2,26},{10... | collective-permute-start | bytes 1179656 | tf_op jit(solution)/shard_map/ppermute | solution.py:31
  10.0 8.3 %all-to-all-start = ((bf16[8,64,512]{2,1,0:T(8,128)(2,1)}), bf16[8,64,512]{2,1,0:T(8,128)(2,1)S(1)}, u32[]{:S(2)}, u32[]{:S(2)}) async-start(bf16[8,64,512]{2,1,0:T(8,128)(2,1)} %broadcast_in_dim.16), calls=%async_computation | async-start | bytes 1048576 | tf_op jit(solution)/shard_map/all_to_all | solution.py:18
  20.4 1.7 collective-permute-start.1
  26.2 2.3 %dynamic-slice_bitcast_fusion.3 = (bf16[2048,128]{1,0:T(8,128)(2,1)}, bf16[2048,128]{1,0:T(8,128)(2,1)}) fusion(bf16[2,2048,128]{2,1,0:T(8,128)(2,1)} %param.37, s32[]{:T(128)S(6)} %select_n.227, s32[]{:T(128)S(6)} %select_n.228), kind=kLoop, calls=%fused_computation.38 | loop fusion | bytes 2097160 | tf_op jit(solution)/shard_map/jit(dynamic_index_in_dim)/squeeze | solution.py:95
  30.2 4.7 %all-to-all-done = bf16[8,64,512]{2,1,0:T(8,128)(2,1)S(1)} async-done(((bf16[8,64,512]{2,1,0:T(8,128)(2,1)}), bf16[8,64,512]{2,1,0:T(8,128)(2,1)S(1)}, u32[]{:S(2)}, u32[]{:S(2)}) %all-to-all-start) | async-done | bytes 524320 | tf_op jit(solution)/shard_map/all_to_all | solution.py:18
  35.8 1.9 %collective-permute-start.4 = (bf16[48,512]{1,0:T(8,128)(2,1)S(1)}, bf16[48,512]{1,0:T(8,128)(2,1)S(1)}, u32[]{:S(2)}, u32[]{:S(2)}) collective-permute-start(bf16[48,512]{1,0:T(8,128)(2,1)S(1)} %get-tuple-element.49), channel_id=1, source_target_pairs={{0,16},{8,24},{16,0},{24,8},{1,17},{9,25},{17,1},{25,9},{2,18},{10... | collective-permute-start | bytes 147464 | tf_op jit(solution)/shard_map/ppermute | solution.py:31
  37.8 2.0 %collective-permute-start.3 = (bf16[48,512]{1,0:T(8,128)(2,1)S(1)}, bf16[48,512]{1,0:T(8,128)(2,1)S(1)}, u32[]{:S(2)}, u32[]{:S(2)}) collective-permute-start(bf16[48,512]{1,0:T(8,128)(2,1)S(1)} %get-tuple-element.47), channel_id=1, source_target_pairs={{0,24},{8,0},{16,8},{24,16},{1,25},{9,1},{17,9},{25,17},{2,26},{10... | collective-permute-start | bytes 147464 | tf_op jit(solution)/shard_map/ppermute | solution.py:31
  40.3 3.9 %collective-permute-start.7 = (bf16[2048,128]{1,0:T(8,128)(2,1)}, bf16[2048,128]{1,0:T(8,128)(2,1)}, u32[]{:S(2)}, u32[]{:S(2)}) collective-permute-start(bf16[2048,128]{1,0:T(8,128)(2,1)} %get-tuple-element.27), channel_id=1, source_target_pairs={{0,1},{1,0},{2,3},{3,2},{4,5},{5,4},{6,7},{7,6},{8,9},{9,8},{10,11... | collective-permute-start | bytes 1572872 | tf_op jit(solution)/shard_map/ppermute | solution.py:26
  44.4 3.4 %fusion = f32[48,1,128]{2,1,0:T(1,128)S(1)} fusion(bf16[48,128,1]{1,0,2:T(8,128)(2,1)S(1)} %slice_bitcast_fusion, f32[48,128]{1,0:T(8,128)S(1)} %split.18, f32[48,128]{1,0:T(8,128)S(1)} %get-tuple-element.55, f32[48,1,128,128]{3,2,1,0:T(8,128)} %param.24, f32[48,128]{1,0:T(8,128)S(1)} %get-tuple-element.54), kind=kOutput, calls=%fused_computation | convolution fusion | flops 3932160 | bytes 3256320 | tf_op jit(solution)/shard_map/bhk,bhkv->bhv/dot_general | solution.py:125
  49.3 1.3 pad_maximum_fusion
  50.6 3.6 %collective-permute-start.13 = (bf16[4,3,256,256]{2,3,0,1:T(8,128)(2,1)S(1)}, bf16[4,3,256,256]{2,3,0,1:T(8,128)(2,1)}, u32[]{:S(2)}, u32[]{:S(2)}) collective-permute-start(bf16[4,3,256,256]{2,3,0,1:T(8,128)(2,1)S(1)} %pad_maximum_fusion), channel_id=1, source_target_pairs={{0,1},{1,0},{2,3},{3,2},{4,5},{5,4},{6,7},{7,6},{8,9},{9,8},{10,11... | collective-permute-start | bytes 4718600 | tf_op jit(solution)/shard_map/ppermute | solution.py:26
  54.9 4.2 %all-to-all-start.1 = ((bf16[4,48,256]{2,1,0:T(8,128)(2,1)}), bf16[4,48,256]{2,1,0:T(8,128)(2,1)S(1)}, u32[]{:S(2)}, u32[]{:S(2)}) async-start(bf16[4,48,256]{2,1,0:T(8,128)(2,1)} %fusion.36), calls=%async_computation.1 | async-start | bytes 196608 | tf_op jit(solution)/shard_map/all_to_all | solution.py:18
  60.4 3.3 %all-to-all-done.1 = bf16[4,48,256]{2,1,0:T(8,128)(2,1)S(1)} async-done(((bf16[4,48,256]{2,1,0:T(8,128)(2,1)}), bf16[4,48,256]{2,1,0:T(8,128)(2,1)S(1)}, u32[]{:S(2)}, u32[]{:S(2)}) %all-to-all-start.1) | async-done | bytes 98336 | tf_op jit(solution)/shard_map/all_to_all | solution.py:18
  66.7 5.5 %all-to-all-start.2 = ((bf16[64,24,128]{2,1,0:T(8,128)(2,1)}), bf16[64,24,128]{2,1,0:T(8,128)(2,1)S(1)}, u32[]{:S(2)}, u32[]{:S(2)}) async-start(bf16[64,24,128]{2,1,0:T(8,128)(2,1)} %copy.273), calls=%async_computation.2 | async-start | bytes 786432 | tf_op jit(solution)/shard_map/all_to_all | solution.py:18
  72.3 2.4 %pad_maximum_fusion.1 = bf16[2048,256]{1,0:T(8,128)(2,1)} fusion(bf16[2048,128]{1,0:T(8,128)(2,1)} %collective-permute-done.7, bf16[2048,128]{1,0:T(8,128)(2,1)} %get-tuple-element.26), kind=kLoop, calls=%fused_computation.23 | loop fusion | flops 2097152 | bytes 2097152 | tf_op jit(solution)/shard_map/concatenate | solution.py:97
  74.6 2.1 %pad_maximum_fusion.2 = bf16[2048,256]{1,0:T(8,128)(2,1)} fusion(bf16[2048,128]{1,0:T(8,128)(2,1)} %collective-permute-done.8, bf16[2048,128]{1,0:T(8,128)(2,1)S(1)} %copy-done.2), kind=kLoop, calls=%fused_computation.24 | loop fusion | flops 2097152 | bytes 2097152 | tf_op jit(solution)/shard_map/concatenate | solution.py:97
  77.3 2.1 %pad_maximum_fusion.3 = bf16[256,2048]{1,0:T(8,128)(2,1)} fusion(bf16[128,2048]{1,0:T(8,128)(2,1)} %collective-permute-done.9, bf16[128,2048]{1,0:T(8,128)(2,1)S(1)} %copy-done.1), kind=kLoop, calls=%fused_computation.25 | loop fusion | flops 2097152 | bytes 2097152 | tf_op jit(solution)/shard_map/concatenate | solution.py:97
  80.1 7.5 %all-to-all-done.2 = bf16[64,24,128]{2,1,0:T(8,128)(2,1)S(1)} async-done(((bf16[64,24,128]{2,1,0:T(8,128)(2,1)}), bf16[64,24,128]{2,1,0:T(8,128)(2,1)S(1)}, u32[]{:S(2)}, u32[]{:S(2)}) %all-to-all-start.2) | async-done | bytes 393248 | tf_op jit(solution)/shard_map/all_to_all | solution.py:18
  88.3 2.5 %fusion.110 = (bf16[4,1,256,256]{2,3,0,1:T(8,128)(2,1)S(1)}, bf16[4,1,256,256]{2,3,0,1:T(8,128)(2,1)}, bf16[4,1,256,256]{2,3,0,1:T(8,128)(2,1)}) fusion(bf16[4,3,256,256]{2,3,0,1:T(8,128)(2,1)} %collective-permute-done.13), kind=kLoop, calls=%fused_computation.205 | loop fusion | bytes 3145728 | tf_op jit(solution)/shard_map/slice | solution.py:117
  96.8 1.8 %convolution_convert_fusion = bf16[192,2048]{1,0:T(8,128)(2,1)S(1)} fusion(bf16[512,2048]{0,1:T(8,128)(2,1)S(1)} %maximum_maximum_fusion, f32[192,512]{1,0:T(8,128)} %reshape.248, f32[512]{0:T(512)S(1)} %copy-done.31), kind=kOutput, calls=%fused_computation.3 | convolution fusion | flops 403243008 | bytes 3278848 | tf_op jit(solution)/shard_map/dot_general | solution.py:39
  103.3 4.2 %all-to-all-start.3 = ((bf16[4,240,512]{2,1,0:T(8,128)(2,1)}), bf16[4,240,512]{2,1,0:T(8,128)(2,1)S(1)}, u32[]{:S(2)}, u32[]{:S(2)}) async-start(bf16[4,240,512]{2,1,0:T(8,128)(2,1)} %broadcast_in_dim.19), calls=%async_computation.3 | async-start | bytes 1966080 | tf_op jit(solution)/shard_map/all_to_all | solution.py:18
  108.6 5.3 %collective-permute-done.15 = bf16[48,2176]{1,0:T(8,128)(2,1)S(1)} collective-permute-done((bf16[48,2176]{1,0:T(8,128)(2,1)S(1)}, bf16[48,2176]{1,0:T(8,128)(2,1)S(1)}, u32[]{:S(2)}, u32[]{:S(2)}) %collective-permute-start.15) | collective-permute-done | bytes 208928 | tf_op jit(solution)/shard_map/ppermute | solution.py:31
  117.0 6.6 %all-to-all-done.3 = bf16[4,240,512]{2,1,0:T(8,128)(2,1)S(1)} async-done(((bf16[4,240,512]{2,1,0:T(8,128)(2,1)}), bf16[4,240,512]{2,1,0:T(8,128)(2,1)S(1)}, u32[]{:S(2)}, u32[]{:S(2)}) %all-to-all-start.3) | async-done | bytes 983072 | tf_op jit(solution)/shard_map/all_to_all | solution.py:18
  126.8 1.4 convolution_convert_fusion.2
  128.2 2.4 %convolution_convert_fusion.1 = bf16[192,2048]{1,0:T(8,128)(2,1)S(1)} fusion(bf16[256,2048]{1,0:T(8,128)(2,1)} %pad_maximum_fusion.3, bf16[2048,256]{1,0:T(8,128)(2,1)S(1)} %copy-done.8, bf16[240,2048]{1,0:T(8,128)(2,1)S(1)} %multiply_convert_fusion, f32[192,256]{1,0:T(8,128)} %fusion.7), kind=kOutput, calls=%fused_computation.4 | convolution fusion | flops 403341312 | bytes 3866624 | tf_op jit(solution)/shard_map/dot_general | solution.py:39
  131.7 3.5 %all-to-all-start.4 = ((bf16[4,240,512]{2,1,0:T(8,128)(2,1)}), bf16[4,240,512]{2,1,0:T(8,128)(2,1)S(1)}, u32[]{:S(2)}, u32[]{:S(2)}) async-start(bf16[4,240,512]{2,1,0:T(8,128)(2,1)} %bitcast.181), calls=%async_computation.4 | async-start | bytes 1966080 | tf_op jit(solution)/shard_map/all_to_all | solution.py:18
  135.4 1.4 convolution_convert_fusion.5
  137.4 9.6 %all-to-all-done.4 = bf16[4,240,512]{2,1,0:T(8,128)(2,1)S(1)} async-done(((bf16[4,240,512]{2,1,0:T(8,128)(2,1)}), bf16[4,240,512]{2,1,0:T(8,128)(2,1)S(1)}, u32[]{:S(2)}, u32[]{:S(2)}) %all-to-all-start.4) | async-done | bytes 983072 | tf_op jit(solution)/shard_map/all_to_all | solution.py:18
  149.5 8.1 %all-to-all-start.5 = ((bf16[64,24,128]{2,1,0:T(8,128)(2,1)}), bf16[64,24,128]{2,1,0:T(8,128)(2,1)S(1)}, u32[]{:S(2)}, u32[]{:S(2)}) async-start(bf16[64,24,128]{2,1,0:T(8,128)(2,1)} %copy.295), calls=%async_computation.5 | async-start | bytes 786432 | tf_op jit(solution)/shard_map/all_to_all | solution.py:18
  157.8 5.1 %multiply_add_fusion = f32[48,1,128,128]{3,2,1,0:T(8,128)} fusion(f32[48,1,128,128]{3,2,1,0:T(8,128)} %param.24, f32[48,128]{1,0:T(8,128)S(1)} %copy-done.18, f32[48,128]{1,0:T(8,128)S(1)} %copy-done.22, f32[48,128]{1,0:T(8,128)S(1)} %copy-done.20), kind=kLoop, calls=%fused_computation.2 | loop fusion | flops 2359296 | bytes 6365184 | tf_op jit(solution)/shard_map/add | solution.py:124
  163.4 9.3 %all-to-all-done.5 = bf16[64,24,128]{2,1,0:T(8,128)(2,1)S(1)} async-done(((bf16[64,24,128]{2,1,0:T(8,128)(2,1)}), bf16[64,24,128]{2,1,0:T(8,128)(2,1)S(1)}, u32[]{:S(2)}, u32[]{:S(2)}) %all-to-all-start.5) | async-done | bytes 393248 | tf_op jit(solution)/shard_map/all_to_all | solution.py:18
  173.5 1.6 fusion.65
  (232 shorter events, 46.7 us)
Async XLA Ops:
  0.6 47.4 %copy-start = (bf16[128,2048]{1,0:T(8,128)(2,1)S(1)}, bf16[128,2048]{1,0:T(8,128)(2,1)}, u32[]{:S(2)}) copy-start(bf16[128,2048]{1,0:T(8,128)(2,1)} %param.32) | copy-start | bytes 1572868
  0.6 17.8 %copy-start.11 = (bf16[48,2048]{1,0:T(8,128)(2,1)S(1)}, bf16[48,2048]{1,0:T(8,128)(2,1)}, u32[]{:S(2)}) copy-start(bf16[48,2048]{1,0:T(8,128)(2,1)} %param.23) | copy-start | bytes 589828
  0.7 17.9 %copy-start.29 = (f32[2048]{0:T(1024)S(1)}, f32[2048]{0:T(1024)}, u32[]{:S(2)}) copy-start(f32[2048]{0:T(1024)} %param.25) | copy-start | bytes 24580
  4.6 43.9 %collective-permute-start.12 = (bf16[3,256,256]{1,2,0:T(8,128)(2,1)}, bf16[3,256,256]{1,2,0:T(8,128)(2,1)}, u32[]{:S(2)}, u32[]{:S(2)}) collective-permute-start(bf16[3,256,256]{1,2,0:T(8,128)(2,1)} %get-tuple-element.36), channel_id=1, source_target_pairs={{0,24},{8,0},{16,8},{24,16},{1,25},{9,1},{17,9},{25,17},{2,26},{10... | collective-permute-start | bytes 1179656 | tf_op jit(solution)/shard_map/ppermute | solution.py:31
  7.9 41.1 %collective-permute-start.11 = (bf16[3,256,256]{1,2,0:T(8,128)(2,1)}, bf16[3,256,256]{1,2,0:T(8,128)(2,1)}, u32[]{:S(2)}, u32[]{:S(2)}) collective-permute-start(bf16[3,256,256]{1,2,0:T(8,128)(2,1)} %get-tuple-element.36), channel_id=1, source_target_pairs={{0,16},{8,24},{16,0},{24,8},{1,17},{9,25},{17,1},{25,9},{2,18},{10... | collective-permute-start | bytes 1179656 | tf_op jit(solution)/shard_map/ppermute | solution.py:31
  10.0 24.8 %all-to-all-start = ((bf16[8,64,512]{2,1,0:T(8,128)(2,1)}), bf16[8,64,512]{2,1,0:T(8,128)(2,1)S(1)}, u32[]{:S(2)}, u32[]{:S(2)}) async-start(bf16[8,64,512]{2,1,0:T(8,128)(2,1)} %broadcast_in_dim.16), calls=%async_computation | async-start | bytes 1048576 | tf_op jit(solution)/shard_map/all_to_all | solution.py:18
  19.5 10.7 %collective-permute-start.2 = (bf16[48,512]{1,0:T(8,128)(2,1)S(1)}, bf16[48,512]{1,0:T(8,128)(2,1)S(1)}, u32[]{:S(2)}, u32[]{:S(2)}) collective-permute-start(bf16[48,512]{1,0:T(8,128)(2,1)S(1)} %get-tuple-element.51), channel_id=1, source_target_pairs={{0,24},{8,0},{16,8},{24,16},{1,25},{9,1},{17,9},{25,17},{2,26},{10... | collective-permute-start | bytes 147464 | tf_op jit(solution)/shard_map/ppermute | solution.py:31
  20.4 9.8 %collective-permute-start.1 = (bf16[48,512]{1,0:T(8,128)(2,1)S(1)}, bf16[48,512]{1,0:T(8,128)(2,1)S(1)}, u32[]{:S(2)}, u32[]{:S(2)}) collective-permute-start(bf16[48,512]{1,0:T(8,128)(2,1)S(1)} %get-tuple-element.52), channel_id=1, source_target_pairs={{0,16},{8,24},{16,0},{24,8},{1,17},{9,25},{17,1},{25,9},{2,18},{10... | collective-permute-start | bytes 147464 | tf_op jit(solution)/shard_map/ppermute | solution.py:31
  22.1 8.1 %collective-permute-start = (bf16[48,512]{1,0:T(8,128)(2,1)S(1)}, bf16[48,512]{1,0:T(8,128)(2,1)S(1)}, u32[]{:S(2)}, u32[]{:S(2)}) collective-permute-start(bf16[48,512]{1,0:T(8,128)(2,1)S(1)} %get-tuple-element.53), channel_id=1, source_target_pairs={{0,8},{8,16},{16,24},{24,0},{1,9},{9,17},{17,25},{25,1},{2,10},{10... | collective-permute-start | bytes 147464 | tf_op jit(solution)/shard_map/ppermute | solution.py:31
  35.1 4.7 %collective-permute-start.5 = (bf16[48,512]{1,0:T(8,128)(2,1)S(1)}, bf16[48,512]{1,0:T(8,128)(2,1)S(1)}, u32[]{:S(2)}, u32[]{:S(2)}) collective-permute-start(bf16[48,512]{1,0:T(8,128)(2,1)S(1)} %get-tuple-element.48), channel_id=1, source_target_pairs={{0,8},{8,16},{16,24},{24,0},{1,9},{9,17},{17,25},{25,1},{2,10},{10... | collective-permute-start | bytes 147464 | tf_op jit(solution)/shard_map/ppermute | solution.py:31
  35.8 4.4 %collective-permute-start.4 = (bf16[48,512]{1,0:T(8,128)(2,1)S(1)}, bf16[48,512]{1,0:T(8,128)(2,1)S(1)}, u32[]{:S(2)}, u32[]{:S(2)}) collective-permute-start(bf16[48,512]{1,0:T(8,128)(2,1)S(1)} %get-tuple-element.49), channel_id=1, source_target_pairs={{0,16},{8,24},{16,0},{24,8},{1,17},{9,25},{17,1},{25,9},{2,18},{10... | collective-permute-start | bytes 147464 | tf_op jit(solution)/shard_map/ppermute | solution.py:31
  37.8 6.4 %collective-permute-start.3 = (bf16[48,512]{1,0:T(8,128)(2,1)S(1)}, bf16[48,512]{1,0:T(8,128)(2,1)S(1)}, u32[]{:S(2)}, u32[]{:S(2)}) collective-permute-start(bf16[48,512]{1,0:T(8,128)(2,1)S(1)} %get-tuple-element.47), channel_id=1, source_target_pairs={{0,24},{8,0},{16,8},{24,16},{1,25},{9,1},{17,9},{25,17},{2,26},{10... | collective-permute-start | bytes 147464 | tf_op jit(solution)/shard_map/ppermute | solution.py:31
  39.7 24.8 %copy-start.33 = (pred[768]{0:T(1024)(128)(4,1)}, pred[768]{0:T(1024)(128)(4,1)S(1)}, u32[]{:S(2)}) copy-start(pred[768]{0:T(1024)(128)(4,1)S(1)} %fusion.99) | copy-start | bytes 2308
  39.8 9.5 %collective-permute-start.10 = (bf16[3,256,256]{1,2,0:T(8,128)(2,1)}, bf16[3,256,256]{1,2,0:T(8,128)(2,1)S(1)}, u32[]{:S(2)}, u32[]{:S(2)}) collective-permute-start(bf16[3,256,256]{1,2,0:T(8,128)(2,1)} %get-tuple-element.36), channel_id=1, source_target_pairs={{0,8},{8,16},{16,24},{24,0},{1,9},{9,17},{17,25},{25,1},{2,10},{10... | collective-permute-start | bytes 1179656 | tf_op jit(solution)/shard_map/ppermute | solution.py:31
  40.3 32.0 %collective-permute-start.7 = (bf16[2048,128]{1,0:T(8,128)(2,1)}, bf16[2048,128]{1,0:T(8,128)(2,1)}, u32[]{:S(2)}, u32[]{:S(2)}) collective-permute-start(bf16[2048,128]{1,0:T(8,128)(2,1)} %get-tuple-element.27), channel_id=1, source_target_pairs={{0,1},{1,0},{2,3},{3,2},{4,5},{5,4},{6,7},{7,6},{8,9},{9,8},{10,11... | collective-permute-start | bytes 1572872 | tf_op jit(solution)/shard_map/ppermute | solution.py:26
  44.2 30.4 %collective-permute-start.8 = (bf16[2048,128]{1,0:T(8,128)(2,1)}, bf16[2048,128]{1,0:T(8,128)(2,1)}, u32[]{:S(2)}, u32[]{:S(2)}) collective-permute-start(bf16[2048,128]{1,0:T(8,128)(2,1)} %get-tuple-element.25), channel_id=1, source_target_pairs={{0,1},{1,0},{2,3},{3,2},{4,5},{5,4},{6,7},{7,6},{8,9},{9,8},{10,11... | collective-permute-start | bytes 1572872 | tf_op jit(solution)/shard_map/ppermute | solution.py:26
  48.5 28.9 %collective-permute-start.9 = (bf16[128,2048]{1,0:T(8,128)(2,1)}, bf16[128,2048]{1,0:T(8,128)(2,1)}, u32[]{:S(2)}, u32[]{:S(2)}) collective-permute-start(bf16[128,2048]{1,0:T(8,128)(2,1)} %get-tuple-element.23), channel_id=1, source_target_pairs={{0,1},{1,0},{2,3},{3,2},{4,5},{5,4},{6,7},{7,6},{8,9},{9,8},{10,11... | collective-permute-start | bytes 1572872 | tf_op jit(solution)/shard_map/ppermute | solution.py:26
  49.0 5.2 %collective-permute-start.6 = (bf16[4,48,256]{2,1,0:T(8,128)(2,1)S(1)}, bf16[4,48,256]{2,1,0:T(8,128)(2,1)S(1)}, u32[]{:S(2)}, u32[]{:S(2)}) collective-permute-start(bf16[4,48,256]{2,1,0:T(8,128)(2,1)S(1)} %select_bitcast_fusion), channel_id=1, source_target_pairs={{0,1},{1,0},{2,3},{3,2},{4,5},{5,4},{6,7},{7,6},{8,9},{9,8},{10,11... | collective-permute-start | bytes 294920 | tf_op jit(solution)/shard_map/ppermute | solution.py:26
  50.6 37.7 %collective-permute-start.13 = (bf16[4,3,256,256]{2,3,0,1:T(8,128)(2,1)S(1)}, bf16[4,3,256,256]{2,3,0,1:T(8,128)(2,1)}, u32[]{:S(2)}, u32[]{:S(2)}) collective-permute-start(bf16[4,3,256,256]{2,3,0,1:T(8,128)(2,1)S(1)} %pad_maximum_fusion), channel_id=1, source_target_pairs={{0,1},{1,0},{2,3},{3,2},{4,5},{5,4},{6,7},{7,6},{8,9},{9,8},{10,11... | collective-permute-start | bytes 4718600 | tf_op jit(solution)/shard_map/ppermute | solution.py:26
  54.9 8.8 %all-to-all-start.1 = ((bf16[4,48,256]{2,1,0:T(8,128)(2,1)}), bf16[4,48,256]{2,1,0:T(8,128)(2,1)S(1)}, u32[]{:S(2)}, u32[]{:S(2)}) async-start(bf16[4,48,256]{2,1,0:T(8,128)(2,1)} %fusion.36), calls=%async_computation.1 | async-start | bytes 196608 | tf_op jit(solution)/shard_map/all_to_all | solution.py:18
  66.7 20.9 %all-to-all-start.2 = ((bf16[64,24,128]{2,1,0:T(8,128)(2,1)}), bf16[64,24,128]{2,1,0:T(8,128)(2,1)S(1)}, u32[]{:S(2)}, u32[]{:S(2)}) async-start(bf16[64,24,128]{2,1,0:T(8,128)(2,1)} %copy.273), calls=%async_computation.2 | async-start | bytes 786432 | tf_op jit(solution)/shard_map/all_to_all | solution.py:18
  76.8 2.7 %collective-permute-start.14 = (bf16[48,256]{1,0:T(8,128)(2,1)S(1)}, bf16[48,256]{1,0:T(8,128)(2,1)S(1)}, u32[]{:S(2)}, u32[]{:S(2)}) collective-permute-start(bf16[48,256]{1,0:T(8,128)(2,1)S(1)} %copy-done.24), channel_id=1, source_target_pairs={{0,1},{1,0},{2,3},{3,2},{4,5},{5,4},{6,7},{7,6},{8,9},{9,8},{10,11... | collective-permute-start | bytes 73736 | tf_op jit(solution)/shard_map/ppermute | solution.py:26
  99.9 7.6 %collective-permute-start.17 = (bf16[48,2176]{1,0:T(8,128)(2,1)}, bf16[48,2176]{1,0:T(8,128)(2,1)S(1)}, u32[]{:S(2)}, u32[]{:S(2)}) collective-permute-start(bf16[48,2176]{1,0:T(8,128)(2,1)} %get-tuple-element.29), channel_id=1, source_target_pairs={{0,6},{2,0},{4,2},{6,4},{1,7},{3,1},{5,3},{7,5},{8,14},{10,8},{12,... | collective-permute-start | bytes 626696 | tf_op jit(solution)/shard_map/ppermute | solution.py:31
  100.8 7.8 %collective-permute-start.16 = (bf16[48,2176]{1,0:T(8,128)(2,1)S(1)}, bf16[48,2176]{1,0:T(8,128)(2,1)S(1)}, u32[]{:S(2)}, u32[]{:S(2)}) collective-permute-start(bf16[48,2176]{1,0:T(8,128)(2,1)S(1)} %get-tuple-element.30), channel_id=1, source_target_pairs={{0,4},{2,6},{4,0},{6,2},{1,5},{3,7},{5,1},{7,3},{8,12},{10,14},{12... | collective-permute-start | bytes 626696 | tf_op jit(solution)/shard_map/ppermute | solution.py:31
  102.0 11.9 %collective-permute-start.15 = (bf16[48,2176]{1,0:T(8,128)(2,1)S(1)}, bf16[48,2176]{1,0:T(8,128)(2,1)S(1)}, u32[]{:S(2)}, u32[]{:S(2)}) collective-permute-start(bf16[48,2176]{1,0:T(8,128)(2,1)S(1)} %get-tuple-element.28), channel_id=1, source_target_pairs={{0,2},{2,4},{4,6},{6,0},{1,3},{3,5},{5,7},{7,1},{8,10},{10,12},{12... | collective-permute-start | bytes 626696 | tf_op jit(solution)/shard_map/ppermute | solution.py:31
  103.3 20.3 %all-to-all-start.3 = ((bf16[4,240,512]{2,1,0:T(8,128)(2,1)}), bf16[4,240,512]{2,1,0:T(8,128)(2,1)S(1)}, u32[]{:S(2)}, u32[]{:S(2)}) async-start(bf16[4,240,512]{2,1,0:T(8,128)(2,1)} %broadcast_in_dim.19), calls=%async_computation.3 | async-start | bytes 1966080 | tf_op jit(solution)/shard_map/all_to_all | solution.py:18
  115.0 20.4 %collective-permute-start.20 = (bf16[48,1024]{1,0:T(8,128)(2,1)}, bf16[48,1024]{1,0:T(8,128)(2,1)}, u32[]{:S(2)}, u32[]{:S(2)}) collective-permute-start(bf16[48,1024]{1,0:T(8,128)(2,1)} %fusion.27), channel_id=1, source_target_pairs={{0,6},{2,0},{4,2},{6,4},{1,7},{3,1},{5,3},{7,5},{8,14},{10,8},{12,... | collective-permute-start | bytes 294920 | tf_op jit(solution)/shard_map/ppermute | solution.py:31
  115.0 20.4 %collective-permute-start.19 = (bf16[48,1024]{1,0:T(8,128)(2,1)}, bf16[48,1024]{1,0:T(8,128)(2,1)}, u32[]{:S(2)}, u32[]{:S(2)}) collective-permute-start(bf16[48,1024]{1,0:T(8,128)(2,1)} %fusion.27), channel_id=1, source_target_pairs={{0,4},{2,6},{4,0},{6,2},{1,5},{3,7},{5,1},{7,3},{8,12},{10,14},{12... | collective-permute-start | bytes 294920 | tf_op jit(solution)/shard_map/ppermute | solution.py:31
  116.1 19.2 %collective-permute-start.18 = (bf16[48,1024]{1,0:T(8,128)(2,1)}, bf16[48,1024]{1,0:T(8,128)(2,1)}, u32[]{:S(2)}, u32[]{:S(2)}) collective-permute-start(bf16[48,1024]{1,0:T(8,128)(2,1)} %fusion.27), channel_id=1, source_target_pairs={{0,2},{2,4},{4,6},{6,0},{1,3},{3,5},{5,7},{7,1},{8,10},{10,12},{12... | collective-permute-start | bytes 294920 | tf_op jit(solution)/shard_map/ppermute | solution.py:31
  131.7 15.3 %all-to-all-start.4 = ((bf16[4,240,512]{2,1,0:T(8,128)(2,1)}), bf16[4,240,512]{2,1,0:T(8,128)(2,1)S(1)}, u32[]{:S(2)}, u32[]{:S(2)}) async-start(bf16[4,240,512]{2,1,0:T(8,128)(2,1)} %bitcast.181), calls=%async_computation.4 | async-start | bytes 1966080 | tf_op jit(solution)/shard_map/all_to_all | solution.py:18
  149.5 23.2 %all-to-all-start.5 = ((bf16[64,24,128]{2,1,0:T(8,128)(2,1)}), bf16[64,24,128]{2,1,0:T(8,128)(2,1)S(1)}, u32[]{:S(2)}, u32[]{:S(2)}) async-start(bf16[64,24,128]{2,1,0:T(8,128)(2,1)} %copy.295), calls=%async_computation.5 | async-start | bytes 786432 | tf_op jit(solution)/shard_map/all_to_all | solution.py:18
  162.9 10.6 %collective-permute-start.21 = (bf16[48,256]{1,0:T(8,128)(2,1)S(1)}, bf16[48,256]{1,0:T(8,128)(2,1)S(1)}, u32[]{:S(2)}, u32[]{:S(2)}) collective-permute-start(bf16[48,256]{1,0:T(8,128)(2,1)S(1)} %select_convert_fusion), channel_id=1, source_target_pairs={{0,1},{1,0},{2,3},{3,2},{4,5},{5,4},{6,7},{7,6},{8,9},{9,8},{10,11... | collective-permute-start | bytes 73736 | tf_op jit(solution)/shard_map/ppermute | solution.py:26
  (34 other events, 196.2 us)

commit v3 on v2

v3 whole, which is shorter than its diff:
```python
import jax
import jax.numpy as jnp
from jax import lax
from jax.experimental import pallas as pl
from jax.experimental.pallas import tpu as pltpu
from jax.sharding import Mesh
from jax.sharding import PartitionSpec as P

EP = ("z", "x")
TP = ("y", "c")
HUB = ("z", "x", "c")


EPS = 1e-06
BF = jnp.bfloat16
F32 = jnp.float32


def swap(x, axis):
    return lax.all_to_all(x, axis, split_axis=0, concat_axis=0, tiled=True)


def spread(x, axis):
    return swap(jnp.broadcast_to(x, (lax.axis_size(axis), *x.shape)), axis)


def partner(x):
    return lax.ppermute(x, "c", [(0, 1), (1, 0)])


def shift(x, axis, by):
    size = lax.axis_size(axis)
    return lax.ppermute(x, axis, [(i, (i + by) % size) for i in range(size)])


def pick(x, index):
    return lax.dynamic_index_in_dim(x, index, 0, keepdims=False)


def dot(a, b):
    return jnp.dot(a, b, preferred_element_type=F32)


def silu(x):
    return x * jax.nn.sigmoid(x)


def call(body, outs, flops, *args):
    moved = sum(a.size * a.dtype.itemsize for a in args) + sum(
        o.size * o.dtype.itemsize for o in outs
    )
    specs = [
        pl.BlockSpec(memory_space=pltpu.SMEM if a.dtype == jnp.int32 and a.ndim == 1 else pltpu.VMEM)
        for a in args
    ]
    return pl.pallas_call(
        body,
        out_shape=outs,
        in_specs=specs,
        out_specs=[pl.BlockSpec(memory_space=pltpu.VMEM) for _ in outs],
        cost_estimate=pl.CostEstimate(flops=flops, bytes_accessed=moved, transcendentals=0),
    )(*args)


def shaped(*dims, dtype=BF):
    return jax.ShapeDtypeStruct(dims, dtype)


def unpack_rows(at, line_of, lines, own, other, both, dense):
    first = at[1] == 0
    group = line_of.shape[1]
    count = dense.shape[1]
    cols = dense.shape[2]
    half = cols // 2
    part = group // 8
    groups = lines.shape[0] // group
    move = jnp.where(
        lax.broadcasted_iota(jnp.int32, (group, group), 0) == line_of[...], 1.0, 0.0
    ).astype(BF)
    mine, others = own[...], other[...]
    both_rows = [
        jnp.where(first, mine, others),
        jnp.where(first, others, mine),
    ]
    for g in range(groups):
        rows = dot(move, lines[g * group : (g + 1) * group, :]).astype(BF)
        here = slice(g * part, (g + 1) * part)
        for side in range(2):
            for h in range(2):
                base = (side * 2 + h) * 2 * part
                at_col = side * cols + h * half
                for copy in range(both.shape[0]):
                    both[copy, here, at_col : at_col + half] = rows[base : base + part]
                dense[side, here, h * half : (h + 1) * half] = rows[base + part : base + 2 * part]
    for side in range(2):
        for copy in range(both.shape[0]):
            both[copy, count:, side * cols : (side + 1) * cols] = both_rows[side]


def dense_first_half(at, rows, gain, *refs):
    y, c = at[0], at[1]
    own_w, other_w, outs = refs[:4], refs[4:8], refs[8:]
    ny = len(outs)
    size = rows.shape[1] // ny
    cols = rows.shape[2]

    def turned(side):
        return jnp.concatenate(
            [
                rows[side, pl.ds(pl.multiple_of(lax.rem(y + d, ny) * size, size), size), :]
                for d in range(ny)
            ],
            axis=0,
        ).astype(F32)

    own, other = turned(c), turned(1 - c)
    square = jnp.sum(own * own + other * other, axis=1, keepdims=True)
    high = square.astype(BF).astype(F32)
    low = square - high
    own = (own * gain[pl.ds(2 * y + c, 1), :]).astype(BF)
    other = (other * gain[pl.ds(2 * y + 1 - c, 1), :]).astype(BF)
    for kind in range(2):
        for i in range(4):
            value = (dot(own, own_w[i][kind]) + dot(other, other_w[i][kind])).astype(BF)
            at_col = (kind * 4 + i) * cols
            for d in range(ny):
                outs[d][:, at_col : at_col + cols] = value[d * size : (d + 1) * size]
    lane = lax.broadcasted_iota(jnp.int32, (square.shape[0], 128), 1)
    both = jnp.where(lane < 64, high, low).astype(BF)
    for d in range(ny):
        outs[d][:, 8 * cols : 8 * cols + 128] = both[d * size : (d + 1) * size]


def dense_activation(a, b, c, d, out):
    width = out.shape[1]
    features = 2048

    def summed(cut):
        return (
            a[:, cut].astype(F32) + b[:, cut].astype(F32) + c[:, cut].astype(F32) + d[:, cut].astype(F32)
        )

    square = summed(slice(2 * width, 2 * width + 128))
    total = square[:, 0:1] + square[:, 64:65]
    scale = lax.rsqrt(total / features + EPS)
    gate = summed(slice(0, width)) * scale
    up = summed(slice(width, 2 * width)) * scale
    out[...] = (silu(gate) * up).astype(BF)


def dense_second_half(at, *refs):
    y = at[0]
    hidden, own_w, other_w, out = refs[:4], refs[4:8], refs[8:12], refs[12]
    ny = len(hidden)
    size, cols = hidden[0].shape[0], out.shape[2]
    rows = jnp.concatenate([h[...] for h in hidden], axis=0)
    for side, weights in enumerate((own_w, other_w)):
        total = None
        for i in range(4):
            term = dot(rows[:, i * cols : (i + 1) * cols], weights[i][2])
            total = term if total is None else total + term
        total = total.astype(BF)
        for d in range(ny):
            start = pl.multiple_of(lax.rem(y + ny - d, ny) * size, size)
            out[side, pl.ds(start, size), :] = total[d * size : (d + 1) * size]


def experts_and_shared(
    at, whole, gain, gate, gate_other, up, up_other, down, down_other,
    shared_gate, shared_up, shared_down, parts,
):
    c = at[1]
    ny, lines, block = whole.shape
    count = lines - 48
    square = jnp.zeros((lines, 1), F32)
    rows = []
    for i in range(ny):
        value = whole[i].astype(F32)
        square = square + jnp.sum(value * value, axis=1, keepdims=True)
        rows.append(value)
    scale = lax.rsqrt(square / (ny * block) + EPS)
    rows = [
        (value * scale * gain[:, i * block : (i + 1) * block]).astype(BF)
        for i, value in enumerate(rows)
    ]
    gate_pre = up_pre = gate_shared = up_shared = None

    def more(total, term):
        return term if total is None else total + term

    for i in range(ny):
        cut = slice(i * block, (i + 1) * block)
        gates = jnp.concatenate([gate[c, cut, :], gate_other[cut, :]], axis=1)
        ups = jnp.concatenate([up[c, cut, :], up_other[cut, :]], axis=1)
        shared = jnp.concatenate([shared_gate[cut, :], shared_up[cut, :]], axis=1)
        gate_pre = more(gate_pre, dot(rows[i][:count], gates))
        up_pre = more(up_pre, dot(rows[i][:count], ups))
        gate_shared = more(gate_shared, dot(rows[i][count:], shared))
    half = gate.shape[2]
    hidden = (silu(gate_pre) * up_pre).astype(BF)
    shared_hidden = (silu(gate_shared[:, :half]) * gate_shared[:, half:]).astype(BF)
    for i in range(ny):
        cut = slice(i * block, (i + 1) * block)
        downs = jnp.concatenate([down[c, :, cut], down_other[:, cut]], axis=0)
        parts[i, :count, :] = dot(hidden, downs).astype(BF)
        parts[i, count:, :] = dot(shared_hidden, shared_down[:, cut]).astype(BF)


def pack_lines(at, line_of, parts, dense, lines, shared_own, shared_send):
    first = at[1] == 0
    group = line_of.shape[0]
    part = group // 8
    cols = dense.shape[2]
    half = cols // 2
    count = dense.shape[1]
    groups = lines.shape[0] // group
    move = jnp.where(
        lax.broadcasted_iota(jnp.int32, (group, group), 1) == line_of[...], 1.0, 0.0
    ).astype(BF)
    total = parts[0].astype(F32)
    for i in range(1, parts.shape[0]):
        total = total + parts[i].astype(F32)
    routed = total[:count].astype(BF)
    shared = total[count:]
    shared_own[...] = jnp.where(first, shared[:, :cols], shared[:, cols:])
    shared_send[...] = jnp.where(first, shared[:, cols:], shared[:, :cols]).astype(BF)
    for g in range(groups):
        here = slice(g * part, (g + 1) * part)
        own, other = dense[0, here, :], dense[1, here, :]
        sides = [jnp.where(first, own, other), jnp.where(first, other, own)]
        stack = []
        for side in range(2):
            for h in range(2):
                at_col = side * cols + h * half
                stack.append(routed[here, at_col : at_col + half])
                stack.append(sides[side][:, h * half : (h + 1) * half])
        rows = jnp.concatenate(stack, axis=0)
        lines[g * group : (g + 1) * group, :] = dot(move, rows).astype(BF)


def step(
    tokens,
    state,
    norm_gain,
    w_query,
    w_forget,
    w_input,
    w_outgate,
    lower_bound,
    head_gain,
    w_output,
    ffn_gain,
    route_ids,
    route_weight,
    expert_gate,
    expert_up,
    expert_down,
    shared_gate,
    shared_up,
    shared_down,
    dense_gate,
    dense_up,
    dense_down,
    dense_mix,
):
    nz, nx, ny, nc = (lax.axis_size(a) for a in ("z", "x", "y", "c"))
    x, y, c = (lax.axis_index(a) for a in ("x", "y", "c"))
    seq, width = tokens.shape
    rows_w, chan = w_query.shape
    head_dim = state.shape[2]
    cols = width // (ny * nc)
    own_at = (y * nc + c) * cols

    joined = jnp.concatenate([w_query, w_forget, w_input, w_outgate], axis=1)
    weights = spread(joined, "z").reshape(nz * rows_w, 4 * chan)
    wide = tokens.astype(F32)
    normed = wide * lax.rsqrt(jnp.mean(wide * wide, axis=-1, keepdims=True) + EPS) * norm_gain
    normed = normed.astype(BF).reshape(seq, nz, nx, rows_w)
    normed = jnp.transpose(normed, (2, 0, 1, 3)).reshape(nx, seq, nz * rows_w)
    mine = [pick(normed, x)] + [shift(pick(normed, (x + d) % nx), "x", d) for d in range(1, nx)]
    part = dot(jnp.concatenate(mine, axis=0), weights).astype(BF)
    part = part.reshape(nx, seq, 4 * chan)
    projected = part[0].astype(F32)
    for d in range(1, nx):
        projected = projected + shift(part[d], "x", -d).astype(F32)
    projected = lax.optimization_barrier(projected.astype(BF)).astype(F32)
    query, forget_pre, values, out_gate = jnp.split(projected, 4, axis=1)

    at = jnp.stack([y, c]).astype(jnp.int32)
    dense_block = jnp.stack([dense_gate, dense_up, dense_down])
    dense_own = [dense_block] + [shift(dense_block, "x", d) for d in range(1, nx)]
    dense_other = [partner(block) for block in dense_own]
    gate_other, up_other, down_other = (
        partner(pick(stack, 1 - c)) for stack in (expert_gate, expert_up, expert_down)
    )

    forget_sig = jax.nn.sigmoid(forget_pre)
    shape = (seq, 1, head_dim)
    decay = (lower_bound + (1.0 - lower_bound) * forget_sig).reshape(shape)
    keygate = ((1.0 - lower_bound) * (1.0 - forget_sig)).reshape(shape)
    new_state = decay[..., None] * state + keygate[..., None] * values.reshape(shape)[:, :, None, :]
    readout = jnp.einsum("bhk,bhkv->bhv", query.reshape(shape), new_state)
    readout = readout * lax.rsqrt(jnp.mean(readout * readout, axis=-1, keepdims=True) + EPS)
    head_out = (readout.reshape(seq, chan) * head_gain * jax.nn.silu(out_gate)).astype(BF)

    head_part = dot(head_out, w_output).astype(BF)
    head_part = jnp.moveaxis(head_part.reshape(seq, ny, nc, cols), 2, 0)
    head_first, head_second = (jnp.moveaxis(h, 1, 0) for h in (head_part[0], head_part[1]))
    keep = jnp.where(c == 0, head_first, head_second)
    give = jnp.where(c == 0, head_second, head_first)
    pair = (keep.astype(F32) + partner(give).astype(F32)).astype(BF)
    resid = swap(pair, "y").astype(F32).sum(axis=0)
    resid = resid + lax.dynamic_slice_in_dim(tokens, own_at, cols, 1).astype(F32)
    own = resid.astype(BF)

    topk = route_ids.shape[1]
    experts = nz * nx * nc
    cap = max(2, 2 * seq * topk // experts)
    flat_ids = route_ids.reshape(-1)
    onehot = (flat_ids[:, None] == jnp.arange(experts, dtype=jnp.int32)[None, :]).astype(jnp.int32)
    rank = jnp.sum((jnp.cumsum(onehot, axis=0) - onehot) * onehot, axis=1)
    slots = 2 * cap
    slot_index = (flat_ids * slots + rank).reshape(seq, topk)
    slot_ids = jnp.arange(experts * slots, dtype=jnp.int32)
    place = slot_ids % slots
    line = (slot_ids // slots) % (nx * nc) * cap + place - cap
    is_dense = place >= cap
    token_ids = jnp.arange(seq, dtype=jnp.int32)
    dense_hits = is_dense[None, :] & (line[None, :] == token_ids[:, None])
    hits = slot_index[:, :, None] == slot_ids[None, None, :]
    routed_hits = jnp.any(hits, axis=1)
    half = cols // 2

    def as_lines(table):
        blocks = table.reshape(seq, experts, slots)
        none = jnp.zeros_like(blocks)
        pair = [jnp.stack([blocks, none], axis=2), jnp.stack([none, blocks], axis=2)]
        return [p.reshape(seq, experts * 2 * slots) for p in pair]

    select = jnp.concatenate(as_lines((routed_hits | dense_hits).astype(BF)), axis=0)
    halves = jnp.concatenate([own[:, :half], own[:, half:]], axis=0)
    outgoing = jnp.einsum("bs,bw->sw", select, halves, preferred_element_type=F32).astype(BF)
    arrived = swap(outgoing.reshape(experts, 2 * slots, half), HUB)
    other = partner(own)
    count = nz * nx * cap

    group = 8 * nc * 2 * slots
    lines = jnp.arange(group, dtype=jnp.int32)
    source, rest = lines // (4 * slots), lines % (4 * slots)
    side, h, kind, r = (
        rest // (2 * slots),
        rest // slots % 2,
        rest // cap % 2,
        rest % cap,
    )
    line_of = ((side * 2 + h) * 2 + kind) * (8 * cap) + source * cap + r
    both, dense_rows = call(
        unpack_rows,
        [shaped(ny, count + seq, nc * cols), shaped(nc, count, cols)],
        4 * 2 * group * group * half,
        at,
        line_of.reshape(1, group),
        arrived.reshape(-1, half),
        own,
        other,
    )
    whole = swap(both, "y")

    hidden_width = nx * dense_gate.shape[1]
    quarter = count // ny
    pre = call(
        dense_first_half,
        [shaped(quarter, 2 * hidden_width + 128)] * ny,
        2 * count * nc * cols * 2 * hidden_width,
        at,
        dense_rows,
        ffn_gain.reshape(ny * nc, cols),
        *dense_own,
        *dense_other,
    )
    pre = [pre[0]] + [shift(pre[d], "y", d) for d in range(1, ny)]
    (hidden,) = call(dense_activation, [shaped(quarter, hidden_width)], 10**6, *pre)
    hidden = [hidden] + [shift(hidden, "y", d) for d in range(1, ny)]
    (dense_part,) = call(
        dense_second_half,
        [shaped(nc, count, cols)],
        2 * count * nc * cols * hidden_width,
        at,
        *hidden,
        *dense_own,
        *dense_other,
    )

    (parts,) = call(
        experts_and_shared,
        [shaped(ny, count + seq, nc * cols)],
        2 * 3 * (count * 2 + seq) * width * expert_gate.shape[2],
        at,
        whole,
        ffn_gain.reshape(1, width),
        expert_gate,
        gate_other,
        expert_up,
        up_other,
        expert_down,
        down_other,
        shared_gate,
        shared_up,
        shared_down,
    )
    parts = swap(parts, "y")
    back, shared_own, shared_send = call(
        pack_lines,
        [
            shaped(experts * 2 * slots, half),
            shaped(seq, cols, dtype=F32),
            shaped(seq, cols),
        ],
        4 * 2 * group * group * half,
        at,
        line_of.reshape(group, 1),
        parts,
        dense_part,
    )

    results = swap(back.reshape(experts, 2 * slots, half), HUB)
    results = results.reshape(experts * 2 * slots, half)
    shared_out = shared_own + partner(shared_send).astype(F32)
    combine = jnp.sum(jnp.where(hits, route_weight[:, :, None], F32(0.0)), axis=1)
    sums = jnp.concatenate(
        as_lines(combine.astype(BF)) + as_lines(dense_hits.astype(BF)), axis=0
    )
    sums = dot(sums, results).reshape(2, 2, seq, half)
    routed = jnp.concatenate([sums[0, 0], sums[0, 1]], axis=1)
    dense_out = jnp.concatenate([sums[1, 0], sums[1, 1]], axis=1)
    mixed = (resid + routed + shared_out + jax.nn.sigmoid(dense_mix) * dense_out).astype(BF)
    return (mixed, new_state)


def solution(mesh):
    torus = Mesh(mesh.devices.reshape(8, 4, 4, 2), ("z", "x", "y", "c"))
    return jax.shard_map(
        step,
        mesh=torus,
        in_specs=(
            P(EP, None),
            P(EP, TP, None, None),
            P(),
            P(EP, TP),
            P(EP, TP),
            P(EP, TP),
            P(EP, TP),
            P(TP),
            P(TP),
            P(TP, None),
            P(),
            P(EP, None),
            P(EP, None),
            P(EP, None, TP),
            P(EP, None, TP),
            P(EP, TP, None),
            P(None, TP),
            P(None, TP),
            P(TP, None),
            P(TP, EP),
            P(TP, EP),
            P(EP, TP),
            P(TP),
        ),
        out_specs=(P(EP, TP), P(EP, TP, None, None)),
        check_vma=False,
    )
```

time: 176 us -> 187 us (1.062)
  the two profiles are of different devices: /device:TPU:1 before, /device:TPU:8 now
where the time goes in v3:
time: 187 us; the launch traced here: 183 us
  starting transfers between devices  60.7 us (32%)
  waiting for transfers between devices  58.7 us (31%)
  Pallas kernels  19.2 us (10%)
  other arithmetic  18.5 us (10%)
  local copies, waits for them, and re-layouts  17.4 us (9%)
  matrix products  7.3 us (4%)
    ppermute x15, waiting for transfers between devices, shift(): return lax.ppermute(x, axis, [(i, (i + by) % size) for i in range(size)])  34.8 us
    all_to_all x6, starting transfers between devices, swap(): return lax.all_to_all(x, axis, split_axis=0, concat_axis=0, tiled=True)  34.6 us
    ppermute x15, starting transfers between devices, shift(): return lax.ppermute(x, axis, [(i, (i + by) % size) for i in range(size)])  24.9 us
    all_to_all x6, waiting for transfers between devices, swap(): return lax.all_to_all(x, axis, split_axis=0, concat_axis=0, tiled=True)  22.4 us
    pallas_call x6, Pallas kernels, call(): pl.pallas_call(body, out_shape=outs, in_specs=specs, out_specs=[pl.BlockS...  19.2 us
    add x1, other arithmetic, step(): decay[..., None] * state  5.09 us
    reshape x6, local copies, waits for them, and re-layouts, as_lines(): return [p.reshape(seq, experts * 2 * slots) for p in pair]  4.74 us
    unnamed x65, local copies, waits for them, and re-layouts  4.1 us
  transfers between devices with their start and end apart: 31, of which 16 were waited for; matrix products, arithmetic and copies ran while one was open for 15% of the time, Pallas kernels for 9%

profile of v3, /device:TPU:8, one launch (start us, length us, event | category | flops | bytes accessed | tf_op | source)
XLA Modules:
  0.0 183.2 jit_solution(1650200995707182489)
XLA Ops:
  2.3 8.5 %all-to-all-start = ((bf16[8,64,512]{2,1,0:T(8,128)(2,1)}), bf16[8,64,512]{2,1,0:T(8,128)(2,1)S(1)}, u32[]{:S(2)}, u32[]{:S(2)}) async-start(bf16[8,64,512]{2,1,0:T(8,128)(2,1)} %broadcast_in_dim.10), calls=%async_computation | async-start | bytes 1048576 | tf_op jit(solution)/shard_map/all_to_all | solution.py:20
  13.7 2.8 %collective-permute-start.2 = (bf16[48,512]{1,0:T(8,128)(2,1)S(1)}, bf16[48,512]{1,0:T(8,128)(2,1)S(1)}, u32[]{:S(2)}, u32[]{:S(2)}) collective-permute-start(bf16[48,512]{1,0:T(8,128)(2,1)S(1)} %get-tuple-element.30), channel_id=1, source_target_pairs={{0,24},{8,0},{16,8},{24,16},{1,25},{9,1},{17,9},{25,17},{2,26},{10... | collective-permute-start | bytes 147464 | tf_op jit(solution)/shard_map/ppermute | solution.py:33
  19.9 2.2 %collective-permute-done.1 = bf16[48,512]{1,0:T(8,128)(2,1)S(1)} collective-permute-done((bf16[48,512]{1,0:T(8,128)(2,1)S(1)}, bf16[48,512]{1,0:T(8,128)(2,1)S(1)}, u32[]{:S(2)}, u32[]{:S(2)}) %collective-permute-start.1) | collective-permute-done | bytes 49184 | tf_op jit(solution)/shard_map/ppermute | solution.py:33
  22.6 5.6 %all-to-all-done = bf16[8,64,512]{2,1,0:T(8,128)(2,1)S(1)} async-done(((bf16[8,64,512]{2,1,0:T(8,128)(2,1)}), bf16[8,64,512]{2,1,0:T(8,128)(2,1)S(1)}, u32[]{:S(2)}, u32[]{:S(2)}) %all-to-all-start) | async-done | bytes 524320 | tf_op jit(solution)/shard_map/all_to_all | solution.py:20
  30.2 2.7 %collective-permute-start.4 = (bf16[48,512]{1,0:T(8,128)(2,1)S(1)}, bf16[48,512]{1,0:T(8,128)(2,1)S(1)}, u32[]{:S(2)}, u32[]{:S(2)}) collective-permute-start(bf16[48,512]{1,0:T(8,128)(2,1)S(1)} %get-tuple-element.28), channel_id=1, source_target_pairs={{0,16},{8,24},{16,0},{24,8},{1,17},{9,25},{17,1},{25,9},{2,18},{10... | collective-permute-start | bytes 147464 | tf_op jit(solution)/shard_map/ppermute | solution.py:33
  37.1 3.4 %fusion = f32[48,1,128]{2,1,0:T(1,128)S(1)} fusion(bf16[48,128,1]{1,0,2:T(8,128)(2,1)S(1)} %slice_bitcast_fusion.4, f32[48,128]{1,0:T(8,128)S(1)} %split.18, f32[48,128]{1,0:T(8,128)S(1)} %get-tuple-element.34, f32[48,1,128,128]{3,2,1,0:T(8,128)} %param.24, f32[48,128]{1,0:T(8,128)S(1)} %get-tuple-element.33), kind=kOutput, calls=%fused_computation | convolution fusion | flops 3932160 | bytes 3256320 | tf_op jit(solution)/shard_map/bhk,bhkv->bhv/dot_general | solution.py:302
  43.2 4.9 %all-to-all-start.1 = ((bf16[4,48,256]{2,1,0:T(8,128)(2,1)}), bf16[4,48,256]{2,1,0:T(8,128)(2,1)}, u32[]{:S(2)}, u32[]{:S(2)}) async-start(bf16[4,48,256]{2,1,0:T(8,128)(2,1)} %fusion.52), calls=%async_computation.1 | async-start | bytes 196608 | tf_op jit(solution)/shard_map/all_to_all | solution.py:20
  50.8 2.0 %reshape.674 = bf16[48,1536]{0,1:T(8,128)(2,1)} reshape(bf16[48,64,2,12]{0,3,2,1:T(8,128)(2,1)} %get-tuple-element.20) | data formatting | bytes 294912 | tf_op jit(solution)/shard_map/reshape | solution.py:338
  55.7 2.1 %convolution_convert_fusion = bf16[1536,128]{1,0:T(8,128)(2,1)} fusion(bf16[48,1536]{0,1:T(8,128)(2,1)S(1)} %reshape.675, bf16[48,1536]{0,1:T(8,128)(2,1)} %reshape.674, bf16[48,128]{1,0:T(8,128)(2,1)S(1)} %get-tuple-element.42, bf16[48,128]{1,0:T(8,128)(2,1)S(1)} %get-tuple-element.41), kind=kOutput, calls=%fused_computation.3 | convolution fusion | flops 38584320 | bytes 712704 | tf_op jit(solution)/shard_map/bs,bw->sw/dot_general | solution.py:342
  57.8 5.6 %all-to-all-start.2 = ((bf16[64,24,128]{2,1,0:T(8,128)(2,1)}), bf16[64,24,128]{2,1,0:T(8,128)(2,1)}, u32[]{:S(2)}, u32[]{:S(2)}) async-start(bf16[64,24,128]{2,1,0:T(8,128)(2,1)} %bitcast.119), calls=%async_computation.2 | async-start | bytes 786432 | tf_op jit(solution)/shard_map/all_to_all | solution.py:20
  66.6 1.7 collective-permute-start.11
  70.1 8.1 %all-to-all-done.2 = bf16[64,24,128]{2,1,0:T(8,128)(2,1)} async-done(((bf16[64,24,128]{2,1,0:T(8,128)(2,1)}), bf16[64,24,128]{2,1,0:T(8,128)(2,1)}, u32[]{:S(2)}, u32[]{:S(2)}) %all-to-all-start.2) | async-done | bytes 393248 | tf_op jit(solution)/shard_map/all_to_all | solution.py:20
  78.2 2.5 %shard_map.230 = (bf16[4,240,512]{2,1,0:T(8,128)(2,1)}, bf16[2,192,256]{2,1,0:T(8,128)(2,1)}) custom-call(s32[2]{0:T(128)} %pad_add_fusion.at, s32[1,384]{1,0:T(1,128)} %fusion.84.line_of, bf16[1536,128]{1,0:T(8,128)(2,1)} %bitcast.20.lines, bf16[48,256]{1,0:T(8,128)(2,1)} %copy-done.19, bf16[48,256]{1,0:T(8,128)(2,1)} %copy-done.31), custom_call_target="tpu_custom_call" | custom-call | flops 150994944 | bytes 1623560 | tf_op jit(solution)/shard_map/pallas_call | solution.py:56
  80.7 4.8 %all-to-all-start.3 = ((bf16[4,240,512]{2,1,0:T(8,128)(2,1)}), bf16[4,240,512]{2,1,0:T(8,128)(2,1)S(1)}, u32[]{:S(2)}, u32[]{:S(2)}) async-start(bf16[4,240,512]{2,1,0:T(8,128)(2,1)} %get-tuple-element.11), calls=%async_computation.3 | async-start | bytes 1966080 | tf_op jit(solution)/shard_map/all_to_all | solution.py:20
  85.6 2.9 %collective-permute-start.12 = (bf16[3,256,256]{2,1,0:T(8,128)(2,1)S(1)}, bf16[3,256,256]{2,1,0:T(8,128)(2,1)}, u32[]{:S(2)}, u32[]{:S(2)}) collective-permute-start(bf16[3,256,256]{2,1,0:T(8,128)(2,1)S(1)} %pad_maximum_fusion.1.refs_0_.refs_4_), channel_id=1, source_target_pairs={{0,16},{8,24},{16,0},{24,8},{1,17},{9,25},{17,1},{25,9},{2,18},{10... | collective-permute-start | bytes 1179656 | tf_op jit(solution)/shard_map/ppermute | solution.py:33
  89.7 9.0 %collective-permute-done.12.refs_2_.refs_6_ = bf16[3,256,256]{2,1,0:T(8,128)(2,1)} collective-permute-done((bf16[3,256,256]{2,1,0:T(8,128)(2,1)S(1)}, bf16[3,256,256]{2,1,0:T(8,128)(2,1)}, u32[]{:S(2)}, u32[]{:S(2)}) %collective-permute-start.12) | collective-permute-done | bytes 393248 | tf_op jit(solution)/shard_map/ppermute | solution.py:33
  98.8 8.3 %collective-permute-done.13.refs_3_.refs_7_ = bf16[3,256,256]{2,1,0:T(8,128)(2,1)} collective-permute-done((bf16[3,256,256]{2,1,0:T(8,128)(2,1)S(1)}, bf16[3,256,256]{2,1,0:T(8,128)(2,1)}, u32[]{:S(2)}, u32[]{:S(2)}) %collective-permute-start.13) | collective-permute-done | bytes 393248 | tf_op jit(solution)/shard_map/ppermute | solution.py:33
  108.9 5.6 %shard_map.231 = bf16[4,240,512]{2,1,0:T(8,128)(2,1)} custom-call(s32[2]{0:T(128)} %pad_add_fusion.at, bf16[4,240,512]{2,1,0:T(8,128)(2,1)} %copy-done.2, f32[1,2048]{1,0:T(1,128)} %bitcast.128, bf16[2,2048,128]{2,1,0:T(8,128)(2,1)} %gate.1, bf16[2048,128]{1,0:T(8,128)(2,1)} %collective-permute-done.8.gate_other, bf16[2,2048,128]{2,1,0:T(8,128)(2,1)} %up.1, ...), custom_call_target="tpu_custom_call" | custom-call | flops 679477248 | bytes 8265736 | tf_op jit(solution)/shard_map/pallas_call | solution.py:56
  114.5 4.8 %all-to-all-start.4 = ((bf16[4,240,512]{2,1,0:T(8,128)(2,1)}), bf16[4,240,512]{2,1,0:T(8,128)(2,1)S(1)}, u32[]{:S(2)}, u32[]{:S(2)}) async-start(bf16[4,240,512]{2,1,0:T(8,128)(2,1)} %shard_map.231), calls=%async_computation.4 | async-start | bytes 1966080 | tf_op jit(solution)/shard_map/all_to_all | solution.py:20
  120.3 3.4 %shard_map.232 = (bf16[48,2176]{1,0:T(8,128)(2,1)}, bf16[48,2176]{1,0:T(8,128)(2,1)}, bf16[48,2176]{1,0:T(8,128)(2,1)}, bf16[48,2176]{1,0:T(8,128)(2,1)}) custom-call(s32[2]{0:T(128)} %pad_add_fusion.at, bf16[2,192,256]{2,1,0:T(8,128)(2,1)} %get-tuple-element.12.rows, f32[8,256]{1,0:T(8,128)} %reshape.679.gain, bf16[3,256,256]{2,1,0:T(8,128)(2,1)} %copy-done.3, ...), custom_call_target="tpu_custom_call" | custom-call | flops 402653184 | bytes 4186120 | tf_op jit(solution)/shard_map/pallas_call | solution.py:56
  125.8 2.5 %collective-permute-start.20 = (bf16[48,2176]{1,0:T(8,128)(2,1)}, bf16[48,2176]{1,0:T(8,128)(2,1)}, u32[]{:S(2)}, u32[]{:S(2)}) collective-permute-start(bf16[48,2176]{1,0:T(8,128)(2,1)} %get-tuple-element.16), channel_id=1, source_target_pairs={{0,6},{2,0},{4,2},{6,4},{1,7},{3,1},{5,3},{7,5},{8,14},{10,8},{12,... | collective-permute-start | bytes 626696 | tf_op jit(solution)/shard_map/ppermute | solution.py:33
  132.5 3.6 %collective-permute-done.18.b = bf16[48,2176]{1,0:T(8,128)(2,1)S(1)} collective-permute-done((bf16[48,2176]{1,0:T(8,128)(2,1)}, bf16[48,2176]{1,0:T(8,128)(2,1)S(1)}, u32[]{:S(2)}, u32[]{:S(2)}) %collective-permute-start.18) | collective-permute-done | bytes 208928 | tf_op jit(solution)/shard_map/ppermute | solution.py:33
  136.1 2.2 %collective-permute-done.19.c = bf16[48,2176]{1,0:T(8,128)(2,1)} collective-permute-done((bf16[48,2176]{1,0:T(8,128)(2,1)}, bf16[48,2176]{1,0:T(8,128)(2,1)}, u32[]{:S(2)}, u32[]{:S(2)}) %collective-permute-start.19) | collective-permute-done | bytes 208928 | tf_op jit(solution)/shard_map/ppermute | solution.py:33
  138.3 3.5 %collective-permute-done.20.d = bf16[48,2176]{1,0:T(8,128)(2,1)} collective-permute-done((bf16[48,2176]{1,0:T(8,128)(2,1)}, bf16[48,2176]{1,0:T(8,128)(2,1)}, u32[]{:S(2)}, u32[]{:S(2)}) %collective-permute-start.20) | collective-permute-done | bytes 208928 | tf_op jit(solution)/shard_map/ppermute | solution.py:33
  141.8 2.1 %shard_map.233.refs_0_ = bf16[48,1024]{1,0:T(8,128)(2,1)} custom-call(bf16[48,2176]{1,0:T(8,128)(2,1)} %get-tuple-element.13.a, bf16[48,2176]{1,0:T(8,128)(2,1)} %copy-done.18, bf16[48,2176]{1,0:T(8,128)(2,1)} %collective-permute-done.19.c, bf16[48,2176]{1,0:T(8,128)(2,1)} %collective-permute-done.20.d), custom_call_target="tpu_custom_call" | custom-call | flops 1000000 | bytes 933888 | tf_op jit(solution)/shard_map/pallas_call | solution.py:56
  144.6 3.0 %collective-permute-start.22 = (bf16[48,1024]{1,0:T(8,128)(2,1)}, bf16[48,1024]{1,0:T(8,128)(2,1)S(1)}, u32[]{:S(2)}, u32[]{:S(2)}) collective-permute-start(bf16[48,1024]{1,0:T(8,128)(2,1)} %shard_map.233.refs_0_), channel_id=1, source_target_pairs={{0,4},{2,6},{4,0},{6,2},{1,5},{3,7},{5,1},{7,3},{8,12},{10,14},{12... | collective-permute-start | bytes 294920 | tf_op jit(solution)/shard_map/ppermute | solution.py:33
  149.3 2.0 %collective-permute-done.22.refs_2_ = bf16[48,1024]{1,0:T(8,128)(2,1)S(1)} collective-permute-done((bf16[48,1024]{1,0:T(8,128)(2,1)}, bf16[48,1024]{1,0:T(8,128)(2,1)S(1)}, u32[]{:S(2)}, u32[]{:S(2)}) %collective-permute-start.22) | collective-permute-done | bytes 98336 | tf_op jit(solution)/shard_map/ppermute | solution.py:33
  153.0 3.1 %shard_map.234.dense = bf16[2,192,256]{2,1,0:T(8,128)(2,1)} custom-call(s32[2]{0:T(128)} %pad_add_fusion.at, bf16[48,1024]{1,0:T(8,128)(2,1)} %shard_map.233.refs_0_, bf16[48,1024]{1,0:T(8,128)(2,1)} %copy-done.21, bf16[48,1024]{1,0:T(8,128)(2,1)} %copy-done.22, bf16[48,1024]{1,0:T(8,128)(2,1)} %copy-done.23, bf16[3,256,256]{2,1,0:T(8,128)(2,1)} %copy-done.3, ...), custom_call_target="tpu_custom_call" | custom-call | flops 201326592 | bytes 3735560 | tf_op jit(solution)/shard_map/pallas_call | solution.py:56
  157.0 2.6 %shard_map.235 = (bf16[1536,128]{1,0:T(8,128)(2,1)}, f32[48,256]{1,0:T(8,128)}, bf16[48,256]{1,0:T(8,128)(2,1)}) custom-call(s32[2]{0:T(128)} %pad_add_fusion.at, s32[384,1]{1,0:T(8,128)} %fusion.23.line_of, bf16[4,240,512]{2,1,0:T(8,128)(2,1)} %copy-done.1, bf16[2,192,256]{2,1,0:T(8,128)(2,1)} %shard_map.234.dense), custom_call_target="tpu_custom_call" | custom-call | flops 150994944 | bytes 1648136 | tf_op jit(solution)/shard_map/pallas_call | solution.py:56
  159.6 6.0 %all-to-all-start.5 = ((bf16[64,24,128]{2,1,0:T(8,128)(2,1)}), bf16[64,24,128]{2,1,0:T(8,128)(2,1)}, u32[]{:S(2)}, u32[]{:S(2)}) async-start(bf16[64,24,128]{2,1,0:T(8,128)(2,1)} %bitcast.122), calls=%async_computation.5 | async-start | bytes 786432 | tf_op jit(solution)/shard_map/all_to_all | solution.py:20
  166.7 5.1 %multiply_add_fusion = f32[48,1,128,128]{3,2,1,0:T(8,128)} fusion(f32[48,1,128,128]{3,2,1,0:T(8,128)} %param.24, f32[48,128]{1,0:T(8,128)S(1)} %copy-done.13, f32[48,128]{1,0:T(8,128)S(1)} %copy-done.17, f32[48,128]{1,0:T(8,128)S(1)} %copy-done.15), kind=kLoop, calls=%fused_computation.2 | loop fusion | flops 2359296 | bytes 6365184 | tf_op jit(solution)/shard_map/add | solution.py:301
  171.8 8.7 %all-to-all-done.5 = bf16[64,24,128]{2,1,0:T(8,128)(2,1)} async-done(((bf16[64,24,128]{2,1,0:T(8,128)(2,1)}), bf16[64,24,128]{2,1,0:T(8,128)(2,1)}, u32[]{:S(2)}, u32[]{:S(2)}) %all-to-all-start.5) | async-done | bytes 393248 | tf_op jit(solution)/shard_map/all_to_all | solution.py:20
  (174 shorter events, 46.6 us)
Async XLA Ops:
  2.3 26.0 %all-to-all-start = ((bf16[8,64,512]{2,1,0:T(8,128)(2,1)}), bf16[8,64,512]{2,1,0:T(8,128)(2,1)S(1)}, u32[]{:S(2)}, u32[]{:S(2)}) async-start(bf16[8,64,512]{2,1,0:T(8,128)(2,1)} %broadcast_in_dim.10), calls=%async_computation | async-start | bytes 1048576 | tf_op jit(solution)/shard_map/all_to_all | solution.py:20
  13.7 6.2 %collective-permute-start.2 = (bf16[48,512]{1,0:T(8,128)(2,1)S(1)}, bf16[48,512]{1,0:T(8,128)(2,1)S(1)}, u32[]{:S(2)}, u32[]{:S(2)}) collective-permute-start(bf16[48,512]{1,0:T(8,128)(2,1)S(1)} %get-tuple-element.30), channel_id=1, source_target_pairs={{0,24},{8,0},{16,8},{24,16},{1,25},{9,1},{17,9},{25,17},{2,26},{10... | collective-permute-start | bytes 147464 | tf_op jit(solution)/shard_map/ppermute | solution.py:33
  16.5 5.6 %collective-permute-start.1 = (bf16[48,512]{1,0:T(8,128)(2,1)S(1)}, bf16[48,512]{1,0:T(8,128)(2,1)S(1)}, u32[]{:S(2)}, u32[]{:S(2)}) collective-permute-start(bf16[48,512]{1,0:T(8,128)(2,1)S(1)} %get-tuple-element.31), channel_id=1, source_target_pairs={{0,16},{8,24},{16,0},{24,8},{1,17},{9,25},{17,1},{25,9},{2,18},{10... | collective-permute-start | bytes 147464 | tf_op jit(solution)/shard_map/ppermute | solution.py:33
  17.3 5.3 %collective-permute-start = (bf16[48,512]{1,0:T(8,128)(2,1)S(1)}, bf16[48,512]{1,0:T(8,128)(2,1)S(1)}, u32[]{:S(2)}, u32[]{:S(2)}) collective-permute-start(bf16[48,512]{1,0:T(8,128)(2,1)S(1)} %get-tuple-element.32), channel_id=1, source_target_pairs={{0,8},{8,16},{16,24},{24,0},{1,9},{9,17},{17,25},{25,1},{2,10},{10... | collective-permute-start | bytes 147464 | tf_op jit(solution)/shard_map/ppermute | solution.py:33
  28.6 6.1 %collective-permute-start.5 = (bf16[48,512]{1,0:T(8,128)(2,1)S(1)}, bf16[48,512]{1,0:T(8,128)(2,1)S(1)}, u32[]{:S(2)}, u32[]{:S(2)}) collective-permute-start(bf16[48,512]{1,0:T(8,128)(2,1)S(1)} %get-tuple-element.27), channel_id=1, source_target_pairs={{0,8},{8,16},{16,24},{24,0},{1,9},{9,17},{17,25},{25,1},{2,10},{10... | collective-permute-start | bytes 147464 | tf_op jit(solution)/shard_map/ppermute | solution.py:33
  30.2 5.6 %collective-permute-start.4 = (bf16[48,512]{1,0:T(8,128)(2,1)S(1)}, bf16[48,512]{1,0:T(8,128)(2,1)S(1)}, u32[]{:S(2)}, u32[]{:S(2)}) collective-permute-start(bf16[48,512]{1,0:T(8,128)(2,1)S(1)} %get-tuple-element.28), channel_id=1, source_target_pairs={{0,16},{8,24},{16,0},{24,8},{1,17},{9,25},{17,1},{25,9},{2,18},{10... | collective-permute-start | bytes 147464 | tf_op jit(solution)/shard_map/ppermute | solution.py:33
  32.9 4.1 %collective-permute-start.3 = (bf16[48,512]{1,0:T(8,128)(2,1)S(1)}, bf16[48,512]{1,0:T(8,128)(2,1)S(1)}, u32[]{:S(2)}, u32[]{:S(2)}) collective-permute-start(bf16[48,512]{1,0:T(8,128)(2,1)S(1)} %get-tuple-element.26), channel_id=1, source_target_pairs={{0,24},{8,0},{16,8},{24,16},{1,25},{9,1},{17,9},{25,17},{2,26},{10... | collective-permute-start | bytes 147464 | tf_op jit(solution)/shard_map/ppermute | solution.py:33
  41.2 1.4 collective-permute-start.6
  43.2 9.6 %all-to-all-start.1 = ((bf16[4,48,256]{2,1,0:T(8,128)(2,1)}), bf16[4,48,256]{2,1,0:T(8,128)(2,1)}, u32[]{:S(2)}, u32[]{:S(2)}) async-start(bf16[4,48,256]{2,1,0:T(8,128)(2,1)} %fusion.52), calls=%async_computation.1 | async-start | bytes 196608 | tf_op jit(solution)/shard_map/all_to_all | solution.py:20
  57.8 20.4 %all-to-all-start.2 = ((bf16[64,24,128]{2,1,0:T(8,128)(2,1)}), bf16[64,24,128]{2,1,0:T(8,128)(2,1)}, u32[]{:S(2)}, u32[]{:S(2)}) async-start(bf16[64,24,128]{2,1,0:T(8,128)(2,1)} %bitcast.119), calls=%async_computation.2 | async-start | bytes 786432 | tf_op jit(solution)/shard_map/all_to_all | solution.py:20
  64.2 42.9 %collective-permute-start.8 = (bf16[2048,128]{1,0:T(8,128)(2,1)}, bf16[2048,128]{1,0:T(8,128)(2,1)}, u32[]{:S(2)}, u32[]{:S(2)}) collective-permute-start(bf16[2048,128]{1,0:T(8,128)(2,1)} %dynamic-slice_bitcast_fusion.2), channel_id=1, source_target_pairs={{0,1},{1,0},{2,3},{3,2},{4,5},{5,4},{6,7},{7,6},{8,9},{9,8},{10,11... | collective-permute-start | bytes 1572872 | tf_op jit(solution)/shard_map/ppermute | solution.py:28
  65.0 42.6 %collective-permute-start.9 = (bf16[2048,128]{1,0:T(8,128)(2,1)}, bf16[2048,128]{1,0:T(8,128)(2,1)}, u32[]{:S(2)}, u32[]{:S(2)}) collective-permute-start(bf16[2048,128]{1,0:T(8,128)(2,1)} %dynamic-slice_bitcast_fusion.1), channel_id=1, source_target_pairs={{0,1},{1,0},{2,3},{3,2},{4,5},{5,4},{6,7},{7,6},{8,9},{9,8},{10,11... | collective-permute-start | bytes 1572872 | tf_op jit(solution)/shard_map/ppermute | solution.py:28
  66.6 47.8 %copy-start.3 = (bf16[3,256,256]{2,1,0:T(8,128)(2,1)}, bf16[3,256,256]{2,1,0:T(8,128)(2,1)S(1)}, u32[]{:S(2)}) copy-start(bf16[3,256,256]{2,1,0:T(8,128)(2,1)S(1)} %pad_maximum_fusion.1.refs_0_.refs_4_) | copy-start | bytes 1179652
  66.6 21.9 %collective-permute-start.11 = (bf16[3,256,256]{2,1,0:T(8,128)(2,1)S(1)}, bf16[3,256,256]{2,1,0:T(8,128)(2,1)}, u32[]{:S(2)}, u32[]{:S(2)}) collective-permute-start(bf16[3,256,256]{2,1,0:T(8,128)(2,1)S(1)} %pad_maximum_fusion.1.refs_0_.refs_4_), channel_id=1, source_target_pairs={{0,8},{8,16},{16,24},{24,0},{1,9},{9,17},{17,25},{25,1},{2,10},{10... | collective-permute-start | bytes 1179656 | tf_op jit(solution)/shard_map/ppermute | solution.py:33
  68.9 1.2 collective-permute-start.7
  80.7 27.0 %all-to-all-start.3 = ((bf16[4,240,512]{2,1,0:T(8,128)(2,1)}), bf16[4,240,512]{2,1,0:T(8,128)(2,1)S(1)}, u32[]{:S(2)}, u32[]{:S(2)}) async-start(bf16[4,240,512]{2,1,0:T(8,128)(2,1)} %get-tuple-element.11), calls=%async_computation.3 | async-start | bytes 1966080 | tf_op jit(solution)/shard_map/all_to_all | solution.py:20
  85.5 22.2 %collective-permute-start.10 = (bf16[128,2048]{1,0:T(8,128)(2,1)S(1)}, bf16[128,2048]{1,0:T(8,128)(2,1)S(1)}, u32[]{:S(2)}, u32[]{:S(2)}) collective-permute-start(bf16[128,2048]{1,0:T(8,128)(2,1)S(1)} %dynamic-slice_bitcast_fusion), channel_id=1, source_target_pairs={{0,1},{1,0},{2,3},{3,2},{4,5},{5,4},{6,7},{7,6},{8,9},{9,8},{10,11... | collective-permute-start | bytes 1572872 | tf_op jit(solution)/shard_map/ppermute | solution.py:28
  85.6 13.1 %collective-permute-start.12 = (bf16[3,256,256]{2,1,0:T(8,128)(2,1)S(1)}, bf16[3,256,256]{2,1,0:T(8,128)(2,1)}, u32[]{:S(2)}, u32[]{:S(2)}) collective-permute-start(bf16[3,256,256]{2,1,0:T(8,128)(2,1)S(1)} %pad_maximum_fusion.1.refs_0_.refs_4_), channel_id=1, source_target_pairs={{0,16},{8,24},{16,0},{24,8},{1,17},{9,25},{17,1},{25,9},{2,18},{10... | collective-permute-start | bytes 1179656 | tf_op jit(solution)/shard_map/ppermute | solution.py:33
  88.6 18.6 %collective-permute-start.13 = (bf16[3,256,256]{2,1,0:T(8,128)(2,1)S(1)}, bf16[3,256,256]{2,1,0:T(8,128)(2,1)}, u32[]{:S(2)}, u32[]{:S(2)}) collective-permute-start(bf16[3,256,256]{2,1,0:T(8,128)(2,1)S(1)} %pad_maximum_fusion.1.refs_0_.refs_4_), channel_id=1, source_target_pairs={{0,24},{8,0},{16,8},{24,16},{1,25},{9,1},{17,9},{25,17},{2,26},{10... | collective-permute-start | bytes 1179656 | tf_op jit(solution)/shard_map/ppermute | solution.py:33
  98.8 21.5 %collective-permute-start.14 = (bf16[3,256,256]{2,1,0:T(8,128)(2,1)S(1)}, bf16[3,256,256]{2,1,0:T(8,128)(2,1)}, u32[]{:S(2)}, u32[]{:S(2)}) collective-permute-start(bf16[3,256,256]{2,1,0:T(8,128)(2,1)S(1)} %pad_maximum_fusion.1.refs_0_.refs_4_), channel_id=1, source_target_pairs={{0,1},{1,0},{2,3},{3,2},{4,5},{5,4},{6,7},{7,6},{8,9},{9,8},{10,11... | collective-permute-start | bytes 1179656 | tf_op jit(solution)/shard_map/ppermute | solution.py:28
  107.1 13.1 %collective-permute-start.15 = (bf16[3,256,256]{2,1,0:T(8,128)(2,1)}, bf16[3,256,256]{2,1,0:T(8,128)(2,1)}, u32[]{:S(2)}, u32[]{:S(2)}) collective-permute-start(bf16[3,256,256]{2,1,0:T(8,128)(2,1)} %collective-permute-done.11.refs_1_.refs_5_), channel_id=1, source_target_pairs={{0,1},{1,0},{2,3},{3,2},{4,5},{5,4},{6,7},{7,6},{8,9},{9,8},{10,11... | collective-permute-start | bytes 1179656 | tf_op jit(solution)/shard_map/ppermute | solution.py:28
  107.1 13.2 %collective-permute-start.16 = (bf16[3,256,256]{2,1,0:T(8,128)(2,1)}, bf16[3,256,256]{2,1,0:T(8,128)(2,1)}, u32[]{:S(2)}, u32[]{:S(2)}) collective-permute-start(bf16[3,256,256]{2,1,0:T(8,128)(2,1)} %collective-permute-done.12.refs_2_.refs_6_), channel_id=1, source_target_pairs={{0,1},{1,0},{2,3},{3,2},{4,5},{5,4},{6,7},{7,6},{8,9},{9,8},{10,11... | collective-permute-start | bytes 1179656 | tf_op jit(solution)/shard_map/ppermute | solution.py:28
  107.6 12.6 %collective-permute-start.17 = (bf16[3,256,256]{2,1,0:T(8,128)(2,1)}, bf16[3,256,256]{2,1,0:T(8,128)(2,1)}, u32[]{:S(2)}, u32[]{:S(2)}) collective-permute-start(bf16[3,256,256]{2,1,0:T(8,128)(2,1)} %collective-permute-done.13.refs_3_.refs_7_), channel_id=1, source_target_pairs={{0,1},{1,0},{2,3},{3,2},{4,5},{5,4},{6,7},{7,6},{8,9},{9,8},{10,11... | collective-permute-start | bytes 1179656 | tf_op jit(solution)/shard_map/ppermute | solution.py:28
  114.5 41.6 %all-to-all-start.4 = ((bf16[4,240,512]{2,1,0:T(8,128)(2,1)}), bf16[4,240,512]{2,1,0:T(8,128)(2,1)S(1)}, u32[]{:S(2)}, u32[]{:S(2)}) async-start(bf16[4,240,512]{2,1,0:T(8,128)(2,1)} %shard_map.231), calls=%async_computation.4 | async-start | bytes 1966080 | tf_op jit(solution)/shard_map/all_to_all | solution.py:20
  123.7 12.4 %collective-permute-start.18 = (bf16[48,2176]{1,0:T(8,128)(2,1)}, bf16[48,2176]{1,0:T(8,128)(2,1)S(1)}, u32[]{:S(2)}, u32[]{:S(2)}) collective-permute-start(bf16[48,2176]{1,0:T(8,128)(2,1)} %get-tuple-element.14), channel_id=1, source_target_pairs={{0,2},{2,4},{4,6},{6,0},{1,3},{3,5},{5,7},{7,1},{8,10},{10,12},{12... | collective-permute-start | bytes 626696 | tf_op jit(solution)/shard_map/ppermute | solution.py:33
  125.1 13.1 %collective-permute-start.19 = (bf16[48,2176]{1,0:T(8,128)(2,1)}, bf16[48,2176]{1,0:T(8,128)(2,1)}, u32[]{:S(2)}, u32[]{:S(2)}) collective-permute-start(bf16[48,2176]{1,0:T(8,128)(2,1)} %get-tuple-element.15), channel_id=1, source_target_pairs={{0,4},{2,6},{4,0},{6,2},{1,5},{3,7},{5,1},{7,3},{8,12},{10,14},{12... | collective-permute-start | bytes 626696 | tf_op jit(solution)/shard_map/ppermute | solution.py:33
  125.8 16.0 %collective-permute-start.20 = (bf16[48,2176]{1,0:T(8,128)(2,1)}, bf16[48,2176]{1,0:T(8,128)(2,1)}, u32[]{:S(2)}, u32[]{:S(2)}) collective-permute-start(bf16[48,2176]{1,0:T(8,128)(2,1)} %get-tuple-element.16), channel_id=1, source_target_pairs={{0,6},{2,0},{4,2},{6,4},{1,7},{3,1},{5,3},{7,5},{8,14},{10,8},{12,... | collective-permute-start | bytes 626696 | tf_op jit(solution)/shard_map/ppermute | solution.py:33
  143.9 5.5 %collective-permute-start.21 = (bf16[48,1024]{1,0:T(8,128)(2,1)}, bf16[48,1024]{1,0:T(8,128)(2,1)S(1)}, u32[]{:S(2)}, u32[]{:S(2)}) collective-permute-start(bf16[48,1024]{1,0:T(8,128)(2,1)} %shard_map.233.refs_0_), channel_id=1, source_target_pairs={{0,2},{2,4},{4,6},{6,0},{1,3},{3,5},{5,7},{7,1},{8,10},{10,12},{12... | collective-permute-start | bytes 294920 | tf_op jit(solution)/shard_map/ppermute | solution.py:33
  144.6 6.7 %collective-permute-start.22 = (bf16[48,1024]{1,0:T(8,128)(2,1)}, bf16[48,1024]{1,0:T(8,128)(2,1)S(1)}, u32[]{:S(2)}, u32[]{:S(2)}) collective-permute-start(bf16[48,1024]{1,0:T(8,128)(2,1)} %shard_map.233.refs_0_), channel_id=1, source_target_pairs={{0,4},{2,6},{4,0},{6,2},{1,5},{3,7},{5,1},{7,3},{8,12},{10,14},{12... | collective-permute-start | bytes 294920 | tf_op jit(solution)/shard_map/ppermute | solution.py:33
  147.5 4.8 %collective-permute-start.23 = (bf16[48,1024]{1,0:T(8,128)(2,1)}, bf16[48,1024]{1,0:T(8,128)(2,1)S(1)}, u32[]{:S(2)}, u32[]{:S(2)}) collective-permute-start(bf16[48,1024]{1,0:T(8,128)(2,1)} %shard_map.233.refs_0_), channel_id=1, source_target_pairs={{0,6},{2,0},{4,2},{6,4},{1,7},{3,1},{5,3},{7,5},{8,14},{10,8},{12,... | collective-permute-start | bytes 294920 | tf_op jit(solution)/shard_map/ppermute | solution.py:33
  159.6 20.9 %all-to-all-start.5 = ((bf16[64,24,128]{2,1,0:T(8,128)(2,1)}), bf16[64,24,128]{2,1,0:T(8,128)(2,1)}, u32[]{:S(2)}, u32[]{:S(2)}) async-start(bf16[64,24,128]{2,1,0:T(8,128)(2,1)} %bitcast.122), calls=%async_computation.5 | async-start | bytes 786432 | tf_op jit(solution)/shard_map/all_to_all | solution.py:20
  171.8 10.0 %collective-permute-start.24 = (bf16[48,256]{1,0:T(8,128)(2,1)S(1)}, bf16[48,256]{1,0:T(8,128)(2,1)S(1)}, u32[]{:S(2)}, u32[]{:S(2)}) collective-permute-start(bf16[48,256]{1,0:T(8,128)(2,1)S(1)} %copy-done.30), channel_id=1, source_target_pairs={{0,1},{1,0},{2,3},{3,2},{4,5},{5,4},{6,7},{7,6},{8,9},{9,8},{10,11... | collective-permute-start | bytes 73736 | tf_op jit(solution)/shard_map/ppermute | solution.py:28
  (31 other events, 315.7 us)

commit v4 on v3

--- a/solution.py
+++ b/solution.py
@@ -45,7 +45,7 @@
     return x * jax.nn.sigmoid(x)
 
 
-def call(body, outs, flops, *args):
+def call(body, outs, flops, *args, mib=12):
     moved = sum(a.size * a.dtype.itemsize for a in args) + sum(
         o.size * o.dtype.itemsize for o in outs
     )
@@ -59,6 +59,7 @@
         in_specs=specs,
         out_specs=[pl.BlockSpec(memory_space=pltpu.VMEM) for _ in outs],
         cost_estimate=pl.CostEstimate(flops=flops, bytes_accessed=moved, transcendentals=0),
+        compiler_params=pltpu.CompilerParams(vmem_limit_bytes=mib * 2**20),
     )(*args)
 
 
@@ -283,7 +284,7 @@
     projected = part[0].astype(F32)
     for d in range(1, nx):
         projected = projected + shift(part[d], "x", -d).astype(F32)
-    projected = lax.optimization_barrier(projected.astype(BF)).astype(F32)
+    projected = projected.astype(BF).astype(F32)
     query, forget_pre, values, out_gate = jnp.split(projected, 4, axis=1)
 
     at = jnp.stack([y, c]).astype(jnp.int32)
@@ -363,6 +364,7 @@
         arrived.reshape(-1, half),
         own,
         other,
+        mib=60,
     )
     whole = swap(both, "y")
 
@@ -407,6 +409,7 @@
         shared_gate,
         shared_up,
         shared_down,
+        mib=24,
     )
     parts = swap(parts, "y")
     back, shared_own, shared_send = call(

time: 187 us -> 184 us (0.984)
  local copies, waits for them, and re-layouts: 17.4 us -> 29 us
  Pallas kernels: 19.2 us -> 13.1 us
  waiting for transfers between devices: 58.7 us -> 53.3 us
    pallas_call x6, Pallas kernels: 19.2 us -> 13.1 us  [call(): pl.pallas_call(body, out_shape=outs, in_specs=specs, out_specs=[pl.BlockS...]
    ppermute x15, waiting for transfers between devices: 34.8 us -> 29.5 us  [shift(): return lax.ppermute(x, axis, [(i, (i + by) % size) for i in range(size)])]
    reshape x6, local copies, waits for them, and re-layouts: 4.74 us -> 9.91 us  [as_lines(): return [p.reshape(seq, experts * 2 * slots) for p in pair]]
    unnamed x65 -> x67, local copies, waits for them, and re-layouts: 4.1 us -> 8.23 us
  transfers between devices with their start and end apart: 31 -> 31, of which waited for: 16 -> 15; matrix products, arithmetic and copies ran while one was open for 15% -> 18% of each run, Pallas kernels for 9% -> 6%
where the time goes in v4:
time: 184 us; the launch traced here: 181 us
  starting transfers between devices  60.7 us (33%)
  waiting for transfers between devices  53.3 us (29%)
  local copies, waits for them, and re-layouts  29 us (16%)
  other arithmetic  17.1 us (9%)
  Pallas kernels  13.1 us (7%)
  matrix products  6.43 us (3%)
    all_to_all x6, starting transfers between devices, swap(): return lax.all_to_all(x, axis, split_axis=0, concat_axis=0, tiled=True)  34.5 us
    ppermute x15, waiting for transfers between devices, shift(): return lax.ppermute(x, axis, [(i, (i + by) % size) for i in range(size)])  29.5 us
    ppermute x15, starting transfers between devices, shift(): return lax.ppermute(x, axis, [(i, (i + by) % size) for i in range(size)])  24.8 us
    all_to_all x6, waiting for transfers between devices, swap(): return lax.all_to_all(x, axis, split_axis=0, concat_axis=0, tiled=True)  22.3 us
    pallas_call x6, Pallas kernels, call(): pl.pallas_call(body, out_shape=outs, in_specs=specs, out_specs=[pl.BlockS...  13.1 us
    reshape x6, local copies, waits for them, and re-layouts, as_lines(): return [p.reshape(seq, experts * 2 * slots) for p in pair]  9.91 us
    unnamed x67, local copies, waits for them, and re-layouts  8.23 us
    add x1, other arithmetic, step(): decay[..., None] * state  5.08 us
  transfers between devices with their start and end apart: 31, of which 15 were waited for; matrix products, arithmetic and copies ran while one was open for 18% of the time, Pallas kernels for 6%

profile of v4, /device:TPU:8, one launch (start us, length us, event | category | flops | bytes accessed | tf_op | source)
XLA Modules:
  0.0 181.0 jit_solution(2831546954319944253)
XLA Ops:
  2.3 8.5 %all-to-all-start = ((bf16[8,64,512]{2,1,0:T(8,128)(2,1)}), bf16[8,64,512]{2,1,0:T(8,128)(2,1)S(1)}, u32[]{:S(2)}, u32[]{:S(2)}) async-start(bf16[8,64,512]{2,1,0:T(8,128)(2,1)} %broadcast_in_dim.10), calls=%async_computation | async-start | bytes 1048576 | tf_op jit(solution)/shard_map/all_to_all | solution.py:20
  13.7 2.8 %collective-permute-start.2 = (bf16[48,512]{1,0:T(8,128)(2,1)S(1)}, bf16[48,512]{1,0:T(8,128)(2,1)S(1)}, u32[]{:S(2)}, u32[]{:S(2)}) collective-permute-start(bf16[48,512]{1,0:T(8,128)(2,1)S(1)} %get-tuple-element.32), channel_id=1, source_target_pairs={{0,24},{8,0},{16,8},{24,16},{1,25},{9,1},{17,9},{25,17},{2,26},{10... | collective-permute-start | bytes 147464 | tf_op jit(solution)/shard_map/ppermute | solution.py:33
  19.9 2.2 %collective-permute-done.1 = bf16[48,512]{1,0:T(8,128)(2,1)S(1)} collective-permute-done((bf16[48,512]{1,0:T(8,128)(2,1)S(1)}, bf16[48,512]{1,0:T(8,128)(2,1)S(1)}, u32[]{:S(2)}, u32[]{:S(2)}) %collective-permute-start.1) | collective-permute-done | bytes 49184 | tf_op jit(solution)/shard_map/ppermute | solution.py:33
  22.6 5.6 %all-to-all-done = bf16[8,64,512]{2,1,0:T(8,128)(2,1)S(1)} async-done(((bf16[8,64,512]{2,1,0:T(8,128)(2,1)}), bf16[8,64,512]{2,1,0:T(8,128)(2,1)S(1)}, u32[]{:S(2)}, u32[]{:S(2)}) %all-to-all-start) | async-done | bytes 524320 | tf_op jit(solution)/shard_map/all_to_all | solution.py:20
  30.2 2.7 %collective-permute-start.4 = (bf16[48,512]{1,0:T(8,128)(2,1)S(1)}, bf16[48,512]{1,0:T(8,128)(2,1)S(1)}, u32[]{:S(2)}, u32[]{:S(2)}) collective-permute-start(bf16[48,512]{1,0:T(8,128)(2,1)S(1)} %get-tuple-element.30), channel_id=1, source_target_pairs={{0,16},{8,24},{16,0},{24,8},{1,17},{9,25},{17,1},{25,9},{2,18},{10... | collective-permute-start | bytes 147464 | tf_op jit(solution)/shard_map/ppermute | solution.py:33
  37.1 3.4 %fusion = f32[48,1,128]{2,1,0:T(1,128)S(1)} fusion(bf16[48,128,1]{1,0,2:T(8,128)(2,1)S(1)} %slice_bitcast_fusion.4, f32[48,128]{1,0:T(8,128)S(1)} %split.18, f32[48,128]{1,0:T(8,128)S(1)} %get-tuple-element.36, f32[48,1,128,128]{3,2,1,0:T(8,128)} %param.24, f32[48,128]{1,0:T(8,128)S(1)} %get-tuple-element.35), kind=kOutput, calls=%fused_computation | convolution fusion | flops 3932160 | bytes 3256320 | tf_op jit(solution)/shard_map/bhk,bhkv->bhv/dot_general | solution.py:303
  43.2 4.9 %all-to-all-start.1 = ((bf16[4,48,256]{2,1,0:T(8,128)(2,1)}), bf16[4,48,256]{2,1,0:T(8,128)(2,1)S(1)}, u32[]{:S(2)}, u32[]{:S(2)}) async-start(bf16[4,48,256]{2,1,0:T(8,128)(2,1)} %fusion.52), calls=%async_computation.1 | async-start | bytes 196608 | tf_op jit(solution)/shard_map/all_to_all | solution.py:20
  49.5 2.1 %reshape.675 = bf16[48,1536]{0,1:T(8,128)(2,1)} reshape(bf16[48,64,2,12]{0,3,2,1:T(8,128)(2,1)} %get-tuple-element.23) | data formatting | bytes 294912 | tf_op jit(solution)/shard_map/reshape | solution.py:339
  53.9 2.2 %convolution_convert_fusion = bf16[1536,128]{1,0:T(8,128)(2,1)} fusion(bf16[48,1536]{0,1:T(8,128)(2,1)} %reshape.675, bf16[48,1536]{0,1:T(8,128)(2,1)} %reshape.674, bf16[48,128]{1,0:T(8,128)(2,1)S(1)} %get-tuple-element.44, bf16[48,128]{1,0:T(8,128)(2,1)S(1)} %get-tuple-element.43), kind=kOutput, calls=%fused_computation.3 | convolution fusion | flops 38584320 | bytes 712704 | tf_op jit(solution)/shard_map/bs,bw->sw/dot_general | solution.py:343
  56.1 5.5 %all-to-all-start.2 = ((bf16[64,24,128]{2,1,0:T(8,128)(2,1)}), bf16[64,24,128]{2,1,0:T(8,128)(2,1)}, u32[]{:S(2)}, u32[]{:S(2)}) async-start(bf16[64,24,128]{2,1,0:T(8,128)(2,1)} %bitcast.19), calls=%async_computation.2 | async-start | bytes 786432 | tf_op jit(solution)/shard_map/all_to_all | solution.py:20
  67.3 9.1 %all-to-all-done.2 = bf16[64,24,128]{2,1,0:T(8,128)(2,1)} async-done(((bf16[64,24,128]{2,1,0:T(8,128)(2,1)}), bf16[64,24,128]{2,1,0:T(8,128)(2,1)}, u32[]{:S(2)}, u32[]{:S(2)}) %all-to-all-start.2) | async-done | bytes 393248 | tf_op jit(solution)/shard_map/all_to_all | solution.py:20
  76.4 2.5 %shard_map.230 = (bf16[4,240,512]{2,1,0:T(8,128)(2,1)}, bf16[2,192,256]{2,1,0:T(8,128)(2,1)}) custom-call(s32[2]{0:T(128)} %pad_add_fusion.at, s32[1,384]{1,0:T(1,128)} %fusion.84.line_of, bf16[1536,128]{1,0:T(8,128)(2,1)} %bitcast.20.lines, bf16[48,256]{1,0:T(8,128)(2,1)} %copy-done.26, bf16[48,256]{1,0:T(8,128)(2,1)} %copy-done.32), custom_call_target="tpu_custom_call" | custom-call | flops 150994944 | bytes 1623560 | tf_op jit(solution)/shard_map/pallas_call | solution.py:56
  78.9 4.9 %all-to-all-start.3 = ((bf16[4,240,512]{2,1,0:T(8,128)(2,1)}), bf16[4,240,512]{2,1,0:T(8,128)(2,1)S(1)}, u32[]{:S(2)}, u32[]{:S(2)}) async-start(bf16[4,240,512]{2,1,0:T(8,128)(2,1)} %get-tuple-element.11), calls=%async_computation.3 | async-start | bytes 1966080 | tf_op jit(solution)/shard_map/all_to_all | solution.py:20
  85.0 2.9 %collective-permute-start.12 = (bf16[3,256,256]{2,1,0:T(8,128)(2,1)S(1)}, bf16[3,256,256]{2,1,0:T(8,128)(2,1)}, u32[]{:S(2)}, u32[]{:S(2)}) collective-permute-start(bf16[3,256,256]{2,1,0:T(8,128)(2,1)S(1)} %pad_maximum_fusion.1.refs_0_.refs_4_), channel_id=1, source_target_pairs={{0,16},{8,24},{16,0},{24,8},{1,17},{9,25},{17,1},{25,9},{2,18},{10... | collective-permute-start | bytes 1179656 | tf_op jit(solution)/shard_map/ppermute | solution.py:33
  89.1 9.0 %collective-permute-done.12.refs_2_.refs_6_ = bf16[3,256,256]{2,1,0:T(8,128)(2,1)} collective-permute-done((bf16[3,256,256]{2,1,0:T(8,128)(2,1)S(1)}, bf16[3,256,256]{2,1,0:T(8,128)(2,1)}, u32[]{:S(2)}, u32[]{:S(2)}) %collective-permute-start.12) | collective-permute-done | bytes 393248 | tf_op jit(solution)/shard_map/ppermute | solution.py:33
  98.1 8.3 %collective-permute-done.13.refs_3_.refs_7_ = bf16[3,256,256]{2,1,0:T(8,128)(2,1)} collective-permute-done((bf16[3,256,256]{2,1,0:T(8,128)(2,1)S(1)}, bf16[3,256,256]{2,1,0:T(8,128)(2,1)}, u32[]{:S(2)}, u32[]{:S(2)}) %collective-permute-start.13) | collective-permute-done | bytes 393248 | tf_op jit(solution)/shard_map/ppermute | solution.py:33
  114.5 3.7 %shard_map.231 = bf16[4,240,512]{2,1,0:T(8,128)(2,1)} custom-call(s32[2]{0:T(128)S(1)} %copy-done.12, bf16[4,240,512]{2,1,0:T(8,128)(2,1)S(1)} %all-to-all-done.3.whole, f32[1,2048]{1,0:T(1,128)S(1)} %bitcast.115, bf16[2,2048,128]{2,1,0:T(8,128)(2,1)S(1)} %copy-done.1, bf16[2048,128]{1,0:T(8,128)(2,1)} %collective-permute-done.8.gate_other, ...), custom_call_target="tpu_custom_call" | custom-call | flops 679477248 | bytes 8265736 | tf_op jit(solution)/shard_map/pallas_call | solution.py:56
  118.2 5.0 %all-to-all-start.4 = ((bf16[4,240,512]{2,1,0:T(8,128)(2,1)}), bf16[4,240,512]{2,1,0:T(8,128)(2,1)S(1)}, u32[]{:S(2)}, u32[]{:S(2)}) async-start(bf16[4,240,512]{2,1,0:T(8,128)(2,1)} %shard_map.231), calls=%async_computation.4 | async-start | bytes 1966080 | tf_op jit(solution)/shard_map/all_to_all | solution.py:20
  123.2 2.0 %reshape.673 = bf16[48,1536]{0,1:T(8,128)(2,1)} reshape(bf16[48,64,2,12]{0,3,2,1:T(8,128)(2,1)} %get-tuple-element.45) | data formatting | bytes 294912 | tf_op jit(solution)/shard_map/reshape | solution.py:339
  126.1 2.9 %shard_map.232 = (bf16[48,2176]{1,0:T(8,128)(2,1)S(1)}, bf16[48,2176]{1,0:T(8,128)(2,1)}, bf16[48,2176]{1,0:T(8,128)(2,1)}, bf16[48,2176]{1,0:T(8,128)(2,1)S(1)}) custom-call(s32[2]{0:T(128)S(1)} %copy-done.12, bf16[2,192,256]{2,1,0:T(8,128)(2,1)S(1)} %copy-done.10, f32[8,256]{1,0:T(8,128)S(1)} %reshape.679.gain, ...), custom_call_target="tpu_custom_call" | custom-call | flops 402653184 | bytes 4186120 | tf_op jit(solution)/shard_map/pallas_call | solution.py:56
  131.2 2.6 %collective-permute-start.20 = (bf16[48,2176]{1,0:T(8,128)(2,1)S(1)}, bf16[48,2176]{1,0:T(8,128)(2,1)S(1)}, u32[]{:S(2)}, u32[]{:S(2)}) collective-permute-start(bf16[48,2176]{1,0:T(8,128)(2,1)S(1)} %get-tuple-element.16), channel_id=1, source_target_pairs={{0,6},{2,0},{4,2},{6,4},{1,7},{3,1},{5,3},{7,5},{8,14},{10,8},{12,... | collective-permute-start | bytes 626696 | tf_op jit(solution)/shard_map/ppermute | solution.py:33
  136.4 2.2 %fusion.95 = (bf16[48,64,2,12]{0,3,2,1:T(8,128)(2,1)}, bf16[48,64,2,12]{0,3,2,1:T(8,128)(2,1)}) fusion(bf16[48,64,1,12]{0,3,2,1:T(8,128)(2,1)} %bitcast.121), kind=kLoop, calls=%fused_computation.182 | loop fusion | bytes 368640 | tf_op jit(solution)/shard_map/stack | solution.py:338
  138.6 2.0 %reshape.671 = bf16[48,1536]{0,1:T(8,128)(2,1)} reshape(bf16[48,64,2,12]{0,3,2,1:T(8,128)(2,1)} %get-tuple-element.25) | data formatting | bytes 294912 | tf_op jit(solution)/shard_map/reshape | solution.py:339
  140.6 2.0 %reshape.670 = bf16[48,1536]{0,1:T(8,128)(2,1)} reshape(bf16[48,64,2,12]{0,3,2,1:T(8,128)(2,1)} %get-tuple-element.24) | data formatting | bytes 294912 | tf_op jit(solution)/shard_map/reshape | solution.py:339
  142.6 3.1 %collective-permute-done.20.d = bf16[48,2176]{1,0:T(8,128)(2,1)S(1)} collective-permute-done((bf16[48,2176]{1,0:T(8,128)(2,1)S(1)}, bf16[48,2176]{1,0:T(8,128)(2,1)S(1)}, u32[]{:S(2)}, u32[]{:S(2)}) %collective-permute-start.20) | collective-permute-done | bytes 208928 | tf_op jit(solution)/shard_map/ppermute | solution.py:33
  146.5 3.0 %collective-permute-start.22 = (bf16[48,1024]{1,0:T(8,128)(2,1)S(1)}, bf16[48,1024]{1,0:T(8,128)(2,1)S(1)}, u32[]{:S(2)}, u32[]{:S(2)}) collective-permute-start(bf16[48,1024]{1,0:T(8,128)(2,1)S(1)} %shard_map.233.refs_0_), channel_id=1, source_target_pairs={{0,4},{2,6},{4,0},{6,2},{1,5},{3,7},{5,1},{7,3},{8,12},{10,14},{12... | collective-permute-start | bytes 294920 | tf_op jit(solution)/shard_map/ppermute | solution.py:33
  151.0 2.6 %collective-permute-done.22.refs_2_ = bf16[48,1024]{1,0:T(8,128)(2,1)S(1)} collective-permute-done((bf16[48,1024]{1,0:T(8,128)(2,1)S(1)}, bf16[48,1024]{1,0:T(8,128)(2,1)S(1)}, u32[]{:S(2)}, u32[]{:S(2)}) %collective-permute-start.22) | collective-permute-done | bytes 98336 | tf_op jit(solution)/shard_map/ppermute | solution.py:33
  154.6 2.0 %shard_map.234.dense = bf16[2,192,256]{2,1,0:T(8,128)(2,1)S(1)} custom-call(s32[2]{0:T(128)S(1)} %copy-done.12, bf16[48,1024]{1,0:T(8,128)(2,1)S(1)} %shard_map.233.refs_0_, bf16[48,1024]{1,0:T(8,128)(2,1)S(1)} %collective-permute-done.21.refs_1_, bf16[48,1024]{1,0:T(8,128)(2,1)S(1)} %collective-permute-done.22.refs_2_, ...), custom_call_target="tpu_custom_call" | custom-call | flops 201326592 | bytes 3735560 | tf_op jit(solution)/shard_map/pallas_call | solution.py:56
  158.5 5.8 %all-to-all-start.5 = ((bf16[64,24,128]{2,1,0:T(8,128)(2,1)}), bf16[64,24,128]{2,1,0:T(8,128)(2,1)S(1)}, u32[]{:S(2)}, u32[]{:S(2)}) async-start(bf16[64,24,128]{2,1,0:T(8,128)(2,1)} %bitcast.28), calls=%async_computation.5 | async-start | bytes 786432 | tf_op jit(solution)/shard_map/all_to_all | solution.py:20
  164.3 1.9 %pad_maximum_fusion = bf16[192,1536]{0,1:T(8,128)(2,1)S(1)} fusion(bf16[48,1536]{0,1:T(8,128)(2,1)S(1)} %copy-done.14, bf16[48,1536]{0,1:T(8,128)(2,1)} %reshape.672, bf16[48,1536]{0,1:T(8,128)(2,1)} %reshape.671, bf16[48,1536]{0,1:T(8,128)(2,1)} %reshape.670), kind=kLoop, calls=%fused_computation.6 | loop fusion | flops 2359296 | bytes 1179648 | tf_op jit(solution)/shard_map/concatenate | solution.py:433
  166.5 5.1 %multiply_add_fusion = f32[48,1,128,128]{3,2,1,0:T(8,128)} fusion(f32[48,1,128,128]{3,2,1,0:T(8,128)} %param.24, f32[48,128]{1,0:T(8,128)S(1)} %copy-done.18, f32[48,128]{1,0:T(8,128)S(1)} %copy-done.22, f32[48,128]{1,0:T(8,128)S(1)} %copy-done.20), kind=kLoop, calls=%fused_computation.2 | loop fusion | flops 2359296 | bytes 6365184 | tf_op jit(solution)/shard_map/add | solution.py:302
  171.7 7.6 %all-to-all-done.5 = bf16[64,24,128]{2,1,0:T(8,128)(2,1)S(1)} async-done(((bf16[64,24,128]{2,1,0:T(8,128)(2,1)}), bf16[64,24,128]{2,1,0:T(8,128)(2,1)S(1)}, u32[]{:S(2)}, u32[]{:S(2)}) %all-to-all-start.5) | async-done | bytes 393248 | tf_op jit(solution)/shard_map/all_to_all | solution.py:20
  (175 shorter events, 49.6 us)
Async XLA Ops:
  2.3 26.0 %all-to-all-start = ((bf16[8,64,512]{2,1,0:T(8,128)(2,1)}), bf16[8,64,512]{2,1,0:T(8,128)(2,1)S(1)}, u32[]{:S(2)}, u32[]{:S(2)}) async-start(bf16[8,64,512]{2,1,0:T(8,128)(2,1)} %broadcast_in_dim.10), calls=%async_computation | async-start | bytes 1048576 | tf_op jit(solution)/shard_map/all_to_all | solution.py:20
  13.7 6.2 %collective-permute-start.2 = (bf16[48,512]{1,0:T(8,128)(2,1)S(1)}, bf16[48,512]{1,0:T(8,128)(2,1)S(1)}, u32[]{:S(2)}, u32[]{:S(2)}) collective-permute-start(bf16[48,512]{1,0:T(8,128)(2,1)S(1)} %get-tuple-element.32), channel_id=1, source_target_pairs={{0,24},{8,0},{16,8},{24,16},{1,25},{9,1},{17,9},{25,17},{2,26},{10... | collective-permute-start | bytes 147464 | tf_op jit(solution)/shard_map/ppermute | solution.py:33
  16.5 5.6 %collective-permute-start.1 = (bf16[48,512]{1,0:T(8,128)(2,1)S(1)}, bf16[48,512]{1,0:T(8,128)(2,1)S(1)}, u32[]{:S(2)}, u32[]{:S(2)}) collective-permute-start(bf16[48,512]{1,0:T(8,128)(2,1)S(1)} %get-tuple-element.33), channel_id=1, source_target_pairs={{0,16},{8,24},{16,0},{24,8},{1,17},{9,25},{17,1},{25,9},{2,18},{10... | collective-permute-start | bytes 147464 | tf_op jit(solution)/shard_map/ppermute | solution.py:33
  17.3 5.3 %collective-permute-start = (bf16[48,512]{1,0:T(8,128)(2,1)S(1)}, bf16[48,512]{1,0:T(8,128)(2,1)S(1)}, u32[]{:S(2)}, u32[]{:S(2)}) collective-permute-start(bf16[48,512]{1,0:T(8,128)(2,1)S(1)} %get-tuple-element.34), channel_id=1, source_target_pairs={{0,8},{8,16},{16,24},{24,0},{1,9},{9,17},{17,25},{25,1},{2,10},{10... | collective-permute-start | bytes 147464 | tf_op jit(solution)/shard_map/ppermute | solution.py:33
  28.6 6.1 %collective-permute-start.5 = (bf16[48,512]{1,0:T(8,128)(2,1)S(1)}, bf16[48,512]{1,0:T(8,128)(2,1)S(1)}, u32[]{:S(2)}, u32[]{:S(2)}) collective-permute-start(bf16[48,512]{1,0:T(8,128)(2,1)S(1)} %get-tuple-element.29), channel_id=1, source_target_pairs={{0,8},{8,16},{16,24},{24,0},{1,9},{9,17},{17,25},{25,1},{2,10},{10... | collective-permute-start | bytes 147464 | tf_op jit(solution)/shard_map/ppermute | solution.py:33
  30.2 5.6 %collective-permute-start.4 = (bf16[48,512]{1,0:T(8,128)(2,1)S(1)}, bf16[48,512]{1,0:T(8,128)(2,1)S(1)}, u32[]{:S(2)}, u32[]{:S(2)}) collective-permute-start(bf16[48,512]{1,0:T(8,128)(2,1)S(1)} %get-tuple-element.30), channel_id=1, source_target_pairs={{0,16},{8,24},{16,0},{24,8},{1,17},{9,25},{17,1},{25,9},{2,18},{10... | collective-permute-start | bytes 147464 | tf_op jit(solution)/shard_map/ppermute | solution.py:33
  32.9 4.1 %collective-permute-start.3 = (bf16[48,512]{1,0:T(8,128)(2,1)S(1)}, bf16[48,512]{1,0:T(8,128)(2,1)S(1)}, u32[]{:S(2)}, u32[]{:S(2)}) collective-permute-start(bf16[48,512]{1,0:T(8,128)(2,1)S(1)} %get-tuple-element.28), channel_id=1, source_target_pairs={{0,24},{8,0},{16,8},{24,16},{1,25},{9,1},{17,9},{25,17},{2,26},{10... | collective-permute-start | bytes 147464 | tf_op jit(solution)/shard_map/ppermute | solution.py:33
  41.1 1.4 collective-permute-start.6
  43.2 9.3 %all-to-all-start.1 = ((bf16[4,48,256]{2,1,0:T(8,128)(2,1)}), bf16[4,48,256]{2,1,0:T(8,128)(2,1)S(1)}, u32[]{:S(2)}, u32[]{:S(2)}) async-start(bf16[4,48,256]{2,1,0:T(8,128)(2,1)} %fusion.52), calls=%async_computation.1 | async-start | bytes 196608 | tf_op jit(solution)/shard_map/all_to_all | solution.py:20
  56.1 20.3 %all-to-all-start.2 = ((bf16[64,24,128]{2,1,0:T(8,128)(2,1)}), bf16[64,24,128]{2,1,0:T(8,128)(2,1)}, u32[]{:S(2)}, u32[]{:S(2)}) async-start(bf16[64,24,128]{2,1,0:T(8,128)(2,1)} %bitcast.19), calls=%async_computation.2 | async-start | bytes 786432 | tf_op jit(solution)/shard_map/all_to_all | solution.py:20
  61.6 46.3 %copy-start.11 = (f32[2048]{0:T(1024)S(1)}, f32[2048]{0:T(1024)}, u32[]{:S(2)}) copy-start(f32[2048]{0:T(1024)} %param.33) | copy-start | bytes 24580
  62.4 44.0 %collective-permute-start.8 = (bf16[2048,128]{1,0:T(8,128)(2,1)}, bf16[2048,128]{1,0:T(8,128)(2,1)}, u32[]{:S(2)}, u32[]{:S(2)}) collective-permute-start(bf16[2048,128]{1,0:T(8,128)(2,1)} %dynamic-slice_bitcast_fusion.2), channel_id=1, source_target_pairs={{0,1},{1,0},{2,3},{3,2},{4,5},{5,4},{6,7},{7,6},{8,9},{9,8},{10,11... | collective-permute-start | bytes 1572872 | tf_op jit(solution)/shard_map/ppermute | solution.py:28
  63.3 43.7 %collective-permute-start.9 = (bf16[2048,128]{1,0:T(8,128)(2,1)}, bf16[2048,128]{1,0:T(8,128)(2,1)}, u32[]{:S(2)}, u32[]{:S(2)}) collective-permute-start(bf16[2048,128]{1,0:T(8,128)(2,1)} %dynamic-slice_bitcast_fusion.1), channel_id=1, source_target_pairs={{0,1},{1,0},{2,3},{3,2},{4,5},{5,4},{6,7},{7,6},{8,9},{9,8},{10,11... | collective-permute-start | bytes 1572872 | tf_op jit(solution)/shard_map/ppermute | solution.py:28
  63.8 24.1 %collective-permute-start.11 = (bf16[3,256,256]{2,1,0:T(8,128)(2,1)S(1)}, bf16[3,256,256]{2,1,0:T(8,128)(2,1)S(1)}, u32[]{:S(2)}, u32[]{:S(2)}) collective-permute-start(bf16[3,256,256]{2,1,0:T(8,128)(2,1)S(1)} %pad_maximum_fusion.1.refs_0_.refs_4_), channel_id=1, source_target_pairs={{0,8},{8,16},{16,24},{24,0},{1,9},{9,17},{17,25},{25,1},{2,10},{10... | collective-permute-start | bytes 1179656 | tf_op jit(solution)/shard_map/ppermute | solution.py:33
  66.1 1.2 collective-permute-start.7
  78.9 29.0 %all-to-all-start.3 = ((bf16[4,240,512]{2,1,0:T(8,128)(2,1)}), bf16[4,240,512]{2,1,0:T(8,128)(2,1)S(1)}, u32[]{:S(2)}, u32[]{:S(2)}) async-start(bf16[4,240,512]{2,1,0:T(8,128)(2,1)} %get-tuple-element.11), calls=%async_computation.3 | async-start | bytes 1966080 | tf_op jit(solution)/shard_map/all_to_all | solution.py:20
  84.9 22.2 %collective-permute-start.10 = (bf16[128,2048]{1,0:T(8,128)(2,1)S(1)}, bf16[128,2048]{1,0:T(8,128)(2,1)S(1)}, u32[]{:S(2)}, u32[]{:S(2)}) collective-permute-start(bf16[128,2048]{1,0:T(8,128)(2,1)S(1)} %dynamic-slice_bitcast_fusion), channel_id=1, source_target_pairs={{0,1},{1,0},{2,3},{3,2},{4,5},{5,4},{6,7},{7,6},{8,9},{9,8},{10,11... | collective-permute-start | bytes 1572872 | tf_op jit(solution)/shard_map/ppermute | solution.py:28
  85.0 13.1 %collective-permute-start.12 = (bf16[3,256,256]{2,1,0:T(8,128)(2,1)S(1)}, bf16[3,256,256]{2,1,0:T(8,128)(2,1)}, u32[]{:S(2)}, u32[]{:S(2)}) collective-permute-start(bf16[3,256,256]{2,1,0:T(8,128)(2,1)S(1)} %pad_maximum_fusion.1.refs_0_.refs_4_), channel_id=1, source_target_pairs={{0,16},{8,24},{16,0},{24,8},{1,17},{9,25},{17,1},{25,9},{2,18},{10... | collective-permute-start | bytes 1179656 | tf_op jit(solution)/shard_map/ppermute | solution.py:33
  87.9 18.6 %collective-permute-start.13 = (bf16[3,256,256]{2,1,0:T(8,128)(2,1)S(1)}, bf16[3,256,256]{2,1,0:T(8,128)(2,1)}, u32[]{:S(2)}, u32[]{:S(2)}) collective-permute-start(bf16[3,256,256]{2,1,0:T(8,128)(2,1)S(1)} %pad_maximum_fusion.1.refs_0_.refs_4_), channel_id=1, source_target_pairs={{0,24},{8,0},{16,8},{24,16},{1,25},{9,1},{17,9},{25,17},{2,26},{10... | collective-permute-start | bytes 1179656 | tf_op jit(solution)/shard_map/ppermute | solution.py:33
  98.1 28.0 %collective-permute-start.14 = (bf16[3,256,256]{2,1,0:T(8,128)(2,1)S(1)}, bf16[3,256,256]{2,1,0:T(8,128)(2,1)}, u32[]{:S(2)}, u32[]{:S(2)}) collective-permute-start(bf16[3,256,256]{2,1,0:T(8,128)(2,1)S(1)} %pad_maximum_fusion.1.refs_0_.refs_4_), channel_id=1, source_target_pairs={{0,1},{1,0},{2,3},{3,2},{4,5},{5,4},{6,7},{7,6},{8,9},{9,8},{10,11... | collective-permute-start | bytes 1179656 | tf_op jit(solution)/shard_map/ppermute | solution.py:28
  106.5 19.7 %collective-permute-start.15 = (bf16[3,256,256]{2,1,0:T(8,128)(2,1)S(1)}, bf16[3,256,256]{2,1,0:T(8,128)(2,1)}, u32[]{:S(2)}, u32[]{:S(2)}) collective-permute-start(bf16[3,256,256]{2,1,0:T(8,128)(2,1)S(1)} %collective-permute-done.11.refs_1_.refs_5_), channel_id=1, source_target_pairs={{0,1},{1,0},{2,3},{3,2},{4,5},{5,4},{6,7},{7,6},{8,9},{9,8},{10,11... | collective-permute-start | bytes 1179656 | tf_op jit(solution)/shard_map/ppermute | solution.py:28
  106.5 19.7 %collective-permute-start.16 = (bf16[3,256,256]{2,1,0:T(8,128)(2,1)}, bf16[3,256,256]{2,1,0:T(8,128)(2,1)}, u32[]{:S(2)}, u32[]{:S(2)}) collective-permute-start(bf16[3,256,256]{2,1,0:T(8,128)(2,1)} %collective-permute-done.12.refs_2_.refs_6_), channel_id=1, source_target_pairs={{0,1},{1,0},{2,3},{3,2},{4,5},{5,4},{6,7},{7,6},{8,9},{9,8},{10,11... | collective-permute-start | bytes 1179656 | tf_op jit(solution)/shard_map/ppermute | solution.py:28
  107.0 19.1 %collective-permute-start.17 = (bf16[3,256,256]{2,1,0:T(8,128)(2,1)}, bf16[3,256,256]{2,1,0:T(8,128)(2,1)}, u32[]{:S(2)}, u32[]{:S(2)}) collective-permute-start(bf16[3,256,256]{2,1,0:T(8,128)(2,1)} %collective-permute-done.13.refs_3_.refs_7_), channel_id=1, source_target_pairs={{0,1},{1,0},{2,3},{3,2},{4,5},{5,4},{6,7},{7,6},{8,9},{9,8},{10,11... | collective-permute-start | bytes 1179656 | tf_op jit(solution)/shard_map/ppermute | solution.py:28
  118.2 38.4 %all-to-all-start.4 = ((bf16[4,240,512]{2,1,0:T(8,128)(2,1)}), bf16[4,240,512]{2,1,0:T(8,128)(2,1)S(1)}, u32[]{:S(2)}, u32[]{:S(2)}) async-start(bf16[4,240,512]{2,1,0:T(8,128)(2,1)} %shard_map.231), calls=%async_computation.4 | async-start | bytes 1966080 | tf_op jit(solution)/shard_map/all_to_all | solution.py:20
  129.1 13.5 %collective-permute-start.18 = (bf16[48,2176]{1,0:T(8,128)(2,1)}, bf16[48,2176]{1,0:T(8,128)(2,1)S(1)}, u32[]{:S(2)}, u32[]{:S(2)}) collective-permute-start(bf16[48,2176]{1,0:T(8,128)(2,1)} %get-tuple-element.14), channel_id=1, source_target_pairs={{0,2},{2,4},{4,6},{6,0},{1,3},{3,5},{5,7},{7,1},{8,10},{10,12},{12... | collective-permute-start | bytes 626696 | tf_op jit(solution)/shard_map/ppermute | solution.py:33
  130.5 12.0 %collective-permute-start.19 = (bf16[48,2176]{1,0:T(8,128)(2,1)}, bf16[48,2176]{1,0:T(8,128)(2,1)S(1)}, u32[]{:S(2)}, u32[]{:S(2)}) collective-permute-start(bf16[48,2176]{1,0:T(8,128)(2,1)} %get-tuple-element.15), channel_id=1, source_target_pairs={{0,4},{2,6},{4,0},{6,2},{1,5},{3,7},{5,1},{7,3},{8,12},{10,14},{12... | collective-permute-start | bytes 626696 | tf_op jit(solution)/shard_map/ppermute | solution.py:33
  131.2 14.5 %collective-permute-start.20 = (bf16[48,2176]{1,0:T(8,128)(2,1)S(1)}, bf16[48,2176]{1,0:T(8,128)(2,1)S(1)}, u32[]{:S(2)}, u32[]{:S(2)}) collective-permute-start(bf16[48,2176]{1,0:T(8,128)(2,1)S(1)} %get-tuple-element.16), channel_id=1, source_target_pairs={{0,6},{2,0},{4,2},{6,4},{1,7},{3,1},{5,3},{7,5},{8,14},{10,8},{12,... | collective-permute-start | bytes 626696 | tf_op jit(solution)/shard_map/ppermute | solution.py:33
  145.9 5.1 %collective-permute-start.21 = (bf16[48,1024]{1,0:T(8,128)(2,1)S(1)}, bf16[48,1024]{1,0:T(8,128)(2,1)S(1)}, u32[]{:S(2)}, u32[]{:S(2)}) collective-permute-start(bf16[48,1024]{1,0:T(8,128)(2,1)S(1)} %shard_map.233.refs_0_), channel_id=1, source_target_pairs={{0,2},{2,4},{4,6},{6,0},{1,3},{3,5},{5,7},{7,1},{8,10},{10,12},{12... | collective-permute-start | bytes 294920 | tf_op jit(solution)/shard_map/ppermute | solution.py:33
  146.5 7.0 %collective-permute-start.22 = (bf16[48,1024]{1,0:T(8,128)(2,1)S(1)}, bf16[48,1024]{1,0:T(8,128)(2,1)S(1)}, u32[]{:S(2)}, u32[]{:S(2)}) collective-permute-start(bf16[48,1024]{1,0:T(8,128)(2,1)S(1)} %shard_map.233.refs_0_), channel_id=1, source_target_pairs={{0,4},{2,6},{4,0},{6,2},{1,5},{3,7},{5,1},{7,3},{8,12},{10,14},{12... | collective-permute-start | bytes 294920 | tf_op jit(solution)/shard_map/ppermute | solution.py:33
  149.5 5.1 %collective-permute-start.23 = (bf16[48,1024]{1,0:T(8,128)(2,1)S(1)}, bf16[48,1024]{1,0:T(8,128)(2,1)S(1)}, u32[]{:S(2)}, u32[]{:S(2)}) collective-permute-start(bf16[48,1024]{1,0:T(8,128)(2,1)S(1)} %shard_map.233.refs_0_), channel_id=1, source_target_pairs={{0,6},{2,0},{4,2},{6,4},{1,7},{3,1},{5,3},{7,5},{8,14},{10,8},{12,... | collective-permute-start | bytes 294920 | tf_op jit(solution)/shard_map/ppermute | solution.py:33
  158.5 20.8 %all-to-all-start.5 = ((bf16[64,24,128]{2,1,0:T(8,128)(2,1)}), bf16[64,24,128]{2,1,0:T(8,128)(2,1)S(1)}, u32[]{:S(2)}, u32[]{:S(2)}) async-start(bf16[64,24,128]{2,1,0:T(8,128)(2,1)} %bitcast.28), calls=%async_computation.5 | async-start | bytes 786432 | tf_op jit(solution)/shard_map/all_to_all | solution.py:20
  171.6 7.9 %collective-permute-start.24 = (bf16[48,256]{1,0:T(8,128)(2,1)S(1)}, bf16[48,256]{1,0:T(8,128)(2,1)S(1)}, u32[]{:S(2)}, u32[]{:S(2)}) collective-permute-start(bf16[48,256]{1,0:T(8,128)(2,1)S(1)} %get-tuple-element.19), channel_id=1, source_target_pairs={{0,1},{1,0},{2,3},{3,2},{4,5},{5,4},{6,7},{7,6},{8,9},{9,8},{10,11... | collective-permute-start | bytes 73736 | tf_op jit(solution)/shard_map/ppermute | solution.py:28
  (32 other events, 358.3 us)

commit v5 on v4

--- a/solution.py
+++ b/solution.py
@@ -20,10 +20,6 @@
     return lax.all_to_all(x, axis, split_axis=0, concat_axis=0, tiled=True)
 
 
-def spread(x, axis):
-    return swap(jnp.broadcast_to(x, (lax.axis_size(axis), *x.shape)), axis)
-
-
 def partner(x):
     return lax.ppermute(x, "c", [(0, 1), (1, 0)])
 
@@ -45,7 +41,7 @@
     return x * jax.nn.sigmoid(x)
 
 
-def call(body, outs, flops, *args, mib=12):
+def call(body, outs, flops, *args, mib=12, scratch=()):
     moved = sum(a.size * a.dtype.itemsize for a in args) + sum(
         o.size * o.dtype.itemsize for o in outs
     )
@@ -58,6 +54,7 @@
         out_shape=outs,
         in_specs=specs,
         out_specs=[pl.BlockSpec(memory_space=pltpu.VMEM) for _ in outs],
+        scratch_shapes=scratch,
         cost_estimate=pl.CostEstimate(flops=flops, bytes_accessed=moved, transcendentals=0),
         compiler_params=pltpu.CompilerParams(vmem_limit_bytes=mib * 2**20),
     )(*args)
@@ -65,6 +62,111 @@
 
 def shaped(*dims, dtype=BF):
     return jax.ShapeDtypeStruct(dims, dtype)
+
+
+def prepare(at, tokens, gain, wq, wf, wi, wo, dg, du, dd, spread_w, dense, t0, t1, t2, t3, held):
+    x = at[2]
+    for i, block in enumerate((dg, du, dd)):
+        dense[i] = block[...]
+    for i, block in enumerate((wq, wf, wi, wo)):
+        width = block.shape[1]
+        value = block[...]
+        for z in range(spread_w.shape[0]):
+            spread_w[z, :, i * width : (i + 1) * width] = value
+    wide = tokens[...].astype(F32)
+    wide = wide * lax.rsqrt(jnp.mean(wide * wide, axis=1, keepdims=True) + EPS) * gain[...]
+    low = lax.broadcasted_iota(jnp.int32, (wide.shape[0], 128), 1) < 64
+
+    def tile(i):
+        return wide[:, i * 128 : (i + 1) * 128]
+
+    for to in range(4):
+        for k in range(4):
+            a, b = tile(4 * k + to // 2), tile(4 * k + 2 + to // 2)
+            if to % 2 == 0:
+                value = jnp.where(low, a, pltpu.roll(b, 64, 1))
+            else:
+                value = jnp.where(low, pltpu.roll(a, 64, 1), b)
+            held[to, :, k * 128 : (k + 1) * 128] = value.astype(BF)
+    for d, out in enumerate((t0, t1, t2, t3)):
+        out[...] = held[lax.rem(x + d, 4)]
+
+
+def recur(at, p0, p1, p2, p3, bound, gain, state, w_out, decay_out, key_out, value_out, keep, give, read):
+    first = at[1] == 0
+    seq = p0.shape[0]
+    total = (
+        p0[...].astype(F32) + p1[...].astype(F32) + p2[...].astype(F32) + p3[...].astype(F32)
+    )
+    total = total.astype(BF).astype(F32)
+    query, forget, values, gate = (total[:, i * 128 : (i + 1) * 128] for i in range(4))
+    forget = jax.nn.sigmoid(forget)
+    low = bound[...]
+    decay = low + (1.0 - low) * forget
+    key = (1.0 - low) * (1.0 - forget)
+    decay_out[...] = decay
+    key_out[...] = key
+    value_out[...] = values
+    turned = jnp.transpose(query * decay)
+    for b in range(seq):
+        read[b : b + 1, :] = jnp.sum(turned[:, b : b + 1] * state[b], axis=0, keepdims=True)
+    readout = read[...] + jnp.sum(query * key, axis=1, keepdims=True) * values
+    readout = readout * lax.rsqrt(jnp.mean(readout * readout, axis=1, keepdims=True) + EPS)
+    head = (readout * gain[...] * silu(gate)).astype(BF)
+    cols = keep.shape[2]
+    for y in range(keep.shape[0]):
+        cut = slice(2 * y * cols, (2 * y + 1) * cols)
+        cut_next = slice((2 * y + 1) * cols, (2 * y + 2) * cols)
+        even = dot(head, w_out[:, cut]).astype(BF)
+        odd = dot(head, w_out[:, cut_next]).astype(BF)
+        keep[y] = jnp.where(first, even, odd)
+        give[y] = jnp.where(first, odd, even)
+
+
+def dispatch(at, heads, tokens, slots, resid, own, lines):
+    cols = resid.shape[1]
+    half = cols // 2
+    seq = resid.shape[0]
+    start = pl.multiple_of((2 * at[0] + at[1]) * cols, cols)
+    total = tokens[:, pl.ds(start, cols)].astype(F32)
+    for i in range(heads.shape[0]):
+        total = total + heads[i].astype(F32)
+    resid[...] = total
+    rows = total.astype(BF)
+    own[...] = rows
+    chunk = 192
+    place = lax.broadcasted_iota(jnp.int32, (chunk, seq), 0)
+    for h in range(2):
+        shifted = place - 12 * h
+        dense = shifted == slots[4:5, :]
+        for z in range(lines.shape[0] // chunk):
+            here = shifted + z * chunk
+            hit = dense
+            for k in range(4):
+                hit = hit | (here == slots[k : k + 1, :])
+            part = dot(jnp.where(hit, 1.0, 0.0).astype(BF), rows[:, h * half : (h + 1) * half])
+            if h == 0:
+                lines[z * chunk : (z + 1) * chunk, :] = part.astype(BF)
+            else:
+                before = lines[z * chunk : (z + 1) * chunk, :].astype(F32)
+                lines[z * chunk : (z + 1) * chunk, :] = (before + part).astype(BF)
+
+
+def finish(lines, within, slots, weight, resid, shared, shared_other, mix, out):
+    seq, cols = out.shape
+    half = cols // 2
+    place = lax.broadcasted_iota(jnp.int32, (seq, lines.shape[0]), 1)
+    gate = jax.nn.sigmoid(mix[...])
+    base = resid[...] + shared[...] + shared_other[...].astype(F32)
+    for h in range(2):
+        routed = jnp.zeros(place.shape, F32)
+        for k in range(4):
+            routed = jnp.where(place == slots[:, k : k + 1] + 12 * h, weight[:, k : k + 1], routed)
+        dense = jnp.where(within[...] == slots[:, 4:5] + 12 * h, 1.0, 0.0)
+        cut = slice(h * half, (h + 1) * half)
+        total = base[:, cut] + dot(routed.astype(BF), lines[...])
+        total = total + gate[:, cut] * dot(dense.astype(BF), lines[...])
+        out[:, cut] = total.astype(BF)
 
 
 def unpack_rows(at, line_of, lines, own, other, both, dense):
@@ -270,77 +372,88 @@
     rows_w, chan = w_query.shape
     head_dim = state.shape[2]
     cols = width // (ny * nc)
-    own_at = (y * nc + c) * cols
-
-    joined = jnp.concatenate([w_query, w_forget, w_input, w_outgate], axis=1)
-    weights = spread(joined, "z").reshape(nz * rows_w, 4 * chan)
-    wide = tokens.astype(F32)
-    normed = wide * lax.rsqrt(jnp.mean(wide * wide, axis=-1, keepdims=True) + EPS) * norm_gain
-    normed = normed.astype(BF).reshape(seq, nz, nx, rows_w)
-    normed = jnp.transpose(normed, (2, 0, 1, 3)).reshape(nx, seq, nz * rows_w)
-    mine = [pick(normed, x)] + [shift(pick(normed, (x + d) % nx), "x", d) for d in range(1, nx)]
+
+    at = jnp.stack([y, c, x]).astype(jnp.int32)
+
+    topk = route_ids.shape[1]
+    experts = nz * nx * nc
+    cap = max(2, 2 * seq * topk // experts)
+    slots = 2 * cap
+    half = cols // 2
+    flat_ids = route_ids.reshape(-1)
+    onehot = (flat_ids[:, None] == jnp.arange(experts, dtype=jnp.int32)[None, :]).astype(jnp.int32)
+    rank = jnp.sum((jnp.cumsum(onehot, axis=0) - onehot) * onehot, axis=1)
+    lines_of = (flat_ids * (2 * slots) + rank).reshape(seq, topk)
+    token_ids = jnp.arange(seq, dtype=jnp.int32)
+    dense_of = (token_ids // cap) * (2 * slots) + cap + token_ids % cap
+    slot_cols = jnp.concatenate(
+        [lines_of, dense_of[:, None], jnp.zeros((seq, 8 - topk - 1), jnp.int32)], axis=1
+    )
+    slot_rows = slot_cols.T
+    within = (jnp.arange(experts * 2 * slots, dtype=jnp.int32) % (nx * nc * 2 * slots))[None, :]
+
+    spread_w, dense_block, *columns = call(
+        prepare,
+        [shaped(nz, rows_w, 4 * chan), shaped(3, *dense_gate.shape)]
+        + [shaped(seq, nz * rows_w)] * nx,
+        10**6,
+        at,
+        tokens,
+        norm_gain.reshape(1, width),
+        w_query,
+        w_forget,
+        w_input,
+        w_outgate,
+        dense_gate,
+        dense_up,
+        dense_down,
+        scratch=[pltpu.VMEM((nx, seq, nz * rows_w), BF)],
+    )
+    weights = swap(spread_w, "z").reshape(nz * rows_w, 4 * chan)
+    mine = [columns[0]] + [shift(columns[d], "x", d) for d in range(1, nx)]
     part = dot(jnp.concatenate(mine, axis=0), weights).astype(BF)
     part = part.reshape(nx, seq, 4 * chan)
-    projected = part[0].astype(F32)
-    for d in range(1, nx):
-        projected = projected + shift(part[d], "x", -d).astype(F32)
-    projected = projected.astype(BF).astype(F32)
-    query, forget_pre, values, out_gate = jnp.split(projected, 4, axis=1)
-
-    at = jnp.stack([y, c]).astype(jnp.int32)
-    dense_block = jnp.stack([dense_gate, dense_up, dense_down])
+    pieces = [part[0]] + [shift(part[d], "x", -d) for d in range(1, nx)]
+
     dense_own = [dense_block] + [shift(dense_block, "x", d) for d in range(1, nx)]
     dense_other = [partner(block) for block in dense_own]
     gate_other, up_other, down_other = (
         partner(pick(stack, 1 - c)) for stack in (expert_gate, expert_up, expert_down)
     )
 
-    forget_sig = jax.nn.sigmoid(forget_pre)
+    decay, keygate, values, keep, give = call(
+        recur,
+        [shaped(seq, chan, dtype=F32)] * 3 + [shaped(ny, seq, cols)] * 2,
+        4 * state.size,
+        at,
+        *pieces,
+        lower_bound.reshape(1, chan),
+        head_gain.reshape(1, chan),
+        state.reshape(seq, head_dim, head_dim),
+        w_output,
+        scratch=[pltpu.VMEM((seq, head_dim), F32)],
+    )
     shape = (seq, 1, head_dim)
-    decay = (lower_bound + (1.0 - lower_bound) * forget_sig).reshape(shape)
-    keygate = ((1.0 - lower_bound) * (1.0 - forget_sig)).reshape(shape)
-    new_state = decay[..., None] * state + keygate[..., None] * values.reshape(shape)[:, :, None, :]
-    readout = jnp.einsum("bhk,bhkv->bhv", query.reshape(shape), new_state)
-    readout = readout * lax.rsqrt(jnp.mean(readout * readout, axis=-1, keepdims=True) + EPS)
-    head_out = (readout.reshape(seq, chan) * head_gain * jax.nn.silu(out_gate)).astype(BF)
-
-    head_part = dot(head_out, w_output).astype(BF)
-    head_part = jnp.moveaxis(head_part.reshape(seq, ny, nc, cols), 2, 0)
-    head_first, head_second = (jnp.moveaxis(h, 1, 0) for h in (head_part[0], head_part[1]))
-    keep = jnp.where(c == 0, head_first, head_second)
-    give = jnp.where(c == 0, head_second, head_first)
+    new_state = (
+        decay.reshape(shape)[..., None] * state
+        + keygate.reshape(shape)[..., None] * values.reshape(shape)[:, :, None, :]
+    )
+
     pair = (keep.astype(F32) + partner(give).astype(F32)).astype(BF)
-    resid = swap(pair, "y").astype(F32).sum(axis=0)
-    resid = resid + lax.dynamic_slice_in_dim(tokens, own_at, cols, 1).astype(F32)
-    own = resid.astype(BF)
-
-    topk = route_ids.shape[1]
-    experts = nz * nx * nc
-    cap = max(2, 2 * seq * topk // experts)
-    flat_ids = route_ids.reshape(-1)
-    onehot = (flat_ids[:, None] == jnp.arange(experts, dtype=jnp.int32)[None, :]).astype(jnp.int32)
-    rank = jnp.sum((jnp.cumsum(onehot, axis=0) - onehot) * onehot, axis=1)
-    slots = 2 * cap
-    slot_index = (flat_ids * slots + rank).reshape(seq, topk)
-    slot_ids = jnp.arange(experts * slots, dtype=jnp.int32)
-    place = slot_ids % slots
-    line = (slot_ids // slots) % (nx * nc) * cap + place - cap
-    is_dense = place >= cap
-    token_ids = jnp.arange(seq, dtype=jnp.int32)
-    dense_hits = is_dense[None, :] & (line[None, :] == token_ids[:, None])
-    hits = slot_index[:, :, None] == slot_ids[None, None, :]
-    routed_hits = jnp.any(hits, axis=1)
-    half = cols // 2
-
-    def as_lines(table):
-        blocks = table.reshape(seq, experts, slots)
-        none = jnp.zeros_like(blocks)
-        pair = [jnp.stack([blocks, none], axis=2), jnp.stack([none, blocks], axis=2)]
-        return [p.reshape(seq, experts * 2 * slots) for p in pair]
-
-    select = jnp.concatenate(as_lines((routed_hits | dense_hits).astype(BF)), axis=0)
-    halves = jnp.concatenate([own[:, :half], own[:, half:]], axis=0)
-    outgoing = jnp.einsum("bs,bw->sw", select, halves, preferred_element_type=F32).astype(BF)
+    heads = swap(pair, "y")
+    resid, own, outgoing = call(
+        dispatch,
+        [
+            shaped(seq, cols, dtype=F32),
+            shaped(seq, cols),
+            shaped(experts * 2 * slots, half),
+        ],
+        4 * experts * 2 * slots * seq * half,
+        at,
+        heads,
+        tokens,
+        slot_rows,
+    )
     arrived = swap(outgoing.reshape(experts, 2 * slots, half), HUB)
     other = partner(own)
     count = nz * nx * cap
@@ -364,7 +477,6 @@
         arrived.reshape(-1, half),
         own,
         other,
-        mib=60,
     )
     whole = swap(both, "y")
 
@@ -427,16 +539,19 @@
     )
 
     results = swap(back.reshape(experts, 2 * slots, half), HUB)
-    results = results.reshape(experts * 2 * slots, half)
-    shared_out = shared_own + partner(shared_send).astype(F32)
-    combine = jnp.sum(jnp.where(hits, route_weight[:, :, None], F32(0.0)), axis=1)
-    sums = jnp.concatenate(
-        as_lines(combine.astype(BF)) + as_lines(dense_hits.astype(BF)), axis=0
-    )
-    sums = dot(sums, results).reshape(2, 2, seq, half)
-    routed = jnp.concatenate([sums[0, 0], sums[0, 1]], axis=1)
-    dense_out = jnp.concatenate([sums[1, 0], sums[1, 1]], axis=1)
-    mixed = (resid + routed + shared_out + jax.nn.sigmoid(dense_mix) * dense_out).astype(BF)
+    (mixed,) = call(
+        finish,
+        [shaped(seq, cols)],
+        8 * experts * 2 * slots * seq * half,
+        results.reshape(experts * 2 * slots, half),
+        within,
+        slot_cols,
+        route_weight,
+        resid,
+        shared_own,
+        partner(shared_send),
+        dense_mix.reshape(1, cols),
+    )
     return (mixed, new_state)
 
 

time: 184 us -> 220 us (1.20)
  the two profiles are of different devices: /device:TPU:8 before, /device:TPU:1 now
where the time goes in v5:
time: 220 us; the launch traced here: 217 us
  starting transfers between devices  67.1 us (30%)
  local copies, waits for them, and re-layouts  56.8 us (26%)
  waiting for transfers between devices  52 us (24%)
  other arithmetic  19.2 us (9%)
  Pallas kernels  19 us (9%)
    unnamed x126, local copies, waits for them, and re-layouts  44.6 us
    all_to_all x6, starting transfers between devices, swap(): return lax.all_to_all(x, axis, split_axis=0, concat_axis=0, tiled=True)  39.3 us
    ppermute x15, waiting for transfers between devices, shift(): return lax.ppermute(x, axis, [(i, (i + by) % size) for i in range(size)])  30.5 us
    ppermute x15, starting transfers between devices, shift(): return lax.ppermute(x, axis, [(i, (i + by) % size) for i in range(size)])  21.9 us
    all_to_all x6, waiting for transfers between devices, swap(): return lax.all_to_all(x, axis, split_axis=0, concat_axis=0, tiled=True)  19.5 us
    pallas_call x10, Pallas kernels, call(): pl.pallas_call(body, out_shape=outs, in_specs=specs, out_specs=[pl.BlockS...  19 us
    ppermute x10, starting transfers between devices, partner(): return lax.ppermute(x, 'c', [(0, 1), (1, 0)])  5.89 us
    another operation x4, other arithmetic  5.35 us
  transfers between devices with their start and end apart: 31, of which 11 were waited for; matrix products, arithmetic and copies ran while one was open for 15% of the time, Pallas kernels for 5%

profile of v5, /device:TPU:1, one launch (start us, length us, event | category | flops | bytes accessed | tf_op | source)
XLA Modules:
  0.0 216.5 jit_solution(9814107045974580949)
XLA Ops:
  12.2 9.1 %all-to-all-start = ((bf16[8,64,512]{2,1,0:T(8,128)(2,1)}), bf16[8,64,512]{2,1,0:T(8,128)(2,1)}, u32[]{:S(2)}, u32[]{:S(2)}) async-start(bf16[8,64,512]{2,1,0:T(8,128)(2,1)} %copy-done.17), calls=%async_computation | async-start | bytes 1048576 | tf_op jit(solution)/shard_map/all_to_all | solution.py:20
  22.6 2.5 %collective-permute-start.1 = (bf16[48,512]{1,0:T(8,128)(2,1)}, bf16[48,512]{1,0:T(8,128)(2,1)}, u32[]{:S(2)}, u32[]{:S(2)}) collective-permute-start(bf16[48,512]{1,0:T(8,128)(2,1)} %copy-done.52), channel_id=1, source_target_pairs={{0,16},{8,24},{16,0},{24,8},{1,17},{9,25},{17,1},{25,9},{2,18},{10... | collective-permute-start | bytes 147464 | tf_op jit(solution)/shard_map/ppermute | solution.py:29
  29.1 2.0 reduce-window.6
  31.0 1.6 slice_reduce_fusion
  37.3 2.2 %all-to-all-done = bf16[8,64,512]{2,1,0:T(8,128)(2,1)} async-done(((bf16[8,64,512]{2,1,0:T(8,128)(2,1)}), bf16[8,64,512]{2,1,0:T(8,128)(2,1)}, u32[]{:S(2)}, u32[]{:S(2)}) %all-to-all-start) | async-done | bytes 524320 | tf_op jit(solution)/shard_map/all_to_all | solution.py:20
  41.5 2.5 %collective-permute-start.3 = (bf16[48,512]{1,0:T(8,128)(2,1)}, bf16[48,512]{1,0:T(8,128)(2,1)}, u32[]{:S(2)}, u32[]{:S(2)}) collective-permute-start(bf16[48,512]{1,0:T(8,128)(2,1)} %get-tuple-element.50), channel_id=1, source_target_pairs={{0,24},{8,0},{16,8},{24,16},{1,25},{9,1},{17,9},{25,17},{2,26},{10... | collective-permute-start | bytes 147464 | tf_op jit(solution)/shard_map/ppermute | solution.py:29
  52.6 2.3 %shard_map.231 = (f32[48,128]{1,0:T(8,128)S(1)}, f32[48,128]{1,0:T(8,128)S(1)}, f32[48,128]{1,0:T(8,128)S(1)}, bf16[4,48,256]{2,1,0:T(8,128)(2,1)S(1)}, bf16[4,48,256]{2,1,0:T(8,128)(2,1)S(1)}) custom-call(s32[3]{0:T(128)S(1)} %pad_add_fusion.at, bf16[48,512]{1,0:T(8,128)(2,1)S(1)} %copy-done.22, bf16[48,512]{1,0:T(8,128)(2,1)} %collective-permute-done.3.p1, ...), custom_call_target="tpu_custom_call" | custom-call | flops 3145728 | bytes 4137996 | tf_op jit(solution)/shard_map/pallas_call | solution.py:52
  59.7 4.2 %all-to-all-start.1 = ((bf16[4,48,256]{2,1,0:T(8,128)(2,1)}), bf16[4,48,256]{2,1,0:T(8,128)(2,1)}, u32[]{:S(2)}, u32[]{:S(2)}) async-start(bf16[4,48,256]{2,1,0:T(8,128)(2,1)} %add_convert_fusion), calls=%async_computation.1 | async-start | bytes 196608 | tf_op jit(solution)/shard_map/all_to_all | solution.py:20
  66.1 2.5 %all-to-all-done.1.heads = bf16[4,48,256]{2,1,0:T(8,128)(2,1)} async-done(((bf16[4,48,256]{2,1,0:T(8,128)(2,1)}), bf16[4,48,256]{2,1,0:T(8,128)(2,1)}, u32[]{:S(2)}, u32[]{:S(2)}) %all-to-all-start.1) | async-done | bytes 98336 | tf_op jit(solution)/shard_map/all_to_all | solution.py:20
  69.6 1.9 shard_map.232
  73.4 10.1 %all-to-all-start.2 = ((bf16[64,24,128]{2,1,0:T(8,128)(2,1)}), bf16[64,24,128]{2,1,0:T(8,128)(2,1)}, u32[]{:S(2)}, u32[]{:S(2)}) async-start(bf16[64,24,128]{2,1,0:T(8,128)(2,1)} %bitcast.37), calls=%async_computation.2 | async-start | bytes 786432 | tf_op jit(solution)/shard_map/all_to_all | solution.py:20
  85.0 1.9 dynamic-slice_bitcast_fusion
  87.6 1.9 dynamic-slice_bitcast_fusion.2
  90.0 1.7 collective-permute-done.7.other
  92.3 6.4 %all-to-all-done.2 = bf16[64,24,128]{2,1,0:T(8,128)(2,1)} async-done(((bf16[64,24,128]{2,1,0:T(8,128)(2,1)}), bf16[64,24,128]{2,1,0:T(8,128)(2,1)}, u32[]{:S(2)}, u32[]{:S(2)}) %all-to-all-start.2) | async-done | bytes 393248 | tf_op jit(solution)/shard_map/all_to_all | solution.py:20
  103.3 4.2 %all-to-all-start.3 = ((bf16[4,240,512]{2,1,0:T(8,128)(2,1)}), bf16[4,240,512]{2,1,0:T(8,128)(2,1)}, u32[]{:S(2)}, u32[]{:S(2)}) async-start(bf16[4,240,512]{2,1,0:T(8,128)(2,1)} %copy-done.5), calls=%async_computation.3 | async-start | bytes 1966080 | tf_op jit(solution)/shard_map/all_to_all | solution.py:20
  109.0 2.5 %collective-permute-start.12 = (bf16[3,256,256]{2,1,0:T(8,128)(2,1)S(1)}, bf16[3,256,256]{2,1,0:T(8,128)(2,1)}, u32[]{:S(2)}, u32[]{:S(2)}) collective-permute-start(bf16[3,256,256]{2,1,0:T(8,128)(2,1)S(1)} %get-tuple-element.36.refs_0_.refs_4_), channel_id=1, source_target_pairs={{0,16},{8,24},{16,0},{24,8},{1,17},{9,25},{17,1},{25,9},{2,18},{10... | collective-permute-start | bytes 1179656 | tf_op jit(solution)/shard_map/ppermute | solution.py:29
  112.4 8.6 %collective-permute-done.12.refs_2_.refs_6_ = bf16[3,256,256]{2,1,0:T(8,128)(2,1)} collective-permute-done((bf16[3,256,256]{2,1,0:T(8,128)(2,1)S(1)}, bf16[3,256,256]{2,1,0:T(8,128)(2,1)}, u32[]{:S(2)}, u32[]{:S(2)}) %collective-permute-start.12) | collective-permute-done | bytes 393248 | tf_op jit(solution)/shard_map/ppermute | solution.py:29
  122.1 7.4 %collective-permute-done.13.refs_3_.refs_7_ = bf16[3,256,256]{2,1,0:T(8,128)(2,1)} collective-permute-done((bf16[3,256,256]{2,1,0:T(8,128)(2,1)S(1)}, bf16[3,256,256]{2,1,0:T(8,128)(2,1)}, u32[]{:S(2)}, u32[]{:S(2)}) %collective-permute-start.13) | collective-permute-done | bytes 393248 | tf_op jit(solution)/shard_map/ppermute | solution.py:29
  139.6 3.0 %shard_map.234 = bf16[4,240,512]{2,1,0:T(8,128)(2,1)S(1)} custom-call(s32[3]{0:T(128)S(1)} %pad_add_fusion.at, bf16[4,240,512]{2,1,0:T(8,128)(2,1)} %all-to-all-done.3.whole, f32[1,2048]{1,0:T(1,128)S(1)} %bitcast.39, bf16[2,2048,128]{2,1,0:T(8,128)(2,1)S(1)} %copy-done.2, bf16[2048,128]{1,0:T(8,128)(2,1)} %collective-permute-done.8.gate_other, ...), custom_call_target="tpu_custom_call" | custom-call | flops 679477248 | bytes 8265740 | tf_op jit(solution)/shard_map/pallas_call | solution.py:52
  143.6 4.5 %all-to-all-start.4 = ((bf16[4,240,512]{2,1,0:T(8,128)(2,1)}), bf16[4,240,512]{2,1,0:T(8,128)(2,1)}, u32[]{:S(2)}, u32[]{:S(2)}) async-start(bf16[4,240,512]{2,1,0:T(8,128)(2,1)} %copy-done.1), calls=%async_computation.4 | async-start | bytes 1966080 | tf_op jit(solution)/shard_map/all_to_all | solution.py:20
  149.7 3.2 %shard_map.235 = (bf16[48,2176]{1,0:T(8,128)(2,1)S(1)}, bf16[48,2176]{1,0:T(8,128)(2,1)}, bf16[48,2176]{1,0:T(8,128)(2,1)}, bf16[48,2176]{1,0:T(8,128)(2,1)}) custom-call(s32[3]{0:T(128)S(1)} %copy-done.36, bf16[2,192,256]{2,1,0:T(8,128)(2,1)S(1)} %copy-done.24, f32[8,256]{1,0:T(8,128)S(1)} %reshape.582.gain, ...), custom_call_target="tpu_custom_call" | custom-call | flops 402653184 | bytes 4186124 | tf_op jit(solution)/shard_map/pallas_call | solution.py:52
  155.0 2.4 %collective-permute-start.19 = (bf16[48,2176]{1,0:T(8,128)(2,1)}, bf16[48,2176]{1,0:T(8,128)(2,1)}, u32[]{:S(2)}, u32[]{:S(2)}) collective-permute-start(bf16[48,2176]{1,0:T(8,128)(2,1)} %get-tuple-element.39), channel_id=1, source_target_pairs={{0,4},{2,6},{4,0},{6,2},{1,5},{3,7},{5,1},{7,3},{8,12},{10,14},{12... | collective-permute-start | bytes 626696 | tf_op jit(solution)/shard_map/ppermute | solution.py:29
  159.2 8.0 %collective-permute-done.18.b = bf16[48,2176]{1,0:T(8,128)(2,1)} collective-permute-done((bf16[48,2176]{1,0:T(8,128)(2,1)}, bf16[48,2176]{1,0:T(8,128)(2,1)}, u32[]{:S(2)}, u32[]{:S(2)}) %collective-permute-start.18) | collective-permute-done | bytes 208928 | tf_op jit(solution)/shard_map/ppermute | solution.py:29
  167.2 4.0 %collective-permute-done.19.c = bf16[48,2176]{1,0:T(8,128)(2,1)} collective-permute-done((bf16[48,2176]{1,0:T(8,128)(2,1)}, bf16[48,2176]{1,0:T(8,128)(2,1)}, u32[]{:S(2)}, u32[]{:S(2)}) %collective-permute-start.19) | collective-permute-done | bytes 208928 | tf_op jit(solution)/shard_map/ppermute | solution.py:29
  174.6 1.8 collective-permute-start.22
  178.4 2.5 %collective-permute-done.22.refs_2_ = bf16[48,1024]{1,0:T(8,128)(2,1)S(1)} collective-permute-done((bf16[48,1024]{1,0:T(8,128)(2,1)S(1)}, bf16[48,1024]{1,0:T(8,128)(2,1)S(1)}, u32[]{:S(2)}, u32[]{:S(2)}) %collective-permute-start.22) | collective-permute-done | bytes 98336 | tf_op jit(solution)/shard_map/ppermute | solution.py:29
  180.9 2.1 shard_map.237.dense
  185.5 1.7 shard_map.238
  189.3 7.2 %all-to-all-start.5 = ((bf16[64,24,128]{2,1,0:T(8,128)(2,1)}), bf16[64,24,128]{2,1,0:T(8,128)(2,1)S(1)}, u32[]{:S(2)}, u32[]{:S(2)}) async-start(bf16[64,24,128]{2,1,0:T(8,128)(2,1)} %bitcast.38), calls=%async_computation.5 | async-start | bytes 786432 | tf_op jit(solution)/shard_map/all_to_all | solution.py:20
  198.4 4.2 %multiply_add_fusion = f32[48,1,128,128]{3,2,1,0:T(8,128)} fusion(f32[48,1,128,128]{3,2,1,0:T(8,128)S(1)} %copy-done, f32[48,128]{1,0:T(8,128)} %copy-done.39, f32[48,128]{1,0:T(8,128)} %copy-done.38, f32[48,128]{1,0:T(8,128)} %copy-done.37), kind=kLoop, calls=%fused_computation | loop fusion | flops 2359296 | bytes 6365184 | tf_op jit(solution)/shard_map/add | solution.py:438
  203.2 8.4 %all-to-all-done.5 = bf16[64,24,128]{2,1,0:T(8,128)(2,1)S(1)} async-done(((bf16[64,24,128]{2,1,0:T(8,128)(2,1)}), bf16[64,24,128]{2,1,0:T(8,128)(2,1)S(1)}, u32[]{:S(2)}, u32[]{:S(2)}) %all-to-all-start.5) | async-done | bytes 393248 | tf_op jit(solution)/shard_map/all_to_all | solution.py:20
  (197 shorter events, 87.3 us)
Async XLA Ops:
  0.7 131.1 %copy-start.35 = (s32[3]{0:T(128)}, s32[3]{0:T(128)S(1)}, u32[]{:S(2)}) copy-start(s32[3]{0:T(128)S(1)} %pad_add_fusion.at) | copy-start | bytes 40
  12.2 27.2 %all-to-all-start = ((bf16[8,64,512]{2,1,0:T(8,128)(2,1)}), bf16[8,64,512]{2,1,0:T(8,128)(2,1)}, u32[]{:S(2)}, u32[]{:S(2)}) async-start(bf16[8,64,512]{2,1,0:T(8,128)(2,1)} %copy-done.17), calls=%async_computation | async-start | bytes 1048576 | tf_op jit(solution)/shard_map/all_to_all | solution.py:20
  21.4 15.9 %collective-permute-start = (bf16[48,512]{1,0:T(8,128)(2,1)}, bf16[48,512]{1,0:T(8,128)(2,1)}, u32[]{:S(2)}, u32[]{:S(2)}) collective-permute-start(bf16[48,512]{1,0:T(8,128)(2,1)} %copy-done.53), channel_id=1, source_target_pairs={{0,8},{8,16},{16,24},{24,0},{1,9},{9,17},{17,25},{25,1},{2,10},{10... | collective-permute-start | bytes 147464 | tf_op jit(solution)/shard_map/ppermute | solution.py:29
  22.6 14.7 %collective-permute-start.1 = (bf16[48,512]{1,0:T(8,128)(2,1)}, bf16[48,512]{1,0:T(8,128)(2,1)}, u32[]{:S(2)}, u32[]{:S(2)}) collective-permute-start(bf16[48,512]{1,0:T(8,128)(2,1)} %copy-done.52), channel_id=1, source_target_pairs={{0,16},{8,24},{16,0},{24,8},{1,17},{9,25},{17,1},{25,9},{2,18},{10... | collective-permute-start | bytes 147464 | tf_op jit(solution)/shard_map/ppermute | solution.py:29
  25.0 12.2 %collective-permute-start.2 = (bf16[48,512]{1,0:T(8,128)(2,1)}, bf16[48,512]{1,0:T(8,128)(2,1)}, u32[]{:S(2)}, u32[]{:S(2)}) collective-permute-start(bf16[48,512]{1,0:T(8,128)(2,1)} %copy-done.51), channel_id=1, source_target_pairs={{0,24},{8,0},{16,8},{24,16},{1,25},{9,1},{17,9},{25,17},{2,26},{10... | collective-permute-start | bytes 147464 | tf_op jit(solution)/shard_map/ppermute | solution.py:29
  41.5 9.2 %collective-permute-start.3 = (bf16[48,512]{1,0:T(8,128)(2,1)}, bf16[48,512]{1,0:T(8,128)(2,1)}, u32[]{:S(2)}, u32[]{:S(2)}) collective-permute-start(bf16[48,512]{1,0:T(8,128)(2,1)} %get-tuple-element.50), channel_id=1, source_target_pairs={{0,24},{8,0},{16,8},{24,16},{1,25},{9,1},{17,9},{25,17},{2,26},{10... | collective-permute-start | bytes 147464 | tf_op jit(solution)/shard_map/ppermute | solution.py:29
  44.0 6.7 %collective-permute-start.4 = (bf16[48,512]{1,0:T(8,128)(2,1)}, bf16[48,512]{1,0:T(8,128)(2,1)}, u32[]{:S(2)}, u32[]{:S(2)}) collective-permute-start(bf16[48,512]{1,0:T(8,128)(2,1)} %get-tuple-element.49), channel_id=1, source_target_pairs={{0,16},{8,24},{16,0},{24,8},{1,17},{9,25},{17,1},{25,9},{2,18},{10... | collective-permute-start | bytes 147464 | tf_op jit(solution)/shard_map/ppermute | solution.py:29
  44.5 6.2 %collective-permute-start.5 = (bf16[48,512]{1,0:T(8,128)(2,1)}, bf16[48,512]{1,0:T(8,128)(2,1)}, u32[]{:S(2)}, u32[]{:S(2)}) collective-permute-start(bf16[48,512]{1,0:T(8,128)(2,1)} %get-tuple-element.48), channel_id=1, source_target_pairs={{0,8},{8,16},{16,24},{24,0},{1,9},{9,17},{17,25},{25,1},{2,10},{10... | collective-permute-start | bytes 147464 | tf_op jit(solution)/shard_map/ppermute | solution.py:29
  56.8 2.3 %collective-permute-start.6 = (bf16[4,48,256]{2,1,0:T(8,128)(2,1)S(1)}, bf16[4,48,256]{2,1,0:T(8,128)(2,1)S(1)}, u32[]{:S(2)}, u32[]{:S(2)}) collective-permute-start(bf16[4,48,256]{2,1,0:T(8,128)(2,1)S(1)} %get-tuple-element.31), channel_id=1, source_target_pairs={{0,1},{1,0},{2,3},{3,2},{4,5},{5,4},{6,7},{7,6},{8,9},{9,8},{10,11... | collective-permute-start | bytes 294920 | tf_op jit(solution)/shard_map/ppermute | solution.py:24
  59.7 8.9 %all-to-all-start.1 = ((bf16[4,48,256]{2,1,0:T(8,128)(2,1)}), bf16[4,48,256]{2,1,0:T(8,128)(2,1)}, u32[]{:S(2)}, u32[]{:S(2)}) async-start(bf16[4,48,256]{2,1,0:T(8,128)(2,1)} %add_convert_fusion), calls=%async_computation.1 | async-start | bytes 196608 | tf_op jit(solution)/shard_map/all_to_all | solution.py:20
  73.4 25.3 %all-to-all-start.2 = ((bf16[64,24,128]{2,1,0:T(8,128)(2,1)}), bf16[64,24,128]{2,1,0:T(8,128)(2,1)}, u32[]{:S(2)}, u32[]{:S(2)}) async-start(bf16[64,24,128]{2,1,0:T(8,128)(2,1)} %bitcast.37), calls=%async_computation.2 | async-start | bytes 786432 | tf_op jit(solution)/shard_map/all_to_all | solution.py:20
  83.6 27.9 %collective-permute-start.11 = (bf16[3,256,256]{2,1,0:T(8,128)(2,1)S(1)}, bf16[3,256,256]{2,1,0:T(8,128)(2,1)}, u32[]{:S(2)}, u32[]{:S(2)}) collective-permute-start(bf16[3,256,256]{2,1,0:T(8,128)(2,1)S(1)} %get-tuple-element.36.refs_0_.refs_4_), channel_id=1, source_target_pairs={{0,8},{8,16},{16,24},{24,0},{1,9},{9,17},{17,25},{25,1},{2,10},{10... | collective-permute-start | bytes 1179656 | tf_op jit(solution)/shard_map/ppermute | solution.py:29
  86.9 43.6 %collective-permute-start.10 = (bf16[128,2048]{1,0:T(8,128)(2,1)}, bf16[128,2048]{1,0:T(8,128)(2,1)}, u32[]{:S(2)}, u32[]{:S(2)}) collective-permute-start(bf16[128,2048]{1,0:T(8,128)(2,1)} %dynamic-slice_bitcast_fusion), channel_id=1, source_target_pairs={{0,1},{1,0},{2,3},{3,2},{4,5},{5,4},{6,7},{7,6},{8,9},{9,8},{10,11... | collective-permute-start | bytes 1572872 | tf_op jit(solution)/shard_map/ppermute | solution.py:24
  89.4 41.0 %collective-permute-start.8 = (bf16[2048,128]{1,0:T(8,128)(2,1)}, bf16[2048,128]{1,0:T(8,128)(2,1)}, u32[]{:S(2)}, u32[]{:S(2)}) collective-permute-start(bf16[2048,128]{1,0:T(8,128)(2,1)} %dynamic-slice_bitcast_fusion.2), channel_id=1, source_target_pairs={{0,1},{1,0},{2,3},{3,2},{4,5},{5,4},{6,7},{7,6},{8,9},{9,8},{10,11... | collective-permute-start | bytes 1572872 | tf_op jit(solution)/shard_map/ppermute | solution.py:24
  89.4 2.2 %collective-permute-start.7 = (bf16[48,256]{1,0:T(8,128)(2,1)}, bf16[48,256]{1,0:T(8,128)(2,1)S(1)}, u32[]{:S(2)}, u32[]{:S(2)}) collective-permute-start(bf16[48,256]{1,0:T(8,128)(2,1)} %copy-done.54), channel_id=1, source_target_pairs={{0,1},{1,0},{2,3},{3,2},{4,5},{5,4},{6,7},{7,6},{8,9},{9,8},{10,11... | collective-permute-start | bytes 73736 | tf_op jit(solution)/shard_map/ppermute | solution.py:24
  103.3 28.5 %all-to-all-start.3 = ((bf16[4,240,512]{2,1,0:T(8,128)(2,1)}), bf16[4,240,512]{2,1,0:T(8,128)(2,1)}, u32[]{:S(2)}, u32[]{:S(2)}) async-start(bf16[4,240,512]{2,1,0:T(8,128)(2,1)} %copy-done.5), calls=%async_computation.3 | async-start | bytes 1966080 | tf_op jit(solution)/shard_map/all_to_all | solution.py:20
  108.6 22.4 %collective-permute-start.9 = (bf16[2048,128]{1,0:T(8,128)(2,1)S(1)}, bf16[2048,128]{1,0:T(8,128)(2,1)S(1)}, u32[]{:S(2)}, u32[]{:S(2)}) collective-permute-start(bf16[2048,128]{1,0:T(8,128)(2,1)S(1)} %dynamic-slice_bitcast_fusion.1), channel_id=1, source_target_pairs={{0,1},{1,0},{2,3},{3,2},{4,5},{5,4},{6,7},{7,6},{8,9},{9,8},{10,11... | collective-permute-start | bytes 1572872 | tf_op jit(solution)/shard_map/ppermute | solution.py:24
  109.0 12.0 %collective-permute-start.12 = (bf16[3,256,256]{2,1,0:T(8,128)(2,1)S(1)}, bf16[3,256,256]{2,1,0:T(8,128)(2,1)}, u32[]{:S(2)}, u32[]{:S(2)}) collective-permute-start(bf16[3,256,256]{2,1,0:T(8,128)(2,1)S(1)} %get-tuple-element.36.refs_0_.refs_4_), channel_id=1, source_target_pairs={{0,16},{8,24},{16,0},{24,8},{1,17},{9,25},{17,1},{25,9},{2,18},{10... | collective-permute-start | bytes 1179656 | tf_op jit(solution)/shard_map/ppermute | solution.py:29
  111.5 18.0 %collective-permute-start.13 = (bf16[3,256,256]{2,1,0:T(8,128)(2,1)S(1)}, bf16[3,256,256]{2,1,0:T(8,128)(2,1)}, u32[]{:S(2)}, u32[]{:S(2)}) collective-permute-start(bf16[3,256,256]{2,1,0:T(8,128)(2,1)S(1)} %get-tuple-element.36.refs_0_.refs_4_), channel_id=1, source_target_pairs={{0,24},{8,0},{16,8},{24,16},{1,25},{9,1},{17,9},{25,17},{2,26},{10... | collective-permute-start | bytes 1179656 | tf_op jit(solution)/shard_map/ppermute | solution.py:29
  121.0 27.0 %collective-permute-start.14 = (bf16[3,256,256]{2,1,0:T(8,128)(2,1)S(1)}, bf16[3,256,256]{2,1,0:T(8,128)(2,1)}, u32[]{:S(2)}, u32[]{:S(2)}) collective-permute-start(bf16[3,256,256]{2,1,0:T(8,128)(2,1)S(1)} %get-tuple-element.36.refs_0_.refs_4_), channel_id=1, source_target_pairs={{0,1},{1,0},{2,3},{3,2},{4,5},{5,4},{6,7},{7,6},{8,9},{9,8},{10,11... | collective-permute-start | bytes 1179656 | tf_op jit(solution)/shard_map/ppermute | solution.py:24
  129.5 18.6 %collective-permute-start.15 = (bf16[3,256,256]{2,1,0:T(8,128)(2,1)}, bf16[3,256,256]{2,1,0:T(8,128)(2,1)}, u32[]{:S(2)}, u32[]{:S(2)}) collective-permute-start(bf16[3,256,256]{2,1,0:T(8,128)(2,1)} %collective-permute-done.11.refs_1_.refs_5_), channel_id=1, source_target_pairs={{0,1},{1,0},{2,3},{3,2},{4,5},{5,4},{6,7},{7,6},{8,9},{9,8},{10,11... | collective-permute-start | bytes 1179656 | tf_op jit(solution)/shard_map/ppermute | solution.py:24
  130.4 17.6 %collective-permute-start.16 = (bf16[3,256,256]{2,1,0:T(8,128)(2,1)}, bf16[3,256,256]{2,1,0:T(8,128)(2,1)}, u32[]{:S(2)}, u32[]{:S(2)}) collective-permute-start(bf16[3,256,256]{2,1,0:T(8,128)(2,1)} %collective-permute-done.12.refs_2_.refs_6_), channel_id=1, source_target_pairs={{0,1},{1,0},{2,3},{3,2},{4,5},{5,4},{6,7},{7,6},{8,9},{9,8},{10,11... | collective-permute-start | bytes 1179656 | tf_op jit(solution)/shard_map/ppermute | solution.py:24
  130.5 17.6 %collective-permute-start.17 = (bf16[3,256,256]{2,1,0:T(8,128)(2,1)}, bf16[3,256,256]{2,1,0:T(8,128)(2,1)}, u32[]{:S(2)}, u32[]{:S(2)}) collective-permute-start(bf16[3,256,256]{2,1,0:T(8,128)(2,1)} %collective-permute-done.13.refs_3_.refs_7_), channel_id=1, source_target_pairs={{0,1},{1,0},{2,3},{3,2},{4,5},{5,4},{6,7},{7,6},{8,9},{9,8},{10,11... | collective-permute-start | bytes 1179656 | tf_op jit(solution)/shard_map/ppermute | solution.py:24
  143.6 40.1 %all-to-all-start.4 = ((bf16[4,240,512]{2,1,0:T(8,128)(2,1)}), bf16[4,240,512]{2,1,0:T(8,128)(2,1)}, u32[]{:S(2)}, u32[]{:S(2)}) async-start(bf16[4,240,512]{2,1,0:T(8,128)(2,1)} %copy-done.1), calls=%async_computation.4 | async-start | bytes 1966080 | tf_op jit(solution)/shard_map/all_to_all | solution.py:20
  153.5 13.8 %collective-permute-start.18 = (bf16[48,2176]{1,0:T(8,128)(2,1)}, bf16[48,2176]{1,0:T(8,128)(2,1)}, u32[]{:S(2)}, u32[]{:S(2)}) collective-permute-start(bf16[48,2176]{1,0:T(8,128)(2,1)} %get-tuple-element.38), channel_id=1, source_target_pairs={{0,2},{2,4},{4,6},{6,0},{1,3},{3,5},{5,7},{7,1},{8,10},{10,12},{12... | collective-permute-start | bytes 626696 | tf_op jit(solution)/shard_map/ppermute | solution.py:29
  155.0 16.3 %collective-permute-start.19 = (bf16[48,2176]{1,0:T(8,128)(2,1)}, bf16[48,2176]{1,0:T(8,128)(2,1)}, u32[]{:S(2)}, u32[]{:S(2)}) collective-permute-start(bf16[48,2176]{1,0:T(8,128)(2,1)} %get-tuple-element.39), channel_id=1, source_target_pairs={{0,4},{2,6},{4,0},{6,2},{1,5},{3,7},{5,1},{7,3},{8,12},{10,14},{12... | collective-permute-start | bytes 626696 | tf_op jit(solution)/shard_map/ppermute | solution.py:29
  157.4 13.9 %collective-permute-start.20 = (bf16[48,2176]{1,0:T(8,128)(2,1)}, bf16[48,2176]{1,0:T(8,128)(2,1)}, u32[]{:S(2)}, u32[]{:S(2)}) collective-permute-start(bf16[48,2176]{1,0:T(8,128)(2,1)} %get-tuple-element.40), channel_id=1, source_target_pairs={{0,6},{2,0},{4,2},{6,4},{1,7},{3,1},{5,3},{7,5},{8,14},{10,8},{12,... | collective-permute-start | bytes 626696 | tf_op jit(solution)/shard_map/ppermute | solution.py:29
  173.5 4.9 %collective-permute-start.21 = (bf16[48,1024]{1,0:T(8,128)(2,1)S(1)}, bf16[48,1024]{1,0:T(8,128)(2,1)S(1)}, u32[]{:S(2)}, u32[]{:S(2)}) collective-permute-start(bf16[48,1024]{1,0:T(8,128)(2,1)S(1)} %shard_map.236.refs_0_), channel_id=1, source_target_pairs={{0,2},{2,4},{4,6},{6,0},{1,3},{3,5},{5,7},{7,1},{8,10},{10,12},{12... | collective-permute-start | bytes 294920 | tf_op jit(solution)/shard_map/ppermute | solution.py:29
  174.6 6.3 %collective-permute-start.22 = (bf16[48,1024]{1,0:T(8,128)(2,1)S(1)}, bf16[48,1024]{1,0:T(8,128)(2,1)S(1)}, u32[]{:S(2)}, u32[]{:S(2)}) collective-permute-start(bf16[48,1024]{1,0:T(8,128)(2,1)S(1)} %shard_map.236.refs_0_), channel_id=1, source_target_pairs={{0,4},{2,6},{4,0},{6,2},{1,5},{3,7},{5,1},{7,3},{8,12},{10,14},{12... | collective-permute-start | bytes 294920 | tf_op jit(solution)/shard_map/ppermute | solution.py:29
  176.4 4.5 %collective-permute-start.23 = (bf16[48,1024]{1,0:T(8,128)(2,1)S(1)}, bf16[48,1024]{1,0:T(8,128)(2,1)S(1)}, u32[]{:S(2)}, u32[]{:S(2)}) collective-permute-start(bf16[48,1024]{1,0:T(8,128)(2,1)S(1)} %shard_map.236.refs_0_), channel_id=1, source_target_pairs={{0,6},{2,0},{4,2},{6,4},{1,7},{3,1},{5,3},{7,5},{8,14},{10,8},{12,... | collective-permute-start | bytes 294920 | tf_op jit(solution)/shard_map/ppermute | solution.py:29
  189.3 22.3 %all-to-all-start.5 = ((bf16[64,24,128]{2,1,0:T(8,128)(2,1)}), bf16[64,24,128]{2,1,0:T(8,128)(2,1)S(1)}, u32[]{:S(2)}, u32[]{:S(2)}) async-start(bf16[64,24,128]{2,1,0:T(8,128)(2,1)} %bitcast.38), calls=%async_computation.5 | async-start | bytes 786432 | tf_op jit(solution)/shard_map/all_to_all | solution.py:20
  197.9 4.7 %collective-permute-start.24 = (bf16[48,256]{1,0:T(8,128)(2,1)}, bf16[48,256]{1,0:T(8,128)(2,1)S(1)}, u32[]{:S(2)}, u32[]{:S(2)}) collective-permute-start(bf16[48,256]{1,0:T(8,128)(2,1)} %copy-done.56), channel_id=1, source_target_pairs={{0,1},{1,0},{2,3},{3,2},{4,5},{5,4},{6,7},{7,6},{8,9},{9,8},{10,11... | collective-permute-start | bytes 73736 | tf_op jit(solution)/shard_map/ppermute | solution.py:24
  (61 other events, 301.3 us)

commit v6 on v5

--- a/solution.py
+++ b/solution.py
@@ -41,7 +41,7 @@
     return x * jax.nn.sigmoid(x)
 
 
-def call(body, outs, flops, *args, mib=12, scratch=()):
+def call(body, outs, flops, *args, mib=0, scratch=()):
     moved = sum(a.size * a.dtype.itemsize for a in args) + sum(
         o.size * o.dtype.itemsize for o in outs
     )
@@ -56,7 +56,7 @@
         out_specs=[pl.BlockSpec(memory_space=pltpu.VMEM) for _ in outs],
         scratch_shapes=scratch,
         cost_estimate=pl.CostEstimate(flops=flops, bytes_accessed=moved, transcendentals=0),
-        compiler_params=pltpu.CompilerParams(vmem_limit_bytes=mib * 2**20),
+        compiler_params=pltpu.CompilerParams(vmem_limit_bytes=mib * 2**20) if mib else None,
     )(*args)
 
 
@@ -521,7 +521,7 @@
         shared_gate,
         shared_up,
         shared_down,
-        mib=24,
+        mib=0,
     )
     parts = swap(parts, "y")
     back, shared_own, shared_send = call(

time: 220 us -> 189 us (0.86)
  the two profiles are of different devices: /device:TPU:1 before, /device:TPU:8 now
where the time goes in v6:
time: 189 us; the launch traced here: 186 us
  waiting for transfers between devices  67.2 us (36%)
  starting transfers between devices  60.2 us (32%)
  Pallas kernels  30.9 us (16%)
  other arithmetic  14.6 us (8%)
  local copies, waits for them, and re-layouts  11 us (6%)
    ppermute x15, waiting for transfers between devices, shift(): return lax.ppermute(x, axis, [(i, (i + by) % size) for i in range(size)])  36.5 us
    all_to_all x6, starting transfers between devices, swap(): return lax.all_to_all(x, axis, split_axis=0, concat_axis=0, tiled=True)  34.5 us
    pallas_call x10, Pallas kernels, call(): pl.pallas_call(body, out_shape=outs, in_specs=specs, out_specs=[pl.BlockS...  30.9 us
    all_to_all x6, waiting for transfers between devices, swap(): return lax.all_to_all(x, axis, split_axis=0, concat_axis=0, tiled=True)  28.6 us
    ppermute x15, starting transfers between devices, shift(): return lax.ppermute(x, axis, [(i, (i + by) % size) for i in range(size)])  24.4 us
    unnamed x50, local copies, waits for them, and re-layouts  6.13 us
    add x1, other arithmetic, step(): decay.reshape(shape)[..., None] * state  4.19 us
  transfers between devices with their start and end apart: 31, of which 16 were waited for; matrix products, arithmetic and copies ran while one was open for 10% of the time, Pallas kernels for 9%

profile of v6, /device:TPU:8, one launch (start us, length us, event | category | flops | bytes accessed | tf_op | source)
XLA Modules:
  0.0 185.7 jit_solution(11195898927999869040)
XLA Ops:
  1.2 2.4 %shard_map.230 = (bf16[8,64,512]{2,1,0:T(8,128)(2,1)}, bf16[3,256,256]{2,1,0:T(8,128)(2,1)}, bf16[48,512]{1,0:T(8,128)(2,1)}, bf16[48,512]{1,0:T(8,128)(2,1)}, b...) custom-call(s32[3]{0:T(128)} %pad_add_fusion.at, bf16[48,2048]{1,0:T(8,128)(2,1)} %tokens.3, f32[1,2048]{1,0:T(1,128)} %bitcast.41, ...), custom_call_target="tpu_custom_call" | custom-call | flops 1000000 | bytes 1777676 | tf_op jit(solution)/shard_map/pallas_call | solution.py:52
  3.6 8.5 %all-to-all-start = ((bf16[8,64,512]{2,1,0:T(8,128)(2,1)}), bf16[8,64,512]{2,1,0:T(8,128)(2,1)S(1)}, u32[]{:S(2)}, u32[]{:S(2)}) async-start(bf16[8,64,512]{2,1,0:T(8,128)(2,1)} %get-tuple-element.29), calls=%async_computation | async-start | bytes 1048576 | tf_op jit(solution)/shard_map/all_to_all | solution.py:20
  13.6 2.7 %collective-permute-start.1 = (bf16[48,512]{1,0:T(8,128)(2,1)}, bf16[48,512]{1,0:T(8,128)(2,1)S(1)}, u32[]{:S(2)}, u32[]{:S(2)}) collective-permute-start(bf16[48,512]{1,0:T(8,128)(2,1)} %get-tuple-element.27), channel_id=1, source_target_pairs={{0,16},{8,24},{16,0},{24,8},{1,17},{9,25},{17,1},{25,9},{2,18},{10... | collective-permute-start | bytes 147464 | tf_op jit(solution)/shard_map/ppermute | solution.py:29
  20.6 9.0 %all-to-all-done = bf16[8,64,512]{2,1,0:T(8,128)(2,1)S(1)} async-done(((bf16[8,64,512]{2,1,0:T(8,128)(2,1)}), bf16[8,64,512]{2,1,0:T(8,128)(2,1)S(1)}, u32[]{:S(2)}, u32[]{:S(2)}) %all-to-all-start) | async-done | bytes 524320 | tf_op jit(solution)/shard_map/all_to_all | solution.py:20
  31.3 2.8 %collective-permute-start.3 = (bf16[48,512]{1,0:T(8,128)(2,1)S(1)}, bf16[48,512]{1,0:T(8,128)(2,1)S(1)}, u32[]{:S(2)}, u32[]{:S(2)}) collective-permute-start(bf16[48,512]{1,0:T(8,128)(2,1)S(1)} %get-tuple-element.50), channel_id=1, source_target_pairs={{0,24},{8,0},{16,8},{24,16},{1,25},{9,1},{17,9},{25,17},{2,26},{10... | collective-permute-start | bytes 147464 | tf_op jit(solution)/shard_map/ppermute | solution.py:29
  36.7 3.0 %collective-permute-done.4.p2 = bf16[48,512]{1,0:T(8,128)(2,1)S(1)} collective-permute-done((bf16[48,512]{1,0:T(8,128)(2,1)S(1)}, bf16[48,512]{1,0:T(8,128)(2,1)S(1)}, u32[]{:S(2)}, u32[]{:S(2)}) %collective-permute-start.4) | collective-permute-done | bytes 49184 | tf_op jit(solution)/shard_map/ppermute | solution.py:29
  40.8 4.4 %shard_map.231 = (f32[48,128]{1,0:T(8,128)}, f32[48,128]{1,0:T(8,128)}, f32[48,128]{1,0:T(8,128)}, bf16[4,48,256]{2,1,0:T(8,128)(2,1)}, bf16[4,48,256]{2,1,0:T(8,128)(2,1)}) custom-call(s32[3]{0:T(128)} %pad_add_fusion.at, bf16[48,512]{1,0:T(8,128)(2,1)} %get-tuple-element.51.p0, bf16[48,512]{1,0:T(8,128)(2,1)} %copy-done.18, bf16[48,512]{1,0:T(8,128)(2,1)} %copy-done.19, ...), custom_call_target="tpu_custom_call" | custom-call | flops 3145728 | bytes 4137996 | tf_op jit(solution)/shard_map/pallas_call | solution.py:52
  48.4 4.9 %all-to-all-start.1 = ((bf16[4,48,256]{2,1,0:T(8,128)(2,1)}), bf16[4,48,256]{2,1,0:T(8,128)(2,1)}, u32[]{:S(2)}, u32[]{:S(2)}) async-start(bf16[4,48,256]{2,1,0:T(8,128)(2,1)} %add_convert_fusion), calls=%async_computation.1 | async-start | bytes 196608 | tf_op jit(solution)/shard_map/all_to_all | solution.py:20
  57.7 2.7 %shard_map.232 = (f32[48,256]{1,0:T(8,128)}, bf16[48,256]{1,0:T(8,128)(2,1)}, bf16[1536,128]{1,0:T(8,128)(2,1)}) custom-call(s32[3]{0:T(128)} %pad_add_fusion.at, bf16[4,48,256]{2,1,0:T(8,128)(2,1)} %all-to-all-done.1.heads, bf16[48,2048]{1,0:T(8,128)(2,1)} %tokens.3, s32[8,48]{1,0:T(8,128)} %copy.55.slots), custom_call_target="tpu_custom_call" | custom-call | flops 37748736 | bytes 763404 | tf_op jit(solution)/shard_map/pallas_call | solution.py:52
  60.4 5.5 %all-to-all-start.2 = ((bf16[64,24,128]{2,1,0:T(8,128)(2,1)}), bf16[64,24,128]{2,1,0:T(8,128)(2,1)}, u32[]{:S(2)}, u32[]{:S(2)}) async-start(bf16[64,24,128]{2,1,0:T(8,128)(2,1)} %bitcast.38), calls=%async_computation.2 | async-start | bytes 786432 | tf_op jit(solution)/shard_map/all_to_all | solution.py:20
  71.4 9.3 %all-to-all-done.2 = bf16[64,24,128]{2,1,0:T(8,128)(2,1)} async-done(((bf16[64,24,128]{2,1,0:T(8,128)(2,1)}), bf16[64,24,128]{2,1,0:T(8,128)(2,1)}, u32[]{:S(2)}, u32[]{:S(2)}) %all-to-all-start.2) | async-done | bytes 393248 | tf_op jit(solution)/shard_map/all_to_all | solution.py:20
  80.8 2.5 %shard_map.233 = (bf16[4,240,512]{2,1,0:T(8,128)(2,1)}, bf16[2,192,256]{2,1,0:T(8,128)(2,1)}) custom-call(s32[3]{0:T(128)} %pad_add_fusion.at, s32[1,384]{1,0:T(1,128)} %fusion.53.line_of, bf16[1536,128]{1,0:T(8,128)(2,1)} %bitcast.11.lines, bf16[48,256]{1,0:T(8,128)(2,1)} %get-tuple-element.33.own, bf16[48,256]{1,0:T(8,128)(2,1)} %copy-done.23), custom_call_target="tpu_custom_call" | custom-call | flops 150994944 | bytes 1623564 | tf_op jit(solution)/shard_map/pallas_call | solution.py:52
  83.2 4.9 %all-to-all-start.3 = ((bf16[4,240,512]{2,1,0:T(8,128)(2,1)}), bf16[4,240,512]{2,1,0:T(8,128)(2,1)S(1)}, u32[]{:S(2)}, u32[]{:S(2)}) async-start(bf16[4,240,512]{2,1,0:T(8,128)(2,1)} %get-tuple-element.34), calls=%async_computation.3 | async-start | bytes 1966080 | tf_op jit(solution)/shard_map/all_to_all | solution.py:20
  88.3 2.9 %collective-permute-start.12 = (bf16[3,256,256]{2,1,0:T(8,128)(2,1)S(1)}, bf16[3,256,256]{2,1,0:T(8,128)(2,1)S(1)}, u32[]{:S(2)}, u32[]{:S(2)}) collective-permute-start(bf16[3,256,256]{2,1,0:T(8,128)(2,1)S(1)} %copy-done.6), channel_id=1, source_target_pairs={{0,16},{8,24},{16,0},{24,8},{1,17},{9,25},{17,1},{25,9},{2,18},{10... | collective-permute-start | bytes 1179656 | tf_op jit(solution)/shard_map/ppermute | solution.py:29
  92.4 8.9 %collective-permute-done.12.refs_2_.refs_6_ = bf16[3,256,256]{2,1,0:T(8,128)(2,1)S(1)} collective-permute-done((bf16[3,256,256]{2,1,0:T(8,128)(2,1)S(1)}, bf16[3,256,256]{2,1,0:T(8,128)(2,1)S(1)}, u32[]{:S(2)}, u32[]{:S(2)}) %collective-permute-start.12) | collective-permute-done | bytes 393248 | tf_op jit(solution)/shard_map/ppermute | solution.py:29
  101.3 8.3 %collective-permute-done.13.refs_3_.refs_7_ = bf16[3,256,256]{2,1,0:T(8,128)(2,1)S(1)} collective-permute-done((bf16[3,256,256]{2,1,0:T(8,128)(2,1)S(1)}, bf16[3,256,256]{2,1,0:T(8,128)(2,1)S(1)}, u32[]{:S(2)}, u32[]{:S(2)}) %collective-permute-start.13) | collective-permute-done | bytes 393248 | tf_op jit(solution)/shard_map/ppermute | solution.py:29
  111.4 5.6 %shard_map.234 = bf16[4,240,512]{2,1,0:T(8,128)(2,1)} custom-call(s32[3]{0:T(128)} %pad_add_fusion.at, bf16[4,240,512]{2,1,0:T(8,128)(2,1)} %copy-done.1, f32[1,2048]{1,0:T(1,128)} %bitcast.40, bf16[2,2048,128]{2,1,0:T(8,128)(2,1)} %gate.1, bf16[2048,128]{1,0:T(8,128)(2,1)} %collective-permute-done.8.gate_other, bf16[2,2048,128]{2,1,0:T(8,128)(2,1)} %up.1, ...), custom_call_target="tpu_custom_call" | custom-call | flops 679477248 | bytes 8265740 | tf_op jit(solution)/shard_map/pallas_call | solution.py:52
  117.0 4.9 %all-to-all-start.4 = ((bf16[4,240,512]{2,1,0:T(8,128)(2,1)}), bf16[4,240,512]{2,1,0:T(8,128)(2,1)}, u32[]{:S(2)}, u32[]{:S(2)}) async-start(bf16[4,240,512]{2,1,0:T(8,128)(2,1)} %shard_map.234), calls=%async_computation.4 | async-start | bytes 1966080 | tf_op jit(solution)/shard_map/all_to_all | solution.py:20
  123.4 3.4 %shard_map.235 = (bf16[48,2176]{1,0:T(8,128)(2,1)}, bf16[48,2176]{1,0:T(8,128)(2,1)}, bf16[48,2176]{1,0:T(8,128)(2,1)}, bf16[48,2176]{1,0:T(8,128)(2,1)}) custom-call(s32[3]{0:T(128)} %pad_add_fusion.at, bf16[2,192,256]{2,1,0:T(8,128)(2,1)} %get-tuple-element.35.rows, f32[8,256]{1,0:T(8,128)} %reshape.582.gain, ...), custom_call_target="tpu_custom_call" | custom-call | flops 402653184 | bytes 4186124 | tf_op jit(solution)/shard_map/pallas_call | solution.py:52
  128.9 2.5 %collective-permute-start.20 = (bf16[48,2176]{1,0:T(8,128)(2,1)}, bf16[48,2176]{1,0:T(8,128)(2,1)S(1)}, u32[]{:S(2)}, u32[]{:S(2)}) collective-permute-start(bf16[48,2176]{1,0:T(8,128)(2,1)} %get-tuple-element.40), channel_id=1, source_target_pairs={{0,6},{2,0},{4,2},{6,4},{1,7},{3,1},{5,3},{7,5},{8,14},{10,8},{12,... | collective-permute-start | bytes 626696 | tf_op jit(solution)/shard_map/ppermute | solution.py:29
  132.2 6.6 %collective-permute-done.18.b = bf16[48,2176]{1,0:T(8,128)(2,1)S(1)} collective-permute-done((bf16[48,2176]{1,0:T(8,128)(2,1)}, bf16[48,2176]{1,0:T(8,128)(2,1)S(1)}, u32[]{:S(2)}, u32[]{:S(2)}) %collective-permute-start.18) | collective-permute-done | bytes 208928 | tf_op jit(solution)/shard_map/ppermute | solution.py:29
  138.7 2.1 %collective-permute-done.19.c = bf16[48,2176]{1,0:T(8,128)(2,1)S(1)} collective-permute-done((bf16[48,2176]{1,0:T(8,128)(2,1)}, bf16[48,2176]{1,0:T(8,128)(2,1)S(1)}, u32[]{:S(2)}, u32[]{:S(2)}) %collective-permute-start.19) | collective-permute-done | bytes 208928 | tf_op jit(solution)/shard_map/ppermute | solution.py:29
  140.8 3.6 %collective-permute-done.20.d = bf16[48,2176]{1,0:T(8,128)(2,1)S(1)} collective-permute-done((bf16[48,2176]{1,0:T(8,128)(2,1)}, bf16[48,2176]{1,0:T(8,128)(2,1)S(1)}, u32[]{:S(2)}, u32[]{:S(2)}) %collective-permute-start.20) | collective-permute-done | bytes 208928 | tf_op jit(solution)/shard_map/ppermute | solution.py:29
  145.1 2.1 %shard_map.236.refs_0_ = bf16[48,1024]{1,0:T(8,128)(2,1)} custom-call(bf16[48,2176]{1,0:T(8,128)(2,1)} %get-tuple-element.37.a, bf16[48,2176]{1,0:T(8,128)(2,1)} %copy-done.12, bf16[48,2176]{1,0:T(8,128)(2,1)} %copy-done.13, bf16[48,2176]{1,0:T(8,128)(2,1)} %copy-done.14), custom_call_target="tpu_custom_call" | custom-call | flops 1000000 | bytes 933888 | tf_op jit(solution)/shard_map/pallas_call | solution.py:52
  147.8 3.1 %collective-permute-start.22 = (bf16[48,1024]{1,0:T(8,128)(2,1)}, bf16[48,1024]{1,0:T(8,128)(2,1)S(1)}, u32[]{:S(2)}, u32[]{:S(2)}) collective-permute-start(bf16[48,1024]{1,0:T(8,128)(2,1)} %shard_map.236.refs_0_), channel_id=1, source_target_pairs={{0,4},{2,6},{4,0},{6,2},{1,5},{3,7},{5,1},{7,3},{8,12},{10,14},{12... | collective-permute-start | bytes 294920 | tf_op jit(solution)/shard_map/ppermute | solution.py:29
  152.6 2.1 %collective-permute-done.22.refs_2_ = bf16[48,1024]{1,0:T(8,128)(2,1)S(1)} collective-permute-done((bf16[48,1024]{1,0:T(8,128)(2,1)}, bf16[48,1024]{1,0:T(8,128)(2,1)S(1)}, u32[]{:S(2)}, u32[]{:S(2)}) %collective-permute-start.22) | collective-permute-done | bytes 98336 | tf_op jit(solution)/shard_map/ppermute | solution.py:29
  156.3 3.1 %shard_map.237.dense = bf16[2,192,256]{2,1,0:T(8,128)(2,1)} custom-call(s32[3]{0:T(128)} %pad_add_fusion.at, bf16[48,1024]{1,0:T(8,128)(2,1)} %shard_map.236.refs_0_, bf16[48,1024]{1,0:T(8,128)(2,1)} %copy-done.15, bf16[48,1024]{1,0:T(8,128)(2,1)} %copy-done.16, bf16[48,1024]{1,0:T(8,128)(2,1)} %copy-done.17, ...), custom_call_target="tpu_custom_call" | custom-call | flops 201326592 | bytes 3735564 | tf_op jit(solution)/shard_map/pallas_call | solution.py:52
  159.4 2.6 %shard_map.238 = (bf16[1536,128]{1,0:T(8,128)(2,1)}, f32[48,256]{1,0:T(8,128)}, bf16[48,256]{1,0:T(8,128)(2,1)}) custom-call(s32[3]{0:T(128)} %pad_add_fusion.at, s32[384,1]{1,0:T(8,128)} %fusion.8.line_of, bf16[4,240,512]{2,1,0:T(8,128)(2,1)} %all-to-all-done.4.parts, bf16[2,192,256]{2,1,0:T(8,128)(2,1)} %shard_map.237.dense), custom_call_target="tpu_custom_call" | custom-call | flops 150994944 | bytes 1648140 | tf_op jit(solution)/shard_map/pallas_call | solution.py:52
  162.0 5.8 %all-to-all-start.5 = ((bf16[64,24,128]{2,1,0:T(8,128)(2,1)}), bf16[64,24,128]{2,1,0:T(8,128)(2,1)S(1)}, u32[]{:S(2)}, u32[]{:S(2)}) async-start(bf16[64,24,128]{2,1,0:T(8,128)(2,1)} %bitcast.39), calls=%async_computation.5 | async-start | bytes 786432 | tf_op jit(solution)/shard_map/all_to_all | solution.py:20
  169.9 4.2 %multiply_add_fusion = f32[48,1,128,128]{3,2,1,0:T(8,128)} fusion(f32[48,1,128,128]{3,2,1,0:T(8,128)S(1)} %copy-done, f32[48,128]{1,0:T(8,128)} %get-tuple-element.47, f32[48,128]{1,0:T(8,128)} %get-tuple-element.46, f32[48,128]{1,0:T(8,128)} %get-tuple-element.45), kind=kLoop, calls=%fused_computation | loop fusion | flops 2359296 | bytes 6365184 | tf_op jit(solution)/shard_map/add | solution.py:438
  174.1 8.7 %all-to-all-done.5 = bf16[64,24,128]{2,1,0:T(8,128)(2,1)S(1)} async-done(((bf16[64,24,128]{2,1,0:T(8,128)(2,1)}), bf16[64,24,128]{2,1,0:T(8,128)(2,1)S(1)}, u32[]{:S(2)}, u32[]{:S(2)}) %all-to-all-start.5) | async-done | bytes 393248 | tf_op jit(solution)/shard_map/all_to_all | solution.py:20
  183.5 2.2 %shard_map.239 = bf16[48,256]{1,0:T(8,128)(2,1)} custom-call(bf16[1536,128]{1,0:T(8,128)(2,1)} %bitcast.36, s32[1,1536]{1,0:T(1,128)} %and_select_fusion.within, s32[48,8]{1,0:T(8,128)} %add_add_fusion.slots, f32[48,4]{1,0:T(8,128)} %copy.56.weight, f32[48,256]{1,0:T(8,128)} %get-tuple-element.42.resid, f32[48,256]{1,0:T(8,128)} %get-tuple-element.43.shared, ...), custom_call_target="tpu_custom_call" | custom-call | flops 75497472 | bytes 550144 | tf_op jit(solution)/shard_map/pallas_call | solution.py:52
  (121 shorter events, 39.8 us)
Async XLA Ops:
  3.6 26.0 %all-to-all-start = ((bf16[8,64,512]{2,1,0:T(8,128)(2,1)}), bf16[8,64,512]{2,1,0:T(8,128)(2,1)S(1)}, u32[]{:S(2)}, u32[]{:S(2)}) async-start(bf16[8,64,512]{2,1,0:T(8,128)(2,1)} %get-tuple-element.29), calls=%async_computation | async-start | bytes 1048576 | tf_op jit(solution)/shard_map/all_to_all | solution.py:20
  12.1 8.2 %collective-permute-start = (bf16[48,512]{1,0:T(8,128)(2,1)}, bf16[48,512]{1,0:T(8,128)(2,1)S(1)}, u32[]{:S(2)}, u32[]{:S(2)}) collective-permute-start(bf16[48,512]{1,0:T(8,128)(2,1)} %get-tuple-element.26), channel_id=1, source_target_pairs={{0,8},{8,16},{16,24},{24,0},{1,9},{9,17},{17,25},{25,1},{2,10},{10... | collective-permute-start | bytes 147464 | tf_op jit(solution)/shard_map/ppermute | solution.py:29
  13.6 6.7 %collective-permute-start.1 = (bf16[48,512]{1,0:T(8,128)(2,1)}, bf16[48,512]{1,0:T(8,128)(2,1)S(1)}, u32[]{:S(2)}, u32[]{:S(2)}) collective-permute-start(bf16[48,512]{1,0:T(8,128)(2,1)} %get-tuple-element.27), channel_id=1, source_target_pairs={{0,16},{8,24},{16,0},{24,8},{1,17},{9,25},{17,1},{25,9},{2,18},{10... | collective-permute-start | bytes 147464 | tf_op jit(solution)/shard_map/ppermute | solution.py:29
  16.3 4.3 %collective-permute-start.2 = (bf16[48,512]{1,0:T(8,128)(2,1)}, bf16[48,512]{1,0:T(8,128)(2,1)S(1)}, u32[]{:S(2)}, u32[]{:S(2)}) collective-permute-start(bf16[48,512]{1,0:T(8,128)(2,1)} %get-tuple-element.28), channel_id=1, source_target_pairs={{0,24},{8,0},{16,8},{24,16},{1,25},{9,1},{17,9},{25,17},{2,26},{10... | collective-permute-start | bytes 147464 | tf_op jit(solution)/shard_map/ppermute | solution.py:29
  31.3 5.4 %collective-permute-start.3 = (bf16[48,512]{1,0:T(8,128)(2,1)S(1)}, bf16[48,512]{1,0:T(8,128)(2,1)S(1)}, u32[]{:S(2)}, u32[]{:S(2)}) collective-permute-start(bf16[48,512]{1,0:T(8,128)(2,1)S(1)} %get-tuple-element.50), channel_id=1, source_target_pairs={{0,24},{8,0},{16,8},{24,16},{1,25},{9,1},{17,9},{25,17},{2,26},{10... | collective-permute-start | bytes 147464 | tf_op jit(solution)/shard_map/ppermute | solution.py:29
  34.1 5.6 %collective-permute-start.4 = (bf16[48,512]{1,0:T(8,128)(2,1)S(1)}, bf16[48,512]{1,0:T(8,128)(2,1)S(1)}, u32[]{:S(2)}, u32[]{:S(2)}) collective-permute-start(bf16[48,512]{1,0:T(8,128)(2,1)S(1)} %get-tuple-element.49), channel_id=1, source_target_pairs={{0,16},{8,24},{16,0},{24,8},{1,17},{9,25},{17,1},{25,9},{2,18},{10... | collective-permute-start | bytes 147464 | tf_op jit(solution)/shard_map/ppermute | solution.py:29
  34.9 5.3 %collective-permute-start.5 = (bf16[48,512]{1,0:T(8,128)(2,1)S(1)}, bf16[48,512]{1,0:T(8,128)(2,1)S(1)}, u32[]{:S(2)}, u32[]{:S(2)}) collective-permute-start(bf16[48,512]{1,0:T(8,128)(2,1)S(1)} %get-tuple-element.48), channel_id=1, source_target_pairs={{0,8},{8,16},{16,24},{24,0},{1,9},{9,17},{17,25},{25,1},{2,10},{10... | collective-permute-start | bytes 147464 | tf_op jit(solution)/shard_map/ppermute | solution.py:29
  45.2 1.5 collective-permute-start.6
  46.7 41.5 %copy-start.3 = (bf16[2,2048,128]{2,1,0:T(8,128)(2,1)S(1)}, bf16[2,2048,128]{2,1,0:T(8,128)(2,1)}, u32[]{:S(2)}) copy-start(bf16[2,2048,128]{2,1,0:T(8,128)(2,1)} %up.1) | copy-start | bytes 3145732
  48.4 9.4 %all-to-all-start.1 = ((bf16[4,48,256]{2,1,0:T(8,128)(2,1)}), bf16[4,48,256]{2,1,0:T(8,128)(2,1)}, u32[]{:S(2)}, u32[]{:S(2)}) async-start(bf16[4,48,256]{2,1,0:T(8,128)(2,1)} %add_convert_fusion), calls=%async_computation.1 | async-start | bytes 196608 | tf_op jit(solution)/shard_map/all_to_all | solution.py:20
  60.4 20.3 %all-to-all-start.2 = ((bf16[64,24,128]{2,1,0:T(8,128)(2,1)}), bf16[64,24,128]{2,1,0:T(8,128)(2,1)}, u32[]{:S(2)}, u32[]{:S(2)}) async-start(bf16[64,24,128]{2,1,0:T(8,128)(2,1)} %bitcast.38), calls=%async_computation.2 | async-start | bytes 786432 | tf_op jit(solution)/shard_map/all_to_all | solution.py:20
  65.9 25.3 %collective-permute-start.11 = (bf16[3,256,256]{2,1,0:T(8,128)(2,1)S(1)}, bf16[3,256,256]{2,1,0:T(8,128)(2,1)}, u32[]{:S(2)}, u32[]{:S(2)}) collective-permute-start(bf16[3,256,256]{2,1,0:T(8,128)(2,1)S(1)} %copy-done.6), channel_id=1, source_target_pairs={{0,8},{8,16},{16,24},{24,0},{1,9},{9,17},{17,25},{25,1},{2,10},{10... | collective-permute-start | bytes 1179656 | tf_op jit(solution)/shard_map/ppermute | solution.py:29
  68.2 41.4 %collective-permute-start.10 = (bf16[128,2048]{1,0:T(8,128)(2,1)}, bf16[128,2048]{1,0:T(8,128)(2,1)}, u32[]{:S(2)}, u32[]{:S(2)}) collective-permute-start(bf16[128,2048]{1,0:T(8,128)(2,1)} %dynamic-slice_bitcast_fusion), channel_id=1, source_target_pairs={{0,1},{1,0},{2,3},{3,2},{4,5},{5,4},{6,7},{7,6},{8,9},{9,8},{10,11... | collective-permute-start | bytes 1572872 | tf_op jit(solution)/shard_map/ppermute | solution.py:24
  69.1 41.1 %collective-permute-start.8 = (bf16[2048,128]{1,0:T(8,128)(2,1)}, bf16[2048,128]{1,0:T(8,128)(2,1)}, u32[]{:S(2)}, u32[]{:S(2)}) collective-permute-start(bf16[2048,128]{1,0:T(8,128)(2,1)} %dynamic-slice_bitcast_fusion.2), channel_id=1, source_target_pairs={{0,1},{1,0},{2,3},{3,2},{4,5},{5,4},{6,7},{7,6},{8,9},{9,8},{10,11... | collective-permute-start | bytes 1572872 | tf_op jit(solution)/shard_map/ppermute | solution.py:24
  69.6 1.9 %collective-permute-start.7 = (bf16[48,256]{1,0:T(8,128)(2,1)}, bf16[48,256]{1,0:T(8,128)(2,1)S(1)}, u32[]{:S(2)}, u32[]{:S(2)}) collective-permute-start(bf16[48,256]{1,0:T(8,128)(2,1)} %get-tuple-element.33.own), channel_id=1, source_target_pairs={{0,1},{1,0},{2,3},{3,2},{4,5},{5,4},{6,7},{7,6},{8,9},{9,8},{10,11... | collective-permute-start | bytes 73736 | tf_op jit(solution)/shard_map/ppermute | solution.py:24
  83.2 27.1 %all-to-all-start.3 = ((bf16[4,240,512]{2,1,0:T(8,128)(2,1)}), bf16[4,240,512]{2,1,0:T(8,128)(2,1)S(1)}, u32[]{:S(2)}, u32[]{:S(2)}) async-start(bf16[4,240,512]{2,1,0:T(8,128)(2,1)} %get-tuple-element.34), calls=%async_computation.3 | async-start | bytes 1966080 | tf_op jit(solution)/shard_map/all_to_all | solution.py:20
  88.2 22.1 %collective-permute-start.9 = (bf16[2048,128]{1,0:T(8,128)(2,1)S(1)}, bf16[2048,128]{1,0:T(8,128)(2,1)S(1)}, u32[]{:S(2)}, u32[]{:S(2)}) collective-permute-start(bf16[2048,128]{1,0:T(8,128)(2,1)S(1)} %dynamic-slice_bitcast_fusion.1), channel_id=1, source_target_pairs={{0,1},{1,0},{2,3},{3,2},{4,5},{5,4},{6,7},{7,6},{8,9},{9,8},{10,11... | collective-permute-start | bytes 1572872 | tf_op jit(solution)/shard_map/ppermute | solution.py:24
  88.3 13.0 %collective-permute-start.12 = (bf16[3,256,256]{2,1,0:T(8,128)(2,1)S(1)}, bf16[3,256,256]{2,1,0:T(8,128)(2,1)S(1)}, u32[]{:S(2)}, u32[]{:S(2)}) collective-permute-start(bf16[3,256,256]{2,1,0:T(8,128)(2,1)S(1)} %copy-done.6), channel_id=1, source_target_pairs={{0,16},{8,24},{16,0},{24,8},{1,17},{9,25},{17,1},{25,9},{2,18},{10... | collective-permute-start | bytes 1179656 | tf_op jit(solution)/shard_map/ppermute | solution.py:29
  91.2 18.4 %collective-permute-start.13 = (bf16[3,256,256]{2,1,0:T(8,128)(2,1)S(1)}, bf16[3,256,256]{2,1,0:T(8,128)(2,1)S(1)}, u32[]{:S(2)}, u32[]{:S(2)}) collective-permute-start(bf16[3,256,256]{2,1,0:T(8,128)(2,1)S(1)} %copy-done.6), channel_id=1, source_target_pairs={{0,24},{8,0},{16,8},{24,16},{1,25},{9,1},{17,9},{25,17},{2,26},{10... | collective-permute-start | bytes 1179656 | tf_op jit(solution)/shard_map/ppermute | solution.py:29
  101.3 21.2 %collective-permute-start.14 = (bf16[3,256,256]{2,1,0:T(8,128)(2,1)S(1)}, bf16[3,256,256]{2,1,0:T(8,128)(2,1)S(1)}, u32[]{:S(2)}, u32[]{:S(2)}) collective-permute-start(bf16[3,256,256]{2,1,0:T(8,128)(2,1)S(1)} %copy-done.6), channel_id=1, source_target_pairs={{0,1},{1,0},{2,3},{3,2},{4,5},{5,4},{6,7},{7,6},{8,9},{9,8},{10,11... | collective-permute-start | bytes 1179656 | tf_op jit(solution)/shard_map/ppermute | solution.py:24
  109.7 12.9 %collective-permute-start.15 = (bf16[3,256,256]{2,1,0:T(8,128)(2,1)}, bf16[3,256,256]{2,1,0:T(8,128)(2,1)S(1)}, u32[]{:S(2)}, u32[]{:S(2)}) collective-permute-start(bf16[3,256,256]{2,1,0:T(8,128)(2,1)} %collective-permute-done.11.refs_1_.refs_5_), channel_id=1, source_target_pairs={{0,1},{1,0},{2,3},{3,2},{4,5},{5,4},{6,7},{7,6},{8,9},{9,8},{10,11... | collective-permute-start | bytes 1179656 | tf_op jit(solution)/shard_map/ppermute | solution.py:24
  109.7 12.9 %collective-permute-start.16 = (bf16[3,256,256]{2,1,0:T(8,128)(2,1)S(1)}, bf16[3,256,256]{2,1,0:T(8,128)(2,1)}, u32[]{:S(2)}, u32[]{:S(2)}) collective-permute-start(bf16[3,256,256]{2,1,0:T(8,128)(2,1)S(1)} %collective-permute-done.12.refs_2_.refs_6_), channel_id=1, source_target_pairs={{0,1},{1,0},{2,3},{3,2},{4,5},{5,4},{6,7},{7,6},{8,9},{9,8},{10,11... | collective-permute-start | bytes 1179656 | tf_op jit(solution)/shard_map/ppermute | solution.py:24
  110.2 12.4 %collective-permute-start.17 = (bf16[3,256,256]{2,1,0:T(8,128)(2,1)S(1)}, bf16[3,256,256]{2,1,0:T(8,128)(2,1)}, u32[]{:S(2)}, u32[]{:S(2)}) collective-permute-start(bf16[3,256,256]{2,1,0:T(8,128)(2,1)S(1)} %collective-permute-done.13.refs_3_.refs_7_), channel_id=1, source_target_pairs={{0,1},{1,0},{2,3},{3,2},{4,5},{5,4},{6,7},{7,6},{8,9},{9,8},{10,11... | collective-permute-start | bytes 1179656 | tf_op jit(solution)/shard_map/ppermute | solution.py:24
  117.0 42.4 %all-to-all-start.4 = ((bf16[4,240,512]{2,1,0:T(8,128)(2,1)}), bf16[4,240,512]{2,1,0:T(8,128)(2,1)}, u32[]{:S(2)}, u32[]{:S(2)}) async-start(bf16[4,240,512]{2,1,0:T(8,128)(2,1)} %shard_map.234), calls=%async_computation.4 | async-start | bytes 1966080 | tf_op jit(solution)/shard_map/all_to_all | solution.py:20
  126.8 12.0 %collective-permute-start.18 = (bf16[48,2176]{1,0:T(8,128)(2,1)}, bf16[48,2176]{1,0:T(8,128)(2,1)S(1)}, u32[]{:S(2)}, u32[]{:S(2)}) collective-permute-start(bf16[48,2176]{1,0:T(8,128)(2,1)} %get-tuple-element.38), channel_id=1, source_target_pairs={{0,2},{2,4},{4,6},{6,0},{1,3},{3,5},{5,7},{7,1},{8,10},{10,12},{12... | collective-permute-start | bytes 626696 | tf_op jit(solution)/shard_map/ppermute | solution.py:29
  128.2 12.6 %collective-permute-start.19 = (bf16[48,2176]{1,0:T(8,128)(2,1)}, bf16[48,2176]{1,0:T(8,128)(2,1)S(1)}, u32[]{:S(2)}, u32[]{:S(2)}) collective-permute-start(bf16[48,2176]{1,0:T(8,128)(2,1)} %get-tuple-element.39), channel_id=1, source_target_pairs={{0,4},{2,6},{4,0},{6,2},{1,5},{3,7},{5,1},{7,3},{8,12},{10,14},{12... | collective-permute-start | bytes 626696 | tf_op jit(solution)/shard_map/ppermute | solution.py:29
  128.9 15.5 %collective-permute-start.20 = (bf16[48,2176]{1,0:T(8,128)(2,1)}, bf16[48,2176]{1,0:T(8,128)(2,1)S(1)}, u32[]{:S(2)}, u32[]{:S(2)}) collective-permute-start(bf16[48,2176]{1,0:T(8,128)(2,1)} %get-tuple-element.40), channel_id=1, source_target_pairs={{0,6},{2,0},{4,2},{6,4},{1,7},{3,1},{5,3},{7,5},{8,14},{10,8},{12,... | collective-permute-start | bytes 626696 | tf_op jit(solution)/shard_map/ppermute | solution.py:29
  147.2 5.4 %collective-permute-start.21 = (bf16[48,1024]{1,0:T(8,128)(2,1)}, bf16[48,1024]{1,0:T(8,128)(2,1)S(1)}, u32[]{:S(2)}, u32[]{:S(2)}) collective-permute-start(bf16[48,1024]{1,0:T(8,128)(2,1)} %shard_map.236.refs_0_), channel_id=1, source_target_pairs={{0,2},{2,4},{4,6},{6,0},{1,3},{3,5},{5,7},{7,1},{8,10},{10,12},{12... | collective-permute-start | bytes 294920 | tf_op jit(solution)/shard_map/ppermute | solution.py:29
  147.8 6.9 %collective-permute-start.22 = (bf16[48,1024]{1,0:T(8,128)(2,1)}, bf16[48,1024]{1,0:T(8,128)(2,1)S(1)}, u32[]{:S(2)}, u32[]{:S(2)}) collective-permute-start(bf16[48,1024]{1,0:T(8,128)(2,1)} %shard_map.236.refs_0_), channel_id=1, source_target_pairs={{0,4},{2,6},{4,0},{6,2},{1,5},{3,7},{5,1},{7,3},{8,12},{10,14},{12... | collective-permute-start | bytes 294920 | tf_op jit(solution)/shard_map/ppermute | solution.py:29
  150.8 4.9 %collective-permute-start.23 = (bf16[48,1024]{1,0:T(8,128)(2,1)}, bf16[48,1024]{1,0:T(8,128)(2,1)S(1)}, u32[]{:S(2)}, u32[]{:S(2)}) collective-permute-start(bf16[48,1024]{1,0:T(8,128)(2,1)} %shard_map.236.refs_0_), channel_id=1, source_target_pairs={{0,6},{2,0},{4,2},{6,4},{1,7},{3,1},{5,3},{7,5},{8,14},{10,8},{12,... | collective-permute-start | bytes 294920 | tf_op jit(solution)/shard_map/ppermute | solution.py:29
  162.0 20.8 %all-to-all-start.5 = ((bf16[64,24,128]{2,1,0:T(8,128)(2,1)}), bf16[64,24,128]{2,1,0:T(8,128)(2,1)S(1)}, u32[]{:S(2)}, u32[]{:S(2)}) async-start(bf16[64,24,128]{2,1,0:T(8,128)(2,1)} %bitcast.39), calls=%async_computation.5 | async-start | bytes 786432 | tf_op jit(solution)/shard_map/all_to_all | solution.py:20
  169.8 4.2 %collective-permute-start.24 = (bf16[48,256]{1,0:T(8,128)(2,1)}, bf16[48,256]{1,0:T(8,128)(2,1)}, u32[]{:S(2)}, u32[]{:S(2)}) collective-permute-start(bf16[48,256]{1,0:T(8,128)(2,1)} %get-tuple-element.44), channel_id=1, source_target_pairs={{0,1},{1,0},{2,3},{3,2},{4,5},{5,4},{6,7},{7,6},{8,9},{9,8},{10,11... | collective-permute-start | bytes 73736 | tf_op jit(solution)/shard_map/ppermute | solution.py:24
  (23 other events, 214.4 us)

commit v7 on v5

--- a/solution.py
+++ b/solution.py
@@ -41,20 +41,60 @@
     return x * jax.nn.sigmoid(x)
 
 
-def call(body, outs, flops, *args, mib=12, scratch=()):
+def call(body, outs, flops, kinds, *args, mib=53, scratch=()):
+    kinds, out_kinds = kinds.split()
     moved = sum(a.size * a.dtype.itemsize for a in args) + sum(
         o.size * o.dtype.itemsize for o in outs
     )
-    specs = [
-        pl.BlockSpec(memory_space=pltpu.SMEM if a.dtype == jnp.int32 and a.ndim == 1 else pltpu.VMEM)
-        for a in args
-    ]
+    space = {"s": pltpu.SMEM, "v": pltpu.VMEM, "h": pltpu.HBM, "l": pltpu.HBM}
+    fetched = [i for i, k in enumerate(kinds) if k in "hl"]
+    stored = [i for i, k in enumerate(out_kinds) if k == "h"]
+    room = [pltpu.VMEM(args[i].shape, args[i].dtype) for i in fetched]
+    out_room = [pltpu.VMEM(outs[i].shape, outs[i].dtype) for i in stored]
+
+    def whole(*refs):
+        ins, rest = list(refs[: len(args)]), refs[len(args) :]
+        results, rest = list(rest[: len(outs)]), rest[len(outs) :]
+        in_room, rest = rest[: len(room)], rest[len(room) :]
+        result_room, rest = rest[: len(out_room)], rest[len(out_room) :]
+        in_sem, out_sem, extra = rest[0], rest[1], rest[2:]
+        late = []
+        now = []
+        for n, i in enumerate(fetched):
+            copy = pltpu.make_async_copy(ins[i], in_room[n], in_sem.at[n])
+            copy.start()
+            (late if kinds[i] == "l" else now).append(copy)
+            ins[i] = in_room[n]
+        targets = list(results)
+        for n, i in enumerate(stored):
+            results[i] = result_room[n]
+        for copy in now:
+            copy.wait()
+        if late:
+            body([copy.wait for copy in late], *ins, *results, *extra)
+        else:
+            body(*ins, *results, *extra)
+        back = [
+            pltpu.make_async_copy(result_room[n], targets[i], out_sem.at[n])
+            for n, i in enumerate(stored)
+        ]
+        for copy in back:
+            copy.start()
+        for copy in back:
+            copy.wait()
+
     return pl.pallas_call(
-        body,
+        whole,
         out_shape=outs,
-        in_specs=specs,
-        out_specs=[pl.BlockSpec(memory_space=pltpu.VMEM) for _ in outs],
-        scratch_shapes=scratch,
+        in_specs=[pl.BlockSpec(memory_space=space[k]) for k in kinds],
+        out_specs=[pl.BlockSpec(memory_space=space[k]) for k in out_kinds],
+        scratch_shapes=[
+            *room,
+            *out_room,
+            pltpu.SemaphoreType.DMA((max(1, len(room)),)),
+            pltpu.SemaphoreType.DMA((max(1, len(out_room)),)),
+            *scratch,
+        ],
         cost_estimate=pl.CostEstimate(flops=flops, bytes_accessed=moved, transcendentals=0),
         compiler_params=pltpu.CompilerParams(vmem_limit_bytes=mib * 2**20),
     )(*args)
@@ -92,7 +132,7 @@
         out[...] = held[lax.rem(x + d, 4)]
 
 
-def recur(at, p0, p1, p2, p3, bound, gain, state, w_out, decay_out, key_out, value_out, keep, give, read):
+def recur(wait, at, p0, p1, p2, p3, bound, gain, state, w_out, decay_out, key_out, value_out, keep, give, read):
     first = at[1] == 0
     seq = p0.shape[0]
     total = (
@@ -108,11 +148,13 @@
     key_out[...] = key
     value_out[...] = values
     turned = jnp.transpose(query * decay)
+    wait[0]()
     for b in range(seq):
         read[b : b + 1, :] = jnp.sum(turned[:, b : b + 1] * state[b], axis=0, keepdims=True)
     readout = read[...] + jnp.sum(query * key, axis=1, keepdims=True) * values
     readout = readout * lax.rsqrt(jnp.mean(readout * readout, axis=1, keepdims=True) + EPS)
     head = (readout * gain[...] * silu(gate)).astype(BF)
+    wait[1]()
     cols = keep.shape[2]
     for y in range(keep.shape[0]):
         cut = slice(2 * y * cols, (2 * y + 1) * cols)
@@ -269,7 +311,7 @@
 
 
 def experts_and_shared(
-    at, whole, gain, gate, gate_other, up, up_other, down, down_other,
+    wait, at, whole, gain, gate, gate_other, up, up_other, down, down_other,
     shared_gate, shared_up, shared_down, parts,
 ):
     c = at[1]
@@ -286,7 +328,9 @@
         (value * scale * gain[:, i * block : (i + 1) * block]).astype(BF)
         for i, value in enumerate(rows)
     ]
-    gate_pre = up_pre = gate_shared = up_shared = None
+    gate_pre = up_pre = gate_shared = None
+    for i in (0, 1, 2, 3, 6, 7):
+        wait[i]()
 
     def more(total, term):
         return term if total is None else total + term
@@ -299,6 +343,8 @@
         gate_pre = more(gate_pre, dot(rows[i][:count], gates))
         up_pre = more(up_pre, dot(rows[i][:count], ups))
         gate_shared = more(gate_shared, dot(rows[i][count:], shared))
+    for i in (4, 5, 8):
+        wait[i]()
     half = gate.shape[2]
     hidden = (silu(gate_pre) * up_pre).astype(BF)
     shared_hidden = (silu(gate_shared[:, :half]) * gate_shared[:, half:]).astype(BF)
@@ -397,6 +443,7 @@
         [shaped(nz, rows_w, 4 * chan), shaped(3, *dense_gate.shape)]
         + [shaped(seq, nz * rows_w)] * nx,
         10**6,
+        "shhhhhhhhh hhhhhh",
         at,
         tokens,
         norm_gain.reshape(1, width),
@@ -407,6 +454,7 @@
         dense_gate,
         dense_up,
         dense_down,
+        mib=58,
         scratch=[pltpu.VMEM((nx, seq, nz * rows_w), BF)],
     )
     weights = swap(spread_w, "z").reshape(nz * rows_w, 4 * chan)
@@ -425,6 +473,7 @@
         recur,
         [shaped(seq, chan, dtype=F32)] * 3 + [shaped(ny, seq, cols)] * 2,
         4 * state.size,
+        "shvvvhhll hhhvh",
         at,
         *pieces,
         lower_bound.reshape(1, chan),
@@ -449,6 +498,7 @@
             shaped(experts * 2 * slots, half),
         ],
         4 * experts * 2 * slots * seq * half,
+        "svhh hhh",
         at,
         heads,
         tokens,
@@ -472,6 +522,7 @@
         unpack_rows,
         [shaped(ny, count + seq, nc * cols), shaped(nc, count, cols)],
         4 * 2 * group * group * half,
+        "shvhv hh",
         at,
         line_of.reshape(1, group),
         arrived.reshape(-1, half),
@@ -486,6 +537,7 @@
         dense_first_half,
         [shaped(quarter, 2 * hidden_width + 128)] * ny,
         2 * count * nc * cols * 2 * hidden_width,
+        "shhhhhhhhhh hhhh",
         at,
         dense_rows,
         ffn_gain.reshape(ny * nc, cols),
@@ -493,12 +545,15 @@
         *dense_other,
     )
     pre = [pre[0]] + [shift(pre[d], "y", d) for d in range(1, ny)]
-    (hidden,) = call(dense_activation, [shaped(quarter, hidden_width)], 10**6, *pre)
+    (hidden,) = call(
+        dense_activation, [shaped(quarter, hidden_width)], 10**6, "hvvv h", *pre
+    )
     hidden = [hidden] + [shift(hidden, "y", d) for d in range(1, ny)]
     (dense_part,) = call(
         dense_second_half,
         [shaped(nc, count, cols)],
         2 * count * nc * cols * hidden_width,
+        "shvvvhhhhhhhh h",
         at,
         *hidden,
         *dense_own,
@@ -509,6 +564,7 @@
         experts_and_shared,
         [shaped(ny, count + seq, nc * cols)],
         2 * 3 * (count * 2 + seq) * width * expert_gate.shape[2],
+        "svhlllllllll h",
         at,
         whole,
         ffn_gain.reshape(1, width),
@@ -521,7 +577,6 @@
         shared_gate,
         shared_up,
         shared_down,
-        mib=24,
     )
     parts = swap(parts, "y")
     back, shared_own, shared_send = call(
@@ -532,6 +587,7 @@
             shaped(seq, cols),
         ],
         4 * 2 * group * group * half,
+        "shvh hhh",
         at,
         line_of.reshape(group, 1),
         parts,
@@ -543,6 +599,7 @@
         finish,
         [shaped(seq, cols)],
         8 * experts * 2 * slots * seq * half,
+        "vhhhhhvh h",
         results.reshape(experts * 2 * slots, half),
         within,
         slot_cols,

time: 220 us -> 184 us (0.84)
  the two profiles are of different devices: /device:TPU:1 before, /device:TPU:8 now
where the time goes in v7:
time: 184 us; the launch traced here: 181 us
  waiting for transfers between devices  72.6 us (39%)
  starting transfers between devices  59.7 us (32%)
  Pallas kernels  31.4 us (17%)
  other arithmetic  8.71 us (5%)
  local copies, waits for them, and re-layouts  6.34 us (3%)
    ppermute x15, waiting for transfers between devices, shift(): return lax.ppermute(x, axis, [(i, (i + by) % size) for i in range(size)])  38.3 us
    all_to_all x6, starting transfers between devices, swap(): return lax.all_to_all(x, axis, split_axis=0, concat_axis=0, tiled=True)  33.6 us
    pallas_call x10, Pallas kernels, call(): pl.pallas_call(whole, out_shape=outs, in_specs=[pl.BlockSpec(memory_space...  31.4 us
    all_to_all x6, waiting for transfers between devices, swap(): return lax.all_to_all(x, axis, split_axis=0, concat_axis=0, tiled=True)  31.3 us
    ppermute x15, starting transfers between devices, shift(): return lax.ppermute(x, axis, [(i, (i + by) % size) for i in range(size)])  24.7 us
    add x1, other arithmetic, step(): decay.reshape(shape)[..., None] * state  5.07 us
  transfers between devices with their start and end apart: 31, of which 18 were waited for; matrix products, arithmetic and copies ran while one was open for 6% of the time, Pallas kernels for 9%

profile of v7, /device:TPU:8, one launch (start us, length us, event | category | flops | bytes accessed | tf_op | source)
XLA Modules:
  0.0 181.1 jit_solution(3202432751174486022)
XLA Ops:
  1.3 3.4 %shard_map.230 = (bf16[8,64,512]{2,1,0:T(8,128)(2,1)}, bf16[3,256,256]{2,1,0:T(8,128)(2,1)}, bf16[48,512]{1,0:T(8,128)(2,1)}, bf16[48,512]{1,0:T(8,128)(2,1)}, b...) custom-call(s32[3]{0:T(128)} %pad_add_fusion.refs_0_, bf16[48,2048]{1,0:T(8,128)(2,1)} %refs_2_.1, f32[1,2048]{1,0:T(1,128)} %bitcast.43, ...), custom_call_target="tpu_custom_call" | custom-call | flops 1000000 | bytes 1777676 | tf_op jit(solution)/shard_map/pallas_call | solution.py:86
  4.6 8.5 %all-to-all-start = ((bf16[8,64,512]{2,1,0:T(8,128)(2,1)}), bf16[8,64,512]{2,1,0:T(8,128)(2,1)S(1)}, u32[]{:S(2)}, u32[]{:S(2)}) async-start(bf16[8,64,512]{2,1,0:T(8,128)(2,1)} %get-tuple-element.29), calls=%async_computation | async-start | bytes 1048576 | tf_op jit(solution)/shard_map/all_to_all | solution.py:20
  14.6 2.7 %collective-permute-start.1 = (bf16[48,512]{1,0:T(8,128)(2,1)}, bf16[48,512]{1,0:T(8,128)(2,1)S(1)}, u32[]{:S(2)}, u32[]{:S(2)}) collective-permute-start(bf16[48,512]{1,0:T(8,128)(2,1)} %get-tuple-element.27), channel_id=1, source_target_pairs={{0,16},{8,24},{16,0},{24,8},{1,17},{9,25},{17,1},{25,9},{2,18},{10... | collective-permute-start | bytes 147464 | tf_op jit(solution)/shard_map/ppermute | solution.py:29
  21.6 9.0 %all-to-all-done = bf16[8,64,512]{2,1,0:T(8,128)(2,1)S(1)} async-done(((bf16[8,64,512]{2,1,0:T(8,128)(2,1)}), bf16[8,64,512]{2,1,0:T(8,128)(2,1)S(1)}, u32[]{:S(2)}, u32[]{:S(2)}) %all-to-all-start) | async-done | bytes 524320 | tf_op jit(solution)/shard_map/all_to_all | solution.py:20
  31.8 2.8 %collective-permute-start.3 = (bf16[48,512]{1,0:T(8,128)(2,1)S(1)}, bf16[48,512]{1,0:T(8,128)(2,1)S(1)}, u32[]{:S(2)}, u32[]{:S(2)}) collective-permute-start(bf16[48,512]{1,0:T(8,128)(2,1)S(1)} %get-tuple-element.50), channel_id=1, source_target_pairs={{0,24},{8,0},{16,8},{24,16},{1,25},{9,1},{17,9},{25,17},{2,26},{10... | collective-permute-start | bytes 147464 | tf_op jit(solution)/shard_map/ppermute | solution.py:29
  36.7 3.5 %collective-permute-done.4.refs_3_ = bf16[48,512]{1,0:T(8,128)(2,1)S(1)} collective-permute-done((bf16[48,512]{1,0:T(8,128)(2,1)S(1)}, bf16[48,512]{1,0:T(8,128)(2,1)S(1)}, u32[]{:S(2)}, u32[]{:S(2)}) %collective-permute-start.4) | collective-permute-done | bytes 49184 | tf_op jit(solution)/shard_map/ppermute | solution.py:29
  40.7 4.1 %shard_map.231 = (f32[48,128]{1,0:T(8,128)S(1)}, f32[48,128]{1,0:T(8,128)S(1)}, f32[48,128]{1,0:T(8,128)S(1)}, bf16[4,48,256]{2,1,0:T(8,128)(2,1)S(1)}, bf16[4,48,256]{2,1,0:T(8,128)(2,1)S(1)}) custom-call(s32[3]{0:T(128)S(1)} %copy-done.2, bf16[48,512]{1,0:T(8,128)(2,1)S(1)} %get-tuple-element.51.refs_1_, ...), custom_call_target="tpu_custom_call" | custom-call | flops 3145728 | bytes 4137996 | tf_op jit(solution)/shard_map/pallas_call | solution.py:86
  46.9 4.9 %all-to-all-start.1 = ((bf16[4,48,256]{2,1,0:T(8,128)(2,1)}), bf16[4,48,256]{2,1,0:T(8,128)(2,1)S(1)}, u32[]{:S(2)}, u32[]{:S(2)}) async-start(bf16[4,48,256]{2,1,0:T(8,128)(2,1)} %add_convert_fusion), calls=%async_computation.1 | async-start | bytes 196608 | tf_op jit(solution)/shard_map/all_to_all | solution.py:20
  52.0 4.2 %all-to-all-done.1.refs_1_ = bf16[4,48,256]{2,1,0:T(8,128)(2,1)S(1)} async-done(((bf16[4,48,256]{2,1,0:T(8,128)(2,1)}), bf16[4,48,256]{2,1,0:T(8,128)(2,1)S(1)}, u32[]{:S(2)}, u32[]{:S(2)}) %all-to-all-start.1) | async-done | bytes 98336 | tf_op jit(solution)/shard_map/all_to_all | solution.py:20
  56.2 2.6 %shard_map.232 = (f32[48,256]{1,0:T(8,128)S(1)}, bf16[48,256]{1,0:T(8,128)(2,1)S(1)}, bf16[1536,128]{1,0:T(8,128)(2,1)}) custom-call(s32[3]{0:T(128)S(1)} %copy-done.2, bf16[4,48,256]{2,1,0:T(8,128)(2,1)S(1)} %all-to-all-done.1.refs_1_, bf16[48,2048]{1,0:T(8,128)(2,1)S(1)} %copy-done, s32[8,48]{1,0:T(8,128)S(1)} %copy.55.refs_3_), custom_call_target="tpu_custom_call" | custom-call | flops 37748736 | bytes 763404 | tf_op jit(solution)/shard_map/pallas_call | solution.py:86
  58.8 4.6 %all-to-all-start.2 = ((bf16[64,24,128]{2,1,0:T(8,128)(2,1)}), bf16[64,24,128]{2,1,0:T(8,128)(2,1)S(1)}, u32[]{:S(2)}, u32[]{:S(2)}) async-start(bf16[64,24,128]{2,1,0:T(8,128)(2,1)} %bitcast.10), calls=%async_computation.2 | async-start | bytes 786432 | tf_op jit(solution)/shard_map/all_to_all | solution.py:20
  65.0 1.9 %dynamic-slice_bitcast_fusion = bf16[128,2048]{1,0:T(8,128)(2,1)} fusion(bf16[2,128,2048]{2,1,0:T(8,128)(2,1)} %refs_7_.3, s32[]{:T(128)S(6)} %select_n.224), kind=kLoop, calls=%fused_computation.2 | loop fusion | bytes 1048580 | tf_op jit(solution)/shard_map/jit(dynamic_index_in_dim)/squeeze | solution.py:33
  70.1 8.4 %all-to-all-done.2 = bf16[64,24,128]{2,1,0:T(8,128)(2,1)S(1)} async-done(((bf16[64,24,128]{2,1,0:T(8,128)(2,1)}), bf16[64,24,128]{2,1,0:T(8,128)(2,1)S(1)}, u32[]{:S(2)}, u32[]{:S(2)}) %all-to-all-start.2) | async-done | bytes 393248 | tf_op jit(solution)/shard_map/all_to_all | solution.py:20
  78.5 2.0 %shard_map.233 = (bf16[4,240,512]{2,1,0:T(8,128)(2,1)}, bf16[2,192,256]{2,1,0:T(8,128)(2,1)S(1)}) custom-call(s32[3]{0:T(128)S(1)} %copy-done.2, s32[1,384]{1,0:T(1,128)S(1)} %fusion.53.refs_1_, bf16[1536,128]{1,0:T(8,128)(2,1)S(1)} %bitcast.36, bf16[48,256]{1,0:T(8,128)(2,1)S(1)} %get-tuple-element.33.refs_3_, ...), custom_call_target="tpu_custom_call" | custom-call | flops 150994944 | bytes 1623564 | tf_op jit(solution)/shard_map/pallas_call | solution.py:86
  80.5 5.0 %all-to-all-start.3 = ((bf16[4,240,512]{2,1,0:T(8,128)(2,1)}), bf16[4,240,512]{2,1,0:T(8,128)(2,1)S(1)}, u32[]{:S(2)}, u32[]{:S(2)}) async-start(bf16[4,240,512]{2,1,0:T(8,128)(2,1)} %get-tuple-element.34), calls=%async_computation.3 | async-start | bytes 1966080 | tf_op jit(solution)/shard_map/all_to_all | solution.py:20
  85.6 2.9 %collective-permute-start.12 = (bf16[3,256,256]{2,1,0:T(8,128)(2,1)S(1)}, bf16[3,256,256]{2,1,0:T(8,128)(2,1)}, u32[]{:S(2)}, u32[]{:S(2)}) collective-permute-start(bf16[3,256,256]{2,1,0:T(8,128)(2,1)S(1)} %copy-done.10), channel_id=1, source_target_pairs={{0,16},{8,24},{16,0},{24,8},{1,17},{9,25},{17,1},{25,9},{2,18},{10... | collective-permute-start | bytes 1179656 | tf_op jit(solution)/shard_map/ppermute | solution.py:29
  89.7 9.0 %collective-permute-done.12.refs_5_.refs_7_ = bf16[3,256,256]{2,1,0:T(8,128)(2,1)} collective-permute-done((bf16[3,256,256]{2,1,0:T(8,128)(2,1)S(1)}, bf16[3,256,256]{2,1,0:T(8,128)(2,1)}, u32[]{:S(2)}, u32[]{:S(2)}) %collective-permute-start.12) | collective-permute-done | bytes 393248 | tf_op jit(solution)/shard_map/ppermute | solution.py:29
  98.7 8.3 %collective-permute-done.13.refs_6_.refs_8_ = bf16[3,256,256]{2,1,0:T(8,128)(2,1)} collective-permute-done((bf16[3,256,256]{2,1,0:T(8,128)(2,1)S(1)}, bf16[3,256,256]{2,1,0:T(8,128)(2,1)}, u32[]{:S(2)}, u32[]{:S(2)}) %collective-permute-start.13) | collective-permute-done | bytes 393248 | tf_op jit(solution)/shard_map/ppermute | solution.py:29
  108.8 6.2 %shard_map.234 = bf16[4,240,512]{2,1,0:T(8,128)(2,1)} custom-call(s32[3]{0:T(128)S(1)} %copy-done.2, bf16[4,240,512]{2,1,0:T(8,128)(2,1)} %copy-done.7, f32[1,2048]{1,0:T(1,128)S(1)} %bitcast.37, bf16[2,2048,128]{2,1,0:T(8,128)(2,1)} %refs_3_.4, bf16[2048,128]{1,0:T(8,128)(2,1)S(1)} %collective-permute-done.8.refs_4_, bf16[2,2048,128]{2,1,0:T(8,128)(2,1)} %refs_5_.3, ...), custom_call_target="tpu_custom_call" | custom-call | flops 679477248 | bytes 8265740 | tf_op jit(solution)/shard_map/pallas_call | solution.py:86
  115.0 4.8 %all-to-all-start.4 = ((bf16[4,240,512]{2,1,0:T(8,128)(2,1)}), bf16[4,240,512]{2,1,0:T(8,128)(2,1)S(1)}, u32[]{:S(2)}, u32[]{:S(2)}) async-start(bf16[4,240,512]{2,1,0:T(8,128)(2,1)} %shard_map.234), calls=%async_computation.4 | async-start | bytes 1966080 | tf_op jit(solution)/shard_map/all_to_all | solution.py:20
  119.9 4.8 %shard_map.235 = (bf16[48,2176]{1,0:T(8,128)(2,1)S(1)}, bf16[48,2176]{1,0:T(8,128)(2,1)S(1)}, bf16[48,2176]{1,0:T(8,128)(2,1)S(1)}, bf16[48,2176]{1,0:T(8,128)(2,1)}) custom-call(s32[3]{0:T(128)S(1)} %copy-done.2, bf16[2,192,256]{2,1,0:T(8,128)(2,1)S(1)} %get-tuple-element.35.refs_1_, f32[8,256]{1,0:T(8,128)S(1)} %reshape.582.refs_2_, ...), custom_call_target="tpu_custom_call" | custom-call | flops 402653184 | bytes 4186124 | tf_op jit(solution)/shard_map/pallas_call | solution.py:86
  127.0 2.5 %collective-permute-start.20 = (bf16[48,2176]{1,0:T(8,128)(2,1)}, bf16[48,2176]{1,0:T(8,128)(2,1)S(1)}, u32[]{:S(2)}, u32[]{:S(2)}) collective-permute-start(bf16[48,2176]{1,0:T(8,128)(2,1)} %get-tuple-element.40), channel_id=1, source_target_pairs={{0,6},{2,0},{4,2},{6,4},{1,7},{3,1},{5,3},{7,5},{8,14},{10,8},{12,... | collective-permute-start | bytes 626696 | tf_op jit(solution)/shard_map/ppermute | solution.py:29
  129.6 7.1 %collective-permute-done.18.refs_1_ = bf16[48,2176]{1,0:T(8,128)(2,1)S(1)} collective-permute-done((bf16[48,2176]{1,0:T(8,128)(2,1)S(1)}, bf16[48,2176]{1,0:T(8,128)(2,1)S(1)}, u32[]{:S(2)}, u32[]{:S(2)}) %collective-permute-start.18) | collective-permute-done | bytes 208928 | tf_op jit(solution)/shard_map/ppermute | solution.py:29
  136.7 2.1 %collective-permute-done.19.refs_2_ = bf16[48,2176]{1,0:T(8,128)(2,1)S(1)} collective-permute-done((bf16[48,2176]{1,0:T(8,128)(2,1)S(1)}, bf16[48,2176]{1,0:T(8,128)(2,1)S(1)}, u32[]{:S(2)}, u32[]{:S(2)}) %collective-permute-start.19) | collective-permute-done | bytes 208928 | tf_op jit(solution)/shard_map/ppermute | solution.py:29
  138.7 3.6 %collective-permute-done.20.refs_3_ = bf16[48,2176]{1,0:T(8,128)(2,1)S(1)} collective-permute-done((bf16[48,2176]{1,0:T(8,128)(2,1)}, bf16[48,2176]{1,0:T(8,128)(2,1)S(1)}, u32[]{:S(2)}, u32[]{:S(2)}) %collective-permute-start.20) | collective-permute-done | bytes 208928 | tf_op jit(solution)/shard_map/ppermute | solution.py:29
  143.6 3.0 %collective-permute-start.22 = (bf16[48,1024]{1,0:T(8,128)(2,1)S(1)}, bf16[48,1024]{1,0:T(8,128)(2,1)S(1)}, u32[]{:S(2)}, u32[]{:S(2)}) collective-permute-start(bf16[48,1024]{1,0:T(8,128)(2,1)S(1)} %shard_map.236.refs_1_), channel_id=1, source_target_pairs={{0,4},{2,6},{4,0},{6,2},{1,5},{3,7},{5,1},{7,3},{8,12},{10,14},{12... | collective-permute-start | bytes 294920 | tf_op jit(solution)/shard_map/ppermute | solution.py:29
  148.1 2.3 %collective-permute-done.22.refs_3_ = bf16[48,1024]{1,0:T(8,128)(2,1)S(1)} collective-permute-done((bf16[48,1024]{1,0:T(8,128)(2,1)S(1)}, bf16[48,1024]{1,0:T(8,128)(2,1)S(1)}, u32[]{:S(2)}, u32[]{:S(2)}) %collective-permute-start.22) | collective-permute-done | bytes 98336 | tf_op jit(solution)/shard_map/ppermute | solution.py:29
  151.4 3.2 %shard_map.237.refs_3_ = bf16[2,192,256]{2,1,0:T(8,128)(2,1)S(1)} custom-call(s32[3]{0:T(128)S(1)} %copy-done.2, bf16[48,1024]{1,0:T(8,128)(2,1)S(1)} %shard_map.236.refs_1_, bf16[48,1024]{1,0:T(8,128)(2,1)S(1)} %collective-permute-done.21.refs_2_, bf16[48,1024]{1,0:T(8,128)(2,1)S(1)} %collective-permute-done.22.refs_3_, ...), custom_call_target="tpu_custom_call" | custom-call | flops 201326592 | bytes 3735564 | tf_op jit(solution)/shard_map/pallas_call | solution.py:86
  155.6 3.0 %shard_map.238 = (bf16[1536,128]{1,0:T(8,128)(2,1)}, f32[48,256]{1,0:T(8,128)S(1)}, bf16[48,256]{1,0:T(8,128)(2,1)S(1)}) custom-call(s32[3]{0:T(128)S(1)} %copy-done.2, s32[384,1]{1,0:T(8,128)S(1)} %fusion.8.refs_1_, bf16[4,240,512]{2,1,0:T(8,128)(2,1)} %copy-done.6, bf16[2,192,256]{2,1,0:T(8,128)(2,1)S(1)} %shard_map.237.refs_3_), custom_call_target="tpu_custom_call" | custom-call | flops 150994944 | bytes 1648140 | tf_op jit(solution)/shard_map/pallas_call | solution.py:86
  158.7 5.8 %all-to-all-start.5 = ((bf16[64,24,128]{2,1,0:T(8,128)(2,1)}), bf16[64,24,128]{2,1,0:T(8,128)(2,1)S(1)}, u32[]{:S(2)}, u32[]{:S(2)}) async-start(bf16[64,24,128]{2,1,0:T(8,128)(2,1)} %bitcast.16), calls=%async_computation.5 | async-start | bytes 786432 | tf_op jit(solution)/shard_map/all_to_all | solution.py:20
  164.7 5.1 %multiply_add_fusion = f32[48,1,128,128]{3,2,1,0:T(8,128)} fusion(f32[48,1,128,128]{3,2,1,0:T(8,128)} %param.24, f32[48,128]{1,0:T(8,128)S(1)} %get-tuple-element.47, f32[48,128]{1,0:T(8,128)S(1)} %get-tuple-element.46, f32[48,128]{1,0:T(8,128)S(1)} %get-tuple-element.45), kind=kLoop, calls=%fused_computation | loop fusion | flops 2359296 | bytes 6365184 | tf_op jit(solution)/shard_map/add | solution.py:487
  169.8 9.7 %all-to-all-done.5 = bf16[64,24,128]{2,1,0:T(8,128)(2,1)S(1)} async-done(((bf16[64,24,128]{2,1,0:T(8,128)(2,1)}), bf16[64,24,128]{2,1,0:T(8,128)(2,1)S(1)}, u32[]{:S(2)}, u32[]{:S(2)}) %all-to-all-start.5) | async-done | bytes 393248 | tf_op jit(solution)/shard_map/all_to_all | solution.py:20
  (99 shorter events, 28.7 us)
Async XLA Ops:
  4.6 26.0 %all-to-all-start = ((bf16[8,64,512]{2,1,0:T(8,128)(2,1)}), bf16[8,64,512]{2,1,0:T(8,128)(2,1)S(1)}, u32[]{:S(2)}, u32[]{:S(2)}) async-start(bf16[8,64,512]{2,1,0:T(8,128)(2,1)} %get-tuple-element.29), calls=%async_computation | async-start | bytes 1048576 | tf_op jit(solution)/shard_map/all_to_all | solution.py:20
  13.1 8.2 %collective-permute-start = (bf16[48,512]{1,0:T(8,128)(2,1)}, bf16[48,512]{1,0:T(8,128)(2,1)S(1)}, u32[]{:S(2)}, u32[]{:S(2)}) collective-permute-start(bf16[48,512]{1,0:T(8,128)(2,1)} %get-tuple-element.26), channel_id=1, source_target_pairs={{0,8},{8,16},{16,24},{24,0},{1,9},{9,17},{17,25},{25,1},{2,10},{10... | collective-permute-start | bytes 147464 | tf_op jit(solution)/shard_map/ppermute | solution.py:29
  14.6 6.7 %collective-permute-start.1 = (bf16[48,512]{1,0:T(8,128)(2,1)}, bf16[48,512]{1,0:T(8,128)(2,1)S(1)}, u32[]{:S(2)}, u32[]{:S(2)}) collective-permute-start(bf16[48,512]{1,0:T(8,128)(2,1)} %get-tuple-element.27), channel_id=1, source_target_pairs={{0,16},{8,24},{16,0},{24,8},{1,17},{9,25},{17,1},{25,9},{2,18},{10... | collective-permute-start | bytes 147464 | tf_op jit(solution)/shard_map/ppermute | solution.py:29
  17.3 4.3 %collective-permute-start.2 = (bf16[48,512]{1,0:T(8,128)(2,1)}, bf16[48,512]{1,0:T(8,128)(2,1)S(1)}, u32[]{:S(2)}, u32[]{:S(2)}) collective-permute-start(bf16[48,512]{1,0:T(8,128)(2,1)} %get-tuple-element.28), channel_id=1, source_target_pairs={{0,24},{8,0},{16,8},{24,16},{1,25},{9,1},{17,9},{25,17},{2,26},{10... | collective-permute-start | bytes 147464 | tf_op jit(solution)/shard_map/ppermute | solution.py:29
  31.8 4.9 %collective-permute-start.3 = (bf16[48,512]{1,0:T(8,128)(2,1)S(1)}, bf16[48,512]{1,0:T(8,128)(2,1)S(1)}, u32[]{:S(2)}, u32[]{:S(2)}) collective-permute-start(bf16[48,512]{1,0:T(8,128)(2,1)S(1)} %get-tuple-element.50), channel_id=1, source_target_pairs={{0,24},{8,0},{16,8},{24,16},{1,25},{9,1},{17,9},{25,17},{2,26},{10... | collective-permute-start | bytes 147464 | tf_op jit(solution)/shard_map/ppermute | solution.py:29
  34.6 5.6 %collective-permute-start.4 = (bf16[48,512]{1,0:T(8,128)(2,1)S(1)}, bf16[48,512]{1,0:T(8,128)(2,1)S(1)}, u32[]{:S(2)}, u32[]{:S(2)}) collective-permute-start(bf16[48,512]{1,0:T(8,128)(2,1)S(1)} %get-tuple-element.49), channel_id=1, source_target_pairs={{0,16},{8,24},{16,0},{24,8},{1,17},{9,25},{17,1},{25,9},{2,18},{10... | collective-permute-start | bytes 147464 | tf_op jit(solution)/shard_map/ppermute | solution.py:29
  35.4 5.3 %collective-permute-start.5 = (bf16[48,512]{1,0:T(8,128)(2,1)S(1)}, bf16[48,512]{1,0:T(8,128)(2,1)S(1)}, u32[]{:S(2)}, u32[]{:S(2)}) collective-permute-start(bf16[48,512]{1,0:T(8,128)(2,1)S(1)} %get-tuple-element.48), channel_id=1, source_target_pairs={{0,8},{8,16},{16,24},{24,0},{1,9},{9,17},{17,25},{25,1},{2,10},{10... | collective-permute-start | bytes 147464 | tf_op jit(solution)/shard_map/ppermute | solution.py:29
  44.9 1.4 collective-permute-start.6
  46.9 9.3 %all-to-all-start.1 = ((bf16[4,48,256]{2,1,0:T(8,128)(2,1)}), bf16[4,48,256]{2,1,0:T(8,128)(2,1)S(1)}, u32[]{:S(2)}, u32[]{:S(2)}) async-start(bf16[4,48,256]{2,1,0:T(8,128)(2,1)} %add_convert_fusion), calls=%async_computation.1 | async-start | bytes 196608 | tf_op jit(solution)/shard_map/all_to_all | solution.py:20
  58.8 50.0 %copy-start.1 = (f32[2048]{0:T(1024)S(1)}, f32[2048]{0:T(1024)}, u32[]{:S(2)}) copy-start(f32[2048]{0:T(1024)} %param.33) | copy-start | bytes 24580
  58.8 19.6 %all-to-all-start.2 = ((bf16[64,24,128]{2,1,0:T(8,128)(2,1)}), bf16[64,24,128]{2,1,0:T(8,128)(2,1)S(1)}, u32[]{:S(2)}, u32[]{:S(2)}) async-start(bf16[64,24,128]{2,1,0:T(8,128)(2,1)} %bitcast.10), calls=%async_computation.2 | async-start | bytes 786432 | tf_op jit(solution)/shard_map/all_to_all | solution.py:20
  63.5 25.0 %collective-permute-start.11 = (bf16[3,256,256]{2,1,0:T(8,128)(2,1)S(1)}, bf16[3,256,256]{2,1,0:T(8,128)(2,1)}, u32[]{:S(2)}, u32[]{:S(2)}) collective-permute-start(bf16[3,256,256]{2,1,0:T(8,128)(2,1)S(1)} %copy-done.10), channel_id=1, source_target_pairs={{0,8},{8,16},{16,24},{24,0},{1,9},{9,17},{17,25},{25,1},{2,10},{10... | collective-permute-start | bytes 1179656 | tf_op jit(solution)/shard_map/ppermute | solution.py:29
  66.9 40.1 %collective-permute-start.10 = (bf16[128,2048]{1,0:T(8,128)(2,1)}, bf16[128,2048]{1,0:T(8,128)(2,1)}, u32[]{:S(2)}, u32[]{:S(2)}) collective-permute-start(bf16[128,2048]{1,0:T(8,128)(2,1)} %dynamic-slice_bitcast_fusion), channel_id=1, source_target_pairs={{0,1},{1,0},{2,3},{3,2},{4,5},{5,4},{6,7},{7,6},{8,9},{9,8},{10,11... | collective-permute-start | bytes 1572872 | tf_op jit(solution)/shard_map/ppermute | solution.py:24
  67.8 39.8 %collective-permute-start.8 = (bf16[2048,128]{1,0:T(8,128)(2,1)}, bf16[2048,128]{1,0:T(8,128)(2,1)S(1)}, u32[]{:S(2)}, u32[]{:S(2)}) collective-permute-start(bf16[2048,128]{1,0:T(8,128)(2,1)} %dynamic-slice_bitcast_fusion.2), channel_id=1, source_target_pairs={{0,1},{1,0},{2,3},{3,2},{4,5},{5,4},{6,7},{7,6},{8,9},{9,8},{10,11... | collective-permute-start | bytes 1572872 | tf_op jit(solution)/shard_map/ppermute | solution.py:24
  68.3 1.8 collective-permute-start.7
  80.5 27.2 %all-to-all-start.3 = ((bf16[4,240,512]{2,1,0:T(8,128)(2,1)}), bf16[4,240,512]{2,1,0:T(8,128)(2,1)S(1)}, u32[]{:S(2)}, u32[]{:S(2)}) async-start(bf16[4,240,512]{2,1,0:T(8,128)(2,1)} %get-tuple-element.34), calls=%async_computation.3 | async-start | bytes 1966080 | tf_op jit(solution)/shard_map/all_to_all | solution.py:20
  85.5 22.2 %collective-permute-start.9 = (bf16[2048,128]{1,0:T(8,128)(2,1)S(1)}, bf16[2048,128]{1,0:T(8,128)(2,1)S(1)}, u32[]{:S(2)}, u32[]{:S(2)}) collective-permute-start(bf16[2048,128]{1,0:T(8,128)(2,1)S(1)} %dynamic-slice_bitcast_fusion.1), channel_id=1, source_target_pairs={{0,1},{1,0},{2,3},{3,2},{4,5},{5,4},{6,7},{7,6},{8,9},{9,8},{10,11... | collective-permute-start | bytes 1572872 | tf_op jit(solution)/shard_map/ppermute | solution.py:24
  85.6 13.1 %collective-permute-start.12 = (bf16[3,256,256]{2,1,0:T(8,128)(2,1)S(1)}, bf16[3,256,256]{2,1,0:T(8,128)(2,1)}, u32[]{:S(2)}, u32[]{:S(2)}) collective-permute-start(bf16[3,256,256]{2,1,0:T(8,128)(2,1)S(1)} %copy-done.10), channel_id=1, source_target_pairs={{0,16},{8,24},{16,0},{24,8},{1,17},{9,25},{17,1},{25,9},{2,18},{10... | collective-permute-start | bytes 1179656 | tf_op jit(solution)/shard_map/ppermute | solution.py:29
  88.5 18.6 %collective-permute-start.13 = (bf16[3,256,256]{2,1,0:T(8,128)(2,1)S(1)}, bf16[3,256,256]{2,1,0:T(8,128)(2,1)}, u32[]{:S(2)}, u32[]{:S(2)}) collective-permute-start(bf16[3,256,256]{2,1,0:T(8,128)(2,1)S(1)} %copy-done.10), channel_id=1, source_target_pairs={{0,24},{8,0},{16,8},{24,16},{1,25},{9,1},{17,9},{25,17},{2,26},{10... | collective-permute-start | bytes 1179656 | tf_op jit(solution)/shard_map/ppermute | solution.py:29
  98.7 21.1 %collective-permute-start.14 = (bf16[3,256,256]{2,1,0:T(8,128)(2,1)S(1)}, bf16[3,256,256]{2,1,0:T(8,128)(2,1)}, u32[]{:S(2)}, u32[]{:S(2)}) collective-permute-start(bf16[3,256,256]{2,1,0:T(8,128)(2,1)S(1)} %copy-done.10), channel_id=1, source_target_pairs={{0,1},{1,0},{2,3},{3,2},{4,5},{5,4},{6,7},{7,6},{8,9},{9,8},{10,11... | collective-permute-start | bytes 1179656 | tf_op jit(solution)/shard_map/ppermute | solution.py:24
  107.1 12.8 %collective-permute-start.15 = (bf16[3,256,256]{2,1,0:T(8,128)(2,1)}, bf16[3,256,256]{2,1,0:T(8,128)(2,1)}, u32[]{:S(2)}, u32[]{:S(2)}) collective-permute-start(bf16[3,256,256]{2,1,0:T(8,128)(2,1)} %collective-permute-done.11.refs_4_.refs_6_), channel_id=1, source_target_pairs={{0,1},{1,0},{2,3},{3,2},{4,5},{5,4},{6,7},{7,6},{8,9},{9,8},{10,11... | collective-permute-start | bytes 1179656 | tf_op jit(solution)/shard_map/ppermute | solution.py:24
  107.1 12.8 %collective-permute-start.16 = (bf16[3,256,256]{2,1,0:T(8,128)(2,1)}, bf16[3,256,256]{2,1,0:T(8,128)(2,1)}, u32[]{:S(2)}, u32[]{:S(2)}) collective-permute-start(bf16[3,256,256]{2,1,0:T(8,128)(2,1)} %collective-permute-done.12.refs_5_.refs_7_), channel_id=1, source_target_pairs={{0,1},{1,0},{2,3},{3,2},{4,5},{5,4},{6,7},{7,6},{8,9},{9,8},{10,11... | collective-permute-start | bytes 1179656 | tf_op jit(solution)/shard_map/ppermute | solution.py:24
  107.6 12.3 %collective-permute-start.17 = (bf16[3,256,256]{2,1,0:T(8,128)(2,1)}, bf16[3,256,256]{2,1,0:T(8,128)(2,1)}, u32[]{:S(2)}, u32[]{:S(2)}) collective-permute-start(bf16[3,256,256]{2,1,0:T(8,128)(2,1)} %collective-permute-done.13.refs_6_.refs_8_), channel_id=1, source_target_pairs={{0,1},{1,0},{2,3},{3,2},{4,5},{5,4},{6,7},{7,6},{8,9},{9,8},{10,11... | collective-permute-start | bytes 1179656 | tf_op jit(solution)/shard_map/ppermute | solution.py:24
  115.0 39.6 %all-to-all-start.4 = ((bf16[4,240,512]{2,1,0:T(8,128)(2,1)}), bf16[4,240,512]{2,1,0:T(8,128)(2,1)S(1)}, u32[]{:S(2)}, u32[]{:S(2)}) async-start(bf16[4,240,512]{2,1,0:T(8,128)(2,1)} %shard_map.234), calls=%async_computation.4 | async-start | bytes 1966080 | tf_op jit(solution)/shard_map/all_to_all | solution.py:20
  124.7 11.9 %collective-permute-start.18 = (bf16[48,2176]{1,0:T(8,128)(2,1)S(1)}, bf16[48,2176]{1,0:T(8,128)(2,1)S(1)}, u32[]{:S(2)}, u32[]{:S(2)}) collective-permute-start(bf16[48,2176]{1,0:T(8,128)(2,1)S(1)} %get-tuple-element.38), channel_id=1, source_target_pairs={{0,2},{2,4},{4,6},{6,0},{1,3},{3,5},{5,7},{7,1},{8,10},{10,12},{12... | collective-permute-start | bytes 626696 | tf_op jit(solution)/shard_map/ppermute | solution.py:29
  126.3 12.5 %collective-permute-start.19 = (bf16[48,2176]{1,0:T(8,128)(2,1)S(1)}, bf16[48,2176]{1,0:T(8,128)(2,1)S(1)}, u32[]{:S(2)}, u32[]{:S(2)}) collective-permute-start(bf16[48,2176]{1,0:T(8,128)(2,1)S(1)} %get-tuple-element.39), channel_id=1, source_target_pairs={{0,4},{2,6},{4,0},{6,2},{1,5},{3,7},{5,1},{7,3},{8,12},{10,14},{12... | collective-permute-start | bytes 626696 | tf_op jit(solution)/shard_map/ppermute | solution.py:29
  127.0 15.4 %collective-permute-start.20 = (bf16[48,2176]{1,0:T(8,128)(2,1)}, bf16[48,2176]{1,0:T(8,128)(2,1)S(1)}, u32[]{:S(2)}, u32[]{:S(2)}) collective-permute-start(bf16[48,2176]{1,0:T(8,128)(2,1)} %get-tuple-element.40), channel_id=1, source_target_pairs={{0,6},{2,0},{4,2},{6,4},{1,7},{3,1},{5,3},{7,5},{8,14},{10,8},{12,... | collective-permute-start | bytes 626696 | tf_op jit(solution)/shard_map/ppermute | solution.py:29
  142.9 5.1 %collective-permute-start.21 = (bf16[48,1024]{1,0:T(8,128)(2,1)S(1)}, bf16[48,1024]{1,0:T(8,128)(2,1)S(1)}, u32[]{:S(2)}, u32[]{:S(2)}) collective-permute-start(bf16[48,1024]{1,0:T(8,128)(2,1)S(1)} %shard_map.236.refs_1_), channel_id=1, source_target_pairs={{0,2},{2,4},{4,6},{6,0},{1,3},{3,5},{5,7},{7,1},{8,10},{10,12},{12... | collective-permute-start | bytes 294920 | tf_op jit(solution)/shard_map/ppermute | solution.py:29
  143.6 6.8 %collective-permute-start.22 = (bf16[48,1024]{1,0:T(8,128)(2,1)S(1)}, bf16[48,1024]{1,0:T(8,128)(2,1)S(1)}, u32[]{:S(2)}, u32[]{:S(2)}) collective-permute-start(bf16[48,1024]{1,0:T(8,128)(2,1)S(1)} %shard_map.236.refs_1_), channel_id=1, source_target_pairs={{0,4},{2,6},{4,0},{6,2},{1,5},{3,7},{5,1},{7,3},{8,12},{10,14},{12... | collective-permute-start | bytes 294920 | tf_op jit(solution)/shard_map/ppermute | solution.py:29
  146.6 4.8 %collective-permute-start.23 = (bf16[48,1024]{1,0:T(8,128)(2,1)S(1)}, bf16[48,1024]{1,0:T(8,128)(2,1)S(1)}, u32[]{:S(2)}, u32[]{:S(2)}) collective-permute-start(bf16[48,1024]{1,0:T(8,128)(2,1)S(1)} %shard_map.236.refs_1_), channel_id=1, source_target_pairs={{0,6},{2,0},{4,2},{6,4},{1,7},{3,1},{5,3},{7,5},{8,14},{10,8},{12,... | collective-permute-start | bytes 294920 | tf_op jit(solution)/shard_map/ppermute | solution.py:29
  158.7 20.8 %all-to-all-start.5 = ((bf16[64,24,128]{2,1,0:T(8,128)(2,1)}), bf16[64,24,128]{2,1,0:T(8,128)(2,1)S(1)}, u32[]{:S(2)}, u32[]{:S(2)}) async-start(bf16[64,24,128]{2,1,0:T(8,128)(2,1)} %bitcast.16), calls=%async_computation.5 | async-start | bytes 786432 | tf_op jit(solution)/shard_map/all_to_all | solution.py:20
  164.6 5.2 %collective-permute-start.24 = (bf16[48,256]{1,0:T(8,128)(2,1)S(1)}, bf16[48,256]{1,0:T(8,128)(2,1)S(1)}, u32[]{:S(2)}, u32[]{:S(2)}) collective-permute-start(bf16[48,256]{1,0:T(8,128)(2,1)S(1)} %get-tuple-element.44), channel_id=1, source_target_pairs={{0,1},{1,0},{2,3},{3,2},{4,5},{5,4},{6,7},{7,6},{8,9},{9,8},{10,11... | collective-permute-start | bytes 73736 | tf_op jit(solution)/shard_map/ppermute | solution.py:24
  (12 other events, 274.5 us)

commit v8 on v7

--- a/solution.py
+++ b/solution.py
@@ -46,10 +46,14 @@
     moved = sum(a.size * a.dtype.itemsize for a in args) + sum(
         o.size * o.dtype.itemsize for o in outs
     )
-    space = {"s": pltpu.SMEM, "v": pltpu.VMEM, "h": pltpu.HBM, "l": pltpu.HBM}
-    fetched = [i for i, k in enumerate(kinds) if k in "hl"]
+    space = {"s": pltpu.SMEM, "v": pltpu.VMEM}
+    fetched = [i for i, k in enumerate(kinds) if k in "hlqe"]
     stored = [i for i, k in enumerate(out_kinds) if k == "h"]
-    room = [pltpu.VMEM(args[i].shape, args[i].dtype) for i in fetched]
+    room = [
+        pltpu.VMEM(args[i].shape[1 if kinds[i] == "e" else 0 :], args[i].dtype) for i in fetched
+    ]
+    pieces = {"h": 1, "l": 1, "q": 4, "e": 4}
+    n_sems = sum(pieces[kinds[i]] for i in fetched)
     out_room = [pltpu.VMEM(outs[i].shape, outs[i].dtype) for i in stored]
 
     def whole(*refs):
@@ -58,20 +62,35 @@
         in_room, rest = rest[: len(room)], rest[len(room) :]
         result_room, rest = rest[: len(out_room)], rest[len(out_room) :]
         in_sem, out_sem, extra = rest[0], rest[1], rest[2:]
-        late = []
-        now = []
+        late, now, order = [], [], []
+        sem = 0
         for n, i in enumerate(fetched):
-            copy = pltpu.make_async_copy(ins[i], in_room[n], in_sem.at[n])
+            kind = kinds[i]
+            source = ins[i].at[ins[0][1]] if kind == "e" else ins[i]
+            parts = pieces[kind]
+            size = in_room[n].shape[0] // parts
+            copies = []
+            for p in range(parts):
+                cut = pl.ds(p * size, size)
+                copies.append(
+                    pltpu.make_async_copy(source.at[cut], in_room[n].at[cut], in_sem.at[sem])
+                )
+                order.append((p, sem, copies[-1]))
+                sem += 1
+            if kind == "h":
+                now.extend(copies)
+            else:
+                late.append([copy.wait for copy in copies])
+            ins[i] = in_room[n]
+        for _, _, copy in sorted(order, key=lambda o: o[:2]):
             copy.start()
-            (late if kinds[i] == "l" else now).append(copy)
-            ins[i] = in_room[n]
         targets = list(results)
         for n, i in enumerate(stored):
             results[i] = result_room[n]
         for copy in now:
             copy.wait()
         if late:
-            body([copy.wait for copy in late], *ins, *results, *extra)
+            body(late, *ins, *results, *extra)
         else:
             body(*ins, *results, *extra)
         back = [
@@ -86,12 +105,12 @@
     return pl.pallas_call(
         whole,
         out_shape=outs,
-        in_specs=[pl.BlockSpec(memory_space=space[k]) for k in kinds],
-        out_specs=[pl.BlockSpec(memory_space=space[k]) for k in out_kinds],
+        in_specs=[pl.BlockSpec(memory_space=space.get(k, pltpu.HBM)) for k in kinds],
+        out_specs=[pl.BlockSpec(memory_space=space.get(k, pltpu.HBM)) for k in out_kinds],
         scratch_shapes=[
             *room,
             *out_room,
-            pltpu.SemaphoreType.DMA((max(1, len(room)),)),
+            pltpu.SemaphoreType.DMA((max(1, n_sems),)),
             pltpu.SemaphoreType.DMA((max(1, len(out_room)),)),
             *scratch,
         ],
@@ -148,13 +167,14 @@
     key_out[...] = key
     value_out[...] = values
     turned = jnp.transpose(query * decay)
-    wait[0]()
     for b in range(seq):
+        if b % (seq // 4) == 0:
+            wait[0][b // (seq // 4)]()
         read[b : b + 1, :] = jnp.sum(turned[:, b : b + 1] * state[b], axis=0, keepdims=True)
     readout = read[...] + jnp.sum(query * key, axis=1, keepdims=True) * values
     readout = readout * lax.rsqrt(jnp.mean(readout * readout, axis=1, keepdims=True) + EPS)
     head = (readout * gain[...] * silu(gate)).astype(BF)
-    wait[1]()
+    wait[1][0]()
     cols = keep.shape[2]
     for y in range(keep.shape[0]):
         cut = slice(2 * y * cols, (2 * y + 1) * cols)
@@ -242,7 +262,7 @@
             both[copy, count:, side * cols : (side + 1) * cols] = both_rows[side]
 
 
-def dense_first_half(at, rows, gain, *refs):
+def dense_first_half(wait, at, rows, gain, *refs):
     y, c = at[0], at[1]
     own_w, other_w, outs = refs[:4], refs[4:8], refs[8:]
     ny = len(outs)
@@ -264,8 +284,10 @@
     low = square - high
     own = (own * gain[pl.ds(2 * y + c, 1), :]).astype(BF)
     other = (other * gain[pl.ds(2 * y + 1 - c, 1), :]).astype(BF)
-    for kind in range(2):
-        for i in range(4):
+    for i in range(4):
+        wait[i][0]()
+        wait[4 + i][0]()
+        for kind in range(2):
             value = (dot(own, own_w[i][kind]) + dot(other, other_w[i][kind])).astype(BF)
             at_col = (kind * 4 + i) * cols
             for d in range(ny):
@@ -293,7 +315,7 @@
     out[...] = (silu(gate) * up).astype(BF)
 
 
-def dense_second_half(at, *refs):
+def dense_second_half(wait, at, *refs):
     y = at[0]
     hidden, own_w, other_w, out = refs[:4], refs[4:8], refs[8:12], refs[12]
     ny = len(hidden)
@@ -302,6 +324,7 @@
     for side, weights in enumerate((own_w, other_w)):
         total = None
         for i in range(4):
+            wait[4 * side + i][0]()
             term = dot(rows[:, i * cols : (i + 1) * cols], weights[i][2])
             total = term if total is None else total + term
         total = total.astype(BF)
@@ -314,43 +337,38 @@
     wait, at, whole, gain, gate, gate_other, up, up_other, down, down_other,
     shared_gate, shared_up, shared_down, parts,
 ):
-    c = at[1]
     ny, lines, block = whole.shape
     count = lines - 48
+    half = gate.shape[1]
     square = jnp.zeros((lines, 1), F32)
-    rows = []
+    gate_pre = up_pre = shared_pre = None
+
+    def more(total, term):
+        return term if total is None else total + term
+
     for i in range(ny):
+        cut = slice(i * block, (i + 1) * block)
+        for k in (0, 1, 2, 3, 4, 7, 8):
+            wait[k][i]()
         value = whole[i].astype(F32)
         square = square + jnp.sum(value * value, axis=1, keepdims=True)
-        rows.append(value)
+        rows = (value * gain[:, cut]).astype(BF)
+        gates = jnp.concatenate([gate[cut, :], gate_other[cut, :]], axis=1)
+        ups = jnp.concatenate([up[cut, :], up_other[cut, :]], axis=1)
+        shared = jnp.concatenate([shared_gate[cut, :], shared_up[cut, :]], axis=1)
+        gate_pre = more(gate_pre, dot(rows[:count], gates))
+        up_pre = more(up_pre, dot(rows[:count], ups))
+        shared_pre = more(shared_pre, dot(rows[count:], shared))
     scale = lax.rsqrt(square / (ny * block) + EPS)
-    rows = [
-        (value * scale * gain[:, i * block : (i + 1) * block]).astype(BF)
-        for i, value in enumerate(rows)
-    ]
-    gate_pre = up_pre = gate_shared = None
-    for i in (0, 1, 2, 3, 6, 7):
-        wait[i]()
-
-    def more(total, term):
-        return term if total is None else total + term
-
+    hidden = (silu(gate_pre * scale[:count]) * (up_pre * scale[:count])).astype(BF)
+    shared_pre = shared_pre * scale[count:]
+    shared_hidden = (silu(shared_pre[:, :half]) * shared_pre[:, half:]).astype(BF)
+    for k in (5, 6, 9):
+        for done in wait[k]:
+            done()
     for i in range(ny):
         cut = slice(i * block, (i + 1) * block)
-        gates = jnp.concatenate([gate[c, cut, :], gate_other[cut, :]], axis=1)
-        ups = jnp.concatenate([up[c, cut, :], up_other[cut, :]], axis=1)
-        shared = jnp.concatenate([shared_gate[cut, :], shared_up[cut, :]], axis=1)
-        gate_pre = more(gate_pre, dot(rows[i][:count], gates))
-        up_pre = more(up_pre, dot(rows[i][:count], ups))
-        gate_shared = more(gate_shared, dot(rows[i][count:], shared))
-    for i in (4, 5, 8):
-        wait[i]()
-    half = gate.shape[2]
-    hidden = (silu(gate_pre) * up_pre).astype(BF)
-    shared_hidden = (silu(gate_shared[:, :half]) * gate_shared[:, half:]).astype(BF)
-    for i in range(ny):
-        cut = slice(i * block, (i + 1) * block)
-        downs = jnp.concatenate([down[c, :, cut], down_other[:, cut]], axis=0)
+        downs = jnp.concatenate([down[:, cut], down_other[:, cut]], axis=0)
         parts[i, :count, :] = dot(hidden, downs).astype(BF)
         parts[i, count:, :] = dot(shared_hidden, shared_down[:, cut]).astype(BF)
 
@@ -473,7 +491,7 @@
         recur,
         [shaped(seq, chan, dtype=F32)] * 3 + [shaped(ny, seq, cols)] * 2,
         4 * state.size,
-        "shvvvhhll hhhvh",
+        "shvvvhhql hhhvh",
         at,
         *pieces,
         lower_bound.reshape(1, chan),
@@ -537,7 +555,7 @@
         dense_first_half,
         [shaped(quarter, 2 * hidden_width + 128)] * ny,
         2 * count * nc * cols * 2 * hidden_width,
-        "shhhhhhhhhh hhhh",
+        "shhllllllll hhhh",
         at,
         dense_rows,
         ffn_gain.reshape(ny * nc, cols),
@@ -553,7 +571,7 @@
         dense_second_half,
         [shaped(nc, count, cols)],
         2 * count * nc * cols * hidden_width,
-        "shvvvhhhhhhhh h",
+        "shvvvllllllll h",
         at,
         *hidden,
         *dense_own,
@@ -564,7 +582,7 @@
         experts_and_shared,
         [shaped(ny, count + seq, nc * cols)],
         2 * 3 * (count * 2 + seq) * width * expert_gate.shape[2],
-        "svhlllllllll h",
+        "sqheqeqeqqqq h",
         at,
         whole,
         ffn_gain.reshape(1, width),

time: 184 us -> 182 us (0.989)
  no operation moved by 1% of the time
where the time goes in v8:
time: 182 us; the launch traced here: 180 us
  waiting for transfers between devices  72.4 us (40%)
  starting transfers between devices  59.7 us (33%)
  Pallas kernels  30.3 us (17%)
  other arithmetic  8.71 us (5%)
  local copies, waits for them, and re-layouts  6.34 us (3%)
    ppermute x15, waiting for transfers between devices, shift(): return lax.ppermute(x, axis, [(i, (i + by) % size) for i in range(size)])  38.1 us
    all_to_all x6, starting transfers between devices, swap(): return lax.all_to_all(x, axis, split_axis=0, concat_axis=0, tiled=True)  33.6 us
    all_to_all x6, waiting for transfers between devices, swap(): return lax.all_to_all(x, axis, split_axis=0, concat_axis=0, tiled=True)  31.3 us
    pallas_call x10, Pallas kernels, call(): pl.pallas_call(whole, out_shape=outs, in_specs=[pl.BlockSpec(memory_space...  30.3 us
    ppermute x15, starting transfers between devices, shift(): return lax.ppermute(x, axis, [(i, (i + by) % size) for i in range(size)])  24.7 us
    add x1, other arithmetic, step(): decay.reshape(shape)[..., None] * state  5.07 us
  transfers between devices with their start and end apart: 31, of which 18 were waited for; matrix products, arithmetic and copies ran while one was open for 6% of the time, Pallas kernels for 9%

profile of v8, /device:TPU:8, one launch (start us, length us, event | category | flops | bytes accessed | tf_op | source)
XLA Modules:
  0.0 179.7 jit_solution(7071022593754834985)
XLA Ops:
  1.3 3.4 %shard_map.230 = (bf16[8,64,512]{2,1,0:T(8,128)(2,1)}, bf16[3,256,256]{2,1,0:T(8,128)(2,1)}, bf16[48,512]{1,0:T(8,128)(2,1)}, bf16[48,512]{1,0:T(8,128)(2,1)}, b...) custom-call(s32[3]{0:T(128)} %pad_add_fusion.refs_0_, bf16[48,2048]{1,0:T(8,128)(2,1)} %refs_2_.1, f32[1,2048]{1,0:T(1,128)} %bitcast.43, ...), custom_call_target="tpu_custom_call" | custom-call | flops 1000000 | bytes 1777676 | tf_op jit(solution)/shard_map/pallas_call | solution.py:105
  4.6 8.5 %all-to-all-start = ((bf16[8,64,512]{2,1,0:T(8,128)(2,1)}), bf16[8,64,512]{2,1,0:T(8,128)(2,1)S(1)}, u32[]{:S(2)}, u32[]{:S(2)}) async-start(bf16[8,64,512]{2,1,0:T(8,128)(2,1)} %get-tuple-element.29), calls=%async_computation | async-start | bytes 1048576 | tf_op jit(solution)/shard_map/all_to_all | solution.py:20
  14.6 2.7 %collective-permute-start.1 = (bf16[48,512]{1,0:T(8,128)(2,1)}, bf16[48,512]{1,0:T(8,128)(2,1)S(1)}, u32[]{:S(2)}, u32[]{:S(2)}) collective-permute-start(bf16[48,512]{1,0:T(8,128)(2,1)} %get-tuple-element.27), channel_id=1, source_target_pairs={{0,16},{8,24},{16,0},{24,8},{1,17},{9,25},{17,1},{25,9},{2,18},{10... | collective-permute-start | bytes 147464 | tf_op jit(solution)/shard_map/ppermute | solution.py:29
  21.6 9.0 %all-to-all-done = bf16[8,64,512]{2,1,0:T(8,128)(2,1)S(1)} async-done(((bf16[8,64,512]{2,1,0:T(8,128)(2,1)}), bf16[8,64,512]{2,1,0:T(8,128)(2,1)S(1)}, u32[]{:S(2)}, u32[]{:S(2)}) %all-to-all-start) | async-done | bytes 524320 | tf_op jit(solution)/shard_map/all_to_all | solution.py:20
  31.8 2.8 %collective-permute-start.3 = (bf16[48,512]{1,0:T(8,128)(2,1)S(1)}, bf16[48,512]{1,0:T(8,128)(2,1)S(1)}, u32[]{:S(2)}, u32[]{:S(2)}) collective-permute-start(bf16[48,512]{1,0:T(8,128)(2,1)S(1)} %get-tuple-element.50), channel_id=1, source_target_pairs={{0,24},{8,0},{16,8},{24,16},{1,25},{9,1},{17,9},{25,17},{2,26},{10... | collective-permute-start | bytes 147464 | tf_op jit(solution)/shard_map/ppermute | solution.py:29
  36.7 3.5 %collective-permute-done.4.refs_3_ = bf16[48,512]{1,0:T(8,128)(2,1)S(1)} collective-permute-done((bf16[48,512]{1,0:T(8,128)(2,1)S(1)}, bf16[48,512]{1,0:T(8,128)(2,1)S(1)}, u32[]{:S(2)}, u32[]{:S(2)}) %collective-permute-start.4) | collective-permute-done | bytes 49184 | tf_op jit(solution)/shard_map/ppermute | solution.py:29
  40.7 3.7 %shard_map.231 = (f32[48,128]{1,0:T(8,128)S(1)}, f32[48,128]{1,0:T(8,128)S(1)}, f32[48,128]{1,0:T(8,128)S(1)}, bf16[4,48,256]{2,1,0:T(8,128)(2,1)S(1)}, bf16[4,48,256]{2,1,0:T(8,128)(2,1)S(1)}) custom-call(s32[3]{0:T(128)S(1)} %copy-done.2, bf16[48,512]{1,0:T(8,128)(2,1)S(1)} %get-tuple-element.51.refs_1_, ...), custom_call_target="tpu_custom_call" | custom-call | flops 3145728 | bytes 4137996 | tf_op jit(solution)/shard_map/pallas_call | solution.py:105
  46.5 4.9 %all-to-all-start.1 = ((bf16[4,48,256]{2,1,0:T(8,128)(2,1)}), bf16[4,48,256]{2,1,0:T(8,128)(2,1)S(1)}, u32[]{:S(2)}, u32[]{:S(2)}) async-start(bf16[4,48,256]{2,1,0:T(8,128)(2,1)} %add_convert_fusion), calls=%async_computation.1 | async-start | bytes 196608 | tf_op jit(solution)/shard_map/all_to_all | solution.py:20
  51.6 4.2 %all-to-all-done.1.refs_1_ = bf16[4,48,256]{2,1,0:T(8,128)(2,1)S(1)} async-done(((bf16[4,48,256]{2,1,0:T(8,128)(2,1)}), bf16[4,48,256]{2,1,0:T(8,128)(2,1)S(1)}, u32[]{:S(2)}, u32[]{:S(2)}) %all-to-all-start.1) | async-done | bytes 98336 | tf_op jit(solution)/shard_map/all_to_all | solution.py:20
  55.8 2.6 %shard_map.232 = (f32[48,256]{1,0:T(8,128)S(1)}, bf16[48,256]{1,0:T(8,128)(2,1)S(1)}, bf16[1536,128]{1,0:T(8,128)(2,1)}) custom-call(s32[3]{0:T(128)S(1)} %copy-done.2, bf16[4,48,256]{2,1,0:T(8,128)(2,1)S(1)} %all-to-all-done.1.refs_1_, bf16[48,2048]{1,0:T(8,128)(2,1)S(1)} %copy-done, s32[8,48]{1,0:T(8,128)S(1)} %copy.55.refs_3_), custom_call_target="tpu_custom_call" | custom-call | flops 37748736 | bytes 763404 | tf_op jit(solution)/shard_map/pallas_call | solution.py:105
  58.4 4.6 %all-to-all-start.2 = ((bf16[64,24,128]{2,1,0:T(8,128)(2,1)}), bf16[64,24,128]{2,1,0:T(8,128)(2,1)S(1)}, u32[]{:S(2)}, u32[]{:S(2)}) async-start(bf16[64,24,128]{2,1,0:T(8,128)(2,1)} %bitcast.10), calls=%async_computation.2 | async-start | bytes 786432 | tf_op jit(solution)/shard_map/all_to_all | solution.py:20
  64.6 1.9 %dynamic-slice_bitcast_fusion = bf16[128,2048]{1,0:T(8,128)(2,1)} fusion(bf16[2,128,2048]{2,1,0:T(8,128)(2,1)} %refs_7_.3, s32[]{:T(128)S(6)} %select_n.224), kind=kLoop, calls=%fused_computation.2 | loop fusion | bytes 1048580 | tf_op jit(solution)/shard_map/jit(dynamic_index_in_dim)/squeeze | solution.py:33
  69.6 8.4 %all-to-all-done.2 = bf16[64,24,128]{2,1,0:T(8,128)(2,1)S(1)} async-done(((bf16[64,24,128]{2,1,0:T(8,128)(2,1)}), bf16[64,24,128]{2,1,0:T(8,128)(2,1)S(1)}, u32[]{:S(2)}, u32[]{:S(2)}) %all-to-all-start.2) | async-done | bytes 393248 | tf_op jit(solution)/shard_map/all_to_all | solution.py:20
  78.1 2.0 %shard_map.233 = (bf16[4,240,512]{2,1,0:T(8,128)(2,1)}, bf16[2,192,256]{2,1,0:T(8,128)(2,1)S(1)}) custom-call(s32[3]{0:T(128)S(1)} %copy-done.2, s32[1,384]{1,0:T(1,128)S(1)} %fusion.53.refs_1_, bf16[1536,128]{1,0:T(8,128)(2,1)S(1)} %bitcast.36, bf16[48,256]{1,0:T(8,128)(2,1)S(1)} %get-tuple-element.33.refs_3_, ...), custom_call_target="tpu_custom_call" | custom-call | flops 150994944 | bytes 1623564 | tf_op jit(solution)/shard_map/pallas_call | solution.py:105
  80.1 5.0 %all-to-all-start.3 = ((bf16[4,240,512]{2,1,0:T(8,128)(2,1)}), bf16[4,240,512]{2,1,0:T(8,128)(2,1)S(1)}, u32[]{:S(2)}, u32[]{:S(2)}) async-start(bf16[4,240,512]{2,1,0:T(8,128)(2,1)} %get-tuple-element.34), calls=%async_computation.3 | async-start | bytes 1966080 | tf_op jit(solution)/shard_map/all_to_all | solution.py:20
  85.2 2.9 %collective-permute-start.12 = (bf16[3,256,256]{2,1,0:T(8,128)(2,1)S(1)}, bf16[3,256,256]{2,1,0:T(8,128)(2,1)}, u32[]{:S(2)}, u32[]{:S(2)}) collective-permute-start(bf16[3,256,256]{2,1,0:T(8,128)(2,1)S(1)} %copy-done.10), channel_id=1, source_target_pairs={{0,16},{8,24},{16,0},{24,8},{1,17},{9,25},{17,1},{25,9},{2,18},{10... | collective-permute-start | bytes 1179656 | tf_op jit(solution)/shard_map/ppermute | solution.py:29
  89.3 9.0 %collective-permute-done.12.refs_5_.refs_7_ = bf16[3,256,256]{2,1,0:T(8,128)(2,1)} collective-permute-done((bf16[3,256,256]{2,1,0:T(8,128)(2,1)S(1)}, bf16[3,256,256]{2,1,0:T(8,128)(2,1)}, u32[]{:S(2)}, u32[]{:S(2)}) %collective-permute-start.12) | collective-permute-done | bytes 393248 | tf_op jit(solution)/shard_map/ppermute | solution.py:29
  98.3 8.3 %collective-permute-done.13.refs_6_.refs_8_ = bf16[3,256,256]{2,1,0:T(8,128)(2,1)} collective-permute-done((bf16[3,256,256]{2,1,0:T(8,128)(2,1)S(1)}, bf16[3,256,256]{2,1,0:T(8,128)(2,1)}, u32[]{:S(2)}, u32[]{:S(2)}) %collective-permute-start.13) | collective-permute-done | bytes 393248 | tf_op jit(solution)/shard_map/ppermute | solution.py:29
  108.4 5.5 %shard_map.234 = bf16[4,240,512]{2,1,0:T(8,128)(2,1)} custom-call(s32[3]{0:T(128)S(1)} %copy-done.2, bf16[4,240,512]{2,1,0:T(8,128)(2,1)} %copy-done.7, f32[1,2048]{1,0:T(1,128)S(1)} %bitcast.37, bf16[2,2048,128]{2,1,0:T(8,128)(2,1)} %refs_3_.4, bf16[2048,128]{1,0:T(8,128)(2,1)S(1)} %collective-permute-done.8.refs_4_, bf16[2,2048,128]{2,1,0:T(8,128)(2,1)} %refs_5_.3, ...), custom_call_target="tpu_custom_call" | custom-call | flops 679477248 | bytes 8265740 | tf_op jit(solution)/shard_map/pallas_call | solution.py:105
  113.9 4.8 %all-to-all-start.4 = ((bf16[4,240,512]{2,1,0:T(8,128)(2,1)}), bf16[4,240,512]{2,1,0:T(8,128)(2,1)S(1)}, u32[]{:S(2)}, u32[]{:S(2)}) async-start(bf16[4,240,512]{2,1,0:T(8,128)(2,1)} %shard_map.234), calls=%async_computation.4 | async-start | bytes 1966080 | tf_op jit(solution)/shard_map/all_to_all | solution.py:20
  118.8 5.0 %shard_map.235 = (bf16[48,2176]{1,0:T(8,128)(2,1)S(1)}, bf16[48,2176]{1,0:T(8,128)(2,1)S(1)}, bf16[48,2176]{1,0:T(8,128)(2,1)S(1)}, bf16[48,2176]{1,0:T(8,128)(2,1)}) custom-call(s32[3]{0:T(128)S(1)} %copy-done.2, bf16[2,192,256]{2,1,0:T(8,128)(2,1)S(1)} %get-tuple-element.35.refs_1_, f32[8,256]{1,0:T(8,128)S(1)} %reshape.582.refs_2_, ...), custom_call_target="tpu_custom_call" | custom-call | flops 402653184 | bytes 4186124 | tf_op jit(solution)/shard_map/pallas_call | solution.py:105
  126.0 2.5 %collective-permute-start.20 = (bf16[48,2176]{1,0:T(8,128)(2,1)}, bf16[48,2176]{1,0:T(8,128)(2,1)S(1)}, u32[]{:S(2)}, u32[]{:S(2)}) collective-permute-start(bf16[48,2176]{1,0:T(8,128)(2,1)} %get-tuple-element.40), channel_id=1, source_target_pairs={{0,6},{2,0},{4,2},{6,4},{1,7},{3,1},{5,3},{7,5},{8,14},{10,8},{12,... | collective-permute-start | bytes 626696 | tf_op jit(solution)/shard_map/ppermute | solution.py:29
  128.6 6.9 %collective-permute-done.18.refs_1_ = bf16[48,2176]{1,0:T(8,128)(2,1)S(1)} collective-permute-done((bf16[48,2176]{1,0:T(8,128)(2,1)S(1)}, bf16[48,2176]{1,0:T(8,128)(2,1)S(1)}, u32[]{:S(2)}, u32[]{:S(2)}) %collective-permute-start.18) | collective-permute-done | bytes 208928 | tf_op jit(solution)/shard_map/ppermute | solution.py:29
  135.5 2.1 %collective-permute-done.19.refs_2_ = bf16[48,2176]{1,0:T(8,128)(2,1)S(1)} collective-permute-done((bf16[48,2176]{1,0:T(8,128)(2,1)S(1)}, bf16[48,2176]{1,0:T(8,128)(2,1)S(1)}, u32[]{:S(2)}, u32[]{:S(2)}) %collective-permute-start.19) | collective-permute-done | bytes 208928 | tf_op jit(solution)/shard_map/ppermute | solution.py:29
  137.6 3.6 %collective-permute-done.20.refs_3_ = bf16[48,2176]{1,0:T(8,128)(2,1)S(1)} collective-permute-done((bf16[48,2176]{1,0:T(8,128)(2,1)}, bf16[48,2176]{1,0:T(8,128)(2,1)S(1)}, u32[]{:S(2)}, u32[]{:S(2)}) %collective-permute-start.20) | collective-permute-done | bytes 208928 | tf_op jit(solution)/shard_map/ppermute | solution.py:29
  142.5 3.0 %collective-permute-start.22 = (bf16[48,1024]{1,0:T(8,128)(2,1)S(1)}, bf16[48,1024]{1,0:T(8,128)(2,1)S(1)}, u32[]{:S(2)}, u32[]{:S(2)}) collective-permute-start(bf16[48,1024]{1,0:T(8,128)(2,1)S(1)} %shard_map.236.refs_1_), channel_id=1, source_target_pairs={{0,4},{2,6},{4,0},{6,2},{1,5},{3,7},{5,1},{7,3},{8,12},{10,14},{12... | collective-permute-start | bytes 294920 | tf_op jit(solution)/shard_map/ppermute | solution.py:29
  146.9 2.3 %collective-permute-done.22.refs_3_ = bf16[48,1024]{1,0:T(8,128)(2,1)S(1)} collective-permute-done((bf16[48,1024]{1,0:T(8,128)(2,1)S(1)}, bf16[48,1024]{1,0:T(8,128)(2,1)S(1)}, u32[]{:S(2)}, u32[]{:S(2)}) %collective-permute-start.22) | collective-permute-done | bytes 98336 | tf_op jit(solution)/shard_map/ppermute | solution.py:29
  150.3 3.0 %shard_map.237.refs_3_ = bf16[2,192,256]{2,1,0:T(8,128)(2,1)S(1)} custom-call(s32[3]{0:T(128)S(1)} %copy-done.2, bf16[48,1024]{1,0:T(8,128)(2,1)S(1)} %shard_map.236.refs_1_, bf16[48,1024]{1,0:T(8,128)(2,1)S(1)} %collective-permute-done.21.refs_2_, bf16[48,1024]{1,0:T(8,128)(2,1)S(1)} %collective-permute-done.22.refs_3_, ...), custom_call_target="tpu_custom_call" | custom-call | flops 201326592 | bytes 3735564 | tf_op jit(solution)/shard_map/pallas_call | solution.py:105
  154.3 3.0 %shard_map.238 = (bf16[1536,128]{1,0:T(8,128)(2,1)}, f32[48,256]{1,0:T(8,128)S(1)}, bf16[48,256]{1,0:T(8,128)(2,1)S(1)}) custom-call(s32[3]{0:T(128)S(1)} %copy-done.2, s32[384,1]{1,0:T(8,128)S(1)} %fusion.8.refs_1_, bf16[4,240,512]{2,1,0:T(8,128)(2,1)} %copy-done.6, bf16[2,192,256]{2,1,0:T(8,128)(2,1)S(1)} %shard_map.237.refs_3_), custom_call_target="tpu_custom_call" | custom-call | flops 150994944 | bytes 1648140 | tf_op jit(solution)/shard_map/pallas_call | solution.py:105
  157.3 5.8 %all-to-all-start.5 = ((bf16[64,24,128]{2,1,0:T(8,128)(2,1)}), bf16[64,24,128]{2,1,0:T(8,128)(2,1)S(1)}, u32[]{:S(2)}, u32[]{:S(2)}) async-start(bf16[64,24,128]{2,1,0:T(8,128)(2,1)} %bitcast.16), calls=%async_computation.5 | async-start | bytes 786432 | tf_op jit(solution)/shard_map/all_to_all | solution.py:20
  163.3 5.1 %multiply_add_fusion = f32[48,1,128,128]{3,2,1,0:T(8,128)} fusion(f32[48,1,128,128]{3,2,1,0:T(8,128)} %param.24, f32[48,128]{1,0:T(8,128)S(1)} %get-tuple-element.47, f32[48,128]{1,0:T(8,128)S(1)} %get-tuple-element.46, f32[48,128]{1,0:T(8,128)S(1)} %get-tuple-element.45), kind=kLoop, calls=%fused_computation | loop fusion | flops 2359296 | bytes 6365184 | tf_op jit(solution)/shard_map/add | solution.py:505
  168.4 9.7 %all-to-all-done.5 = bf16[64,24,128]{2,1,0:T(8,128)(2,1)S(1)} async-done(((bf16[64,24,128]{2,1,0:T(8,128)(2,1)}), bf16[64,24,128]{2,1,0:T(8,128)(2,1)S(1)}, u32[]{:S(2)}, u32[]{:S(2)}) %all-to-all-start.5) | async-done | bytes 393248 | tf_op jit(solution)/shard_map/all_to_all | solution.py:20
  (99 shorter events, 28.7 us)
Async XLA Ops:
  4.6 26.0 %all-to-all-start = ((bf16[8,64,512]{2,1,0:T(8,128)(2,1)}), bf16[8,64,512]{2,1,0:T(8,128)(2,1)S(1)}, u32[]{:S(2)}, u32[]{:S(2)}) async-start(bf16[8,64,512]{2,1,0:T(8,128)(2,1)} %get-tuple-element.29), calls=%async_computation | async-start | bytes 1048576 | tf_op jit(solution)/shard_map/all_to_all | solution.py:20
  13.1 8.2 %collective-permute-start = (bf16[48,512]{1,0:T(8,128)(2,1)}, bf16[48,512]{1,0:T(8,128)(2,1)S(1)}, u32[]{:S(2)}, u32[]{:S(2)}) collective-permute-start(bf16[48,512]{1,0:T(8,128)(2,1)} %get-tuple-element.26), channel_id=1, source_target_pairs={{0,8},{8,16},{16,24},{24,0},{1,9},{9,17},{17,25},{25,1},{2,10},{10... | collective-permute-start | bytes 147464 | tf_op jit(solution)/shard_map/ppermute | solution.py:29
  14.6 6.7 %collective-permute-start.1 = (bf16[48,512]{1,0:T(8,128)(2,1)}, bf16[48,512]{1,0:T(8,128)(2,1)S(1)}, u32[]{:S(2)}, u32[]{:S(2)}) collective-permute-start(bf16[48,512]{1,0:T(8,128)(2,1)} %get-tuple-element.27), channel_id=1, source_target_pairs={{0,16},{8,24},{16,0},{24,8},{1,17},{9,25},{17,1},{25,9},{2,18},{10... | collective-permute-start | bytes 147464 | tf_op jit(solution)/shard_map/ppermute | solution.py:29
  17.3 4.3 %collective-permute-start.2 = (bf16[48,512]{1,0:T(8,128)(2,1)}, bf16[48,512]{1,0:T(8,128)(2,1)S(1)}, u32[]{:S(2)}, u32[]{:S(2)}) collective-permute-start(bf16[48,512]{1,0:T(8,128)(2,1)} %get-tuple-element.28), channel_id=1, source_target_pairs={{0,24},{8,0},{16,8},{24,16},{1,25},{9,1},{17,9},{25,17},{2,26},{10... | collective-permute-start | bytes 147464 | tf_op jit(solution)/shard_map/ppermute | solution.py:29
  31.8 4.9 %collective-permute-start.3 = (bf16[48,512]{1,0:T(8,128)(2,1)S(1)}, bf16[48,512]{1,0:T(8,128)(2,1)S(1)}, u32[]{:S(2)}, u32[]{:S(2)}) collective-permute-start(bf16[48,512]{1,0:T(8,128)(2,1)S(1)} %get-tuple-element.50), channel_id=1, source_target_pairs={{0,24},{8,0},{16,8},{24,16},{1,25},{9,1},{17,9},{25,17},{2,26},{10... | collective-permute-start | bytes 147464 | tf_op jit(solution)/shard_map/ppermute | solution.py:29
  34.6 5.6 %collective-permute-start.4 = (bf16[48,512]{1,0:T(8,128)(2,1)S(1)}, bf16[48,512]{1,0:T(8,128)(2,1)S(1)}, u32[]{:S(2)}, u32[]{:S(2)}) collective-permute-start(bf16[48,512]{1,0:T(8,128)(2,1)S(1)} %get-tuple-element.49), channel_id=1, source_target_pairs={{0,16},{8,24},{16,0},{24,8},{1,17},{9,25},{17,1},{25,9},{2,18},{10... | collective-permute-start | bytes 147464 | tf_op jit(solution)/shard_map/ppermute | solution.py:29
  35.4 5.3 %collective-permute-start.5 = (bf16[48,512]{1,0:T(8,128)(2,1)S(1)}, bf16[48,512]{1,0:T(8,128)(2,1)S(1)}, u32[]{:S(2)}, u32[]{:S(2)}) collective-permute-start(bf16[48,512]{1,0:T(8,128)(2,1)S(1)} %get-tuple-element.48), channel_id=1, source_target_pairs={{0,8},{8,16},{16,24},{24,0},{1,9},{9,17},{17,25},{25,1},{2,10},{10... | collective-permute-start | bytes 147464 | tf_op jit(solution)/shard_map/ppermute | solution.py:29
  44.4 1.4 collective-permute-start.6
  46.5 9.3 %all-to-all-start.1 = ((bf16[4,48,256]{2,1,0:T(8,128)(2,1)}), bf16[4,48,256]{2,1,0:T(8,128)(2,1)S(1)}, u32[]{:S(2)}, u32[]{:S(2)}) async-start(bf16[4,48,256]{2,1,0:T(8,128)(2,1)} %add_convert_fusion), calls=%async_computation.1 | async-start | bytes 196608 | tf_op jit(solution)/shard_map/all_to_all | solution.py:20
  58.4 50.0 %copy-start.1 = (f32[2048]{0:T(1024)S(1)}, f32[2048]{0:T(1024)}, u32[]{:S(2)}) copy-start(f32[2048]{0:T(1024)} %param.33) | copy-start | bytes 24580
  58.4 19.6 %all-to-all-start.2 = ((bf16[64,24,128]{2,1,0:T(8,128)(2,1)}), bf16[64,24,128]{2,1,0:T(8,128)(2,1)S(1)}, u32[]{:S(2)}, u32[]{:S(2)}) async-start(bf16[64,24,128]{2,1,0:T(8,128)(2,1)} %bitcast.10), calls=%async_computation.2 | async-start | bytes 786432 | tf_op jit(solution)/shard_map/all_to_all | solution.py:20
  63.1 25.0 %collective-permute-start.11 = (bf16[3,256,256]{2,1,0:T(8,128)(2,1)S(1)}, bf16[3,256,256]{2,1,0:T(8,128)(2,1)}, u32[]{:S(2)}, u32[]{:S(2)}) collective-permute-start(bf16[3,256,256]{2,1,0:T(8,128)(2,1)S(1)} %copy-done.10), channel_id=1, source_target_pairs={{0,8},{8,16},{16,24},{24,0},{1,9},{9,17},{17,25},{25,1},{2,10},{10... | collective-permute-start | bytes 1179656 | tf_op jit(solution)/shard_map/ppermute | solution.py:29
  66.5 40.1 %collective-permute-start.10 = (bf16[128,2048]{1,0:T(8,128)(2,1)}, bf16[128,2048]{1,0:T(8,128)(2,1)}, u32[]{:S(2)}, u32[]{:S(2)}) collective-permute-start(bf16[128,2048]{1,0:T(8,128)(2,1)} %dynamic-slice_bitcast_fusion), channel_id=1, source_target_pairs={{0,1},{1,0},{2,3},{3,2},{4,5},{5,4},{6,7},{7,6},{8,9},{9,8},{10,11... | collective-permute-start | bytes 1572872 | tf_op jit(solution)/shard_map/ppermute | solution.py:24
  67.4 39.8 %collective-permute-start.8 = (bf16[2048,128]{1,0:T(8,128)(2,1)}, bf16[2048,128]{1,0:T(8,128)(2,1)S(1)}, u32[]{:S(2)}, u32[]{:S(2)}) collective-permute-start(bf16[2048,128]{1,0:T(8,128)(2,1)} %dynamic-slice_bitcast_fusion.2), channel_id=1, source_target_pairs={{0,1},{1,0},{2,3},{3,2},{4,5},{5,4},{6,7},{7,6},{8,9},{9,8},{10,11... | collective-permute-start | bytes 1572872 | tf_op jit(solution)/shard_map/ppermute | solution.py:24
  67.9 1.8 collective-permute-start.7
  80.1 27.2 %all-to-all-start.3 = ((bf16[4,240,512]{2,1,0:T(8,128)(2,1)}), bf16[4,240,512]{2,1,0:T(8,128)(2,1)S(1)}, u32[]{:S(2)}, u32[]{:S(2)}) async-start(bf16[4,240,512]{2,1,0:T(8,128)(2,1)} %get-tuple-element.34), calls=%async_computation.3 | async-start | bytes 1966080 | tf_op jit(solution)/shard_map/all_to_all | solution.py:20
  85.1 22.2 %collective-permute-start.9 = (bf16[2048,128]{1,0:T(8,128)(2,1)S(1)}, bf16[2048,128]{1,0:T(8,128)(2,1)S(1)}, u32[]{:S(2)}, u32[]{:S(2)}) collective-permute-start(bf16[2048,128]{1,0:T(8,128)(2,1)S(1)} %dynamic-slice_bitcast_fusion.1), channel_id=1, source_target_pairs={{0,1},{1,0},{2,3},{3,2},{4,5},{5,4},{6,7},{7,6},{8,9},{9,8},{10,11... | collective-permute-start | bytes 1572872 | tf_op jit(solution)/shard_map/ppermute | solution.py:24
  85.2 13.1 %collective-permute-start.12 = (bf16[3,256,256]{2,1,0:T(8,128)(2,1)S(1)}, bf16[3,256,256]{2,1,0:T(8,128)(2,1)}, u32[]{:S(2)}, u32[]{:S(2)}) collective-permute-start(bf16[3,256,256]{2,1,0:T(8,128)(2,1)S(1)} %copy-done.10), channel_id=1, source_target_pairs={{0,16},{8,24},{16,0},{24,8},{1,17},{9,25},{17,1},{25,9},{2,18},{10... | collective-permute-start | bytes 1179656 | tf_op jit(solution)/shard_map/ppermute | solution.py:29
  88.1 18.6 %collective-permute-start.13 = (bf16[3,256,256]{2,1,0:T(8,128)(2,1)S(1)}, bf16[3,256,256]{2,1,0:T(8,128)(2,1)}, u32[]{:S(2)}, u32[]{:S(2)}) collective-permute-start(bf16[3,256,256]{2,1,0:T(8,128)(2,1)S(1)} %copy-done.10), channel_id=1, source_target_pairs={{0,24},{8,0},{16,8},{24,16},{1,25},{9,1},{17,9},{25,17},{2,26},{10... | collective-permute-start | bytes 1179656 | tf_op jit(solution)/shard_map/ppermute | solution.py:29
  98.3 20.4 %collective-permute-start.14 = (bf16[3,256,256]{2,1,0:T(8,128)(2,1)S(1)}, bf16[3,256,256]{2,1,0:T(8,128)(2,1)}, u32[]{:S(2)}, u32[]{:S(2)}) collective-permute-start(bf16[3,256,256]{2,1,0:T(8,128)(2,1)S(1)} %copy-done.10), channel_id=1, source_target_pairs={{0,1},{1,0},{2,3},{3,2},{4,5},{5,4},{6,7},{7,6},{8,9},{9,8},{10,11... | collective-permute-start | bytes 1179656 | tf_op jit(solution)/shard_map/ppermute | solution.py:24
  106.7 12.1 %collective-permute-start.15 = (bf16[3,256,256]{2,1,0:T(8,128)(2,1)}, bf16[3,256,256]{2,1,0:T(8,128)(2,1)}, u32[]{:S(2)}, u32[]{:S(2)}) collective-permute-start(bf16[3,256,256]{2,1,0:T(8,128)(2,1)} %collective-permute-done.11.refs_4_.refs_6_), channel_id=1, source_target_pairs={{0,1},{1,0},{2,3},{3,2},{4,5},{5,4},{6,7},{7,6},{8,9},{9,8},{10,11... | collective-permute-start | bytes 1179656 | tf_op jit(solution)/shard_map/ppermute | solution.py:24
  106.7 12.1 %collective-permute-start.16 = (bf16[3,256,256]{2,1,0:T(8,128)(2,1)}, bf16[3,256,256]{2,1,0:T(8,128)(2,1)}, u32[]{:S(2)}, u32[]{:S(2)}) collective-permute-start(bf16[3,256,256]{2,1,0:T(8,128)(2,1)} %collective-permute-done.12.refs_5_.refs_7_), channel_id=1, source_target_pairs={{0,1},{1,0},{2,3},{3,2},{4,5},{5,4},{6,7},{7,6},{8,9},{9,8},{10,11... | collective-permute-start | bytes 1179656 | tf_op jit(solution)/shard_map/ppermute | solution.py:24
  107.2 11.6 %collective-permute-start.17 = (bf16[3,256,256]{2,1,0:T(8,128)(2,1)}, bf16[3,256,256]{2,1,0:T(8,128)(2,1)}, u32[]{:S(2)}, u32[]{:S(2)}) collective-permute-start(bf16[3,256,256]{2,1,0:T(8,128)(2,1)} %collective-permute-done.13.refs_6_.refs_8_), channel_id=1, source_target_pairs={{0,1},{1,0},{2,3},{3,2},{4,5},{5,4},{6,7},{7,6},{8,9},{9,8},{10,11... | collective-permute-start | bytes 1179656 | tf_op jit(solution)/shard_map/ppermute | solution.py:24
  113.9 39.4 %all-to-all-start.4 = ((bf16[4,240,512]{2,1,0:T(8,128)(2,1)}), bf16[4,240,512]{2,1,0:T(8,128)(2,1)S(1)}, u32[]{:S(2)}, u32[]{:S(2)}) async-start(bf16[4,240,512]{2,1,0:T(8,128)(2,1)} %shard_map.234), calls=%async_computation.4 | async-start | bytes 1966080 | tf_op jit(solution)/shard_map/all_to_all | solution.py:20
  123.7 11.8 %collective-permute-start.18 = (bf16[48,2176]{1,0:T(8,128)(2,1)S(1)}, bf16[48,2176]{1,0:T(8,128)(2,1)S(1)}, u32[]{:S(2)}, u32[]{:S(2)}) collective-permute-start(bf16[48,2176]{1,0:T(8,128)(2,1)S(1)} %get-tuple-element.38), channel_id=1, source_target_pairs={{0,2},{2,4},{4,6},{6,0},{1,3},{3,5},{5,7},{7,1},{8,10},{10,12},{12... | collective-permute-start | bytes 626696 | tf_op jit(solution)/shard_map/ppermute | solution.py:29
  125.3 12.3 %collective-permute-start.19 = (bf16[48,2176]{1,0:T(8,128)(2,1)S(1)}, bf16[48,2176]{1,0:T(8,128)(2,1)S(1)}, u32[]{:S(2)}, u32[]{:S(2)}) collective-permute-start(bf16[48,2176]{1,0:T(8,128)(2,1)S(1)} %get-tuple-element.39), channel_id=1, source_target_pairs={{0,4},{2,6},{4,0},{6,2},{1,5},{3,7},{5,1},{7,3},{8,12},{10,14},{12... | collective-permute-start | bytes 626696 | tf_op jit(solution)/shard_map/ppermute | solution.py:29
  126.0 15.2 %collective-permute-start.20 = (bf16[48,2176]{1,0:T(8,128)(2,1)}, bf16[48,2176]{1,0:T(8,128)(2,1)S(1)}, u32[]{:S(2)}, u32[]{:S(2)}) collective-permute-start(bf16[48,2176]{1,0:T(8,128)(2,1)} %get-tuple-element.40), channel_id=1, source_target_pairs={{0,6},{2,0},{4,2},{6,4},{1,7},{3,1},{5,3},{7,5},{8,14},{10,8},{12,... | collective-permute-start | bytes 626696 | tf_op jit(solution)/shard_map/ppermute | solution.py:29
  141.8 5.1 %collective-permute-start.21 = (bf16[48,1024]{1,0:T(8,128)(2,1)S(1)}, bf16[48,1024]{1,0:T(8,128)(2,1)S(1)}, u32[]{:S(2)}, u32[]{:S(2)}) collective-permute-start(bf16[48,1024]{1,0:T(8,128)(2,1)S(1)} %shard_map.236.refs_1_), channel_id=1, source_target_pairs={{0,2},{2,4},{4,6},{6,0},{1,3},{3,5},{5,7},{7,1},{8,10},{10,12},{12... | collective-permute-start | bytes 294920 | tf_op jit(solution)/shard_map/ppermute | solution.py:29
  142.5 6.8 %collective-permute-start.22 = (bf16[48,1024]{1,0:T(8,128)(2,1)S(1)}, bf16[48,1024]{1,0:T(8,128)(2,1)S(1)}, u32[]{:S(2)}, u32[]{:S(2)}) collective-permute-start(bf16[48,1024]{1,0:T(8,128)(2,1)S(1)} %shard_map.236.refs_1_), channel_id=1, source_target_pairs={{0,4},{2,6},{4,0},{6,2},{1,5},{3,7},{5,1},{7,3},{8,12},{10,14},{12... | collective-permute-start | bytes 294920 | tf_op jit(solution)/shard_map/ppermute | solution.py:29
  145.5 4.8 %collective-permute-start.23 = (bf16[48,1024]{1,0:T(8,128)(2,1)S(1)}, bf16[48,1024]{1,0:T(8,128)(2,1)S(1)}, u32[]{:S(2)}, u32[]{:S(2)}) collective-permute-start(bf16[48,1024]{1,0:T(8,128)(2,1)S(1)} %shard_map.236.refs_1_), channel_id=1, source_target_pairs={{0,6},{2,0},{4,2},{6,4},{1,7},{3,1},{5,3},{7,5},{8,14},{10,8},{12,... | collective-permute-start | bytes 294920 | tf_op jit(solution)/shard_map/ppermute | solution.py:29
  157.3 20.8 %all-to-all-start.5 = ((bf16[64,24,128]{2,1,0:T(8,128)(2,1)}), bf16[64,24,128]{2,1,0:T(8,128)(2,1)S(1)}, u32[]{:S(2)}, u32[]{:S(2)}) async-start(bf16[64,24,128]{2,1,0:T(8,128)(2,1)} %bitcast.16), calls=%async_computation.5 | async-start | bytes 786432 | tf_op jit(solution)/shard_map/all_to_all | solution.py:20
  163.3 5.2 %collective-permute-start.24 = (bf16[48,256]{1,0:T(8,128)(2,1)S(1)}, bf16[48,256]{1,0:T(8,128)(2,1)S(1)}, u32[]{:S(2)}, u32[]{:S(2)}) collective-permute-start(bf16[48,256]{1,0:T(8,128)(2,1)S(1)} %get-tuple-element.44), channel_id=1, source_target_pairs={{0,1},{1,0},{2,3},{3,2},{4,5},{5,4},{6,7},{7,6},{8,9},{9,8},{10,11... | collective-permute-start | bytes 73736 | tf_op jit(solution)/shard_map/ppermute | solution.py:24
  (12 other events, 273.4 us)

commit v9 on v8

--- a/solution.py
+++ b/solution.py
@@ -41,18 +41,21 @@
     return x * jax.nn.sigmoid(x)
 
 
-def call(body, outs, flops, kinds, *args, mib=53, scratch=()):
+def call(body, outs, flops, kinds, *args, mib=52, scratch=()):
     kinds, out_kinds = kinds.split()
     moved = sum(a.size * a.dtype.itemsize for a in args) + sum(
         o.size * o.dtype.itemsize for o in outs
     )
     space = {"s": pltpu.SMEM, "v": pltpu.VMEM}
-    fetched = [i for i, k in enumerate(kinds) if k in "hlqe"]
+    fetched = [i for i, k in enumerate(kinds) if k in "hlqegd"]
     stored = [i for i, k in enumerate(out_kinds) if k == "h"]
-    room = [
-        pltpu.VMEM(args[i].shape[1 if kinds[i] == "e" else 0 :], args[i].dtype) for i in fetched
-    ]
-    pieces = {"h": 1, "l": 1, "q": 4, "e": 4}
+
+    def held(i):
+        shape = args[i].shape
+        return {"e": shape[1:], "d": shape[1:], "g": (2, *shape[1:])}.get(kinds[i], shape)
+
+    room = [pltpu.VMEM(held(i), args[i].dtype) for i in fetched]
+    pieces = {"h": 1, "l": 1, "q": 4, "e": 4, "g": 1, "d": 1}
     n_sems = sum(pieces[kinds[i]] for i in fetched)
     out_room = [pltpu.VMEM(outs[i].shape, outs[i].dtype) for i in stored]
 
@@ -66,7 +69,11 @@
         sem = 0
         for n, i in enumerate(fetched):
             kind = kinds[i]
-            source = ins[i].at[ins[0][1]] if kind == "e" else ins[i]
+            source = ins[i]
+            if kind == "e":
+                source = source.at[ins[0][1]]
+            elif kind == "d":
+                source = source.at[2]
             parts = pieces[kind]
             size = in_room[n].shape[0] // parts
             copies = []
@@ -123,15 +130,18 @@
     return jax.ShapeDtypeStruct(dims, dtype)
 
 
-def prepare(at, tokens, gain, wq, wf, wi, wo, dg, du, dd, spread_w, dense, t0, t1, t2, t3, held):
-    x = at[2]
-    for i, block in enumerate((dg, du, dd)):
-        dense[i] = block[...]
+def copies(wq, wf, wi, wo, spread_w):
     for i, block in enumerate((wq, wf, wi, wo)):
         width = block.shape[1]
         value = block[...]
         for z in range(spread_w.shape[0]):
             spread_w[z, :, i * width : (i + 1) * width] = value
+
+
+def prepare(at, tokens, gain, dg, du, dd, dense, t0, t1, t2, t3, held):
+    x = at[2]
+    for i, block in enumerate((dg, du, dd)):
+        dense[i] = block[...]
     wide = tokens[...].astype(F32)
     wide = wide * lax.rsqrt(jnp.mean(wide * wide, axis=1, keepdims=True) + EPS) * gain[...]
     low = lax.broadcasted_iota(jnp.int32, (wide.shape[0], 128), 1) < 64
@@ -298,44 +308,9 @@
         outs[d][:, 8 * cols : 8 * cols + 128] = both[d * size : (d + 1) * size]
 
 
-def dense_activation(a, b, c, d, out):
-    width = out.shape[1]
-    features = 2048
-
-    def summed(cut):
-        return (
-            a[:, cut].astype(F32) + b[:, cut].astype(F32) + c[:, cut].astype(F32) + d[:, cut].astype(F32)
-        )
-
-    square = summed(slice(2 * width, 2 * width + 128))
-    total = square[:, 0:1] + square[:, 64:65]
-    scale = lax.rsqrt(total / features + EPS)
-    gate = summed(slice(0, width)) * scale
-    up = summed(slice(width, 2 * width)) * scale
-    out[...] = (silu(gate) * up).astype(BF)
-
-
-def dense_second_half(wait, at, *refs):
-    y = at[0]
-    hidden, own_w, other_w, out = refs[:4], refs[4:8], refs[8:12], refs[12]
-    ny = len(hidden)
-    size, cols = hidden[0].shape[0], out.shape[2]
-    rows = jnp.concatenate([h[...] for h in hidden], axis=0)
-    for side, weights in enumerate((own_w, other_w)):
-        total = None
-        for i in range(4):
-            wait[4 * side + i][0]()
-            term = dot(rows[:, i * cols : (i + 1) * cols], weights[i][2])
-            total = term if total is None else total + term
-        total = total.astype(BF)
-        for d in range(ny):
-            start = pl.multiple_of(lax.rem(y + ny - d, ny) * size, size)
-            out[side, pl.ds(start, size), :] = total[d * size : (d + 1) * size]
-
-
 def experts_and_shared(
     wait, at, whole, gain, gate, gate_other, up, up_other, down, down_other,
-    shared_gate, shared_up, shared_down, parts,
+    shared_gate, shared_up, shared_down, p0, p1, p2, p3, parts,
 ):
     ny, lines, block = whole.shape
     count = lines - 48
@@ -370,30 +345,63 @@
         cut = slice(i * block, (i + 1) * block)
         downs = jnp.concatenate([down[:, cut], down_other[:, cut]], axis=0)
         parts[i, :count, :] = dot(hidden, downs).astype(BF)
-        parts[i, count:, :] = dot(shared_hidden, shared_down[:, cut]).astype(BF)
-
-
-def pack_lines(at, line_of, parts, dense, lines, shared_own, shared_send):
+        parts[i, count:lines, :] = dot(shared_hidden, shared_down[:, cut]).astype(BF)
+
+    width = 2 * block
+
+    def summed(at_col, size):
+        part = slice(at_col, at_col + size)
+        return sum(p[:, part].astype(F32) for p in (p0, p1, p2, p3))
+
+    tail = summed(2 * width, 128)
+    dense_scale = lax.rsqrt((tail[:, 0:1] + tail[:, 64:65]) / (ny * block) + EPS)
+    for j in range(2):
+        dense_gate = summed(j * block, block) * dense_scale
+        dense_up = summed(width + j * block, block) * dense_scale
+        dense_hidden = (silu(dense_gate) * dense_up).astype(BF)
+        start = lines + j * p0.shape[0]
+        for i in range(ny):
+            parts[i, start : start + p0.shape[0], :] = dense_hidden
+
+
+def pack_lines(wait, at, line_of, parts, *refs):
+    own_w, other_w, (lines, shared_own, shared_send) = refs[:4], refs[4:8], refs[8:]
     first = at[1] == 0
     group = line_of.shape[0]
     part = group // 8
-    cols = dense.shape[2]
+    groups = lines.shape[0] // group
+    count = part * groups
+    cols = shared_own.shape[1]
     half = cols // 2
-    count = dense.shape[1]
-    groups = lines.shape[0] // group
+    seq = shared_own.shape[0]
     move = jnp.where(
         lax.broadcasted_iota(jnp.int32, (group, group), 1) == line_of[...], 1.0, 0.0
     ).astype(BF)
-    total = parts[0].astype(F32)
-    for i in range(1, parts.shape[0]):
-        total = total + parts[i].astype(F32)
+    ny = parts.shape[0]
+    total = parts[0, : count + seq].astype(F32)
+    for i in range(1, ny):
+        total = total + parts[i, : count + seq].astype(F32)
     routed = total[:count].astype(BF)
     shared = total[count:]
     shared_own[...] = jnp.where(first, shared[:, :cols], shared[:, cols:])
     shared_send[...] = jnp.where(first, shared[:, cols:], shared[:, :cols]).astype(BF)
+    size = count // ny
+    hidden = [
+        jnp.concatenate([parts[i, start : start + size, :] for i in range(ny)], axis=0)
+        for start in (count + seq, count + seq + size)
+    ]
+    dense = []
+    for side, weights in enumerate((own_w, other_w)):
+        value = None
+        for i in range(4):
+            wait[4 * side + i][0]()
+            at_col = i % 2 * cols
+            term = dot(hidden[i // 2][:, at_col : at_col + cols], weights[i][...])
+            value = term if value is None else value + term
+        dense.append(value.astype(BF))
     for g in range(groups):
         here = slice(g * part, (g + 1) * part)
-        own, other = dense[0, here, :], dense[1, here, :]
+        own, other = dense[0][here], dense[1][here]
         sides = [jnp.where(first, own, other), jnp.where(first, other, own)]
         stack = []
         for side in range(2):
@@ -456,26 +464,31 @@
     slot_rows = slot_cols.T
     within = (jnp.arange(experts * 2 * slots, dtype=jnp.int32) % (nx * nc * 2 * slots))[None, :]
 
-    spread_w, dense_block, *columns = call(
-        prepare,
-        [shaped(nz, rows_w, 4 * chan), shaped(3, *dense_gate.shape)]
-        + [shaped(seq, nz * rows_w)] * nx,
+    (spread_w,) = call(
+        copies,
+        [shaped(nz, rows_w, 4 * chan)],
         10**6,
-        "shhhhhhhhh hhhhhh",
-        at,
-        tokens,
-        norm_gain.reshape(1, width),
+        "hhhh h",
         w_query,
         w_forget,
         w_input,
         w_outgate,
+        mib=58,
+    )
+    weights = swap(spread_w, "z").reshape(nz * rows_w, 4 * chan)
+    dense_block, *columns = call(
+        prepare,
+        [shaped(3, *dense_gate.shape)] + [shaped(seq, nz * rows_w)] * nx,
+        10**6,
+        "shhhhh hhhhh",
+        at,
+        tokens,
+        norm_gain.reshape(1, width),
         dense_gate,
         dense_up,
         dense_down,
-        mib=58,
         scratch=[pltpu.VMEM((nx, seq, nz * rows_w), BF)],
     )
-    weights = swap(spread_w, "z").reshape(nz * rows_w, 4 * chan)
     mine = [columns[0]] + [shift(columns[d], "x", d) for d in range(1, nx)]
     part = dot(jnp.concatenate(mine, axis=0), weights).astype(BF)
     part = part.reshape(nx, seq, 4 * chan)
@@ -555,7 +568,7 @@
         dense_first_half,
         [shaped(quarter, 2 * hidden_width + 128)] * ny,
         2 * count * nc * cols * 2 * hidden_width,
-        "shhllllllll hhhh",
+        "shhgggggggg hhhh",
         at,
         dense_rows,
         ffn_gain.reshape(ny * nc, cols),
@@ -563,26 +576,11 @@
         *dense_other,
     )
     pre = [pre[0]] + [shift(pre[d], "y", d) for d in range(1, ny)]
-    (hidden,) = call(
-        dense_activation, [shaped(quarter, hidden_width)], 10**6, "hvvv h", *pre
-    )
-    hidden = [hidden] + [shift(hidden, "y", d) for d in range(1, ny)]
-    (dense_part,) = call(
-        dense_second_half,
-        [shaped(nc, count, cols)],
-        2 * count * nc * cols * hidden_width,
-        "shvvvllllllll h",
-        at,
-        *hidden,
-        *dense_own,
-        *dense_other,
-    )
-
     (parts,) = call(
         experts_and_shared,
-        [shaped(ny, count + seq, nc * cols)],
+        [shaped(ny, count + seq + 2 * quarter, nc * cols)],
         2 * 3 * (count * 2 + seq) * width * expert_gate.shape[2],
-        "sqheqeqeqqqq h",
+        "sqheqeqeqqqqhvvv h",
         at,
         whole,
         ffn_gain.reshape(1, width),
@@ -595,6 +593,7 @@
         shared_gate,
         shared_up,
         shared_down,
+        *pre,
     )
     parts = swap(parts, "y")
     back, shared_own, shared_send = call(
@@ -605,11 +604,12 @@
             shaped(seq, cols),
         ],
         4 * 2 * group * group * half,
-        "shvh hhh",
+        "shvdddddddd hhh",
         at,
         line_of.reshape(group, 1),
         parts,
-        dense_part,
+        *dense_own,
+        *dense_other,
     )
 
     results = swap(back.reshape(experts, 2 * slots, half), HUB)

time: 182 us -> 181 us (level)
  waiting for transfers between devices: 72.4 us -> 66.1 us
  local copies, waits for them, and re-layouts: 6.34 us -> 11.6 us
    ppermute x15 -> x12, waiting for transfers between devices: 38.1 us -> 31.9 us  [shift(): return lax.ppermute(x, axis, [(i, (i + by) % size) for i in range(size)])]
    all_to_all x6, starting transfers between devices: 33.6 us -> 38.8 us  [swap(): return lax.all_to_all(x, axis, split_axis=0, concat_axis=0, tiled=True)]
    ppermute x15 -> x12, starting transfers between devices: 24.7 us -> 20.8 us  [shift(): return lax.ppermute(x, axis, [(i, (i + by) % size) for i in range(size)])]
    unnamed x28 -> x36, local copies, waits for them, and re-layouts: 2.94 us -> 6.32 us
    squeeze x3, local copies, waits for them, and re-layouts: 2.75 us -> 4.61 us  [pick(): return lax.dynamic_index_in_dim(x, index, 0, keepdims=False)]
    pallas_call x10 -> x9, Pallas kernels: 30.3 us -> 28.6 us  [call(): pl.pallas_call(whole, out_shape=outs, in_specs=[pl.BlockSpec(memory_space...]
  transfers between devices with their start and end apart: 31 -> 28, of which waited for: 18 -> 14; matrix products, arithmetic and copies ran while one was open for 6% -> 8% of each run, Pallas kernels for 9% -> 5%
where the time goes in v9:
time: 181 us; the launch traced here: 177 us
  waiting for transfers between devices  66.1 us (37%)
  starting transfers between devices  61.5 us (34%)
  Pallas kernels  28.6 us (16%)
  local copies, waits for them, and re-layouts  11.6 us (6%)
  other arithmetic  8.17 us (5%)
    all_to_all x6, starting transfers between devices, swap(): return lax.all_to_all(x, axis, split_axis=0, concat_axis=0, tiled=True)  38.8 us
    all_to_all x6, waiting for transfers between devices, swap(): return lax.all_to_all(x, axis, split_axis=0, concat_axis=0, tiled=True)  32.9 us
    ppermute x12, waiting for transfers between devices, shift(): return lax.ppermute(x, axis, [(i, (i + by) % size) for i in range(size)])  31.9 us
    pallas_call x9, Pallas kernels, call(): pl.pallas_call(whole, out_shape=outs, in_specs=[pl.BlockSpec(memory_space...  28.6 us
    ppermute x12, starting transfers between devices, shift(): return lax.ppermute(x, axis, [(i, (i + by) % size) for i in range(size)])  20.8 us
    unnamed x36, local copies, waits for them, and re-layouts  6.32 us
    add x1, other arithmetic, step(): decay.reshape(shape)[..., None] * state  5.07 us
    squeeze x3, local copies, waits for them, and re-layouts, pick(): return lax.dynamic_index_in_dim(x, index, 0, keepdims=False)  4.61 us
  transfers between devices with their start and end apart: 28, of which 14 were waited for; matrix products, arithmetic and copies ran while one was open for 8% of the time, Pallas kernels for 5%

profile of v9, /device:TPU:8, one launch (start us, length us, event | category | flops | bytes accessed | tf_op | source)
XLA Modules:
  0.0 177.2 jit_solution(7759021635699898779)
XLA Ops:
  0.7 1.7 shard_map.231
  2.4 8.5 %all-to-all-start = ((bf16[8,64,512]{2,1,0:T(8,128)(2,1)}), bf16[8,64,512]{2,1,0:T(8,128)(2,1)S(1)}, u32[]{:S(2)}, u32[]{:S(2)}) async-start(bf16[8,64,512]{2,1,0:T(8,128)(2,1)} %shard_map.231), calls=%async_computation | async-start | bytes 1048576 | tf_op jit(solution)/shard_map/all_to_all | solution.py:20
  15.3 2.1 %shard_map.230 = (bf16[3,256,256]{2,1,0:T(8,128)(2,1)S(1)}, bf16[48,512]{1,0:T(8,128)(2,1)S(1)}, bf16[48,512]{1,0:T(8,128)(2,1)S(1)}, bf16[48,512]{1,0:T(8,128)(2,1)S(1)}, bf16[48,512]{1,0:T(8,128)(2,1)S(1)}) custom-call(s32[3]{0:T(128)S(1)} %pad_add_fusion.refs_0_, bf16[48,2048]{1,0:T(8,128)(2,1)S(1)} %copy-done.2, f32[1,2048]{1,0:T(1,128)S(1)} %bitcast.38, ...), custom_call_target="tpu_custom_call" | custom-call | flops 1000000 | bytes 1187852 | tf_op jit(solution)/shard_map/pallas_call | solution.py:112
  19.0 2.7 %collective-permute-start.1 = (bf16[48,512]{1,0:T(8,128)(2,1)S(1)}, bf16[48,512]{1,0:T(8,128)(2,1)S(1)}, u32[]{:S(2)}, u32[]{:S(2)}) collective-permute-start(bf16[48,512]{1,0:T(8,128)(2,1)S(1)} %get-tuple-element.26), channel_id=1, source_target_pairs={{0,16},{8,24},{16,0},{24,8},{1,17},{9,25},{17,1},{25,9},{2,18},{10... | collective-permute-start | bytes 147464 | tf_op jit(solution)/shard_map/ppermute | solution.py:29
  25.8 2.5 %all-to-all-done = bf16[8,64,512]{2,1,0:T(8,128)(2,1)S(1)} async-done(((bf16[8,64,512]{2,1,0:T(8,128)(2,1)}), bf16[8,64,512]{2,1,0:T(8,128)(2,1)S(1)}, u32[]{:S(2)}, u32[]{:S(2)}) %all-to-all-start) | async-done | bytes 524320 | tf_op jit(solution)/shard_map/all_to_all | solution.py:20
  28.7 2.8 %collective-permute-start.3 = (bf16[48,512]{1,0:T(8,128)(2,1)S(1)}, bf16[48,512]{1,0:T(8,128)(2,1)S(1)}, u32[]{:S(2)}, u32[]{:S(2)}) collective-permute-start(bf16[48,512]{1,0:T(8,128)(2,1)S(1)} %get-tuple-element.48), channel_id=1, source_target_pairs={{0,24},{8,0},{16,8},{24,16},{1,25},{9,1},{17,9},{25,17},{2,26},{10... | collective-permute-start | bytes 147464 | tf_op jit(solution)/shard_map/ppermute | solution.py:29
  33.6 3.5 %collective-permute-done.4.refs_3_ = bf16[48,512]{1,0:T(8,128)(2,1)S(1)} collective-permute-done((bf16[48,512]{1,0:T(8,128)(2,1)S(1)}, bf16[48,512]{1,0:T(8,128)(2,1)S(1)}, u32[]{:S(2)}, u32[]{:S(2)}) %collective-permute-start.4) | collective-permute-done | bytes 49184 | tf_op jit(solution)/shard_map/ppermute | solution.py:29
  37.7 3.6 %shard_map.232 = (f32[48,128]{1,0:T(8,128)S(1)}, f32[48,128]{1,0:T(8,128)S(1)}, f32[48,128]{1,0:T(8,128)S(1)}, bf16[4,48,256]{2,1,0:T(8,128)(2,1)S(1)}, bf16[4,48,256]{2,1,0:T(8,128)(2,1)S(1)}) custom-call(s32[3]{0:T(128)S(1)} %pad_add_fusion.refs_0_, bf16[48,512]{1,0:T(8,128)(2,1)S(1)} %get-tuple-element.49.refs_1_, ...), custom_call_target="tpu_custom_call" | custom-call | flops 3145728 | bytes 4137996 | tf_op jit(solution)/shard_map/pallas_call | solution.py:112
  43.3 4.9 %all-to-all-start.1 = ((bf16[4,48,256]{2,1,0:T(8,128)(2,1)}), bf16[4,48,256]{2,1,0:T(8,128)(2,1)S(1)}, u32[]{:S(2)}, u32[]{:S(2)}) async-start(bf16[4,48,256]{2,1,0:T(8,128)(2,1)} %add_convert_fusion), calls=%async_computation.1 | async-start | bytes 196608 | tf_op jit(solution)/shard_map/all_to_all | solution.py:20
  48.4 4.2 %all-to-all-done.1.refs_1_ = bf16[4,48,256]{2,1,0:T(8,128)(2,1)S(1)} async-done(((bf16[4,48,256]{2,1,0:T(8,128)(2,1)}), bf16[4,48,256]{2,1,0:T(8,128)(2,1)S(1)}, u32[]{:S(2)}, u32[]{:S(2)}) %all-to-all-start.1) | async-done | bytes 98336 | tf_op jit(solution)/shard_map/all_to_all | solution.py:20
  52.6 2.6 %shard_map.233 = (f32[48,256]{1,0:T(8,128)S(1)}, bf16[48,256]{1,0:T(8,128)(2,1)S(1)}, bf16[1536,128]{1,0:T(8,128)(2,1)}) custom-call(s32[3]{0:T(128)S(1)} %pad_add_fusion.refs_0_, bf16[4,48,256]{2,1,0:T(8,128)(2,1)S(1)} %all-to-all-done.1.refs_1_, bf16[48,2048]{1,0:T(8,128)(2,1)S(1)} %copy-done.3, s32[8,48]{1,0:T(8,128)S(1)} %copy.55.refs_3_), custom_call_target="tpu_custom_call" | custom-call | flops 37748736 | bytes 763404 | tf_op jit(solution)/shard_map/pallas_call | solution.py:112
  55.2 6.5 %all-to-all-start.2 = ((bf16[64,24,128]{2,1,0:T(8,128)(2,1)}), bf16[64,24,128]{2,1,0:T(8,128)(2,1)S(1)}, u32[]{:S(2)}, u32[]{:S(2)}) async-start(bf16[64,24,128]{2,1,0:T(8,128)(2,1)} %bitcast.10), calls=%async_computation.2 | async-start | bytes 786432 | tf_op jit(solution)/shard_map/all_to_all | solution.py:20
  61.8 1.6 collective-permute-start.11
  63.4 2.7 %collective-permute-start.12 = (bf16[3,256,256]{2,1,0:T(8,128)(2,1)S(1)}, bf16[3,256,256]{2,1,0:T(8,128)(2,1)S(1)}, u32[]{:S(2)}, u32[]{:S(2)}) collective-permute-start(bf16[3,256,256]{2,1,0:T(8,128)(2,1)S(1)} %get-tuple-element.34.refs_3_), channel_id=1, source_target_pairs={{0,16},{8,24},{16,0},{24,8},{1,17},{9,25},{17,1},{25,9},{2,18},{10... | collective-permute-start | bytes 1179656 | tf_op jit(solution)/shard_map/ppermute | solution.py:29
  67.5 1.9 %dynamic-slice_bitcast_fusion = bf16[128,2048]{1,0:T(8,128)(2,1)} fusion(bf16[2,128,2048]{2,1,0:T(8,128)(2,1)} %refs_7_.1, s32[]{:T(128)S(6)} %select_n.224), kind=kLoop, calls=%fused_computation.2 | loop fusion | bytes 1048580 | tf_op jit(solution)/shard_map/jit(dynamic_index_in_dim)/squeeze | solution.py:33
  69.4 9.0 %collective-permute-done.11.refs_4_ = bf16[3,256,256]{2,1,0:T(8,128)(2,1)S(1)} collective-permute-done((bf16[3,256,256]{2,1,0:T(8,128)(2,1)S(1)}, bf16[3,256,256]{2,1,0:T(8,128)(2,1)S(1)}, u32[]{:S(2)}, u32[]{:S(2)}) %collective-permute-start.11) | collective-permute-done | bytes 393248 | tf_op jit(solution)/shard_map/ppermute | solution.py:29
  79.8 7.4 %collective-permute-done.12.refs_5_ = bf16[3,256,256]{2,1,0:T(8,128)(2,1)S(1)} collective-permute-done((bf16[3,256,256]{2,1,0:T(8,128)(2,1)S(1)}, bf16[3,256,256]{2,1,0:T(8,128)(2,1)S(1)}, u32[]{:S(2)}, u32[]{:S(2)}) %collective-permute-start.12) | collective-permute-done | bytes 393248 | tf_op jit(solution)/shard_map/ppermute | solution.py:29
  87.9 2.0 %shard_map.234 = (bf16[4,240,512]{2,1,0:T(8,128)(2,1)}, bf16[2,192,256]{2,1,0:T(8,128)(2,1)S(1)}) custom-call(s32[3]{0:T(128)S(1)} %pad_add_fusion.refs_0_, s32[1,384]{1,0:T(1,128)S(1)} %fusion.53.refs_1_, bf16[1536,128]{1,0:T(8,128)(2,1)S(1)} %bitcast.36, bf16[48,256]{1,0:T(8,128)(2,1)S(1)} %get-tuple-element.31.refs_3_, ...), custom_call_target="tpu_custom_call" | custom-call | flops 150994944 | bytes 1623564 | tf_op jit(solution)/shard_map/pallas_call | solution.py:112
  89.9 5.7 %all-to-all-start.3 = ((bf16[4,240,512]{2,1,0:T(8,128)(2,1)}), bf16[4,240,512]{2,1,0:T(8,128)(2,1)}, u32[]{:S(2)}, u32[]{:S(2)}) async-start(bf16[4,240,512]{2,1,0:T(8,128)(2,1)} %get-tuple-element.32), calls=%async_computation.3 | async-start | bytes 1966080 | tf_op jit(solution)/shard_map/all_to_all | solution.py:20
  95.6 1.9 %dynamic-slice_bitcast_fusion.1 = bf16[2048,128]{1,0:T(8,128)(2,1)} fusion(bf16[2,2048,128]{2,1,0:T(8,128)(2,1)} %refs_5_.3, s32[]{:T(128)S(6)} %select_n.224), kind=kLoop, calls=%fused_computation.3 | loop fusion | bytes 1048580 | tf_op jit(solution)/shard_map/jit(dynamic_index_in_dim)/squeeze | solution.py:33
  98.0 4.2 %shard_map.235 = (bf16[48,2176]{1,0:T(8,128)(2,1)S(1)}, bf16[48,2176]{1,0:T(8,128)(2,1)S(1)}, bf16[48,2176]{1,0:T(8,128)(2,1)S(1)}, bf16[48,2176]{1,0:T(8,128)(2,1)S(1)}) custom-call(s32[3]{0:T(128)S(1)} %pad_add_fusion.refs_0_, bf16[2,192,256]{2,1,0:T(8,128)(2,1)S(1)} %get-tuple-element.33.refs_1_, f32[8,256]{1,0:T(8,128)S(1)} %reshape.582.refs_2_, ...), custom_call_target="tpu_custom_call" | custom-call | flops 402653184 | bytes 4186124 | tf_op jit(solution)/shard_map/pallas_call | solution.py:112
  104.5 2.5 %collective-permute-start.20 = (bf16[48,2176]{1,0:T(8,128)(2,1)S(1)}, bf16[48,2176]{1,0:T(8,128)(2,1)S(1)}, u32[]{:S(2)}, u32[]{:S(2)}) collective-permute-start(bf16[48,2176]{1,0:T(8,128)(2,1)S(1)} %get-tuple-element.38), channel_id=1, source_target_pairs={{0,6},{2,0},{4,2},{6,4},{1,7},{3,1},{5,3},{7,5},{8,14},{10,8},{12,... | collective-permute-start | bytes 626696 | tf_op jit(solution)/shard_map/ppermute | solution.py:29
  107.1 5.3 %collective-permute-done.18.refs_13_ = bf16[48,2176]{1,0:T(8,128)(2,1)S(1)} collective-permute-done((bf16[48,2176]{1,0:T(8,128)(2,1)S(1)}, bf16[48,2176]{1,0:T(8,128)(2,1)S(1)}, u32[]{:S(2)}, u32[]{:S(2)}) %collective-permute-start.18) | collective-permute-done | bytes 208928 | tf_op jit(solution)/shard_map/ppermute | solution.py:29
  112.4 2.0 %collective-permute-done.19.refs_14_ = bf16[48,2176]{1,0:T(8,128)(2,1)S(1)} collective-permute-done((bf16[48,2176]{1,0:T(8,128)(2,1)S(1)}, bf16[48,2176]{1,0:T(8,128)(2,1)S(1)}, u32[]{:S(2)}, u32[]{:S(2)}) %collective-permute-start.19) | collective-permute-done | bytes 208928 | tf_op jit(solution)/shard_map/ppermute | solution.py:29
  114.4 3.9 %collective-permute-done.20.refs_15_ = bf16[48,2176]{1,0:T(8,128)(2,1)S(1)} collective-permute-done((bf16[48,2176]{1,0:T(8,128)(2,1)S(1)}, bf16[48,2176]{1,0:T(8,128)(2,1)S(1)}, u32[]{:S(2)}, u32[]{:S(2)}) %collective-permute-start.20) | collective-permute-done | bytes 208928 | tf_op jit(solution)/shard_map/ppermute | solution.py:29
  118.3 5.9 %shard_map.236 = bf16[4,336,512]{2,1,0:T(8,128)(2,1)} custom-call(s32[3]{0:T(128)S(1)} %pad_add_fusion.refs_0_, bf16[4,240,512]{2,1,0:T(8,128)(2,1)} %all-to-all-done.3.refs_1_, f32[1,2048]{1,0:T(1,128)S(1)} %bitcast.37, bf16[2,2048,128]{2,1,0:T(8,128)(2,1)} %refs_3_.6, bf16[2048,128]{1,0:T(8,128)(2,1)S(1)} %collective-permute-done.8.refs_4_, ...), custom_call_target="tpu_custom_call" | custom-call | flops 679477248 | bytes 9494540 | tf_op jit(solution)/shard_map/pallas_call | solution.py:112
  124.2 5.2 %all-to-all-start.4 = ((bf16[4,336,512]{2,1,0:T(8,128)(2,1)}), bf16[4,336,512]{2,1,0:T(8,128)(2,1)S(1)}, u32[]{:S(2)}, u32[]{:S(2)}) async-start(bf16[4,336,512]{2,1,0:T(8,128)(2,1)} %shard_map.236), calls=%async_computation.4 | async-start | bytes 2752512 | tf_op jit(solution)/shard_map/all_to_all | solution.py:20
  130.1 16.4 %all-to-all-done.4.refs_2_ = bf16[4,336,512]{2,1,0:T(8,128)(2,1)S(1)} async-done(((bf16[4,336,512]{2,1,0:T(8,128)(2,1)}), bf16[4,336,512]{2,1,0:T(8,128)(2,1)S(1)}, u32[]{:S(2)}, u32[]{:S(2)}) %all-to-all-start.4) | async-done | bytes 1376288 | tf_op jit(solution)/shard_map/all_to_all | solution.py:20
  147.6 4.9 %shard_map.237 = (bf16[1536,128]{1,0:T(8,128)(2,1)}, f32[48,256]{1,0:T(8,128)S(1)}, bf16[48,256]{1,0:T(8,128)(2,1)S(1)}) custom-call(s32[3]{0:T(128)S(1)} %pad_add_fusion.refs_0_, s32[384,1]{1,0:T(8,128)S(1)} %fusion.8.refs_1_, bf16[4,336,512]{2,1,0:T(8,128)(2,1)} %copy-done.13, bf16[3,256,256]{2,1,0:T(8,128)(2,1)S(1)} %get-tuple-element.34.refs_3_, ...), custom_call_target="tpu_custom_call" | custom-call | flops 150994944 | bytes 4990476 | tf_op jit(solution)/shard_map/pallas_call | solution.py:112
  152.5 8.1 %all-to-all-start.5 = ((bf16[64,24,128]{2,1,0:T(8,128)(2,1)}), bf16[64,24,128]{2,1,0:T(8,128)(2,1)S(1)}, u32[]{:S(2)}, u32[]{:S(2)}) async-start(bf16[64,24,128]{2,1,0:T(8,128)(2,1)} %bitcast.16), calls=%async_computation.5 | async-start | bytes 786432 | tf_op jit(solution)/shard_map/all_to_all | solution.py:20
  160.9 5.1 %multiply_add_fusion = f32[48,1,128,128]{3,2,1,0:T(8,128)} fusion(f32[48,1,128,128]{3,2,1,0:T(8,128)} %param.24, f32[48,128]{1,0:T(8,128)S(1)} %get-tuple-element.45, f32[48,128]{1,0:T(8,128)S(1)} %get-tuple-element.44, f32[48,128]{1,0:T(8,128)S(1)} %get-tuple-element.43), kind=kLoop, calls=%fused_computation | loop fusion | flops 2359296 | bytes 6365184 | tf_op jit(solution)/shard_map/add | solution.py:518
  165.9 9.7 %all-to-all-done.5 = bf16[64,24,128]{2,1,0:T(8,128)(2,1)S(1)} async-done(((bf16[64,24,128]{2,1,0:T(8,128)(2,1)}), bf16[64,24,128]{2,1,0:T(8,128)(2,1)S(1)}, u32[]{:S(2)}, u32[]{:S(2)}) %all-to-all-start.5) | async-done | bytes 393248 | tf_op jit(solution)/shard_map/all_to_all | solution.py:20
  (100 shorter events, 24.8 us)
Async XLA Ops:
  0.6 37.0 %copy-start.11 = (f32[128]{0:T(128)S(1)}, f32[128]{0:T(128)}, u32[]{:S(2)}) copy-start(f32[128]{0:T(128)} %param.30) | copy-start | bytes 1540
  0.6 37.0 %copy-start.12 = (f32[128]{0:T(128)S(1)}, f32[128]{0:T(128)}, u32[]{:S(2)}) copy-start(f32[128]{0:T(128)} %param.31) | copy-start | bytes 1540
  2.4 26.0 %all-to-all-start = ((bf16[8,64,512]{2,1,0:T(8,128)(2,1)}), bf16[8,64,512]{2,1,0:T(8,128)(2,1)S(1)}, u32[]{:S(2)}, u32[]{:S(2)}) async-start(bf16[8,64,512]{2,1,0:T(8,128)(2,1)} %shard_map.231), calls=%async_computation | async-start | bytes 1048576 | tf_op jit(solution)/shard_map/all_to_all | solution.py:20
  17.4 8.3 %collective-permute-start = (bf16[48,512]{1,0:T(8,128)(2,1)S(1)}, bf16[48,512]{1,0:T(8,128)(2,1)S(1)}, u32[]{:S(2)}, u32[]{:S(2)}) collective-permute-start(bf16[48,512]{1,0:T(8,128)(2,1)S(1)} %get-tuple-element.25), channel_id=1, source_target_pairs={{0,8},{8,16},{16,24},{24,0},{1,9},{9,17},{17,25},{25,1},{2,10},{10... | collective-permute-start | bytes 147464 | tf_op jit(solution)/shard_map/ppermute | solution.py:29
  19.0 6.7 %collective-permute-start.1 = (bf16[48,512]{1,0:T(8,128)(2,1)S(1)}, bf16[48,512]{1,0:T(8,128)(2,1)S(1)}, u32[]{:S(2)}, u32[]{:S(2)}) collective-permute-start(bf16[48,512]{1,0:T(8,128)(2,1)S(1)} %get-tuple-element.26), channel_id=1, source_target_pairs={{0,16},{8,24},{16,0},{24,8},{1,17},{9,25},{17,1},{25,9},{2,18},{10... | collective-permute-start | bytes 147464 | tf_op jit(solution)/shard_map/ppermute | solution.py:29
  21.8 4.1 %collective-permute-start.2 = (bf16[48,512]{1,0:T(8,128)(2,1)S(1)}, bf16[48,512]{1,0:T(8,128)(2,1)S(1)}, u32[]{:S(2)}, u32[]{:S(2)}) collective-permute-start(bf16[48,512]{1,0:T(8,128)(2,1)S(1)} %get-tuple-element.27), channel_id=1, source_target_pairs={{0,24},{8,0},{16,8},{24,16},{1,25},{9,1},{17,9},{25,17},{2,26},{10... | collective-permute-start | bytes 147464 | tf_op jit(solution)/shard_map/ppermute | solution.py:29
  28.7 4.9 %collective-permute-start.3 = (bf16[48,512]{1,0:T(8,128)(2,1)S(1)}, bf16[48,512]{1,0:T(8,128)(2,1)S(1)}, u32[]{:S(2)}, u32[]{:S(2)}) collective-permute-start(bf16[48,512]{1,0:T(8,128)(2,1)S(1)} %get-tuple-element.48), channel_id=1, source_target_pairs={{0,24},{8,0},{16,8},{24,16},{1,25},{9,1},{17,9},{25,17},{2,26},{10... | collective-permute-start | bytes 147464 | tf_op jit(solution)/shard_map/ppermute | solution.py:29
  31.5 5.6 %collective-permute-start.4 = (bf16[48,512]{1,0:T(8,128)(2,1)S(1)}, bf16[48,512]{1,0:T(8,128)(2,1)S(1)}, u32[]{:S(2)}, u32[]{:S(2)}) collective-permute-start(bf16[48,512]{1,0:T(8,128)(2,1)S(1)} %get-tuple-element.47), channel_id=1, source_target_pairs={{0,16},{8,24},{16,0},{24,8},{1,17},{9,25},{17,1},{25,9},{2,18},{10... | collective-permute-start | bytes 147464 | tf_op jit(solution)/shard_map/ppermute | solution.py:29
  32.3 5.3 %collective-permute-start.5 = (bf16[48,512]{1,0:T(8,128)(2,1)S(1)}, bf16[48,512]{1,0:T(8,128)(2,1)S(1)}, u32[]{:S(2)}, u32[]{:S(2)}) collective-permute-start(bf16[48,512]{1,0:T(8,128)(2,1)S(1)} %get-tuple-element.46), channel_id=1, source_target_pairs={{0,8},{8,16},{16,24},{24,0},{1,9},{9,17},{17,25},{25,1},{2,10},{10... | collective-permute-start | bytes 147464 | tf_op jit(solution)/shard_map/ppermute | solution.py:29
  37.7 40.8 %copy-start.14 = (bf16[2,2048,128]{2,1,0:T(8,128)(2,1)S(1)}, bf16[2,2048,128]{2,1,0:T(8,128)(2,1)}, u32[]{:S(2)}) copy-start(bf16[2,2048,128]{2,1,0:T(8,128)(2,1)} %refs_3_.6) | copy-start | bytes 3145732
  41.3 1.4 collective-permute-start.6
  43.3 9.3 %all-to-all-start.1 = ((bf16[4,48,256]{2,1,0:T(8,128)(2,1)}), bf16[4,48,256]{2,1,0:T(8,128)(2,1)S(1)}, u32[]{:S(2)}, u32[]{:S(2)}) async-start(bf16[4,48,256]{2,1,0:T(8,128)(2,1)} %add_convert_fusion), calls=%async_computation.1 | async-start | bytes 196608 | tf_op jit(solution)/shard_map/all_to_all | solution.py:20
  55.2 42.7 %copy-start.8 = (f32[2048]{0:T(1024)S(1)}, f32[2048]{0:T(1024)}, u32[]{:S(2)}) copy-start(f32[2048]{0:T(1024)} %param.33) | copy-start | bytes 24580
  55.2 32.6 %all-to-all-start.2 = ((bf16[64,24,128]{2,1,0:T(8,128)(2,1)}), bf16[64,24,128]{2,1,0:T(8,128)(2,1)S(1)}, u32[]{:S(2)}, u32[]{:S(2)}) async-start(bf16[64,24,128]{2,1,0:T(8,128)(2,1)} %bitcast.10), calls=%async_computation.2 | async-start | bytes 786432 | tf_op jit(solution)/shard_map/all_to_all | solution.py:20
  61.8 16.6 %collective-permute-start.11 = (bf16[3,256,256]{2,1,0:T(8,128)(2,1)S(1)}, bf16[3,256,256]{2,1,0:T(8,128)(2,1)S(1)}, u32[]{:S(2)}, u32[]{:S(2)}) collective-permute-start(bf16[3,256,256]{2,1,0:T(8,128)(2,1)S(1)} %get-tuple-element.34.refs_3_), channel_id=1, source_target_pairs={{0,8},{8,16},{16,24},{24,0},{1,9},{9,17},{17,25},{25,1},{2,10},{10... | collective-permute-start | bytes 1179656 | tf_op jit(solution)/shard_map/ppermute | solution.py:29
  63.4 23.8 %collective-permute-start.12 = (bf16[3,256,256]{2,1,0:T(8,128)(2,1)S(1)}, bf16[3,256,256]{2,1,0:T(8,128)(2,1)S(1)}, u32[]{:S(2)}, u32[]{:S(2)}) collective-permute-start(bf16[3,256,256]{2,1,0:T(8,128)(2,1)S(1)} %get-tuple-element.34.refs_3_), channel_id=1, source_target_pairs={{0,16},{8,24},{16,0},{24,8},{1,17},{9,25},{17,1},{25,9},{2,18},{10... | collective-permute-start | bytes 1179656 | tf_op jit(solution)/shard_map/ppermute | solution.py:29
  66.1 21.2 %collective-permute-start.13 = (bf16[3,256,256]{2,1,0:T(8,128)(2,1)S(1)}, bf16[3,256,256]{2,1,0:T(8,128)(2,1)S(1)}, u32[]{:S(2)}, u32[]{:S(2)}) collective-permute-start(bf16[3,256,256]{2,1,0:T(8,128)(2,1)S(1)} %get-tuple-element.34.refs_3_), channel_id=1, source_target_pairs={{0,24},{8,0},{16,8},{24,16},{1,25},{9,1},{17,9},{25,17},{2,26},{10... | collective-permute-start | bytes 1179656 | tf_op jit(solution)/shard_map/ppermute | solution.py:29
  67.5 29.9 %collective-permute-start.14 = (bf16[3,256,256]{2,1,0:T(8,128)(2,1)S(1)}, bf16[3,256,256]{2,1,0:T(8,128)(2,1)}, u32[]{:S(2)}, u32[]{:S(2)}) collective-permute-start(bf16[3,256,256]{2,1,0:T(8,128)(2,1)S(1)} %get-tuple-element.34.refs_3_), channel_id=1, source_target_pairs={{0,1},{1,0},{2,3},{3,2},{4,5},{5,4},{6,7},{7,6},{8,9},{9,8},{10,11... | collective-permute-start | bytes 1179656 | tf_op jit(solution)/shard_map/ppermute | solution.py:24
  78.4 19.2 %collective-permute-start.15 = (bf16[3,256,256]{2,1,0:T(8,128)(2,1)S(1)}, bf16[3,256,256]{2,1,0:T(8,128)(2,1)}, u32[]{:S(2)}, u32[]{:S(2)}) collective-permute-start(bf16[3,256,256]{2,1,0:T(8,128)(2,1)S(1)} %collective-permute-done.11.refs_4_), channel_id=1, source_target_pairs={{0,1},{1,0},{2,3},{3,2},{4,5},{5,4},{6,7},{7,6},{8,9},{9,8},{10,11... | collective-permute-start | bytes 1179656 | tf_op jit(solution)/shard_map/ppermute | solution.py:24
  79.3 8.5 %collective-permute-start.7 = (bf16[48,256]{1,0:T(8,128)(2,1)S(1)}, bf16[48,256]{1,0:T(8,128)(2,1)S(1)}, u32[]{:S(2)}, u32[]{:S(2)}) collective-permute-start(bf16[48,256]{1,0:T(8,128)(2,1)S(1)} %get-tuple-element.31.refs_3_), channel_id=1, source_target_pairs={{0,1},{1,0},{2,3},{3,2},{4,5},{5,4},{6,7},{7,6},{8,9},{9,8},{10,11... | collective-permute-start | bytes 73736 | tf_op jit(solution)/shard_map/ppermute | solution.py:24
  87.2 17.3 %collective-permute-start.10 = (bf16[128,2048]{1,0:T(8,128)(2,1)}, bf16[128,2048]{1,0:T(8,128)(2,1)}, u32[]{:S(2)}, u32[]{:S(2)}) collective-permute-start(bf16[128,2048]{1,0:T(8,128)(2,1)} %dynamic-slice_bitcast_fusion), channel_id=1, source_target_pairs={{0,1},{1,0},{2,3},{3,2},{4,5},{5,4},{6,7},{7,6},{8,9},{9,8},{10,11... | collective-permute-start | bytes 1572872 | tf_op jit(solution)/shard_map/ppermute | solution.py:24
  87.3 10.7 %collective-permute-start.16 = (bf16[3,256,256]{2,1,0:T(8,128)(2,1)S(1)}, bf16[3,256,256]{2,1,0:T(8,128)(2,1)}, u32[]{:S(2)}, u32[]{:S(2)}) collective-permute-start(bf16[3,256,256]{2,1,0:T(8,128)(2,1)S(1)} %collective-permute-done.12.refs_5_), channel_id=1, source_target_pairs={{0,1},{1,0},{2,3},{3,2},{4,5},{5,4},{6,7},{7,6},{8,9},{9,8},{10,11... | collective-permute-start | bytes 1179656 | tf_op jit(solution)/shard_map/ppermute | solution.py:24
  87.8 10.2 %collective-permute-start.17 = (bf16[3,256,256]{2,1,0:T(8,128)(2,1)S(1)}, bf16[3,256,256]{2,1,0:T(8,128)(2,1)}, u32[]{:S(2)}, u32[]{:S(2)}) collective-permute-start(bf16[3,256,256]{2,1,0:T(8,128)(2,1)S(1)} %collective-permute-done.13.refs_6_), channel_id=1, source_target_pairs={{0,1},{1,0},{2,3},{3,2},{4,5},{5,4},{6,7},{7,6},{8,9},{9,8},{10,11... | collective-permute-start | bytes 1179656 | tf_op jit(solution)/shard_map/ppermute | solution.py:24
  89.9 28.4 %all-to-all-start.3 = ((bf16[4,240,512]{2,1,0:T(8,128)(2,1)}), bf16[4,240,512]{2,1,0:T(8,128)(2,1)}, u32[]{:S(2)}, u32[]{:S(2)}) async-start(bf16[4,240,512]{2,1,0:T(8,128)(2,1)} %get-tuple-element.32), calls=%async_computation.3 | async-start | bytes 1966080 | tf_op jit(solution)/shard_map/all_to_all | solution.py:20
  97.5 9.6 %collective-permute-start.8 = (bf16[2048,128]{1,0:T(8,128)(2,1)}, bf16[2048,128]{1,0:T(8,128)(2,1)S(1)}, u32[]{:S(2)}, u32[]{:S(2)}) collective-permute-start(bf16[2048,128]{1,0:T(8,128)(2,1)} %dynamic-slice_bitcast_fusion.2), channel_id=1, source_target_pairs={{0,1},{1,0},{2,3},{3,2},{4,5},{5,4},{6,7},{7,6},{8,9},{9,8},{10,11... | collective-permute-start | bytes 1572872 | tf_op jit(solution)/shard_map/ppermute | solution.py:24
  97.6 9.5 %collective-permute-start.9 = (bf16[2048,128]{1,0:T(8,128)(2,1)}, bf16[2048,128]{1,0:T(8,128)(2,1)S(1)}, u32[]{:S(2)}, u32[]{:S(2)}) collective-permute-start(bf16[2048,128]{1,0:T(8,128)(2,1)} %dynamic-slice_bitcast_fusion.1), channel_id=1, source_target_pairs={{0,1},{1,0},{2,3},{3,2},{4,5},{5,4},{6,7},{7,6},{8,9},{9,8},{10,11... | collective-permute-start | bytes 1572872 | tf_op jit(solution)/shard_map/ppermute | solution.py:24
  102.3 10.1 %collective-permute-start.18 = (bf16[48,2176]{1,0:T(8,128)(2,1)S(1)}, bf16[48,2176]{1,0:T(8,128)(2,1)S(1)}, u32[]{:S(2)}, u32[]{:S(2)}) collective-permute-start(bf16[48,2176]{1,0:T(8,128)(2,1)S(1)} %get-tuple-element.36), channel_id=1, source_target_pairs={{0,2},{2,4},{4,6},{6,0},{1,3},{3,5},{5,7},{7,1},{8,10},{10,12},{12... | collective-permute-start | bytes 626696 | tf_op jit(solution)/shard_map/ppermute | solution.py:29
  103.8 10.6 %collective-permute-start.19 = (bf16[48,2176]{1,0:T(8,128)(2,1)S(1)}, bf16[48,2176]{1,0:T(8,128)(2,1)S(1)}, u32[]{:S(2)}, u32[]{:S(2)}) collective-permute-start(bf16[48,2176]{1,0:T(8,128)(2,1)S(1)} %get-tuple-element.37), channel_id=1, source_target_pairs={{0,4},{2,6},{4,0},{6,2},{1,5},{3,7},{5,1},{7,3},{8,12},{10,14},{12... | collective-permute-start | bytes 626696 | tf_op jit(solution)/shard_map/ppermute | solution.py:29
  104.5 13.8 %collective-permute-start.20 = (bf16[48,2176]{1,0:T(8,128)(2,1)S(1)}, bf16[48,2176]{1,0:T(8,128)(2,1)S(1)}, u32[]{:S(2)}, u32[]{:S(2)}) collective-permute-start(bf16[48,2176]{1,0:T(8,128)(2,1)S(1)} %get-tuple-element.38), channel_id=1, source_target_pairs={{0,6},{2,0},{4,2},{6,4},{1,7},{3,1},{5,3},{7,5},{8,14},{10,8},{12,... | collective-permute-start | bytes 626696 | tf_op jit(solution)/shard_map/ppermute | solution.py:29
  124.2 22.3 %all-to-all-start.4 = ((bf16[4,336,512]{2,1,0:T(8,128)(2,1)}), bf16[4,336,512]{2,1,0:T(8,128)(2,1)S(1)}, u32[]{:S(2)}, u32[]{:S(2)}) async-start(bf16[4,336,512]{2,1,0:T(8,128)(2,1)} %shard_map.236), calls=%async_computation.4 | async-start | bytes 2752512 | tf_op jit(solution)/shard_map/all_to_all | solution.py:20
  152.5 23.1 %all-to-all-start.5 = ((bf16[64,24,128]{2,1,0:T(8,128)(2,1)}), bf16[64,24,128]{2,1,0:T(8,128)(2,1)S(1)}, u32[]{:S(2)}, u32[]{:S(2)}) async-start(bf16[64,24,128]{2,1,0:T(8,128)(2,1)} %bitcast.16), calls=%async_computation.5 | async-start | bytes 786432 | tf_op jit(solution)/shard_map/all_to_all | solution.py:20
  160.8 5.2 %collective-permute-start.21 = (bf16[48,256]{1,0:T(8,128)(2,1)S(1)}, bf16[48,256]{1,0:T(8,128)(2,1)S(1)}, u32[]{:S(2)}, u32[]{:S(2)}) collective-permute-start(bf16[48,256]{1,0:T(8,128)(2,1)S(1)} %get-tuple-element.42), channel_id=1, source_target_pairs={{0,1},{1,0},{2,3},{3,2},{4,5},{5,4},{6,7},{7,6},{8,9},{9,8},{10,11... | collective-permute-start | bytes 73736 | tf_op jit(solution)/shard_map/ppermute | solution.py:24
  (13 other events, 137.4 us)

commit v10 on v8

--- a/solution.py
+++ b/solution.py
@@ -41,18 +41,21 @@
     return x * jax.nn.sigmoid(x)
 
 
-def call(body, outs, flops, kinds, *args, mib=53, scratch=()):
+def call(body, outs, flops, kinds, *args, mib=52, scratch=()):
     kinds, out_kinds = kinds.split()
     moved = sum(a.size * a.dtype.itemsize for a in args) + sum(
         o.size * o.dtype.itemsize for o in outs
     )
     space = {"s": pltpu.SMEM, "v": pltpu.VMEM}
-    fetched = [i for i, k in enumerate(kinds) if k in "hlqe"]
+    fetched = [i for i, k in enumerate(kinds) if k in "hlqegd"]
     stored = [i for i, k in enumerate(out_kinds) if k == "h"]
-    room = [
-        pltpu.VMEM(args[i].shape[1 if kinds[i] == "e" else 0 :], args[i].dtype) for i in fetched
-    ]
-    pieces = {"h": 1, "l": 1, "q": 4, "e": 4}
+
+    def held(i):
+        shape = args[i].shape
+        return {"e": shape[1:], "d": shape[1:], "g": (2, *shape[1:])}.get(kinds[i], shape)
+
+    room = [pltpu.VMEM(held(i), args[i].dtype) for i in fetched]
+    pieces = {"h": 1, "l": 1, "q": 4, "e": 4, "g": 1, "d": 1}
     n_sems = sum(pieces[kinds[i]] for i in fetched)
     out_room = [pltpu.VMEM(outs[i].shape, outs[i].dtype) for i in stored]
 
@@ -66,7 +69,11 @@
         sem = 0
         for n, i in enumerate(fetched):
             kind = kinds[i]
-            source = ins[i].at[ins[0][1]] if kind == "e" else ins[i]
+            source = ins[i]
+            if kind == "e":
+                source = source.at[ins[0][1]]
+            elif kind == "d":
+                source = source.at[2]
             parts = pieces[kind]
             size = in_room[n].shape[0] // parts
             copies = []
@@ -123,15 +130,18 @@
     return jax.ShapeDtypeStruct(dims, dtype)
 
 
-def prepare(at, tokens, gain, wq, wf, wi, wo, dg, du, dd, spread_w, dense, t0, t1, t2, t3, held):
-    x = at[2]
-    for i, block in enumerate((dg, du, dd)):
-        dense[i] = block[...]
+def copies(wq, wf, wi, wo, spread_w):
     for i, block in enumerate((wq, wf, wi, wo)):
         width = block.shape[1]
         value = block[...]
         for z in range(spread_w.shape[0]):
             spread_w[z, :, i * width : (i + 1) * width] = value
+
+
+def prepare(at, tokens, gain, dg, du, dd, dense, t0, t1, t2, t3, held):
+    x = at[2]
+    for i, block in enumerate((dg, du, dd)):
+        dense[i] = block[...]
     wide = tokens[...].astype(F32)
     wide = wide * lax.rsqrt(jnp.mean(wide * wide, axis=1, keepdims=True) + EPS) * gain[...]
     low = lax.broadcasted_iota(jnp.int32, (wide.shape[0], 128), 1) < 64
@@ -325,7 +335,7 @@
         total = None
         for i in range(4):
             wait[4 * side + i][0]()
-            term = dot(rows[:, i * cols : (i + 1) * cols], weights[i][2])
+            term = dot(rows[:, i * cols : (i + 1) * cols], weights[i][...])
             total = term if total is None else total + term
         total = total.astype(BF)
         for d in range(ny):
@@ -456,26 +466,32 @@
     slot_rows = slot_cols.T
     within = (jnp.arange(experts * 2 * slots, dtype=jnp.int32) % (nx * nc * 2 * slots))[None, :]
 
-    spread_w, dense_block, *columns = call(
-        prepare,
-        [shaped(nz, rows_w, 4 * chan), shaped(3, *dense_gate.shape)]
-        + [shaped(seq, nz * rows_w)] * nx,
+    (spread_w,) = call(
+        copies,
+        [shaped(nz, rows_w, 4 * chan)],
         10**6,
-        "shhhhhhhhh hhhhhh",
-        at,
-        tokens,
-        norm_gain.reshape(1, width),
+        "hhhh h",
         w_query,
         w_forget,
         w_input,
         w_outgate,
+        mib=58,
+    )
+    weights = swap(spread_w, "z").reshape(nz * rows_w, 4 * chan)
+    dense_block, *columns = call(
+        prepare,
+        [shaped(3, *dense_gate.shape)] + [shaped(seq, nz * rows_w)] * nx,
+        10**6,
+        "shhhhh hhhhh",
+        at,
+        tokens,
+        norm_gain.reshape(1, width),
         dense_gate,
         dense_up,
         dense_down,
-        mib=58,
+        mib=59,
         scratch=[pltpu.VMEM((nx, seq, nz * rows_w), BF)],
     )
-    weights = swap(spread_w, "z").reshape(nz * rows_w, 4 * chan)
     mine = [columns[0]] + [shift(columns[d], "x", d) for d in range(1, nx)]
     part = dot(jnp.concatenate(mine, axis=0), weights).astype(BF)
     part = part.reshape(nx, seq, 4 * chan)
@@ -555,7 +571,7 @@
         dense_first_half,
         [shaped(quarter, 2 * hidden_width + 128)] * ny,
         2 * count * nc * cols * 2 * hidden_width,
-        "shhllllllll hhhh",
+        "shhgggggggg hhhh",
         at,
         dense_rows,
         ffn_gain.reshape(ny * nc, cols),
@@ -571,7 +587,7 @@
         dense_second_half,
         [shaped(nc, count, cols)],
         2 * count * nc * cols * hidden_width,
-        "shvvvllllllll h",
+        "shvvvdddddddd h",
         at,
         *hidden,
         *dense_own,

time: 182 us -> 181 us (level)
  waiting for transfers between devices: 72.4 us -> 68.1 us
    all_to_all x6, waiting for transfers between devices: 31.3 us -> 26.6 us  [swap(): return lax.all_to_all(x, axis, split_axis=0, concat_axis=0, tiled=True)]
    squeeze x3, local copies, waits for them, and re-layouts: 2.75 us -> 4.84 us  [pick(): return lax.dynamic_index_in_dim(x, index, 0, keepdims=False)]
    pallas_call x10 -> x11, Pallas kernels: 30.3 us -> 30.5 us  [call(): pl.pallas_call(whole, out_shape=outs, in_specs=[pl.BlockSpec(memory_space...]
  transfers between devices with their start and end apart: 31 -> 31, of which waited for: 18 -> 17; matrix products, arithmetic and copies ran while one was open for 6% -> 8% of each run, Pallas kernels for 9% -> 11%
where the time goes in v10:
time: 181 us; the launch traced here: 178 us
  waiting for transfers between devices  68.1 us (38%)
  starting transfers between devices  60.7 us (34%)
  Pallas kernels  30.5 us (17%)
  other arithmetic  8.68 us (5%)
  local copies, waits for them, and re-layouts  7.99 us (4%)
    ppermute x15, waiting for transfers between devices, shift(): return lax.ppermute(x, axis, [(i, (i + by) % size) for i in range(size)])  38.5 us
    all_to_all x6, starting transfers between devices, swap(): return lax.all_to_all(x, axis, split_axis=0, concat_axis=0, tiled=True)  34.3 us
    pallas_call x11, Pallas kernels, call(): pl.pallas_call(whole, out_shape=outs, in_specs=[pl.BlockSpec(memory_space...  30.5 us
    all_to_all x6, waiting for transfers between devices, swap(): return lax.all_to_all(x, axis, split_axis=0, concat_axis=0, tiled=True)  26.6 us
    ppermute x15, starting transfers between devices, shift(): return lax.ppermute(x, axis, [(i, (i + by) % size) for i in range(size)])  25 us
    add x1, other arithmetic, step(): decay.reshape(shape)[..., None] * state  5.07 us
    squeeze x3, local copies, waits for them, and re-layouts, pick(): return lax.dynamic_index_in_dim(x, index, 0, keepdims=False)  4.84 us
  transfers between devices with their start and end apart: 31, of which 17 were waited for; matrix products, arithmetic and copies ran while one was open for 8% of the time, Pallas kernels for 11%

profile of v10, /device:TPU:8, one launch (start us, length us, event | category | flops | bytes accessed | tf_op | source)
XLA Modules:
  0.0 178.3 jit_solution(14651296926509409415)
XLA Ops:
  2.4 8.5 %all-to-all-start = ((bf16[8,64,512]{2,1,0:T(8,128)(2,1)}), bf16[8,64,512]{2,1,0:T(8,128)(2,1)S(1)}, u32[]{:S(2)}, u32[]{:S(2)}) async-start(bf16[8,64,512]{2,1,0:T(8,128)(2,1)} %shard_map.231), calls=%async_computation | async-start | bytes 1048576 | tf_op jit(solution)/shard_map/all_to_all | solution.py:20
  11.5 2.9 %shard_map.230 = (bf16[3,256,256]{2,1,0:T(8,128)(2,1)}, bf16[48,512]{1,0:T(8,128)(2,1)}, bf16[48,512]{1,0:T(8,128)(2,1)}, bf16[48,512]{1,0:T(8,128)(2,1)}, bf16[48,512]{1,0:T(8,128)(2,1)}) custom-call(s32[3]{0:T(128)} %pad_add_fusion.refs_0_, bf16[48,2048]{1,0:T(8,128)(2,1)} %refs_2_.3, f32[1,2048]{1,0:T(1,128)} %bitcast.43, bf16[256,256]{1,0:T(8,128)(2,1)} %refs_3_.4, ...), custom_call_target="tpu_custom_call" | custom-call | flops 1000000 | bytes 1187852 | tf_op jit(solution)/shard_map/pallas_call | solution.py:112
  16.0 2.7 %collective-permute-start.1 = (bf16[48,512]{1,0:T(8,128)(2,1)}, bf16[48,512]{1,0:T(8,128)(2,1)S(1)}, u32[]{:S(2)}, u32[]{:S(2)}) collective-permute-start(bf16[48,512]{1,0:T(8,128)(2,1)} %get-tuple-element.26), channel_id=1, source_target_pairs={{0,16},{8,24},{16,0},{24,8},{1,17},{9,25},{17,1},{25,9},{2,18},{10... | collective-permute-start | bytes 147464 | tf_op jit(solution)/shard_map/ppermute | solution.py:29
  23.0 5.4 %all-to-all-done = bf16[8,64,512]{2,1,0:T(8,128)(2,1)S(1)} async-done(((bf16[8,64,512]{2,1,0:T(8,128)(2,1)}), bf16[8,64,512]{2,1,0:T(8,128)(2,1)S(1)}, u32[]{:S(2)}, u32[]{:S(2)}) %all-to-all-start) | async-done | bytes 524320 | tf_op jit(solution)/shard_map/all_to_all | solution.py:20
  29.5 2.8 %collective-permute-start.3 = (bf16[48,512]{1,0:T(8,128)(2,1)S(1)}, bf16[48,512]{1,0:T(8,128)(2,1)S(1)}, u32[]{:S(2)}, u32[]{:S(2)}) collective-permute-start(bf16[48,512]{1,0:T(8,128)(2,1)S(1)} %get-tuple-element.48), channel_id=1, source_target_pairs={{0,24},{8,0},{16,8},{24,16},{1,25},{9,1},{17,9},{25,17},{2,26},{10... | collective-permute-start | bytes 147464 | tf_op jit(solution)/shard_map/ppermute | solution.py:29
  34.4 3.5 %collective-permute-done.4.refs_3_ = bf16[48,512]{1,0:T(8,128)(2,1)S(1)} collective-permute-done((bf16[48,512]{1,0:T(8,128)(2,1)S(1)}, bf16[48,512]{1,0:T(8,128)(2,1)S(1)}, u32[]{:S(2)}, u32[]{:S(2)}) %collective-permute-start.4) | collective-permute-done | bytes 49184 | tf_op jit(solution)/shard_map/ppermute | solution.py:29
  39.1 3.6 %shard_map.232 = (f32[48,128]{1,0:T(8,128)S(1)}, f32[48,128]{1,0:T(8,128)S(1)}, f32[48,128]{1,0:T(8,128)S(1)}, bf16[4,48,256]{2,1,0:T(8,128)(2,1)S(1)}, bf16[4,48,256]{2,1,0:T(8,128)(2,1)S(1)}) custom-call(s32[3]{0:T(128)S(1)} %copy-done.6, bf16[48,512]{1,0:T(8,128)(2,1)S(1)} %get-tuple-element.49.refs_1_, ...), custom_call_target="tpu_custom_call" | custom-call | flops 3145728 | bytes 4137996 | tf_op jit(solution)/shard_map/pallas_call | solution.py:112
  44.8 4.9 %all-to-all-start.1 = ((bf16[4,48,256]{2,1,0:T(8,128)(2,1)}), bf16[4,48,256]{2,1,0:T(8,128)(2,1)S(1)}, u32[]{:S(2)}, u32[]{:S(2)}) async-start(bf16[4,48,256]{2,1,0:T(8,128)(2,1)} %add_convert_fusion), calls=%async_computation.1 | async-start | bytes 196608 | tf_op jit(solution)/shard_map/all_to_all | solution.py:20
  49.8 4.2 %all-to-all-done.1.refs_1_ = bf16[4,48,256]{2,1,0:T(8,128)(2,1)S(1)} async-done(((bf16[4,48,256]{2,1,0:T(8,128)(2,1)}), bf16[4,48,256]{2,1,0:T(8,128)(2,1)S(1)}, u32[]{:S(2)}, u32[]{:S(2)}) %all-to-all-start.1) | async-done | bytes 98336 | tf_op jit(solution)/shard_map/all_to_all | solution.py:20
  54.0 2.6 %shard_map.233 = (f32[48,256]{1,0:T(8,128)S(1)}, bf16[48,256]{1,0:T(8,128)(2,1)S(1)}, bf16[1536,128]{1,0:T(8,128)(2,1)}) custom-call(s32[3]{0:T(128)S(1)} %copy-done.6, bf16[4,48,256]{2,1,0:T(8,128)(2,1)S(1)} %all-to-all-done.1.refs_1_, bf16[48,2048]{1,0:T(8,128)(2,1)S(1)} %copy-done.3, s32[8,48]{1,0:T(8,128)S(1)} %copy.55.refs_3_), custom_call_target="tpu_custom_call" | custom-call | flops 37748736 | bytes 763404 | tf_op jit(solution)/shard_map/pallas_call | solution.py:112
  56.7 4.6 %all-to-all-start.2 = ((bf16[64,24,128]{2,1,0:T(8,128)(2,1)}), bf16[64,24,128]{2,1,0:T(8,128)(2,1)S(1)}, u32[]{:S(2)}, u32[]{:S(2)}) async-start(bf16[64,24,128]{2,1,0:T(8,128)(2,1)} %bitcast.10), calls=%async_computation.2 | async-start | bytes 786432 | tf_op jit(solution)/shard_map/all_to_all | solution.py:20
  62.9 1.9 %dynamic-slice_bitcast_fusion = bf16[128,2048]{1,0:T(8,128)(2,1)} fusion(bf16[2,128,2048]{2,1,0:T(8,128)(2,1)} %refs_7_.1, s32[]{:T(128)S(6)} %select_n.224), kind=kLoop, calls=%fused_computation.2 | loop fusion | bytes 1048580 | tf_op jit(solution)/shard_map/jit(dynamic_index_in_dim)/squeeze | solution.py:33
  69.0 7.4 %all-to-all-done.2 = bf16[64,24,128]{2,1,0:T(8,128)(2,1)S(1)} async-done(((bf16[64,24,128]{2,1,0:T(8,128)(2,1)}), bf16[64,24,128]{2,1,0:T(8,128)(2,1)S(1)}, u32[]{:S(2)}, u32[]{:S(2)}) %all-to-all-start.2) | async-done | bytes 393248 | tf_op jit(solution)/shard_map/all_to_all | solution.py:20
  76.3 2.0 %shard_map.234 = (bf16[4,240,512]{2,1,0:T(8,128)(2,1)}, bf16[2,192,256]{2,1,0:T(8,128)(2,1)S(1)}) custom-call(s32[3]{0:T(128)S(1)} %copy-done.6, s32[1,384]{1,0:T(1,128)S(1)} %fusion.53.refs_1_, bf16[1536,128]{1,0:T(8,128)(2,1)S(1)} %bitcast.36, bf16[48,256]{1,0:T(8,128)(2,1)S(1)} %get-tuple-element.31.refs_3_, ...), custom_call_target="tpu_custom_call" | custom-call | flops 150994944 | bytes 1623564 | tf_op jit(solution)/shard_map/pallas_call | solution.py:112
  78.4 5.7 %all-to-all-start.3 = ((bf16[4,240,512]{2,1,0:T(8,128)(2,1)}), bf16[4,240,512]{2,1,0:T(8,128)(2,1)}, u32[]{:S(2)}, u32[]{:S(2)}) async-start(bf16[4,240,512]{2,1,0:T(8,128)(2,1)} %get-tuple-element.32), calls=%async_computation.3 | async-start | bytes 1966080 | tf_op jit(solution)/shard_map/all_to_all | solution.py:20
  85.2 2.9 %collective-permute-start.12 = (bf16[3,256,256]{2,1,0:T(8,128)(2,1)S(1)}, bf16[3,256,256]{2,1,0:T(8,128)(2,1)S(1)}, u32[]{:S(2)}, u32[]{:S(2)}) collective-permute-start(bf16[3,256,256]{2,1,0:T(8,128)(2,1)S(1)} %copy-done), channel_id=1, source_target_pairs={{0,16},{8,24},{16,0},{24,8},{1,17},{9,25},{17,1},{25,9},{2,18},{10... | collective-permute-start | bytes 1179656 | tf_op jit(solution)/shard_map/ppermute | solution.py:29
  89.3 8.9 %collective-permute-done.12.refs_5_.refs_7_ = bf16[3,256,256]{2,1,0:T(8,128)(2,1)S(1)} collective-permute-done((bf16[3,256,256]{2,1,0:T(8,128)(2,1)S(1)}, bf16[3,256,256]{2,1,0:T(8,128)(2,1)S(1)}, u32[]{:S(2)}, u32[]{:S(2)}) %collective-permute-start.12) | collective-permute-done | bytes 393248 | tf_op jit(solution)/shard_map/ppermute | solution.py:29
  98.2 8.4 %collective-permute-done.13.refs_6_.refs_8_ = bf16[3,256,256]{2,1,0:T(8,128)(2,1)} collective-permute-done((bf16[3,256,256]{2,1,0:T(8,128)(2,1)S(1)}, bf16[3,256,256]{2,1,0:T(8,128)(2,1)}, u32[]{:S(2)}, u32[]{:S(2)}) %collective-permute-start.13) | collective-permute-done | bytes 393248 | tf_op jit(solution)/shard_map/ppermute | solution.py:29
  107.3 6.0 %shard_map.235 = bf16[4,240,512]{2,1,0:T(8,128)(2,1)} custom-call(s32[3]{0:T(128)S(1)} %copy-done.6, bf16[4,240,512]{2,1,0:T(8,128)(2,1)} %all-to-all-done.3.refs_1_, f32[1,2048]{1,0:T(1,128)S(1)} %bitcast.37, bf16[2,2048,128]{2,1,0:T(8,128)(2,1)} %refs_3_.6, bf16[2048,128]{1,0:T(8,128)(2,1)S(1)} %collective-permute-done.8.refs_4_, ...), custom_call_target="tpu_custom_call" | custom-call | flops 679477248 | bytes 8265740 | tf_op jit(solution)/shard_map/pallas_call | solution.py:112
  113.3 4.8 %all-to-all-start.4 = ((bf16[4,240,512]{2,1,0:T(8,128)(2,1)}), bf16[4,240,512]{2,1,0:T(8,128)(2,1)S(1)}, u32[]{:S(2)}, u32[]{:S(2)}) async-start(bf16[4,240,512]{2,1,0:T(8,128)(2,1)} %shard_map.235), calls=%async_computation.4 | async-start | bytes 1966080 | tf_op jit(solution)/shard_map/all_to_all | solution.py:20
  118.2 4.2 %shard_map.236 = (bf16[48,2176]{1,0:T(8,128)(2,1)S(1)}, bf16[48,2176]{1,0:T(8,128)(2,1)}, bf16[48,2176]{1,0:T(8,128)(2,1)}, bf16[48,2176]{1,0:T(8,128)(2,1)S(1)}) custom-call(s32[3]{0:T(128)S(1)} %copy-done.7, bf16[2,192,256]{2,1,0:T(8,128)(2,1)S(1)} %get-tuple-element.33.refs_1_, f32[8,256]{1,0:T(8,128)S(1)} %reshape.582.refs_2_, ...), custom_call_target="tpu_custom_call" | custom-call | flops 402653184 | bytes 4186124 | tf_op jit(solution)/shard_map/pallas_call | solution.py:112
  124.6 2.5 %collective-permute-start.20 = (bf16[48,2176]{1,0:T(8,128)(2,1)S(1)}, bf16[48,2176]{1,0:T(8,128)(2,1)S(1)}, u32[]{:S(2)}, u32[]{:S(2)}) collective-permute-start(bf16[48,2176]{1,0:T(8,128)(2,1)S(1)} %get-tuple-element.38), channel_id=1, source_target_pairs={{0,6},{2,0},{4,2},{6,4},{1,7},{3,1},{5,3},{7,5},{8,14},{10,8},{12,... | collective-permute-start | bytes 626696 | tf_op jit(solution)/shard_map/ppermute | solution.py:29
  127.2 7.7 %collective-permute-done.18.refs_1_ = bf16[48,2176]{1,0:T(8,128)(2,1)S(1)} collective-permute-done((bf16[48,2176]{1,0:T(8,128)(2,1)}, bf16[48,2176]{1,0:T(8,128)(2,1)S(1)}, u32[]{:S(2)}, u32[]{:S(2)}) %collective-permute-start.18) | collective-permute-done | bytes 208928 | tf_op jit(solution)/shard_map/ppermute | solution.py:29
  134.9 2.1 %collective-permute-done.19.refs_2_ = bf16[48,2176]{1,0:T(8,128)(2,1)S(1)} collective-permute-done((bf16[48,2176]{1,0:T(8,128)(2,1)}, bf16[48,2176]{1,0:T(8,128)(2,1)S(1)}, u32[]{:S(2)}, u32[]{:S(2)}) %collective-permute-start.19) | collective-permute-done | bytes 208928 | tf_op jit(solution)/shard_map/ppermute | solution.py:29
  137.0 3.4 %collective-permute-done.20.refs_3_ = bf16[48,2176]{1,0:T(8,128)(2,1)S(1)} collective-permute-done((bf16[48,2176]{1,0:T(8,128)(2,1)S(1)}, bf16[48,2176]{1,0:T(8,128)(2,1)S(1)}, u32[]{:S(2)}, u32[]{:S(2)}) %collective-permute-start.20) | collective-permute-done | bytes 208928 | tf_op jit(solution)/shard_map/ppermute | solution.py:29
  141.9 3.0 %collective-permute-start.22 = (bf16[48,1024]{1,0:T(8,128)(2,1)S(1)}, bf16[48,1024]{1,0:T(8,128)(2,1)S(1)}, u32[]{:S(2)}, u32[]{:S(2)}) collective-permute-start(bf16[48,1024]{1,0:T(8,128)(2,1)S(1)} %shard_map.237.refs_1_), channel_id=1, source_target_pairs={{0,4},{2,6},{4,0},{6,2},{1,5},{3,7},{5,1},{7,3},{8,12},{10,14},{12... | collective-permute-start | bytes 294920 | tf_op jit(solution)/shard_map/ppermute | solution.py:29
  146.0 2.3 %collective-permute-done.22.refs_3_ = bf16[48,1024]{1,0:T(8,128)(2,1)S(1)} collective-permute-done((bf16[48,1024]{1,0:T(8,128)(2,1)S(1)}, bf16[48,1024]{1,0:T(8,128)(2,1)S(1)}, u32[]{:S(2)}, u32[]{:S(2)}) %collective-permute-start.22) | collective-permute-done | bytes 98336 | tf_op jit(solution)/shard_map/ppermute | solution.py:29
  150.5 3.0 %shard_map.238.refs_3_ = bf16[2,192,256]{2,1,0:T(8,128)(2,1)S(1)} custom-call(s32[3]{0:T(128)S(1)} %copy-done.7, bf16[48,1024]{1,0:T(8,128)(2,1)S(1)} %shard_map.237.refs_1_, bf16[48,1024]{1,0:T(8,128)(2,1)S(1)} %collective-permute-done.21.refs_2_, bf16[48,1024]{1,0:T(8,128)(2,1)S(1)} %collective-permute-done.22.refs_3_, ...), custom_call_target="tpu_custom_call" | custom-call | flops 201326592 | bytes 3735564 | tf_op jit(solution)/shard_map/pallas_call | solution.py:112
  153.5 2.4 %shard_map.239 = (bf16[1536,128]{1,0:T(8,128)(2,1)}, f32[48,256]{1,0:T(8,128)S(1)}, bf16[48,256]{1,0:T(8,128)(2,1)S(1)}) custom-call(s32[3]{0:T(128)S(1)} %copy-done.7, s32[384,1]{1,0:T(8,128)S(1)} %fusion.8.refs_1_, bf16[4,240,512]{2,1,0:T(8,128)(2,1)S(1)} %all-to-all-done.4.refs_2_, bf16[2,192,256]{2,1,0:T(8,128)(2,1)S(1)} %shard_map.238.refs_3_), custom_call_target="tpu_custom_call" | custom-call | flops 150994944 | bytes 1648140 | tf_op jit(solution)/shard_map/pallas_call | solution.py:112
  155.9 5.8 %all-to-all-start.5 = ((bf16[64,24,128]{2,1,0:T(8,128)(2,1)}), bf16[64,24,128]{2,1,0:T(8,128)(2,1)S(1)}, u32[]{:S(2)}, u32[]{:S(2)}) async-start(bf16[64,24,128]{2,1,0:T(8,128)(2,1)} %bitcast.16), calls=%async_computation.5 | async-start | bytes 786432 | tf_op jit(solution)/shard_map/all_to_all | solution.py:20
  161.9 5.1 %multiply_add_fusion = f32[48,1,128,128]{3,2,1,0:T(8,128)} fusion(f32[48,1,128,128]{3,2,1,0:T(8,128)} %param.24, f32[48,128]{1,0:T(8,128)S(1)} %get-tuple-element.45, f32[48,128]{1,0:T(8,128)S(1)} %get-tuple-element.44, f32[48,128]{1,0:T(8,128)S(1)} %get-tuple-element.43), kind=kLoop, calls=%fused_computation | loop fusion | flops 2359296 | bytes 6365184 | tf_op jit(solution)/shard_map/add | solution.py:521
  167.0 9.7 %all-to-all-done.5 = bf16[64,24,128]{2,1,0:T(8,128)(2,1)S(1)} async-done(((bf16[64,24,128]{2,1,0:T(8,128)(2,1)}), bf16[64,24,128]{2,1,0:T(8,128)(2,1)S(1)}, u32[]{:S(2)}, u32[]{:S(2)}) %all-to-all-start.5) | async-done | bytes 393248 | tf_op jit(solution)/shard_map/all_to_all | solution.py:20
  (98 shorter events, 32.1 us)
Async XLA Ops:
  2.4 26.0 %all-to-all-start = ((bf16[8,64,512]{2,1,0:T(8,128)(2,1)}), bf16[8,64,512]{2,1,0:T(8,128)(2,1)S(1)}, u32[]{:S(2)}, u32[]{:S(2)}) async-start(bf16[8,64,512]{2,1,0:T(8,128)(2,1)} %shard_map.231), calls=%async_computation | async-start | bytes 1048576 | tf_op jit(solution)/shard_map/all_to_all | solution.py:20
  14.4 8.3 %collective-permute-start = (bf16[48,512]{1,0:T(8,128)(2,1)}, bf16[48,512]{1,0:T(8,128)(2,1)S(1)}, u32[]{:S(2)}, u32[]{:S(2)}) collective-permute-start(bf16[48,512]{1,0:T(8,128)(2,1)} %get-tuple-element.25), channel_id=1, source_target_pairs={{0,8},{8,16},{16,24},{24,0},{1,9},{9,17},{17,25},{25,1},{2,10},{10... | collective-permute-start | bytes 147464 | tf_op jit(solution)/shard_map/ppermute | solution.py:29
  16.0 6.7 %collective-permute-start.1 = (bf16[48,512]{1,0:T(8,128)(2,1)}, bf16[48,512]{1,0:T(8,128)(2,1)S(1)}, u32[]{:S(2)}, u32[]{:S(2)}) collective-permute-start(bf16[48,512]{1,0:T(8,128)(2,1)} %get-tuple-element.26), channel_id=1, source_target_pairs={{0,16},{8,24},{16,0},{24,8},{1,17},{9,25},{17,1},{25,9},{2,18},{10... | collective-permute-start | bytes 147464 | tf_op jit(solution)/shard_map/ppermute | solution.py:29
  18.7 4.3 %collective-permute-start.2 = (bf16[48,512]{1,0:T(8,128)(2,1)}, bf16[48,512]{1,0:T(8,128)(2,1)S(1)}, u32[]{:S(2)}, u32[]{:S(2)}) collective-permute-start(bf16[48,512]{1,0:T(8,128)(2,1)} %get-tuple-element.27), channel_id=1, source_target_pairs={{0,24},{8,0},{16,8},{24,16},{1,25},{9,1},{17,9},{25,17},{2,26},{10... | collective-permute-start | bytes 147464 | tf_op jit(solution)/shard_map/ppermute | solution.py:29
  29.5 4.9 %collective-permute-start.3 = (bf16[48,512]{1,0:T(8,128)(2,1)S(1)}, bf16[48,512]{1,0:T(8,128)(2,1)S(1)}, u32[]{:S(2)}, u32[]{:S(2)}) collective-permute-start(bf16[48,512]{1,0:T(8,128)(2,1)S(1)} %get-tuple-element.48), channel_id=1, source_target_pairs={{0,24},{8,0},{16,8},{24,16},{1,25},{9,1},{17,9},{25,17},{2,26},{10... | collective-permute-start | bytes 147464 | tf_op jit(solution)/shard_map/ppermute | solution.py:29
  32.4 5.6 %collective-permute-start.4 = (bf16[48,512]{1,0:T(8,128)(2,1)S(1)}, bf16[48,512]{1,0:T(8,128)(2,1)S(1)}, u32[]{:S(2)}, u32[]{:S(2)}) collective-permute-start(bf16[48,512]{1,0:T(8,128)(2,1)S(1)} %get-tuple-element.47), channel_id=1, source_target_pairs={{0,16},{8,24},{16,0},{24,8},{1,17},{9,25},{17,1},{25,9},{2,18},{10... | collective-permute-start | bytes 147464 | tf_op jit(solution)/shard_map/ppermute | solution.py:29
  33.2 5.3 %collective-permute-start.5 = (bf16[48,512]{1,0:T(8,128)(2,1)S(1)}, bf16[48,512]{1,0:T(8,128)(2,1)S(1)}, u32[]{:S(2)}, u32[]{:S(2)}) collective-permute-start(bf16[48,512]{1,0:T(8,128)(2,1)S(1)} %get-tuple-element.46), channel_id=1, source_target_pairs={{0,8},{8,16},{16,24},{24,0},{1,9},{9,17},{17,25},{25,1},{2,10},{10... | collective-permute-start | bytes 147464 | tf_op jit(solution)/shard_map/ppermute | solution.py:29
  42.7 1.4 collective-permute-start.6
  44.8 9.3 %all-to-all-start.1 = ((bf16[4,48,256]{2,1,0:T(8,128)(2,1)}), bf16[4,48,256]{2,1,0:T(8,128)(2,1)S(1)}, u32[]{:S(2)}, u32[]{:S(2)}) async-start(bf16[4,48,256]{2,1,0:T(8,128)(2,1)} %add_convert_fusion), calls=%async_computation.1 | async-start | bytes 196608 | tf_op jit(solution)/shard_map/all_to_all | solution.py:20
  56.7 50.6 %copy-start.5 = (f32[2048]{0:T(1024)S(1)}, f32[2048]{0:T(1024)}, u32[]{:S(2)}) copy-start(f32[2048]{0:T(1024)} %param.33) | copy-start | bytes 24580
  56.7 19.6 %all-to-all-start.2 = ((bf16[64,24,128]{2,1,0:T(8,128)(2,1)}), bf16[64,24,128]{2,1,0:T(8,128)(2,1)S(1)}, u32[]{:S(2)}, u32[]{:S(2)}) async-start(bf16[64,24,128]{2,1,0:T(8,128)(2,1)} %bitcast.10), calls=%async_computation.2 | async-start | bytes 786432 | tf_op jit(solution)/shard_map/all_to_all | solution.py:20
  61.3 26.8 %collective-permute-start.11 = (bf16[3,256,256]{2,1,0:T(8,128)(2,1)S(1)}, bf16[3,256,256]{2,1,0:T(8,128)(2,1)S(1)}, u32[]{:S(2)}, u32[]{:S(2)}) collective-permute-start(bf16[3,256,256]{2,1,0:T(8,128)(2,1)S(1)} %copy-done), channel_id=1, source_target_pairs={{0,8},{8,16},{16,24},{24,0},{1,9},{9,17},{17,25},{25,1},{2,10},{10... | collective-permute-start | bytes 1179656 | tf_op jit(solution)/shard_map/ppermute | solution.py:29
  64.8 41.9 %collective-permute-start.10 = (bf16[128,2048]{1,0:T(8,128)(2,1)}, bf16[128,2048]{1,0:T(8,128)(2,1)S(1)}, u32[]{:S(2)}, u32[]{:S(2)}) collective-permute-start(bf16[128,2048]{1,0:T(8,128)(2,1)} %dynamic-slice_bitcast_fusion), channel_id=1, source_target_pairs={{0,1},{1,0},{2,3},{3,2},{4,5},{5,4},{6,7},{7,6},{8,9},{9,8},{10,11... | collective-permute-start | bytes 1572872 | tf_op jit(solution)/shard_map/ppermute | solution.py:24
  66.7 40.5 %collective-permute-start.8 = (bf16[2048,128]{1,0:T(8,128)(2,1)}, bf16[2048,128]{1,0:T(8,128)(2,1)S(1)}, u32[]{:S(2)}, u32[]{:S(2)}) collective-permute-start(bf16[2048,128]{1,0:T(8,128)(2,1)} %dynamic-slice_bitcast_fusion.2), channel_id=1, source_target_pairs={{0,1},{1,0},{2,3},{3,2},{4,5},{5,4},{6,7},{7,6},{8,9},{9,8},{10,11... | collective-permute-start | bytes 1572872 | tf_op jit(solution)/shard_map/ppermute | solution.py:24
  67.2 1.8 collective-permute-start.7
  78.4 28.9 %all-to-all-start.3 = ((bf16[4,240,512]{2,1,0:T(8,128)(2,1)}), bf16[4,240,512]{2,1,0:T(8,128)(2,1)}, u32[]{:S(2)}, u32[]{:S(2)}) async-start(bf16[4,240,512]{2,1,0:T(8,128)(2,1)} %get-tuple-element.32), calls=%async_computation.3 | async-start | bytes 1966080 | tf_op jit(solution)/shard_map/all_to_all | solution.py:20
  85.1 22.2 %collective-permute-start.9 = (bf16[2048,128]{1,0:T(8,128)(2,1)S(1)}, bf16[2048,128]{1,0:T(8,128)(2,1)S(1)}, u32[]{:S(2)}, u32[]{:S(2)}) collective-permute-start(bf16[2048,128]{1,0:T(8,128)(2,1)S(1)} %dynamic-slice_bitcast_fusion.1), channel_id=1, source_target_pairs={{0,1},{1,0},{2,3},{3,2},{4,5},{5,4},{6,7},{7,6},{8,9},{9,8},{10,11... | collective-permute-start | bytes 1572872 | tf_op jit(solution)/shard_map/ppermute | solution.py:24
  85.2 13.0 %collective-permute-start.12 = (bf16[3,256,256]{2,1,0:T(8,128)(2,1)S(1)}, bf16[3,256,256]{2,1,0:T(8,128)(2,1)S(1)}, u32[]{:S(2)}, u32[]{:S(2)}) collective-permute-start(bf16[3,256,256]{2,1,0:T(8,128)(2,1)S(1)} %copy-done), channel_id=1, source_target_pairs={{0,16},{8,24},{16,0},{24,8},{1,17},{9,25},{17,1},{25,9},{2,18},{10... | collective-permute-start | bytes 1179656 | tf_op jit(solution)/shard_map/ppermute | solution.py:29
  88.1 18.6 %collective-permute-start.13 = (bf16[3,256,256]{2,1,0:T(8,128)(2,1)S(1)}, bf16[3,256,256]{2,1,0:T(8,128)(2,1)}, u32[]{:S(2)}, u32[]{:S(2)}) collective-permute-start(bf16[3,256,256]{2,1,0:T(8,128)(2,1)S(1)} %copy-done), channel_id=1, source_target_pairs={{0,24},{8,0},{16,8},{24,16},{1,25},{9,1},{17,9},{25,17},{2,26},{10... | collective-permute-start | bytes 1179656 | tf_op jit(solution)/shard_map/ppermute | solution.py:29
  98.2 19.9 %collective-permute-start.14 = (bf16[3,256,256]{2,1,0:T(8,128)(2,1)S(1)}, bf16[3,256,256]{2,1,0:T(8,128)(2,1)}, u32[]{:S(2)}, u32[]{:S(2)}) collective-permute-start(bf16[3,256,256]{2,1,0:T(8,128)(2,1)S(1)} %copy-done), channel_id=1, source_target_pairs={{0,1},{1,0},{2,3},{3,2},{4,5},{5,4},{6,7},{7,6},{8,9},{9,8},{10,11... | collective-permute-start | bytes 1179656 | tf_op jit(solution)/shard_map/ppermute | solution.py:24
  106.7 11.5 %collective-permute-start.15 = (bf16[3,256,256]{2,1,0:T(8,128)(2,1)S(1)}, bf16[3,256,256]{2,1,0:T(8,128)(2,1)}, u32[]{:S(2)}, u32[]{:S(2)}) collective-permute-start(bf16[3,256,256]{2,1,0:T(8,128)(2,1)S(1)} %collective-permute-done.11.refs_4_.refs_6_), channel_id=1, source_target_pairs={{0,1},{1,0},{2,3},{3,2},{4,5},{5,4},{6,7},{7,6},{8,9},{9,8},{10,11... | collective-permute-start | bytes 1179656 | tf_op jit(solution)/shard_map/ppermute | solution.py:24
  106.7 11.5 %collective-permute-start.16 = (bf16[3,256,256]{2,1,0:T(8,128)(2,1)S(1)}, bf16[3,256,256]{2,1,0:T(8,128)(2,1)}, u32[]{:S(2)}, u32[]{:S(2)}) collective-permute-start(bf16[3,256,256]{2,1,0:T(8,128)(2,1)S(1)} %collective-permute-done.12.refs_5_.refs_7_), channel_id=1, source_target_pairs={{0,1},{1,0},{2,3},{3,2},{4,5},{5,4},{6,7},{7,6},{8,9},{9,8},{10,11... | collective-permute-start | bytes 1179656 | tf_op jit(solution)/shard_map/ppermute | solution.py:24
  107.2 11.0 %collective-permute-start.17 = (bf16[3,256,256]{2,1,0:T(8,128)(2,1)}, bf16[3,256,256]{2,1,0:T(8,128)(2,1)}, u32[]{:S(2)}, u32[]{:S(2)}) collective-permute-start(bf16[3,256,256]{2,1,0:T(8,128)(2,1)} %collective-permute-done.13.refs_6_.refs_8_), channel_id=1, source_target_pairs={{0,1},{1,0},{2,3},{3,2},{4,5},{5,4},{6,7},{7,6},{8,9},{9,8},{10,11... | collective-permute-start | bytes 1179656 | tf_op jit(solution)/shard_map/ppermute | solution.py:24
  113.3 40.2 %all-to-all-start.4 = ((bf16[4,240,512]{2,1,0:T(8,128)(2,1)}), bf16[4,240,512]{2,1,0:T(8,128)(2,1)S(1)}, u32[]{:S(2)}, u32[]{:S(2)}) async-start(bf16[4,240,512]{2,1,0:T(8,128)(2,1)} %shard_map.235), calls=%async_computation.4 | async-start | bytes 1966080 | tf_op jit(solution)/shard_map/all_to_all | solution.py:20
  122.4 12.5 %collective-permute-start.18 = (bf16[48,2176]{1,0:T(8,128)(2,1)}, bf16[48,2176]{1,0:T(8,128)(2,1)S(1)}, u32[]{:S(2)}, u32[]{:S(2)}) collective-permute-start(bf16[48,2176]{1,0:T(8,128)(2,1)} %get-tuple-element.36), channel_id=1, source_target_pairs={{0,2},{2,4},{4,6},{6,0},{1,3},{3,5},{5,7},{7,1},{8,10},{10,12},{12... | collective-permute-start | bytes 626696 | tf_op jit(solution)/shard_map/ppermute | solution.py:29
  123.9 13.1 %collective-permute-start.19 = (bf16[48,2176]{1,0:T(8,128)(2,1)}, bf16[48,2176]{1,0:T(8,128)(2,1)S(1)}, u32[]{:S(2)}, u32[]{:S(2)}) collective-permute-start(bf16[48,2176]{1,0:T(8,128)(2,1)} %get-tuple-element.37), channel_id=1, source_target_pairs={{0,4},{2,6},{4,0},{6,2},{1,5},{3,7},{5,1},{7,3},{8,12},{10,14},{12... | collective-permute-start | bytes 626696 | tf_op jit(solution)/shard_map/ppermute | solution.py:29
  124.6 15.8 %collective-permute-start.20 = (bf16[48,2176]{1,0:T(8,128)(2,1)S(1)}, bf16[48,2176]{1,0:T(8,128)(2,1)S(1)}, u32[]{:S(2)}, u32[]{:S(2)}) collective-permute-start(bf16[48,2176]{1,0:T(8,128)(2,1)S(1)} %get-tuple-element.38), channel_id=1, source_target_pairs={{0,6},{2,0},{4,2},{6,4},{1,7},{3,1},{5,3},{7,5},{8,14},{10,8},{12,... | collective-permute-start | bytes 626696 | tf_op jit(solution)/shard_map/ppermute | solution.py:29
  141.0 5.0 %collective-permute-start.21 = (bf16[48,1024]{1,0:T(8,128)(2,1)S(1)}, bf16[48,1024]{1,0:T(8,128)(2,1)S(1)}, u32[]{:S(2)}, u32[]{:S(2)}) collective-permute-start(bf16[48,1024]{1,0:T(8,128)(2,1)S(1)} %shard_map.237.refs_1_), channel_id=1, source_target_pairs={{0,2},{2,4},{4,6},{6,0},{1,3},{3,5},{5,7},{7,1},{8,10},{10,12},{12... | collective-permute-start | bytes 294920 | tf_op jit(solution)/shard_map/ppermute | solution.py:29
  141.9 6.4 %collective-permute-start.22 = (bf16[48,1024]{1,0:T(8,128)(2,1)S(1)}, bf16[48,1024]{1,0:T(8,128)(2,1)S(1)}, u32[]{:S(2)}, u32[]{:S(2)}) collective-permute-start(bf16[48,1024]{1,0:T(8,128)(2,1)S(1)} %shard_map.237.refs_1_), channel_id=1, source_target_pairs={{0,4},{2,6},{4,0},{6,2},{1,5},{3,7},{5,1},{7,3},{8,12},{10,14},{12... | collective-permute-start | bytes 294920 | tf_op jit(solution)/shard_map/ppermute | solution.py:29
  144.8 4.6 %collective-permute-start.23 = (bf16[48,1024]{1,0:T(8,128)(2,1)S(1)}, bf16[48,1024]{1,0:T(8,128)(2,1)S(1)}, u32[]{:S(2)}, u32[]{:S(2)}) collective-permute-start(bf16[48,1024]{1,0:T(8,128)(2,1)S(1)} %shard_map.237.refs_1_), channel_id=1, source_target_pairs={{0,6},{2,0},{4,2},{6,4},{1,7},{3,1},{5,3},{7,5},{8,14},{10,8},{12,... | collective-permute-start | bytes 294920 | tf_op jit(solution)/shard_map/ppermute | solution.py:29
  155.9 20.8 %all-to-all-start.5 = ((bf16[64,24,128]{2,1,0:T(8,128)(2,1)}), bf16[64,24,128]{2,1,0:T(8,128)(2,1)S(1)}, u32[]{:S(2)}, u32[]{:S(2)}) async-start(bf16[64,24,128]{2,1,0:T(8,128)(2,1)} %bitcast.16), calls=%async_computation.5 | async-start | bytes 786432 | tf_op jit(solution)/shard_map/all_to_all | solution.py:20
  161.8 5.2 %collective-permute-start.24 = (bf16[48,256]{1,0:T(8,128)(2,1)S(1)}, bf16[48,256]{1,0:T(8,128)(2,1)S(1)}, u32[]{:S(2)}, u32[]{:S(2)}) collective-permute-start(bf16[48,256]{1,0:T(8,128)(2,1)S(1)} %get-tuple-element.42), channel_id=1, source_target_pairs={{0,1},{1,0},{2,3},{3,2},{4,5},{5,4},{6,7},{7,6},{8,9},{9,8},{10,11... | collective-permute-start | bytes 73736 | tf_op jit(solution)/shard_map/ppermute | solution.py:24
  (11 other events, 232.1 us)

commit v11 on v10

--- a/solution.py
+++ b/solution.py
@@ -41,12 +41,14 @@
     return x * jax.nn.sigmoid(x)
 
 
-def call(body, outs, flops, kinds, *args, mib=52, scratch=()):
+def call(body, outs, flops, kinds, *args, mib=53, scratch=()):
     kinds, out_kinds = kinds.split()
+    placed = kinds[0] == "s"
+    kinds = kinds[1:] if placed else kinds
     moved = sum(a.size * a.dtype.itemsize for a in args) + sum(
         o.size * o.dtype.itemsize for o in outs
     )
-    space = {"s": pltpu.SMEM, "v": pltpu.VMEM}
+    space = {"v": pltpu.VMEM}
     fetched = [i for i, k in enumerate(kinds) if k in "hlqegd"]
     stored = [i for i, k in enumerate(out_kinds) if k == "h"]
 
@@ -65,13 +67,14 @@
         in_room, rest = rest[: len(room)], rest[len(room) :]
         result_room, rest = rest[: len(out_room)], rest[len(out_room) :]
         in_sem, out_sem, extra = rest[0], rest[1], rest[2:]
+        at = tuple(lax.axis_index(a) for a in ("y", "c", "x"))
         late, now, order = [], [], []
         sem = 0
         for n, i in enumerate(fetched):
             kind = kinds[i]
             source = ins[i]
             if kind == "e":
-                source = source.at[ins[0][1]]
+                source = source.at[at[1]]
             elif kind == "d":
                 source = source.at[2]
             parts = pieces[kind]
@@ -96,10 +99,8 @@
             results[i] = result_room[n]
         for copy in now:
             copy.wait()
-        if late:
-            body(late, *ins, *results, *extra)
-        else:
-            body(*ins, *results, *extra)
+        before = ([late] if late else []) + ([at] if placed else [])
+        body(*before, *ins, *results, *extra)
         back = [
             pltpu.make_async_copy(result_room[n], targets[i], out_sem.at[n])
             for n, i in enumerate(stored)
@@ -224,12 +225,12 @@
                 lines[z * chunk : (z + 1) * chunk, :] = (before + part).astype(BF)
 
 
-def finish(lines, within, slots, weight, resid, shared, shared_other, mix, out):
+def finish(lines, within, slots, weight, resid, shared, mix, out):
     seq, cols = out.shape
     half = cols // 2
     place = lax.broadcasted_iota(jnp.int32, (seq, lines.shape[0]), 1)
     gate = jax.nn.sigmoid(mix[...])
-    base = resid[...] + shared[...] + shared_other[...].astype(F32)
+    base = resid[...] + shared[...]
     for h in range(2):
         routed = jnp.zeros(place.shape, F32)
         for k in range(4):
@@ -241,10 +242,8 @@
         out[:, cut] = total.astype(BF)
 
 
-def unpack_rows(at, line_of, lines, own, other, both, dense):
-    first = at[1] == 0
+def unpack_rows(line_of, lines, routed, dense):
     group = line_of.shape[1]
-    count = dense.shape[1]
     cols = dense.shape[2]
     half = cols // 2
     part = group // 8
@@ -252,11 +251,6 @@
     move = jnp.where(
         lax.broadcasted_iota(jnp.int32, (group, group), 0) == line_of[...], 1.0, 0.0
     ).astype(BF)
-    mine, others = own[...], other[...]
-    both_rows = [
-        jnp.where(first, mine, others),
-        jnp.where(first, others, mine),
-    ]
     for g in range(groups):
         rows = dot(move, lines[g * group : (g + 1) * group, :]).astype(BF)
         here = slice(g * part, (g + 1) * part)
@@ -264,12 +258,37 @@
             for h in range(2):
                 base = (side * 2 + h) * 2 * part
                 at_col = side * cols + h * half
-                for copy in range(both.shape[0]):
-                    both[copy, here, at_col : at_col + half] = rows[base : base + part]
+                for copy in range(routed.shape[0]):
+                    routed[copy, here, at_col : at_col + half] = rows[base : base + part]
                 dense[side, here, h * half : (h + 1) * half] = rows[base + part : base + 2 * part]
-    for side in range(2):
-        for copy in range(both.shape[0]):
-            both[copy, count:, side * cols : (side + 1) * cols] = both_rows[side]
+
+
+def shared_expert(wait, at, s0, s1, s2, s3, gain, gate, up, down, keep, give):
+    y, c = at[0], at[1]
+    first = c == 0
+    cols = keep.shape[2]
+    half = gate.shape[1]
+    square = total = None
+    for k in (0, 1):
+        wait[k][0]()
+    for d, piece in enumerate((s0, s1, s2, s3)):
+        for side, core in enumerate((c, 1 - c)):
+            block = 2 * lax.rem(y + 4 - d, 4) + core
+            cut = pl.ds(pl.multiple_of(block * cols, cols), cols)
+            value = piece[:, side * cols : (side + 1) * cols].astype(F32)
+            more = jnp.sum(value * value, axis=1, keepdims=True)
+            square = more if square is None else square + more
+            rows = (value * gain[pl.ds(block, 1), :]).astype(BF)
+            term = dot(rows, jnp.concatenate([gate[cut, :], up[cut, :]], axis=1))
+            total = term if total is None else total + term
+    total = total * lax.rsqrt(square / (8 * cols) + EPS)
+    hidden = (silu(total[:, :half]) * total[:, half:]).astype(BF)
+    wait[2][0]()
+    for i in range(keep.shape[0]):
+        even = dot(hidden, down[:, 2 * i * cols : (2 * i + 1) * cols]).astype(BF)
+        odd = dot(hidden, down[:, (2 * i + 1) * cols : (2 * i + 2) * cols]).astype(BF)
+        keep[i] = jnp.where(first, even, odd)
+        give[i] = jnp.where(first, odd, even)
 
 
 def dense_first_half(wait, at, rows, gain, *refs):
@@ -343,47 +362,44 @@
             out[side, pl.ds(start, size), :] = total[d * size : (d + 1) * size]
 
 
-def experts_and_shared(
+def experts(
     wait, at, whole, gain, gate, gate_other, up, up_other, down, down_other,
-    shared_gate, shared_up, shared_down, parts,
+    shared, shared_other, parts,
 ):
-    ny, lines, block = whole.shape
-    count = lines - 48
-    half = gate.shape[1]
-    square = jnp.zeros((lines, 1), F32)
-    gate_pre = up_pre = shared_pre = None
+    ny, count, block = whole.shape
+    square = jnp.zeros((count, 1), F32)
+    gate_pre = up_pre = None
 
     def more(total, term):
         return term if total is None else total + term
 
     for i in range(ny):
         cut = slice(i * block, (i + 1) * block)
-        for k in (0, 1, 2, 3, 4, 7, 8):
+        for k in (0, 1, 2, 3, 4):
             wait[k][i]()
         value = whole[i].astype(F32)
         square = square + jnp.sum(value * value, axis=1, keepdims=True)
         rows = (value * gain[:, cut]).astype(BF)
         gates = jnp.concatenate([gate[cut, :], gate_other[cut, :]], axis=1)
         ups = jnp.concatenate([up[cut, :], up_other[cut, :]], axis=1)
-        shared = jnp.concatenate([shared_gate[cut, :], shared_up[cut, :]], axis=1)
-        gate_pre = more(gate_pre, dot(rows[:count], gates))
-        up_pre = more(up_pre, dot(rows[:count], ups))
-        shared_pre = more(shared_pre, dot(rows[count:], shared))
+        gate_pre = more(gate_pre, dot(rows, gates))
+        up_pre = more(up_pre, dot(rows, ups))
     scale = lax.rsqrt(square / (ny * block) + EPS)
-    hidden = (silu(gate_pre * scale[:count]) * (up_pre * scale[:count])).astype(BF)
-    shared_pre = shared_pre * scale[count:]
-    shared_hidden = (silu(shared_pre[:, :half]) * shared_pre[:, half:]).astype(BF)
-    for k in (5, 6, 9):
+    hidden = (silu(gate_pre * scale) * (up_pre * scale)).astype(BF)
+    for k in (5, 6):
         for done in wait[k]:
             done()
+    tall, cols = shared.shape[1] // 2, shared.shape[2]
     for i in range(ny):
         cut = slice(i * block, (i + 1) * block)
         downs = jnp.concatenate([down[:, cut], down_other[:, cut]], axis=0)
         parts[i, :count, :] = dot(hidden, downs).astype(BF)
-        parts[i, count:, :] = dot(shared_hidden, shared_down[:, cut]).astype(BF)
-
-
-def pack_lines(at, line_of, parts, dense, lines, shared_own, shared_send):
+        both = (shared[i].astype(F32) + shared_other[i].astype(F32)).astype(BF)
+        parts[i, count:, :cols] = both[:tall]
+        parts[i, count:, cols:] = both[tall:]
+
+
+def pack_lines(at, line_of, parts, dense, lines, shared_out):
     first = at[1] == 0
     group = line_of.shape[0]
     part = group // 8
@@ -398,9 +414,9 @@
     for i in range(1, parts.shape[0]):
         total = total + parts[i].astype(F32)
     routed = total[:count].astype(BF)
-    shared = total[count:]
-    shared_own[...] = jnp.where(first, shared[:, :cols], shared[:, cols:])
-    shared_send[...] = jnp.where(first, shared[:, cols:], shared[:, :cols]).astype(BF)
+    tall = shared_out.shape[0] // 2
+    shared_out[:tall, :] = total[count:, :cols]
+    shared_out[tall:, :] = total[count:, cols:]
     for g in range(groups):
         here = slice(g * part, (g + 1) * part)
         own, other = dense[0, here, :], dense[1, here, :]
@@ -441,21 +457,19 @@
     dense_mix,
 ):
     nz, nx, ny, nc = (lax.axis_size(a) for a in ("z", "x", "y", "c"))
-    x, y, c = (lax.axis_index(a) for a in ("x", "y", "c"))
+    _, _, c = (lax.axis_index(a) for a in ("x", "y", "c"))
     seq, width = tokens.shape
     rows_w, chan = w_query.shape
     head_dim = state.shape[2]
     cols = width // (ny * nc)
 
-    at = jnp.stack([y, c, x]).astype(jnp.int32)
-
     topk = route_ids.shape[1]
-    experts = nz * nx * nc
-    cap = max(2, 2 * seq * topk // experts)
+    n_experts = nz * nx * nc
+    cap = max(2, 2 * seq * topk // n_experts)
     slots = 2 * cap
     half = cols // 2
     flat_ids = route_ids.reshape(-1)
-    onehot = (flat_ids[:, None] == jnp.arange(experts, dtype=jnp.int32)[None, :]).astype(jnp.int32)
+    onehot = (flat_ids[:, None] == jnp.arange(n_experts, dtype=jnp.int32)[None, :]).astype(jnp.int32)
     rank = jnp.sum((jnp.cumsum(onehot, axis=0) - onehot) * onehot, axis=1)
     lines_of = (flat_ids * (2 * slots) + rank).reshape(seq, topk)
     token_ids = jnp.arange(seq, dtype=jnp.int32)
@@ -464,7 +478,7 @@
         [lines_of, dense_of[:, None], jnp.zeros((seq, 8 - topk - 1), jnp.int32)], axis=1
     )
     slot_rows = slot_cols.T
-    within = (jnp.arange(experts * 2 * slots, dtype=jnp.int32) % (nx * nc * 2 * slots))[None, :]
+    within = (jnp.arange(n_experts * 2 * slots, dtype=jnp.int32) % (nx * nc * 2 * slots))[None, :]
 
     (spread_w,) = call(
         copies,
@@ -483,7 +497,6 @@
         [shaped(3, *dense_gate.shape)] + [shaped(seq, nz * rows_w)] * nx,
         10**6,
         "shhhhh hhhhh",
-        at,
         tokens,
         norm_gain.reshape(1, width),
         dense_gate,
@@ -508,7 +521,6 @@
         [shaped(seq, chan, dtype=F32)] * 3 + [shaped(ny, seq, cols)] * 2,
         4 * state.size,
         "shvvvhhql hhhvh",
-        at,
         *pieces,
         lower_bound.reshape(1, chan),
         head_gain.reshape(1, chan),
@@ -529,16 +541,15 @@
         [
             shaped(seq, cols, dtype=F32),
             shaped(seq, cols),
-            shaped(experts * 2 * slots, half),
+            shaped(n_experts * 2 * slots, half),
         ],
-        4 * experts * 2 * slots * seq * half,
+        4 * n_experts * 2 * slots * seq * half,
         "svhh hhh",
-        at,
         heads,
         tokens,
         slot_rows,
     )
-    arrived = swap(outgoing.reshape(experts, 2 * slots, half), HUB)
+    arrived = swap(outgoing.reshape(n_experts, 2 * slots, half), HUB)
     other = partner(own)
     count = nz * nx * cap
 
@@ -552,16 +563,28 @@
         rest % cap,
     )
     line_of = ((side * 2 + h) * 2 + kind) * (8 * cap) + source * cap + r
+    lines_own = jnp.concatenate([own, other], axis=1)
+    pieces = [lines_own] + [shift(lines_own, "y", d) for d in range(1, ny)]
+    shared_keep, shared_give = call(
+        shared_expert,
+        [shaped(ny, seq, cols)] * 2,
+        2 * 3 * seq * width * shared_gate.shape[1],
+        "shvvvhlll hh",
+        *pieces,
+        ffn_gain.reshape(ny * nc, cols),
+        shared_gate,
+        shared_up,
+        shared_down,
+    )
+    shared_other = partner(shared_give)
+
     both, dense_rows = call(
         unpack_rows,
-        [shaped(ny, count + seq, nc * cols), shaped(nc, count, cols)],
+        [shaped(ny, count, nc * cols), shaped(nc, count, cols)],
         4 * 2 * group * group * half,
-        "shvhv hh",
-        at,
+        "hv hh",
         line_of.reshape(1, group),
         arrived.reshape(-1, half),
-        own,
-        other,
     )
     whole = swap(both, "y")
 
@@ -572,7 +595,6 @@
         [shaped(quarter, 2 * hidden_width + 128)] * ny,
         2 * count * nc * cols * 2 * hidden_width,
         "shhgggggggg hhhh",
-        at,
         dense_rows,
         ffn_gain.reshape(ny * nc, cols),
         *dense_own,
@@ -588,18 +610,16 @@
         [shaped(nc, count, cols)],
         2 * count * nc * cols * hidden_width,
         "shvvvdddddddd h",
-        at,
         *hidden,
         *dense_own,
         *dense_other,
     )
 
     (parts,) = call(
-        experts_and_shared,
-        [shaped(ny, count + seq, nc * cols)],
-        2 * 3 * (count * 2 + seq) * width * expert_gate.shape[2],
-        "sqheqeqeqqqq h",
-        at,
+        experts,
+        [shaped(ny, count + seq // 2, nc * cols)],
+        2 * 3 * count * 2 * width * expert_gate.shape[2],
+        "sqheqeqeqhv h",
         whole,
         ffn_gain.reshape(1, width),
         expert_gate,
@@ -608,39 +628,32 @@
         up_other,
         expert_down,
         down_other,
-        shared_gate,
-        shared_up,
-        shared_down,
+        shared_keep,
+        shared_other,
     )
     parts = swap(parts, "y")
-    back, shared_own, shared_send = call(
+    back, shared_out = call(
         pack_lines,
-        [
-            shaped(experts * 2 * slots, half),
-            shaped(seq, cols, dtype=F32),
-            shaped(seq, cols),
-        ],
+        [shaped(n_experts * 2 * slots, half), shaped(seq, cols, dtype=F32)],
         4 * 2 * group * group * half,
-        "shvh hhh",
-        at,
+        "shvh hh",
         line_of.reshape(group, 1),
         parts,
         dense_part,
     )
 
-    results = swap(back.reshape(experts, 2 * slots, half), HUB)
+    results = swap(back.reshape(n_experts, 2 * slots, half), HUB)
     (mixed,) = call(
         finish,
         [shaped(seq, cols)],
-        8 * experts * 2 * slots * seq * half,
-        "vhhhhhvh h",
-        results.reshape(experts * 2 * slots, half),
+        8 * n_experts * 2 * slots * seq * half,
+        "vhhhhhh h",
+        results.reshape(n_experts * 2 * slots, half),
         within,
         slot_cols,
         route_weight,
         resid,
-        shared_own,
-        partner(shared_send),
+        shared_out,
         dense_mix.reshape(1, cols),
     )
     return (mixed, new_state)

time: 181 us -> 187 us (1.033)
  starting transfers between devices: 60.7 us -> 66.9 us
  waiting for transfers between devices: 68.1 us -> 70.8 us
  Pallas kernels: 30.5 us -> 28 us
    ppermute x15 -> x18, starting transfers between devices: 25 us -> 29 us  [shift(): return lax.ppermute(x, axis, [(i, (i + by) % size) for i in range(size)])]
    all_to_all x6, waiting for transfers between devices: 26.6 us -> 29.4 us  [swap(): return lax.all_to_all(x, axis, split_axis=0, concat_axis=0, tiled=True)]
    pallas_call x11 -> x12, Pallas kernels: 30.5 us -> 28 us  [call(): pl.pallas_call(whole, out_shape=outs, in_specs=[pl.BlockSpec(memory_space...]
    ppermute x15 -> x18, waiting for transfers between devices: 38.5 us -> 40.1 us  [shift(): return lax.ppermute(x, axis, [(i, (i + by) % size) for i in range(size)])]
  transfers between devices with their start and end apart: 31 -> 34, of which waited for: 17 -> 17; matrix products, arithmetic and copies ran while one was open for 8% -> 8% of each run, Pallas kernels for 11% -> 12%
where the time goes in v11:
time: 187 us; the launch traced here: 184 us
  waiting for transfers between devices  70.8 us (38%)
  starting transfers between devices  66.9 us (36%)
  Pallas kernels  28 us (15%)
  other arithmetic  8.1 us (4%)
  local copies, waits for them, and re-layouts  7.96 us (4%)
    ppermute x18, waiting for transfers between devices, shift(): return lax.ppermute(x, axis, [(i, (i + by) % size) for i in range(size)])  40.1 us
    all_to_all x6, starting transfers between devices, swap(): return lax.all_to_all(x, axis, split_axis=0, concat_axis=0, tiled=True)  35.5 us
    all_to_all x6, waiting for transfers between devices, swap(): return lax.all_to_all(x, axis, split_axis=0, concat_axis=0, tiled=True)  29.4 us
    ppermute x18, starting transfers between devices, shift(): return lax.ppermute(x, axis, [(i, (i + by) % size) for i in range(size)])  29 us
    pallas_call x12, Pallas kernels, call(): pl.pallas_call(whole, out_shape=outs, in_specs=[pl.BlockSpec(memory_space...  28 us
    add x1, other arithmetic, step(): decay.reshape(shape)[..., None] * state  5.08 us
    squeeze x3, local copies, waits for them, and re-layouts, pick(): return lax.dynamic_index_in_dim(x, index, 0, keepdims=False)  4.6 us
  transfers between devices with their start and end apart: 34, of which 17 were waited for; matrix products, arithmetic and copies ran while one was open for 8% of the time, Pallas kernels for 12%

profile of v11, /device:TPU:8, one launch (start us, length us, event | category | flops | bytes accessed | tf_op | source)
XLA Modules:
  0.0 184.0 jit_solution(13375551239819710521)
XLA Ops:
  2.4 8.5 %all-to-all-start = ((bf16[8,64,512]{2,1,0:T(8,128)(2,1)}), bf16[8,64,512]{2,1,0:T(8,128)(2,1)S(1)}, u32[]{:S(2)}, u32[]{:S(2)}) async-start(bf16[8,64,512]{2,1,0:T(8,128)(2,1)} %shard_map.231), calls=%async_computation | async-start | bytes 1048576 | tf_op jit(solution)/shard_map/all_to_all | solution.py:20
  10.8 2.2 %shard_map.230 = (bf16[3,256,256]{2,1,0:T(8,128)(2,1)}, bf16[48,512]{1,0:T(8,128)(2,1)}, bf16[48,512]{1,0:T(8,128)(2,1)}, bf16[48,512]{1,0:T(8,128)(2,1)}, bf16[48,512]{1,0:T(8,128)(2,1)}) custom-call(bf16[48,2048]{1,0:T(8,128)(2,1)} %refs_1_.3, f32[1,2048]{1,0:T(1,128)} %bitcast.40, bf16[256,256]{1,0:T(8,128)(2,1)} %refs_2_.3, bf16[256,256]{1,0:T(8,128)(2,1)} %refs_3_.3, ...), custom_call_target="tpu_custom_call" | custom-call | flops 1000000 | bytes 1187840 | tf_op jit(solution)/shard_map/pallas_call | solution.py:113
  14.7 2.7 %collective-permute-start.1 = (bf16[48,512]{1,0:T(8,128)(2,1)}, bf16[48,512]{1,0:T(8,128)(2,1)S(1)}, u32[]{:S(2)}, u32[]{:S(2)}) collective-permute-start(bf16[48,512]{1,0:T(8,128)(2,1)} %get-tuple-element.27), channel_id=1, source_target_pairs={{0,16},{8,24},{16,0},{24,8},{1,17},{9,25},{17,1},{25,9},{2,18},{10... | collective-permute-start | bytes 147464 | tf_op jit(solution)/shard_map/ppermute | solution.py:29
  22.0 6.4 %all-to-all-done = bf16[8,64,512]{2,1,0:T(8,128)(2,1)S(1)} async-done(((bf16[8,64,512]{2,1,0:T(8,128)(2,1)}), bf16[8,64,512]{2,1,0:T(8,128)(2,1)S(1)}, u32[]{:S(2)}, u32[]{:S(2)}) %all-to-all-start) | async-done | bytes 524320 | tf_op jit(solution)/shard_map/all_to_all | solution.py:20
  29.5 2.8 %collective-permute-start.3 = (bf16[48,512]{1,0:T(8,128)(2,1)S(1)}, bf16[48,512]{1,0:T(8,128)(2,1)S(1)}, u32[]{:S(2)}, u32[]{:S(2)}) collective-permute-start(bf16[48,512]{1,0:T(8,128)(2,1)S(1)} %get-tuple-element.50), channel_id=1, source_target_pairs={{0,24},{8,0},{16,8},{24,16},{1,25},{9,1},{17,9},{25,17},{2,26},{10... | collective-permute-start | bytes 147464 | tf_op jit(solution)/shard_map/ppermute | solution.py:29
  34.4 3.5 %collective-permute-done.4.refs_2_ = bf16[48,512]{1,0:T(8,128)(2,1)S(1)} collective-permute-done((bf16[48,512]{1,0:T(8,128)(2,1)S(1)}, bf16[48,512]{1,0:T(8,128)(2,1)S(1)}, u32[]{:S(2)}, u32[]{:S(2)}) %collective-permute-start.4) | collective-permute-done | bytes 49184 | tf_op jit(solution)/shard_map/ppermute | solution.py:29
  38.4 3.1 %shard_map.232 = (f32[48,128]{1,0:T(8,128)S(1)}, f32[48,128]{1,0:T(8,128)S(1)}, f32[48,128]{1,0:T(8,128)S(1)}, bf16[4,48,256]{2,1,0:T(8,128)(2,1)S(1)}, bf16[4,48,256]{2,1,0:T(8,128)(2,1)S(1)}) custom-call(bf16[48,512]{1,0:T(8,128)(2,1)S(1)} %get-tuple-element.51.refs_0_, bf16[48,512]{1,0:T(8,128)(2,1)S(1)} %collective-permute-done.3.refs_1_, ...), custom_call_target="tpu_custom_call" | custom-call | flops 3145728 | bytes 4137984 | tf_op jit(solution)/shard_map/pallas_call | solution.py:113
  43.6 4.9 %all-to-all-start.1 = ((bf16[4,48,256]{2,1,0:T(8,128)(2,1)}), bf16[4,48,256]{2,1,0:T(8,128)(2,1)S(1)}, u32[]{:S(2)}, u32[]{:S(2)}) async-start(bf16[4,48,256]{2,1,0:T(8,128)(2,1)} %add_convert_fusion), calls=%async_computation.1 | async-start | bytes 196608 | tf_op jit(solution)/shard_map/all_to_all | solution.py:20
  48.7 4.2 %all-to-all-done.1.refs_0_ = bf16[4,48,256]{2,1,0:T(8,128)(2,1)S(1)} async-done(((bf16[4,48,256]{2,1,0:T(8,128)(2,1)}), bf16[4,48,256]{2,1,0:T(8,128)(2,1)S(1)}, u32[]{:S(2)}, u32[]{:S(2)}) %all-to-all-start.1) | async-done | bytes 98336 | tf_op jit(solution)/shard_map/all_to_all | solution.py:20
  52.9 2.1 %shard_map.233 = (f32[48,256]{1,0:T(8,128)S(1)}, bf16[48,256]{1,0:T(8,128)(2,1)S(1)}, bf16[1536,128]{1,0:T(8,128)(2,1)}) custom-call(bf16[4,48,256]{2,1,0:T(8,128)(2,1)S(1)} %all-to-all-done.1.refs_0_, bf16[48,2048]{1,0:T(8,128)(2,1)S(1)} %copy-done, s32[8,48]{1,0:T(8,128)S(1)} %copy.55.refs_2_), custom_call_target="tpu_custom_call" | custom-call | flops 37748736 | bytes 763392 | tf_op jit(solution)/shard_map/pallas_call | solution.py:113
  55.0 4.8 %all-to-all-start.2 = ((bf16[64,24,128]{2,1,0:T(8,128)(2,1)}), bf16[64,24,128]{2,1,0:T(8,128)(2,1)S(1)}, u32[]{:S(2)}, u32[]{:S(2)}) async-start(bf16[64,24,128]{2,1,0:T(8,128)(2,1)} %bitcast.7), calls=%async_computation.2 | async-start | bytes 786432 | tf_op jit(solution)/shard_map/all_to_all | solution.py:20
  65.8 9.0 %all-to-all-done.2 = bf16[64,24,128]{2,1,0:T(8,128)(2,1)S(1)} async-done(((bf16[64,24,128]{2,1,0:T(8,128)(2,1)}), bf16[64,24,128]{2,1,0:T(8,128)(2,1)S(1)}, u32[]{:S(2)}, u32[]{:S(2)}) %all-to-all-start.2) | async-done | bytes 393248 | tf_op jit(solution)/shard_map/all_to_all | solution.py:20
  76.2 4.9 %all-to-all-start.3 = ((bf16[4,192,512]{2,1,0:T(8,128)(2,1)}), bf16[4,192,512]{2,1,0:T(8,128)(2,1)S(1)}, u32[]{:S(2)}, u32[]{:S(2)}) async-start(bf16[4,192,512]{2,1,0:T(8,128)(2,1)} %get-tuple-element.32), calls=%async_computation.3 | async-start | bytes 1572864 | tf_op jit(solution)/shard_map/all_to_all | solution.py:20
  83.3 9.1 %collective-permute-done.11.refs_1_ = bf16[48,512]{1,0:T(8,128)(2,1)S(1)} collective-permute-done((bf16[48,512]{1,0:T(8,128)(2,1)S(1)}, bf16[48,512]{1,0:T(8,128)(2,1)S(1)}, u32[]{:S(2)}, u32[]{:S(2)}) %collective-permute-start.11) | collective-permute-done | bytes 49184 | tf_op jit(solution)/shard_map/ppermute | solution.py:29
  92.4 2.8 %collective-permute-start.13 = (bf16[48,512]{1,0:T(8,128)(2,1)S(1)}, bf16[48,512]{1,0:T(8,128)(2,1)S(1)}, u32[]{:S(2)}, u32[]{:S(2)}) collective-permute-start(bf16[48,512]{1,0:T(8,128)(2,1)S(1)} %constant_dynamic-update-slice_fusion.refs_0_), channel_id=1, source_target_pairs={{0,6},{2,0},{4,2},{6,4},{1,7},{3,1},{5,3},{7,5},{8,14},{10,8},{12,... | collective-permute-start | bytes 147464 | tf_op jit(solution)/shard_map/ppermute | solution.py:29
  95.2 2.2 %collective-permute-start.16 = (bf16[3,256,256]{2,1,0:T(8,128)(2,1)}, bf16[3,256,256]{2,1,0:T(8,128)(2,1)S(1)}, u32[]{:S(2)}, u32[]{:S(2)}) collective-permute-start(bf16[3,256,256]{2,1,0:T(8,128)(2,1)} %get-tuple-element.37.refs_2_.refs_4_), channel_id=1, source_target_pairs={{0,16},{8,24},{16,0},{24,8},{1,17},{9,25},{17,1},{25,9},{2,18},{10... | collective-permute-start | bytes 1179656 | tf_op jit(solution)/shard_map/ppermute | solution.py:29
  99.2 2.1 %shard_map.235 = (bf16[4,48,256]{2,1,0:T(8,128)(2,1)S(1)}, bf16[4,48,256]{2,1,0:T(8,128)(2,1)S(1)}) custom-call(bf16[48,512]{1,0:T(8,128)(2,1)S(1)} %constant_dynamic-update-slice_fusion.refs_0_, bf16[48,512]{1,0:T(8,128)(2,1)S(1)} %collective-permute-done.11.refs_1_, bf16[48,512]{1,0:T(8,128)(2,1)S(1)} %collective-permute-done.12.refs_2_, ...), custom_call_target="tpu_custom_call" | custom-call | flops 75497472 | bytes 1974272 | tf_op jit(solution)/shard_map/pallas_call | solution.py:113
  101.3 4.6 %collective-permute-done.16.refs_4_.refs_6_ = bf16[3,256,256]{2,1,0:T(8,128)(2,1)S(1)} collective-permute-done((bf16[3,256,256]{2,1,0:T(8,128)(2,1)}, bf16[3,256,256]{2,1,0:T(8,128)(2,1)S(1)}, u32[]{:S(2)}, u32[]{:S(2)}) %collective-permute-start.16) | collective-permute-done | bytes 393248 | tf_op jit(solution)/shard_map/ppermute | solution.py:29
  105.9 6.4 %collective-permute-done.17.refs_5_.refs_7_ = bf16[3,256,256]{2,1,0:T(8,128)(2,1)} collective-permute-done((bf16[3,256,256]{2,1,0:T(8,128)(2,1)}, bf16[3,256,256]{2,1,0:T(8,128)(2,1)}, u32[]{:S(2)}, u32[]{:S(2)}) %collective-permute-start.17) | collective-permute-done | bytes 393248 | tf_op jit(solution)/shard_map/ppermute | solution.py:29
  114.3 3.9 %shard_map.236 = bf16[4,216,512]{2,1,0:T(8,128)(2,1)} custom-call(bf16[4,192,512]{2,1,0:T(8,128)(2,1)} %copy-done.7, f32[1,2048]{1,0:T(1,128)S(1)} %bitcast.34, bf16[2,2048,128]{2,1,0:T(8,128)(2,1)} %refs_2_.5, bf16[2048,128]{1,0:T(8,128)(2,1)S(1)} %collective-permute-done.7.refs_3_, bf16[2,2048,128]{2,1,0:T(8,128)(2,1)} %refs_4_.3, ...), custom_call_target="tpu_custom_call" | custom-call | flops 603979776 | bytes 6594560 | tf_op jit(solution)/shard_map/pallas_call | solution.py:113
  118.2 5.8 %all-to-all-start.4 = ((bf16[4,216,512]{2,1,0:T(8,128)(2,1)}), bf16[4,216,512]{2,1,0:T(8,128)(2,1)S(1)}, u32[]{:S(2)}, u32[]{:S(2)}) async-start(bf16[4,216,512]{2,1,0:T(8,128)(2,1)} %shard_map.236), calls=%async_computation.4 | async-start | bytes 1769472 | tf_op jit(solution)/shard_map/all_to_all | solution.py:20
  124.0 4.2 %shard_map.237 = (bf16[48,2176]{1,0:T(8,128)(2,1)S(1)}, bf16[48,2176]{1,0:T(8,128)(2,1)S(1)}, bf16[48,2176]{1,0:T(8,128)(2,1)S(1)}, bf16[48,2176]{1,0:T(8,128)(2,1)}) custom-call(bf16[2,192,256]{2,1,0:T(8,128)(2,1)S(1)} %get-tuple-element.36.refs_0_, f32[8,256]{1,0:T(8,128)S(1)} %reshape.583.refs_4_.refs_1_, ...), custom_call_target="tpu_custom_call" | custom-call | flops 402653184 | bytes 4186112 | tf_op jit(solution)/shard_map/pallas_call | solution.py:113
  130.5 2.5 %collective-permute-start.24 = (bf16[48,2176]{1,0:T(8,128)(2,1)}, bf16[48,2176]{1,0:T(8,128)(2,1)S(1)}, u32[]{:S(2)}, u32[]{:S(2)}) collective-permute-start(bf16[48,2176]{1,0:T(8,128)(2,1)} %get-tuple-element.41), channel_id=1, source_target_pairs={{0,6},{2,0},{4,2},{6,4},{1,7},{3,1},{5,3},{7,5},{8,14},{10,8},{12,... | collective-permute-start | bytes 626696 | tf_op jit(solution)/shard_map/ppermute | solution.py:29
  133.2 6.6 %collective-permute-done.22.refs_1_ = bf16[48,2176]{1,0:T(8,128)(2,1)S(1)} collective-permute-done((bf16[48,2176]{1,0:T(8,128)(2,1)S(1)}, bf16[48,2176]{1,0:T(8,128)(2,1)S(1)}, u32[]{:S(2)}, u32[]{:S(2)}) %collective-permute-start.22) | collective-permute-done | bytes 208928 | tf_op jit(solution)/shard_map/ppermute | solution.py:29
  141.8 3.6 %collective-permute-done.24.refs_3_ = bf16[48,2176]{1,0:T(8,128)(2,1)S(1)} collective-permute-done((bf16[48,2176]{1,0:T(8,128)(2,1)}, bf16[48,2176]{1,0:T(8,128)(2,1)S(1)}, u32[]{:S(2)}, u32[]{:S(2)}) %collective-permute-start.24) | collective-permute-done | bytes 208928 | tf_op jit(solution)/shard_map/ppermute | solution.py:29
  146.9 3.0 %collective-permute-start.26 = (bf16[48,1024]{1,0:T(8,128)(2,1)S(1)}, bf16[48,1024]{1,0:T(8,128)(2,1)S(1)}, u32[]{:S(2)}, u32[]{:S(2)}) collective-permute-start(bf16[48,1024]{1,0:T(8,128)(2,1)S(1)} %shard_map.238.refs_0_), channel_id=1, source_target_pairs={{0,4},{2,6},{4,0},{6,2},{1,5},{3,7},{5,1},{7,3},{8,12},{10,14},{12... | collective-permute-start | bytes 294920 | tf_op jit(solution)/shard_map/ppermute | solution.py:29
  151.3 2.3 %collective-permute-done.26.refs_2_ = bf16[48,1024]{1,0:T(8,128)(2,1)S(1)} collective-permute-done((bf16[48,1024]{1,0:T(8,128)(2,1)S(1)}, bf16[48,1024]{1,0:T(8,128)(2,1)S(1)}, u32[]{:S(2)}, u32[]{:S(2)}) %collective-permute-start.26) | collective-permute-done | bytes 98336 | tf_op jit(solution)/shard_map/ppermute | solution.py:29
  154.7 2.2 %shard_map.239.refs_2_ = bf16[2,192,256]{2,1,0:T(8,128)(2,1)S(1)} custom-call(bf16[48,1024]{1,0:T(8,128)(2,1)S(1)} %shard_map.238.refs_0_, bf16[48,1024]{1,0:T(8,128)(2,1)S(1)} %collective-permute-done.25.refs_1_, bf16[48,1024]{1,0:T(8,128)(2,1)S(1)} %collective-permute-done.26.refs_2_, bf16[48,1024]{1,0:T(8,128)(2,1)S(1)} %collective-permute-done.27.refs_3_, ...), custom_call_target="tpu_custom_call" | custom-call | flops 201326592 | bytes 3735552 | tf_op jit(solution)/shard_map/pallas_call | solution.py:113
  157.9 2.9 %shard_map.240 = (bf16[1536,128]{1,0:T(8,128)(2,1)}, f32[48,256]{1,0:T(8,128)S(1)}) custom-call(s32[384,1]{1,0:T(8,128)S(1)} %fusion.8.refs_0_, bf16[4,216,512]{2,1,0:T(8,128)(2,1)} %copy-done.6, bf16[2,192,256]{2,1,0:T(8,128)(2,1)S(1)} %shard_map.239.refs_2_), custom_call_target="tpu_custom_call" | custom-call | flops 150994944 | bytes 1525248 | tf_op jit(solution)/shard_map/pallas_call | solution.py:113
  160.8 6.6 %all-to-all-start.5 = ((bf16[64,24,128]{2,1,0:T(8,128)(2,1)}), bf16[64,24,128]{2,1,0:T(8,128)(2,1)S(1)}, u32[]{:S(2)}, u32[]{:S(2)}) async-start(bf16[64,24,128]{2,1,0:T(8,128)(2,1)} %bitcast.13), calls=%async_computation.5 | async-start | bytes 786432 | tf_op jit(solution)/shard_map/all_to_all | solution.py:20
  167.6 5.1 %multiply_add_fusion = f32[48,1,128,128]{3,2,1,0:T(8,128)} fusion(f32[48,1,128,128]{3,2,1,0:T(8,128)} %param.24, f32[48,128]{1,0:T(8,128)S(1)} %get-tuple-element.47, f32[48,128]{1,0:T(8,128)S(1)} %get-tuple-element.46, f32[48,128]{1,0:T(8,128)S(1)} %get-tuple-element.45), kind=kLoop, calls=%fused_computation | loop fusion | flops 2359296 | bytes 6365184 | tf_op jit(solution)/shard_map/add | solution.py:533
  172.6 9.8 %all-to-all-done.5 = bf16[64,24,128]{2,1,0:T(8,128)(2,1)S(1)} async-done(((bf16[64,24,128]{2,1,0:T(8,128)(2,1)}), bf16[64,24,128]{2,1,0:T(8,128)(2,1)S(1)}, u32[]{:S(2)}, u32[]{:S(2)}) %all-to-all-start.5) | async-done | bytes 393248 | tf_op jit(solution)/shard_map/all_to_all | solution.py:20
  (106 shorter events, 37.8 us)
Async XLA Ops:
  2.4 26.0 %all-to-all-start = ((bf16[8,64,512]{2,1,0:T(8,128)(2,1)}), bf16[8,64,512]{2,1,0:T(8,128)(2,1)S(1)}, u32[]{:S(2)}, u32[]{:S(2)}) async-start(bf16[8,64,512]{2,1,0:T(8,128)(2,1)} %shard_map.231), calls=%async_computation | async-start | bytes 1048576 | tf_op jit(solution)/shard_map/all_to_all | solution.py:20
  13.1 8.9 %collective-permute-start = (bf16[48,512]{1,0:T(8,128)(2,1)}, bf16[48,512]{1,0:T(8,128)(2,1)S(1)}, u32[]{:S(2)}, u32[]{:S(2)}) collective-permute-start(bf16[48,512]{1,0:T(8,128)(2,1)} %get-tuple-element.26), channel_id=1, source_target_pairs={{0,8},{8,16},{16,24},{24,0},{1,9},{9,17},{17,25},{25,1},{2,10},{10... | collective-permute-start | bytes 147464 | tf_op jit(solution)/shard_map/ppermute | solution.py:29
  14.7 7.3 %collective-permute-start.1 = (bf16[48,512]{1,0:T(8,128)(2,1)}, bf16[48,512]{1,0:T(8,128)(2,1)S(1)}, u32[]{:S(2)}, u32[]{:S(2)}) collective-permute-start(bf16[48,512]{1,0:T(8,128)(2,1)} %get-tuple-element.27), channel_id=1, source_target_pairs={{0,16},{8,24},{16,0},{24,8},{1,17},{9,25},{17,1},{25,9},{2,18},{10... | collective-permute-start | bytes 147464 | tf_op jit(solution)/shard_map/ppermute | solution.py:29
  18.8 63.8 %collective-permute-start.15 = (bf16[3,256,256]{2,1,0:T(8,128)(2,1)}, bf16[3,256,256]{2,1,0:T(8,128)(2,1)S(1)}, u32[]{:S(2)}, u32[]{:S(2)}) collective-permute-start(bf16[3,256,256]{2,1,0:T(8,128)(2,1)} %get-tuple-element.37.refs_2_.refs_4_), channel_id=1, source_target_pairs={{0,8},{8,16},{16,24},{24,0},{1,9},{9,17},{17,25},{25,1},{2,10},{10... | collective-permute-start | bytes 1179656 | tf_op jit(solution)/shard_map/ppermute | solution.py:29
  29.5 4.9 %collective-permute-start.3 = (bf16[48,512]{1,0:T(8,128)(2,1)S(1)}, bf16[48,512]{1,0:T(8,128)(2,1)S(1)}, u32[]{:S(2)}, u32[]{:S(2)}) collective-permute-start(bf16[48,512]{1,0:T(8,128)(2,1)S(1)} %get-tuple-element.50), channel_id=1, source_target_pairs={{0,24},{8,0},{16,8},{24,16},{1,25},{9,1},{17,9},{25,17},{2,26},{10... | collective-permute-start | bytes 147464 | tf_op jit(solution)/shard_map/ppermute | solution.py:29
  32.3 5.6 %collective-permute-start.4 = (bf16[48,512]{1,0:T(8,128)(2,1)S(1)}, bf16[48,512]{1,0:T(8,128)(2,1)S(1)}, u32[]{:S(2)}, u32[]{:S(2)}) collective-permute-start(bf16[48,512]{1,0:T(8,128)(2,1)S(1)} %get-tuple-element.49), channel_id=1, source_target_pairs={{0,16},{8,24},{16,0},{24,8},{1,17},{9,25},{17,1},{25,9},{2,18},{10... | collective-permute-start | bytes 147464 | tf_op jit(solution)/shard_map/ppermute | solution.py:29
  33.1 5.3 %collective-permute-start.5 = (bf16[48,512]{1,0:T(8,128)(2,1)S(1)}, bf16[48,512]{1,0:T(8,128)(2,1)S(1)}, u32[]{:S(2)}, u32[]{:S(2)}) collective-permute-start(bf16[48,512]{1,0:T(8,128)(2,1)S(1)} %get-tuple-element.48), channel_id=1, source_target_pairs={{0,8},{8,16},{16,24},{24,0},{1,9},{9,17},{17,25},{25,1},{2,10},{10... | collective-permute-start | bytes 147464 | tf_op jit(solution)/shard_map/ppermute | solution.py:29
  43.6 9.3 %all-to-all-start.1 = ((bf16[4,48,256]{2,1,0:T(8,128)(2,1)}), bf16[4,48,256]{2,1,0:T(8,128)(2,1)S(1)}, u32[]{:S(2)}, u32[]{:S(2)}) async-start(bf16[4,48,256]{2,1,0:T(8,128)(2,1)} %add_convert_fusion), calls=%async_computation.1 | async-start | bytes 196608 | tf_op jit(solution)/shard_map/all_to_all | solution.py:20
  55.0 19.8 %all-to-all-start.2 = ((bf16[64,24,128]{2,1,0:T(8,128)(2,1)}), bf16[64,24,128]{2,1,0:T(8,128)(2,1)S(1)}, u32[]{:S(2)}, u32[]{:S(2)}) async-start(bf16[64,24,128]{2,1,0:T(8,128)(2,1)} %bitcast.7), calls=%async_computation.2 | async-start | bytes 786432 | tf_op jit(solution)/shard_map/all_to_all | solution.py:20
  60.6 51.7 %collective-permute-start.7 = (bf16[2048,128]{1,0:T(8,128)(2,1)}, bf16[2048,128]{1,0:T(8,128)(2,1)S(1)}, u32[]{:S(2)}, u32[]{:S(2)}) collective-permute-start(bf16[2048,128]{1,0:T(8,128)(2,1)} %dynamic-slice_bitcast_fusion.2), channel_id=1, source_target_pairs={{0,1},{1,0},{2,3},{3,2},{4,5},{5,4},{6,7},{7,6},{8,9},{9,8},{10,11... | collective-permute-start | bytes 1572872 | tf_op jit(solution)/shard_map/ppermute | solution.py:24
  62.5 50.3 %collective-permute-start.8 = (bf16[2048,128]{1,0:T(8,128)(2,1)}, bf16[2048,128]{1,0:T(8,128)(2,1)}, u32[]{:S(2)}, u32[]{:S(2)}) collective-permute-start(bf16[2048,128]{1,0:T(8,128)(2,1)} %dynamic-slice_bitcast_fusion.1), channel_id=1, source_target_pairs={{0,1},{1,0},{2,3},{3,2},{4,5},{5,4},{6,7},{7,6},{8,9},{9,8},{10,11... | collective-permute-start | bytes 1572872 | tf_op jit(solution)/shard_map/ppermute | solution.py:24
  64.9 48.0 %collective-permute-start.9 = (bf16[128,2048]{1,0:T(8,128)(2,1)}, bf16[128,2048]{1,0:T(8,128)(2,1)}, u32[]{:S(2)}, u32[]{:S(2)}) collective-permute-start(bf16[128,2048]{1,0:T(8,128)(2,1)} %dynamic-slice_bitcast_fusion), channel_id=1, source_target_pairs={{0,1},{1,0},{2,3},{3,2},{4,5},{5,4},{6,7},{7,6},{8,9},{9,8},{10,11... | collective-permute-start | bytes 1572872 | tf_op jit(solution)/shard_map/ppermute | solution.py:24
  65.0 16.1 %collective-permute-start.10 = (bf16[48,256]{1,0:T(8,128)(2,1)S(1)}, bf16[48,256]{1,0:T(8,128)(2,1)S(1)}, u32[]{:S(2)}, u32[]{:S(2)}) collective-permute-start(bf16[48,256]{1,0:T(8,128)(2,1)S(1)} %get-tuple-element.33), channel_id=1, source_target_pairs={{0,1},{1,0},{2,3},{3,2},{4,5},{5,4},{6,7},{7,6},{8,9},{9,8},{10,11... | collective-permute-start | bytes 73736 | tf_op jit(solution)/shard_map/ppermute | solution.py:24
  76.2 37.2 %all-to-all-start.3 = ((bf16[4,192,512]{2,1,0:T(8,128)(2,1)}), bf16[4,192,512]{2,1,0:T(8,128)(2,1)S(1)}, u32[]{:S(2)}, u32[]{:S(2)}) async-start(bf16[4,192,512]{2,1,0:T(8,128)(2,1)} %get-tuple-element.32), calls=%async_computation.3 | async-start | bytes 1572864 | tf_op jit(solution)/shard_map/all_to_all | solution.py:20
  81.1 11.3 %collective-permute-start.11 = (bf16[48,512]{1,0:T(8,128)(2,1)S(1)}, bf16[48,512]{1,0:T(8,128)(2,1)S(1)}, u32[]{:S(2)}, u32[]{:S(2)}) collective-permute-start(bf16[48,512]{1,0:T(8,128)(2,1)S(1)} %constant_dynamic-update-slice_fusion.refs_0_), channel_id=1, source_target_pairs={{0,2},{2,4},{4,6},{6,0},{1,3},{3,5},{5,7},{7,1},{8,10},{10,12},{12... | collective-permute-start | bytes 147464 | tf_op jit(solution)/shard_map/ppermute | solution.py:29
  82.6 12.7 %collective-permute-start.12 = (bf16[48,512]{1,0:T(8,128)(2,1)S(1)}, bf16[48,512]{1,0:T(8,128)(2,1)S(1)}, u32[]{:S(2)}, u32[]{:S(2)}) collective-permute-start(bf16[48,512]{1,0:T(8,128)(2,1)S(1)} %constant_dynamic-update-slice_fusion.refs_0_), channel_id=1, source_target_pairs={{0,4},{2,6},{4,0},{6,2},{1,5},{3,7},{5,1},{7,3},{8,12},{10,14},{12... | collective-permute-start | bytes 147464 | tf_op jit(solution)/shard_map/ppermute | solution.py:29
  92.4 5.1 %collective-permute-start.13 = (bf16[48,512]{1,0:T(8,128)(2,1)S(1)}, bf16[48,512]{1,0:T(8,128)(2,1)S(1)}, u32[]{:S(2)}, u32[]{:S(2)}) collective-permute-start(bf16[48,512]{1,0:T(8,128)(2,1)S(1)} %constant_dynamic-update-slice_fusion.refs_0_), channel_id=1, source_target_pairs={{0,6},{2,0},{4,2},{6,4},{1,7},{3,1},{5,3},{7,5},{8,14},{10,8},{12,... | collective-permute-start | bytes 147464 | tf_op jit(solution)/shard_map/ppermute | solution.py:29
  95.2 10.7 %collective-permute-start.16 = (bf16[3,256,256]{2,1,0:T(8,128)(2,1)}, bf16[3,256,256]{2,1,0:T(8,128)(2,1)S(1)}, u32[]{:S(2)}, u32[]{:S(2)}) collective-permute-start(bf16[3,256,256]{2,1,0:T(8,128)(2,1)} %get-tuple-element.37.refs_2_.refs_4_), channel_id=1, source_target_pairs={{0,16},{8,24},{16,0},{24,8},{1,17},{9,25},{17,1},{25,9},{2,18},{10... | collective-permute-start | bytes 1179656 | tf_op jit(solution)/shard_map/ppermute | solution.py:29
  97.5 14.8 %collective-permute-start.17 = (bf16[3,256,256]{2,1,0:T(8,128)(2,1)}, bf16[3,256,256]{2,1,0:T(8,128)(2,1)}, u32[]{:S(2)}, u32[]{:S(2)}) collective-permute-start(bf16[3,256,256]{2,1,0:T(8,128)(2,1)} %get-tuple-element.37.refs_2_.refs_4_), channel_id=1, source_target_pairs={{0,24},{8,0},{16,8},{24,16},{1,25},{9,1},{17,9},{25,17},{2,26},{10... | collective-permute-start | bytes 1179656 | tf_op jit(solution)/shard_map/ppermute | solution.py:29
  105.9 7.5 %collective-permute-start.14 = (bf16[4,48,256]{2,1,0:T(8,128)(2,1)S(1)}, bf16[4,48,256]{2,1,0:T(8,128)(2,1)S(1)}, u32[]{:S(2)}, u32[]{:S(2)}) collective-permute-start(bf16[4,48,256]{2,1,0:T(8,128)(2,1)S(1)} %get-tuple-element.35), channel_id=1, source_target_pairs={{0,1},{1,0},{2,3},{3,2},{4,5},{5,4},{6,7},{7,6},{8,9},{9,8},{10,11... | collective-permute-start | bytes 294920 | tf_op jit(solution)/shard_map/ppermute | solution.py:24
  112.3 11.7 %collective-permute-start.18 = (bf16[3,256,256]{2,1,0:T(8,128)(2,1)}, bf16[3,256,256]{2,1,0:T(8,128)(2,1)}, u32[]{:S(2)}, u32[]{:S(2)}) collective-permute-start(bf16[3,256,256]{2,1,0:T(8,128)(2,1)} %get-tuple-element.37.refs_2_.refs_4_), channel_id=1, source_target_pairs={{0,1},{1,0},{2,3},{3,2},{4,5},{5,4},{6,7},{7,6},{8,9},{9,8},{10,11... | collective-permute-start | bytes 1179656 | tf_op jit(solution)/shard_map/ppermute | solution.py:24
  112.3 11.7 %collective-permute-start.19 = (bf16[3,256,256]{2,1,0:T(8,128)(2,1)S(1)}, bf16[3,256,256]{2,1,0:T(8,128)(2,1)}, u32[]{:S(2)}, u32[]{:S(2)}) collective-permute-start(bf16[3,256,256]{2,1,0:T(8,128)(2,1)S(1)} %collective-permute-done.15.refs_3_.refs_5_), channel_id=1, source_target_pairs={{0,1},{1,0},{2,3},{3,2},{4,5},{5,4},{6,7},{7,6},{8,9},{9,8},{10,11... | collective-permute-start | bytes 1179656 | tf_op jit(solution)/shard_map/ppermute | solution.py:24
  112.8 11.2 %collective-permute-start.20 = (bf16[3,256,256]{2,1,0:T(8,128)(2,1)S(1)}, bf16[3,256,256]{2,1,0:T(8,128)(2,1)}, u32[]{:S(2)}, u32[]{:S(2)}) collective-permute-start(bf16[3,256,256]{2,1,0:T(8,128)(2,1)S(1)} %collective-permute-done.16.refs_4_.refs_6_), channel_id=1, source_target_pairs={{0,1},{1,0},{2,3},{3,2},{4,5},{5,4},{6,7},{7,6},{8,9},{9,8},{10,11... | collective-permute-start | bytes 1179656 | tf_op jit(solution)/shard_map/ppermute | solution.py:24
  112.9 11.1 %collective-permute-start.21 = (bf16[3,256,256]{2,1,0:T(8,128)(2,1)}, bf16[3,256,256]{2,1,0:T(8,128)(2,1)}, u32[]{:S(2)}, u32[]{:S(2)}) collective-permute-start(bf16[3,256,256]{2,1,0:T(8,128)(2,1)} %collective-permute-done.17.refs_5_.refs_7_), channel_id=1, source_target_pairs={{0,1},{1,0},{2,3},{3,2},{4,5},{5,4},{6,7},{7,6},{8,9},{9,8},{10,11... | collective-permute-start | bytes 1179656 | tf_op jit(solution)/shard_map/ppermute | solution.py:24
  118.2 38.7 %all-to-all-start.4 = ((bf16[4,216,512]{2,1,0:T(8,128)(2,1)}), bf16[4,216,512]{2,1,0:T(8,128)(2,1)S(1)}, u32[]{:S(2)}, u32[]{:S(2)}) async-start(bf16[4,216,512]{2,1,0:T(8,128)(2,1)} %shard_map.236), calls=%async_computation.4 | async-start | bytes 1769472 | tf_op jit(solution)/shard_map/all_to_all | solution.py:20
  128.3 11.5 %collective-permute-start.22 = (bf16[48,2176]{1,0:T(8,128)(2,1)S(1)}, bf16[48,2176]{1,0:T(8,128)(2,1)S(1)}, u32[]{:S(2)}, u32[]{:S(2)}) collective-permute-start(bf16[48,2176]{1,0:T(8,128)(2,1)S(1)} %get-tuple-element.39), channel_id=1, source_target_pairs={{0,2},{2,4},{4,6},{6,0},{1,3},{3,5},{5,7},{7,1},{8,10},{10,12},{12... | collective-permute-start | bytes 626696 | tf_op jit(solution)/shard_map/ppermute | solution.py:29
  129.8 12.0 %collective-permute-start.23 = (bf16[48,2176]{1,0:T(8,128)(2,1)S(1)}, bf16[48,2176]{1,0:T(8,128)(2,1)S(1)}, u32[]{:S(2)}, u32[]{:S(2)}) collective-permute-start(bf16[48,2176]{1,0:T(8,128)(2,1)S(1)} %get-tuple-element.40), channel_id=1, source_target_pairs={{0,4},{2,6},{4,0},{6,2},{1,5},{3,7},{5,1},{7,3},{8,12},{10,14},{12... | collective-permute-start | bytes 626696 | tf_op jit(solution)/shard_map/ppermute | solution.py:29
  130.5 14.8 %collective-permute-start.24 = (bf16[48,2176]{1,0:T(8,128)(2,1)}, bf16[48,2176]{1,0:T(8,128)(2,1)S(1)}, u32[]{:S(2)}, u32[]{:S(2)}) collective-permute-start(bf16[48,2176]{1,0:T(8,128)(2,1)} %get-tuple-element.41), channel_id=1, source_target_pairs={{0,6},{2,0},{4,2},{6,4},{1,7},{3,1},{5,3},{7,5},{8,14},{10,8},{12,... | collective-permute-start | bytes 626696 | tf_op jit(solution)/shard_map/ppermute | solution.py:29
  146.0 5.3 %collective-permute-start.25 = (bf16[48,1024]{1,0:T(8,128)(2,1)S(1)}, bf16[48,1024]{1,0:T(8,128)(2,1)S(1)}, u32[]{:S(2)}, u32[]{:S(2)}) collective-permute-start(bf16[48,1024]{1,0:T(8,128)(2,1)S(1)} %shard_map.238.refs_0_), channel_id=1, source_target_pairs={{0,2},{2,4},{4,6},{6,0},{1,3},{3,5},{5,7},{7,1},{8,10},{10,12},{12... | collective-permute-start | bytes 294920 | tf_op jit(solution)/shard_map/ppermute | solution.py:29
  146.9 6.8 %collective-permute-start.26 = (bf16[48,1024]{1,0:T(8,128)(2,1)S(1)}, bf16[48,1024]{1,0:T(8,128)(2,1)S(1)}, u32[]{:S(2)}, u32[]{:S(2)}) collective-permute-start(bf16[48,1024]{1,0:T(8,128)(2,1)S(1)} %shard_map.238.refs_0_), channel_id=1, source_target_pairs={{0,4},{2,6},{4,0},{6,2},{1,5},{3,7},{5,1},{7,3},{8,12},{10,14},{12... | collective-permute-start | bytes 294920 | tf_op jit(solution)/shard_map/ppermute | solution.py:29
  149.9 4.8 %collective-permute-start.27 = (bf16[48,1024]{1,0:T(8,128)(2,1)S(1)}, bf16[48,1024]{1,0:T(8,128)(2,1)S(1)}, u32[]{:S(2)}, u32[]{:S(2)}) collective-permute-start(bf16[48,1024]{1,0:T(8,128)(2,1)S(1)} %shard_map.238.refs_0_), channel_id=1, source_target_pairs={{0,6},{2,0},{4,2},{6,4},{1,7},{3,1},{5,3},{7,5},{8,14},{10,8},{12,... | collective-permute-start | bytes 294920 | tf_op jit(solution)/shard_map/ppermute | solution.py:29
  160.8 21.6 %all-to-all-start.5 = ((bf16[64,24,128]{2,1,0:T(8,128)(2,1)}), bf16[64,24,128]{2,1,0:T(8,128)(2,1)S(1)}, u32[]{:S(2)}, u32[]{:S(2)}) async-start(bf16[64,24,128]{2,1,0:T(8,128)(2,1)} %bitcast.13), calls=%async_computation.5 | async-start | bytes 786432 | tf_op jit(solution)/shard_map/all_to_all | solution.py:20
  (14 other events, 310.2 us)
